TPU v7x, 512 devices: a whole 4x8x8 slice. The times are simulated.
512 devices in a mesh: sp: 128 (over z, y, core), tp: 4 (over x).
Axes of the slice: x: 4, y: 8, z: 8, core: 2. Of those that a mesh axis runs over, the one named last changes fastest.
Arguments:
- tokens: bfloat16 [65536, 2048], P('sp'), may hold values from -6 to 6
- norm_gain: bfloat16 [2048], replicated, may hold values from 0.099609375 to 1.8984375
- w_conv_value: bfloat16 [2048, 2048], P('sp', 'tp'), may hold values from -0.125 to 0.125
- w_conv_gate: bfloat16 [2048, 2048], P('sp', 'tp'), may hold values from -0.125 to 0.125
- w_query: bfloat16 [2048, 2048], P('sp', 'tp'), may hold values from -0.125 to 0.125
- w_key: bfloat16 [2048, 512], P('sp', 'tp'), may hold values from -0.125 to 0.125
- w_value: bfloat16 [2048, 512], P('sp', 'tp'), may hold values from -0.125 to 0.125
- conv_taps: float32 [31, 2048], P(None, 'tp'), as said below
- ln_gain: float32 [2048], P('tp'), may hold values from 0.1 to 1.9
- sinks: float32 [32], P('tp'), may hold values from 3 to 6
- out_conv: bfloat16 [2048, 2048], P('tp', 'sp'), may hold values from -0.125 to 0.125
- out_attn: bfloat16 [2048, 2048], P('tp', 'sp'), may hold values from -0.5 to 0.5
Outputs:
- mixed: bfloat16 [65536, 2048], P(('sp', 'tp'))
- log_sums: float32 [32, 65536], P('tp', 'sp')
Inputs may be any that keep to these rules, and one draw needn't show every extreme that they name: `conv_taps`: each tap lies within 30 / sqrt(31) in magnitude.
All inputs are finite; a program needn't handle non-finite values.
Results may differ from a plain program's by a relative error of at most 0.017.
Values may be sent and summed in bfloat16 or wider, within the bound.
No kernel may reach another device: no remote copies, remote signals or barrier semaphores. Data moves between devices by JAX's collectives and lax.ppermute only.
A program may use at most 64 MiB of HBM per device.

v0:
```python
import jax
import jax.numpy as jnp
from jax import lax
from jax.experimental import pallas as pl
from jax.experimental.pallas import tpu as pltpu
from jax.sharding import Mesh, PartitionSpec as P

CONV_CH = 2048
HEAD_DIM = 64
WINDOW = 128

NORM_EPS = 1e-06
CHANNEL_EPS = 1e-05
ROPE_BASE = 10000.0

SIDE = 8
PAIRS = SIDE // 2
CORES = 2
SP = ("chip", "core")
CHIP = ("core", "tp")


def place(z, y, core):
    return ((z % SIDE) * SIDE + y % SIDE) * CORES + core


FAR_BOTH = [
    [place(2 * i + a, 2 * j + b, c) for i in range(PAIRS) for j in range(PAIRS) for c in range(CORES)]
    for a in range(2)
    for b in range(2)
]
FAR_ONE = [
    [place(2 * i + a, 2 * j + b, c) for i in range(PAIRS) for j in range(PAIRS)]
    for a in range(2)
    for b in range(2)
    for c in range(CORES)
]


def beside(at, core):
    return ((at + core) ^ 1) - core


NEAR = [
    [
        (place(z, y, c), place(beside(z, c) if along_z else z, beside(y, c) if along_y else y, c))
        for z in range(SIDE)
        for y in range(SIDE)
        for c in range(CORES)
    ]
    for along_z, along_y in ((0, 1), (1, 0), (1, 1))
]
OTHER_CORE = [(i, i ^ 1) for i in range(SIDE * SIDE * CORES)]
NEXT_CHIP = [(i, i + CORES) for i in range(SIDE * SIDE * CORES - CORES)]


def exchanged(pieces, groups):
    return lax.all_to_all(pieces, SP, 0, 0, tiled=True, axis_index_groups=groups)


def repeated(shard, count):
    return jnp.broadcast_to(shard[None], (count, *shard.shape))


VMEM = pl.BlockSpec(memory_space=pltpu.VMEM)
SMEM = pl.BlockSpec(memory_space=pltpu.SMEM)
TILE = 256


def call(body, outs, scratch, flops, *operands):
    return pl.pallas_call(
        body,
        out_shape=outs,
        in_specs=[SMEM] + [VMEM] * (len(operands) - 1),
        out_specs=jax.tree.map(lambda _: VMEM, outs),
        scratch_shapes=scratch,
        compiler_params=pltpu.CompilerParams(vmem_limit_bytes=12 << 20),
        cost_estimate=pl.CostEstimate(flops=flops, bytes_accessed=1 << 20, transcendentals=0),
    )(*operands)


def put_in_order(at_ref, pieces, out_ref, rows):
    for piece, (flip_z, flip_y) in zip(pieces, ((0, 0), (0, 1), (1, 0), (1, 1))):
        odd_z = jnp.bitwise_xor(at_ref[0], flip_z)
        odd_y = jnp.bitwise_xor(at_ref[1], flip_y)
        first = (odd_z * SIDE + odd_y) * rows
        for i in range(PAIRS):
            for j in range(PAIRS):
                to = pl.multiple_of(first + (2 * i * SIDE + 2 * j) * rows, rows)
                out_ref[pl.ds(to, rows), :] = piece[pl.ds((i * PAIRS + j) * rows, rows), :]


def gated_kernel(at_ref, x_ref, a_ref, b_ref, c_ref, d_ref, out_ref, w_ref):
    put_in_order(at_ref, (a_ref, b_ref, c_ref, d_ref), w_ref, a_ref.shape[0] // PAIRS**2)
    half = out_ref.shape[1]

    @pl.loop(0, x_ref.shape[0] // TILE)
    def _(step):
        rows = pl.ds(pl.multiple_of(step * TILE, TILE), TILE)
        both = jnp.dot(x_ref[rows, :], w_ref[...], preferred_element_type=jnp.float32)
        both = both.astype(jnp.bfloat16).astype(jnp.float32)
        out_ref[rows, :] = (both[:, :half] * jax.nn.sigmoid(both[:, half:])).astype(jnp.bfloat16)


def rotated_kernel(at_ref, x_ref, cos_ref, sin_ref, a_ref, b_ref, c_ref, d_ref, out_ref, w_ref):
    put_in_order(at_ref, (a_ref, b_ref, c_ref, d_ref), w_ref, a_ref.shape[0] // PAIRS**2)
    width = out_ref.shape[1]

    @pl.loop(0, x_ref.shape[0] // TILE)
    def _(step):
        rows = pl.ds(pl.multiple_of(step * TILE, TILE), TILE)
        raw = jnp.dot(x_ref[rows, :], w_ref[...], preferred_element_type=jnp.float32)
        raw = raw.astype(jnp.bfloat16).astype(jnp.float32)
        lane = lax.broadcasted_iota(jnp.int32, (TILE, 128), 1)
        front = jnp.bitwise_and(lane, HEAD_DIM - 1) < HEAD_DIM // 2
        cosine, sine = cos_ref[rows, :], sin_ref[rows, :]
        for at in range(0, width, 128):
            part = raw[:, at : at + 128]
            other = jnp.where(
                front,
                pltpu.roll(part, 128 - HEAD_DIM // 2, 1),
                pltpu.roll(part, HEAD_DIM // 2, 1),
            )
            turned = part * cosine + other * sine
            if at + 128 == width:
                turned = jnp.where(lane < HEAD_DIM, turned, part)
            out_ref[rows, at : at + 128] = turned.astype(jnp.bfloat16)


def conv_kernel(at_ref, before_ref, glu_ref, taps_ref, out_ref, sums_ref, ext_ref):
    count, rows = taps_ref.shape[0], glu_ref.shape[0]
    lead = before_ref.shape[0]
    for part in range(2):
        lanes = pl.ds(part * 128, 128)
        ext_ref[part, pl.ds(0, lead), :] = before_ref[:, lanes].astype(jnp.float32)
        ext_ref[part, pl.ds(lead, rows), :] = glu_ref[:, lanes].astype(jnp.float32)

    @pl.loop(0, rows // 128)
    def _(step):
        base = pl.multiple_of(step * 128, 128)
        first = jnp.zeros((128, 128), jnp.float32)
        second = jnp.zeros((128, 128), jnp.float32)
        for part in range(2):
            lanes = pl.ds(part * 128, 128)
            total = jnp.zeros((128, 128), jnp.float32)
            for tap in range(count):
                rows_at = pl.ds(base + (lead - count + 1 + tap), 128)
                total = total + taps_ref[pl.ds(tap, 1), lanes] * ext_ref[part, rows_at, :]
            out_ref[pl.ds(base, 128), lanes] = total
            first = first + total
            second = second + total * total
        sums_ref[pl.ds(0, 1), pl.ds(base, 128)] = jnp.sum(first.T, axis=0, keepdims=True)
        sums_ref[pl.ds(1, 1), pl.ds(base, 128)] = jnp.sum(second.T, axis=0, keepdims=True)


def gather_kernel(at_ref, a_ref, b_ref, c_ref, d_ref, out_ref):
    put_in_order(at_ref, (a_ref, b_ref, c_ref, d_ref), out_ref, a_ref.shape[0] // PAIRS**2)


def output_kernel(at_ref, conv_ref, attn_ref, own_ref, other_ref, out_ref, w_ref):
    core = at_ref[2]
    block = own_ref.shape[0] // SIDE**2
    for source, to_core in ((own_ref, core), (other_ref, 1 - core)):
        for chip in range(SIDE**2):
            to = pl.multiple_of(chip * CORES * block + to_core * block, block)
            w_ref[pl.ds(to, block), :] = source[pl.ds(chip * block, block), :]
    half = conv_ref.shape[1]

    @pl.loop(0, out_ref.shape[1] // TILE)
    def _(step):
        cols = pl.ds(pl.multiple_of(step * TILE, TILE), TILE)
        contract = (((1,), (1,)), ((), ()))
        total = lax.dot_general(
            conv_ref[...], w_ref[cols, :half], contract, preferred_element_type=jnp.float32
        ) + lax.dot_general(
            attn_ref[...], w_ref[cols, half:], contract, preferred_element_type=jnp.float32
        )
        out_ref[:, cols] = total.astype(jnp.bfloat16)


def layer(
    tokens,
    norm_gain,
    w_conv_value,
    w_conv_gate,
    w_query,
    w_key,
    w_value,
    conv_taps,
    ln_gain,
    sinks,
    out_conv,
    out_attn,
):
    core = lax.axis_index("core")
    chip = lax.axis_index("chip")
    own_rows = tokens.shape[0]
    row_count = own_rows * CORES

    tokens_other = lax.ppermute(tokens, SP, OTHER_CORE)

    def own_half(weights):
        halves = jnp.stack(
            [
                jnp.concatenate(
                    [w[:, h * (w.shape[1] // CORES) : (h + 1) * (w.shape[1] // CORES)] for w in weights],
                    axis=1,
                )
                for h in range(CORES)
            ]
        )
        return repeated(halves, PAIRS * PAIRS).reshape(-1, *halves.shape[1:])

    at = jnp.stack([(chip // SIDE) % 2, chip % 2, core]).astype(jnp.int32)

    def from_square(far):
        own = far.reshape(-1, far.shape[-1])
        return (own, *(lax.ppermute(own, SP, pairs) for pairs in NEAR))

    far_conv = exchanged(own_half((w_conv_value, w_conv_gate)), FAR_BOTH)
    far_qkv = exchanged(own_half((w_query, w_key, w_value)), FAR_BOTH)
    near_conv = from_square(far_conv)
    turned = jnp.concatenate([out_conv.T, out_attn.T], axis=1)
    out_depth, out_width = turned.shape
    far_out = exchanged(repeated(turned, PAIRS * PAIRS).reshape(-1, out_width), FAR_ONE)
    near_qkv = from_square(far_qkv)
    near_out = from_square(far_out)
    out_own = call(
        gather_kernel,
        jax.ShapeDtypeStruct((SIDE**2 * out_depth, out_width), jnp.bfloat16),
        [],
        1 << 28,
        at,
        *near_out,
    )
    out_other = lax.ppermute(out_own, SP, OTHER_CORE)

    both = jnp.where(
        core == 0,
        jnp.concatenate([tokens, tokens_other], axis=0),
        jnp.concatenate([tokens_other, tokens], axis=0),
    )
    as_float = both.astype(jnp.float32)
    normed = (
        as_float
        * lax.rsqrt(jnp.mean(as_float * as_float, axis=-1, keepdims=True) + NORM_EPS)
        * norm_gain.astype(jnp.float32)
    ).astype(jnp.bfloat16)

    channels = w_conv_value.shape[1] // CORES
    q_cols = w_query.shape[1] // CORES
    model = normed.shape[1]
    glu = call(
        gated_kernel,
        jax.ShapeDtypeStruct((row_count, channels), jnp.bfloat16),
        [pltpu.VMEM((model, 2 * channels), jnp.bfloat16)],
        2 * row_count * model * 2 * channels,
        at,
        normed,
        *near_conv,
    )
    offset = chip * row_count
    positions = offset + jnp.arange(row_count, dtype=jnp.int32)
    half_dim = HEAD_DIM // 2
    inverse = ROPE_BASE ** (-jnp.arange(half_dim, dtype=jnp.float32) / half_dim)
    angles = positions.astype(jnp.float32)[:, None] * inverse[None, :]
    cosine, sine = jnp.cos(angles), jnp.sin(angles)
    query_heads = q_cols // HEAD_DIM
    qkv = call(
        rotated_kernel,
        jax.ShapeDtypeStruct((row_count, q_cols + 2 * HEAD_DIM), jnp.bfloat16),
        [pltpu.VMEM((model, q_cols + 2 * HEAD_DIM), jnp.bfloat16)],
        2 * row_count * model * (q_cols + 2 * HEAD_DIM),
        at,
        normed,
        jnp.concatenate([cosine] * 4, axis=1),
        jnp.concatenate([-sine, sine] * 2, axis=1),
        *near_qkv,
    )
    query = qkv[:, :q_cols].reshape(row_count, query_heads, HEAD_DIM)
    key_value = qkv[:, q_cols:]
    key = key_value[:, :HEAD_DIM]
    value_rows = key_value[:, HEAD_DIM:]

    glu_before = lax.ppermute(glu[row_count - 32 :], SP, NEXT_CHIP)
    before = lax.ppermute(key_value[row_count - WINDOW :], SP, NEXT_CHIP)
    key_before = before[:, :HEAD_DIM]
    value_before = before[:, HEAD_DIM:]

    taps = lax.dynamic_slice_in_dim(conv_taps, core * channels, channels, 1)
    conv_out, sums = call(
        conv_kernel,
        (
            jax.ShapeDtypeStruct((row_count, channels), jnp.float32),
            jax.ShapeDtypeStruct((2, row_count), jnp.float32),
        ),
        [pltpu.VMEM((2, row_count + 32, 128), jnp.float32)],
        2 * row_count * channels * 32 * 32,
        at,
        glu_before,
        glu,
        taps,
    )
    members = CORES * lax.axis_size("tp")
    everyones = lax.all_to_all(repeated(sums, members), CHIP, 0, 0, tiled=True)
    totals = jnp.sum(everyones, axis=0)
    mean = (totals[0] / CONV_CH)[:, None]
    var = (totals[1] / CONV_CH)[:, None] - mean * mean
    gain = lax.dynamic_slice_in_dim(ln_gain, core * channels, channels, 0)
    conv_branch = jax.nn.silu(
        (conv_out - mean) * lax.rsqrt(var + CHANNEL_EPS) * gain[None, :]
    ).astype(jnp.bfloat16)

    blocks = row_count // WINDOW
    q_blocks = query.reshape(blocks, WINDOW, query_heads, HEAD_DIM)
    key_blocks = jnp.concatenate([key_before, key], axis=0).reshape(blocks + 1, WINDOW, HEAD_DIM)
    value_blocks = jnp.concatenate([value_before, value_rows], axis=0).reshape(
        blocks + 1, WINDOW, HEAD_DIM
    )
    key_window = jnp.concatenate([key_blocks[:-1], key_blocks[1:]], axis=1)
    value_window = jnp.concatenate([value_blocks[:-1], value_blocks[1:]], axis=1)
    scores = jnp.einsum(
        "nqgd,nkd->ngqk", q_blocks, key_window, preferred_element_type=jnp.float32
    ) * HEAD_DIM ** (-0.5)
    query_index = jnp.arange(WINDOW)[:, None] + WINDOW
    key_index = jnp.arange(2 * WINDOW)[None, :]
    band = (key_index <= query_index) & (query_index - key_index < WINDOW)
    block_index = jnp.arange(blocks)[:, None, None]
    allowed = band[None] & (offset + block_index * WINDOW + key_index[None] - WINDOW >= 0)
    allowed = allowed[:, None]
    sums_exp = jnp.sum(jnp.where(allowed, jnp.exp(scores), 0.0), axis=-1)
    own_sinks = lax.dynamic_slice_in_dim(sinks, core * query_heads, query_heads, 0)
    log_total = jnp.log(sums_exp + jnp.exp(own_sinks)[None, :, None])
    weights = jnp.where(allowed, jnp.exp(scores - log_total[..., None]), 0.0).astype(jnp.bfloat16)
    attended = jnp.einsum(
        "ngqk,nkd->nqgd", weights, value_window, preferred_element_type=jnp.float32
    )
    attn_branch = attended.astype(jnp.bfloat16).reshape(row_count, q_cols)
    log_rows = log_total.transpose(1, 0, 2).reshape(query_heads, row_count)

    def swapped(value, axis):
        kept = lax.dynamic_slice_in_dim(value, core * own_rows, own_rows, axis)
        given = lax.dynamic_slice_in_dim(value, (1 - core) * own_rows, own_rows, axis)
        return kept, lax.ppermute(given, SP, OTHER_CORE)

    def joined(kept, got, axis):
        return jnp.where(
            core == 0,
            jnp.concatenate([kept, got], axis=axis),
            jnp.concatenate([got, kept], axis=axis),
        )

    log_sums = joined(*swapped(log_rows, 1), 0)
    attn_full = joined(*swapped(attn_branch, 0), 1)
    conv_full = joined(*swapped(conv_branch, 0), 1)

    partial = call(
        output_kernel,
        jax.ShapeDtypeStruct((own_rows, model), jnp.bfloat16),
        [pltpu.VMEM((model, out_width), jnp.bfloat16)],
        2 * own_rows * model * out_width,
        at,
        conv_full,
        attn_full,
        out_own,
        out_other,
    )
    peers = lax.axis_size("tp")
    arrived = lax.all_to_all(
        partial.reshape(peers, own_rows // peers, -1), "tp", split_axis=0, concat_axis=0, tiled=True
    )
    mixed = arrived.astype(jnp.float32).sum(axis=0)
    return (mixed.astype(jnp.bfloat16), log_sums)


def solution(mesh):
    split = Mesh(mesh.devices.reshape(-1, CORES, mesh.shape["tp"]), ("chip", "core", "tp"))
    in_specs = (
        P(SP, None),
        P(),
        P(SP, "tp"),
        P(SP, "tp"),
        P(SP, "tp"),
        P(SP, "tp"),
        P(SP, "tp"),
        P(None, "tp"),
        P("tp"),
        P("tp"),
        P("tp", SP),
        P("tp", SP),
    )
    out_specs = (P((*SP, "tp"), None), P("tp", SP))
    return jax.shard_map(layer, mesh=split, in_specs=in_specs, out_specs=out_specs, check_vma=False)
```

profile of v0, /device:TPU:1, one launch (start us, length us, event | category | flops | bytes accessed | tf_op | source)
XLA Modules:
  0.0 218.3 jit_solution(16624676760614858398)
XLA Ops:
  3.9 17.3 %all-to-all-start.2 = ((bf16[32,16,384]{2,1,0:T(8,128)(2,1)}), bf16[32,16,384]{2,1,0:T(8,128)(2,1)}, u32[]{:S(2)}, u32[]{:S(2)}) async-start(bf16[32,16,384]{2,1,0:T(8,128)(2,1)} %bitcast.11), calls=%async_computation.2 | async-start | bytes 786432 | tf_op jit(solution)/shard_map/all_to_all | solution.py:58
  21.2 2.2 %collective-permute-start = (bf16[512,2048]{1,0:T(8,128)(2,1)}, bf16[512,2048]{1,0:T(8,128)(2,1)}, u32[]{:S(2)}, u32[]{:S(2)}) collective-permute-start(bf16[512,2048]{1,0:T(8,128)(2,1)} %param.12), channel_id=1, source_target_pairs={{0,4},{4,0},{8,12},{12,8},{16,20},{20,16},{24,28},{28,24},{32,36},... | collective-permute-start | bytes 6291464 | tf_op jit(solution)/shard_map/ppermute | solution.py:200
  24.2 15.2 %all-to-all-done.2 = bf16[32,16,384]{2,1,0:T(8,128)(2,1)} async-done(((bf16[32,16,384]{2,1,0:T(8,128)(2,1)}), bf16[32,16,384]{2,1,0:T(8,128)(2,1)}, u32[]{:S(2)}, u32[]{:S(2)}) %all-to-all-start.2) | async-done | bytes 393248 | tf_op jit(solution)/shard_map/all_to_all | solution.py:58
  40.3 3.6 %all-to-all-start.3 = ((bf16[16,16,1024]{2,1,0:T(8,128)(2,1)}), bf16[16,16,1024]{2,1,0:T(8,128)(2,1)S(1)}, u32[]{:S(2)}, u32[]{:S(2)}) async-start(bf16[16,16,1024]{2,1,0:T(8,128)(2,1)} %broadcast_in_dim.25), calls=%async_computation.3 | async-start | bytes 1048576 | tf_op jit(solution)/shard_map/all_to_all | solution.py:58
  48.7 14.1 %all-to-all-done.3 = bf16[16,16,1024]{2,1,0:T(8,128)(2,1)S(1)} async-done(((bf16[16,16,1024]{2,1,0:T(8,128)(2,1)}), bf16[16,16,1024]{2,1,0:T(8,128)(2,1)S(1)}, u32[]{:S(2)}, u32[]{:S(2)}) %all-to-all-start.3) | async-done | bytes 524320 | tf_op jit(solution)/shard_map/all_to_all | solution.py:58
  63.7 7.7 %all-to-all-start = ((bf16[32,16,512]{2,1,0:T(8,128)(2,1)}), bf16[32,16,512]{2,1,0:T(8,128)(2,1)}, u32[]{:S(2)}, u32[]{:S(2)}) async-start(bf16[32,16,512]{2,1,0:T(8,128)(2,1)} %bitcast.5), calls=%async_computation | async-start | bytes 1048576 | tf_op jit(solution)/shard_map/all_to_all | solution.py:58
  73.3 4.0 %collective-permute-start.11 = (bf16[256,1024]{1,0:T(8,128)(2,1)S(1)}, bf16[256,1024]{1,0:T(8,128)(2,1)S(1)}, u32[]{:S(2)}, u32[]{:S(2)}) collective-permute-start(bf16[256,1024]{1,0:T(8,128)(2,1)S(1)} %bitcast.61), channel_id=1, source_target_pairs={{0,8},{4,60},{8,0},{12,20},{16,24},{20,12},{24,16},{28,36},{32,40}... | collective-permute-start | bytes 1572872 | tf_op jit(solution)/shard_map/ppermute | solution.py:218
  77.2 6.6 %collective-permute-start.12 = (bf16[256,1024]{1,0:T(8,128)(2,1)S(1)}, bf16[256,1024]{1,0:T(8,128)(2,1)S(1)}, u32[]{:S(2)}, u32[]{:S(2)}) collective-permute-start(bf16[256,1024]{1,0:T(8,128)(2,1)S(1)} %bitcast.62), channel_id=1, source_target_pairs={{0,64},{4,452},{8,72},{12,460},{16,80},{20,468},{24,88},{28,476},{... | collective-permute-start | bytes 1572872 | tf_op jit(solution)/shard_map/ppermute | solution.py:218
  86.9 4.3 %collective-permute-start.6 = (bf16[512,384]{1,0:T(8,128)(2,1)}, bf16[512,384]{1,0:T(8,128)(2,1)}, u32[]{:S(2)}, u32[]{:S(2)}) collective-permute-start(bf16[512,384]{1,0:T(8,128)(2,1)} %bitcast.12.a_ref), channel_id=1, source_target_pairs={{0,8},{4,60},{8,0},{12,20},{16,24},{20,12},{24,16},{28,36},{32,40}... | collective-permute-start | bytes 1179656 | tf_op jit(solution)/shard_map/ppermute | solution.py:218
  92.1 6.7 %collective-permute-start.7 = (bf16[512,384]{1,0:T(8,128)(2,1)}, bf16[512,384]{1,0:T(8,128)(2,1)}, u32[]{:S(2)}, u32[]{:S(2)}) collective-permute-start(bf16[512,384]{1,0:T(8,128)(2,1)} %bitcast.12.a_ref), channel_id=1, source_target_pairs={{0,64},{4,452},{8,72},{12,460},{16,80},{20,468},{24,88},{28,476},{... | collective-permute-start | bytes 1179656 | tf_op jit(solution)/shard_map/ppermute | solution.py:218
  99.6 5.0 %collective-permute-start.8 = (bf16[512,384]{1,0:T(8,128)(2,1)}, bf16[512,384]{1,0:T(8,128)(2,1)}, u32[]{:S(2)}, u32[]{:S(2)}) collective-permute-start(bf16[512,384]{1,0:T(8,128)(2,1)} %bitcast.12.a_ref), channel_id=1, source_target_pairs={{0,72},{4,508},{8,64},{12,468},{16,88},{20,460},{24,80},{28,484},{... | collective-permute-start | bytes 1179656 | tf_op jit(solution)/shard_map/ppermute | solution.py:218
  105.5 2.9 %collective-permute-start.1 = (bf16[512,512]{1,0:T(8,128)(2,1)}, bf16[512,512]{1,0:T(8,128)(2,1)S(1)}, u32[]{:S(2)}, u32[]{:S(2)}) collective-permute-start(bf16[512,512]{1,0:T(8,128)(2,1)} %bitcast.6.a_ref), channel_id=1, source_target_pairs={{0,8},{4,60},{8,0},{12,20},{16,24},{20,12},{24,16},{28,36},{32,40}... | collective-permute-start | bytes 1572872 | tf_op jit(solution)/shard_map/ppermute | solution.py:218
  112.2 2.9 %collective-permute-start.2 = (bf16[512,512]{1,0:T(8,128)(2,1)}, bf16[512,512]{1,0:T(8,128)(2,1)S(1)}, u32[]{:S(2)}, u32[]{:S(2)}) collective-permute-start(bf16[512,512]{1,0:T(8,128)(2,1)} %bitcast.6.a_ref), channel_id=1, source_target_pairs={{0,64},{4,452},{8,72},{12,460},{16,80},{20,468},{24,88},{28,476},{... | collective-permute-start | bytes 1572872 | tf_op jit(solution)/shard_map/ppermute | solution.py:218
  115.1 3.2 %fusion = f32[1024]{0:T(1024)S(1)} fusion(bf16[512,2048]{1,0:T(8,128)(2,1)S(1)} %copy-done.10, bf16[512,2048]{1,0:T(8,128)(2,1)} %collective-permute-done, pred[]{:T(512)S(6)} %eq.5), kind=kLoop, calls=%fused_computation.2 | loop fusion | flops 25164800 | bytes 4198401 | tf_op jit(solution)/shard_map/reduce_sum | solution.py:246
  118.3 5.1 %collective-permute-start.3 = (bf16[512,512]{1,0:T(8,128)(2,1)}, bf16[512,512]{1,0:T(8,128)(2,1)S(1)}, u32[]{:S(2)}, u32[]{:S(2)}) collective-permute-start(bf16[512,512]{1,0:T(8,128)(2,1)} %bitcast.6.a_ref), channel_id=1, source_target_pairs={{0,72},{4,508},{8,64},{12,468},{16,88},{20,460},{24,80},{28,484},{... | collective-permute-start | bytes 1572872 | tf_op jit(solution)/shard_map/ppermute | solution.py:218
  123.4 3.2 %fusion.2.x_ref = bf16[1024,2048]{1,0:T(8,128)(2,1)S(1)} fusion(f32[2048]{0:T(1024)S(1)} %convert_element_type.31, f32[1024]{0:T(1024)S(1)} %add_rsqrt_fusion.1, bf16[512,2048]{1,0:T(8,128)(2,1)S(1)} %copy-done.10, bf16[512,2048]{1,0:T(8,128)(2,1)} %collective-permute-done, pred[]{:T(512)S(6)} %eq.5), kind=kLoop, calls=%fused_computation.4 | loop fusion | flops 27262976 | bytes 8400897 | tf_op jit(solution)/shard_map/convert_element_type | solution.py:248
  126.6 2.1 collective-permute-start.14
  128.6 3.1 %collective-permute-done.3.d_ref = bf16[512,512]{1,0:T(8,128)(2,1)S(1)} collective-permute-done((bf16[512,512]{1,0:T(8,128)(2,1)}, bf16[512,512]{1,0:T(8,128)(2,1)S(1)}, u32[]{:S(2)}, u32[]{:S(2)}) %collective-permute-start.3) | collective-permute-done | bytes 524320 | tf_op jit(solution)/shard_map/ppermute | solution.py:218
  131.7 4.2 %shard_map.131.glu_ref = bf16[1024,256]{1,0:T(8,128)(2,1)S(1)} custom-call(s32[3]{0:T(128)S(1)} %pad_add_fusion.at_ref, bf16[1024,2048]{1,0:T(8,128)(2,1)S(1)} %fusion.2.x_ref, bf16[512,512]{1,0:T(8,128)(2,1)} %bitcast.6.a_ref, bf16[512,512]{1,0:T(8,128)(2,1)S(1)} %collective-permute-done.1.b_ref, bf16[512,512]{1,0:T(8,128)(2,1)S(1)} %collective-permute-done.2.c_ref, ...), custom_call_target="tpu_custom_call" | custom-call | flops 2147483648 | bytes 1048576 | tf_op jit(solution)/shard_map/pallas_call | solution.py:71
  137.3 4.8 %shard_map.133 = bf16[1024,384]{1,0:T(8,128)(2,1)S(1)} custom-call(s32[3]{0:T(128)S(1)} %pad_add_fusion.at_ref, bf16[1024,2048]{1,0:T(8,128)(2,1)S(1)} %fusion.2.x_ref, f32[1024,128]{1,0:T(8,128)S(1)} %get-tuple-element.35.cos_ref, f32[1024,128]{1,0:T(8,128)S(1)} %copy-done.2, bf16[512,384]{1,0:T(8,128)(2,1)} %bitcast.12.a_ref, ...), custom_call_target="tpu_custom_call" | custom-call | flops 1610612736 | bytes 1048576 | tf_op jit(solution)/shard_map/pallas_call | solution.py:71
  143.1 2.8 %reshape.178 = bf16[8,128,4,64]{3,2,1,0:T(4,128)(2,1)} reshape(bf16[1024,256]{1,0:T(8,128)(2,1)} %slice.114) | data formatting | bytes 1048576 | tf_op jit(solution)/shard_map/reshape;reshape | solution.py:315
  146.7 2.5 %collective-permute-start.9 = (bf16[128,128]{1,0:T(8,128)(2,1)S(1)}, bf16[128,128]{1,0:T(8,128)(2,1)S(1)}, u32[]{:S(2)}, u32[]{:S(2)}) collective-permute-start(bf16[128,128]{1,0:T(8,128)(2,1)S(1)} %slice.109), channel_id=1, source_target_pairs={{0,8},{4,12},{8,16},{12,20},{16,24},{20,28},{24,32},{28,36},{32,40... | collective-permute-start | bytes 98312 | tf_op jit(solution)/shard_map/ppermute | solution.py:286
  150.0 3.6 %shard_map.132 = (f32[1024,256]{1,0:T(8,128)S(1)}, f32[2,1024]{1,0:T(2,128)S(1)}) custom-call(s32[3]{0:T(128)S(1)} %pad_add_fusion.at_ref, bf16[32,256]{1,0:T(8,128)(2,1)S(1)} %collective-permute-done.4.before_ref, bf16[1024,256]{1,0:T(8,128)(2,1)S(1)} %shard_map.131.glu_ref, f32[31,256]{1,0:T(8,128)S(1)} %constant_dynamic-slice_fusion.6.taps_ref), custom_call_target="tpu_custom_call" | custom-call | flops 536870912 | bytes 1048576 | tf_op jit(solution)/shard_map/pallas_call | solution.py:71
  155.3 4.4 %all-to-all-start.1 = ((f32[8,2,1024]{2,1,0:T(2,128)}), f32[8,2,1024]{2,1,0:T(2,128)}, u32[]{:S(2)}, u32[]{:S(2)}) async-start(f32[8,2,1024]{2,1,0:T(2,128)} %broadcast_in_dim.21), calls=%async_computation.1 | async-start | bytes 131072 | tf_op jit(solution)/shard_map/all_to_all | solution.py:305
  160.0 4.4 %fusion.4 = (f32[8,4,128]{2,1,0:T(4,128)S(1)}, f32[8,256,128,4]{2,1,3,0:T(8,128)}) fusion(pred[8,128,256]{1,2,0:T(8,128)(4,1)} %broadcast_and_fusion, bf16[8,128,4,64]{3,2,1,0:T(4,128)(2,1)} %reshape.178, bf16[8,128,64]{1,2,0:T(8,128)(2,1)} %copy.57, bf16[8,128,64]{1,2,0:T(8,128)(2,1)S(1)} %copy.56), kind=kOutput, calls=%fused_computation.9 | convolution fusion | flops 137883648 | bytes 5259264 | tf_op jit(solution)/shard_map/nqgd,nkd->ngqk/dot_general | solution.py:322
  164.6 3.2 %fusion.17 = bf16[8,128,4,64]{1,3,2,0:T(8,128)(2,1)S(1)} fusion(f32[8,256,128,4]{2,1,3,0:T(8,128)} %get-tuple-element.32, f32[8,4,128]{2,1,0:T(4,128)S(1)} %add_log_fusion, pred[8,128,256]{1,2,0:T(8,128)(4,1)S(1)} %copy-done.11, bf16[8,128,64]{1,2,0:T(8,128)(2,1)} %copy.55, bf16[8,128,64]{1,2,0:T(8,128)(2,1)S(1)} %copy.54), kind=kOutput, calls=%fused_computation.19 | convolution fusion | flops 139198464 | bytes 5259264 | tf_op jit(solution)/shard_map/ngqk,nkd->nqgd/dot_general | solution.py:335
  169.3 2.1 reshape.179
  175.9 2.4 %collective-permute-start.5 = (bf16[512,256]{1,0:T(8,128)(2,1)S(1)}, bf16[512,256]{1,0:T(8,128)(2,1)S(1)}, u32[]{:S(2)}, u32[]{:S(2)}) collective-permute-start(bf16[512,256]{1,0:T(8,128)(2,1)S(1)} %get-tuple-element.11), channel_id=1, source_target_pairs={{0,4},{4,0},{8,12},{12,8},{16,20},{20,16},{24,28},{28,24},{32,36},... | collective-permute-start | bytes 786440 | tf_op jit(solution)/shard_map/ppermute | solution.py:344
  179.6 5.7 %shard_map.135 = bf16[512,2048]{1,0:T(8,128)(2,1)S(1)} custom-call(s32[3]{0:T(128)S(1)} %pad_add_fusion.at_ref, bf16[512,512]{1,0:T(8,128)(2,1)S(1)} %maximum_select_fusion.1.conv_ref, bf16[512,512]{1,0:T(8,128)(2,1)S(1)} %maximum_select_fusion.2.attn_ref, bf16[1024,1024]{1,0:T(8,128)(2,1)S(1)} %shard_map.134.own_ref, ...), custom_call_target="tpu_custom_call" | custom-call | flops 2147483648 | bytes 1048576 | tf_op jit(solution)/shard_map/pallas_call | solution.py:71
  186.6 4.4 %all-to-all-start.4 = ((bf16[4,128,2048]{2,1,0:T(8,128)(2,1)}), bf16[4,128,2048]{2,1,0:T(8,128)(2,1)S(1)}, u32[]{:S(2)}, u32[]{:S(2)}) async-start(bf16[4,128,2048]{2,1,0:T(8,128)(2,1)} %bitcast.65), calls=%async_computation.4 | async-start | bytes 4194304 | tf_op jit(solution)/shard_map/all_to_all | solution.py:369
  191.1 2.3 %collective-permute-start.15 = (f32[4,512]{1,0:T(4,128)S(1)}, f32[4,512]{1,0:T(4,128)S(1)}, u32[]{:S(2)}, u32[]{:S(2)}) collective-permute-start(f32[4,512]{1,0:T(4,128)S(1)} %get-tuple-element.15), channel_id=1, source_target_pairs={{0,4},{4,0},{8,12},{12,8},{16,20},{20,16},{24,28},{28,24},{32,36},... | collective-permute-start | bytes 24584 | tf_op jit(solution)/shard_map/ppermute | solution.py:344
  194.9 22.1 %all-to-all-done.4 = bf16[4,128,2048]{2,1,0:T(8,128)(2,1)S(1)} async-done(((bf16[4,128,2048]{2,1,0:T(8,128)(2,1)}), bf16[4,128,2048]{2,1,0:T(8,128)(2,1)S(1)}, u32[]{:S(2)}, u32[]{:S(2)}) %all-to-all-start.4) | async-done | bytes 2097184 | tf_op jit(solution)/shard_map/all_to_all | solution.py:369
  (101 shorter events, 39.1 us)
Async XLA Ops:
  0.6 22.8 %copy-start = (f32[31,512]{1,0:T(8,128)S(1)}, f32[31,512]{1,0:T(8,128)}, u32[]{:S(2)}) copy-start(f32[31,512]{1,0:T(8,128)} %param.19) | copy-start | bytes 190468
  0.6 70.8 %copy-start.12 = (f32[8]{0:T(128)S(1)}, f32[8]{0:T(128)}, u32[]{:S(2)}) copy-start(f32[8]{0:T(128)} %param.21) | copy-start | bytes 100
  3.9 35.5 %all-to-all-start.2 = ((bf16[32,16,384]{2,1,0:T(8,128)(2,1)}), bf16[32,16,384]{2,1,0:T(8,128)(2,1)}, u32[]{:S(2)}, u32[]{:S(2)}) async-start(bf16[32,16,384]{2,1,0:T(8,128)(2,1)} %bitcast.11), calls=%async_computation.2 | async-start | bytes 786432 | tf_op jit(solution)/shard_map/all_to_all | solution.py:58
  21.2 91.0 %collective-permute-start = (bf16[512,2048]{1,0:T(8,128)(2,1)}, bf16[512,2048]{1,0:T(8,128)(2,1)}, u32[]{:S(2)}, u32[]{:S(2)}) collective-permute-start(bf16[512,2048]{1,0:T(8,128)(2,1)} %param.12), channel_id=1, source_target_pairs={{0,4},{4,0},{8,12},{12,8},{16,20},{20,16},{24,28},{28,24},{32,36},... | collective-permute-start | bytes 6291464 | tf_op jit(solution)/shard_map/ppermute | solution.py:200
  40.3 22.6 %all-to-all-start.3 = ((bf16[16,16,1024]{2,1,0:T(8,128)(2,1)}), bf16[16,16,1024]{2,1,0:T(8,128)(2,1)S(1)}, u32[]{:S(2)}, u32[]{:S(2)}) async-start(bf16[16,16,1024]{2,1,0:T(8,128)(2,1)} %broadcast_in_dim.25), calls=%async_computation.3 | async-start | bytes 1048576 | tf_op jit(solution)/shard_map/all_to_all | solution.py:58
  63.7 41.0 %all-to-all-start = ((bf16[32,16,512]{2,1,0:T(8,128)(2,1)}), bf16[32,16,512]{2,1,0:T(8,128)(2,1)}, u32[]{:S(2)}, u32[]{:S(2)}) async-start(bf16[32,16,512]{2,1,0:T(8,128)(2,1)} %bitcast.5), calls=%async_computation | async-start | bytes 1048576 | tf_op jit(solution)/shard_map/all_to_all | solution.py:58
  73.3 18.1 %collective-permute-start.11 = (bf16[256,1024]{1,0:T(8,128)(2,1)S(1)}, bf16[256,1024]{1,0:T(8,128)(2,1)S(1)}, u32[]{:S(2)}, u32[]{:S(2)}) collective-permute-start(bf16[256,1024]{1,0:T(8,128)(2,1)S(1)} %bitcast.61), channel_id=1, source_target_pairs={{0,8},{4,60},{8,0},{12,20},{16,24},{20,12},{24,16},{28,36},{32,40}... | collective-permute-start | bytes 1572872 | tf_op jit(solution)/shard_map/ppermute | solution.py:218
  77.2 21.6 %collective-permute-start.12 = (bf16[256,1024]{1,0:T(8,128)(2,1)S(1)}, bf16[256,1024]{1,0:T(8,128)(2,1)S(1)}, u32[]{:S(2)}, u32[]{:S(2)}) collective-permute-start(bf16[256,1024]{1,0:T(8,128)(2,1)S(1)} %bitcast.62), channel_id=1, source_target_pairs={{0,64},{4,452},{8,72},{12,460},{16,80},{20,468},{24,88},{28,476},{... | collective-permute-start | bytes 1572872 | tf_op jit(solution)/shard_map/ppermute | solution.py:218
  83.8 20.9 %collective-permute-start.13 = (bf16[256,1024]{1,0:T(8,128)(2,1)S(1)}, bf16[256,1024]{1,0:T(8,128)(2,1)S(1)}, u32[]{:S(2)}, u32[]{:S(2)}) collective-permute-start(bf16[256,1024]{1,0:T(8,128)(2,1)S(1)} %bitcast.63), channel_id=1, source_target_pairs={{0,72},{4,508},{8,64},{12,468},{16,88},{20,460},{24,80},{28,484},{... | collective-permute-start | bytes 1572872 | tf_op jit(solution)/shard_map/ppermute | solution.py:218
  86.9 50.3 %collective-permute-start.6 = (bf16[512,384]{1,0:T(8,128)(2,1)}, bf16[512,384]{1,0:T(8,128)(2,1)}, u32[]{:S(2)}, u32[]{:S(2)}) collective-permute-start(bf16[512,384]{1,0:T(8,128)(2,1)} %bitcast.12.a_ref), channel_id=1, source_target_pairs={{0,8},{4,60},{8,0},{12,20},{16,24},{20,12},{24,16},{28,36},{32,40}... | collective-permute-start | bytes 1179656 | tf_op jit(solution)/shard_map/ppermute | solution.py:218
  92.1 45.1 %collective-permute-start.7 = (bf16[512,384]{1,0:T(8,128)(2,1)}, bf16[512,384]{1,0:T(8,128)(2,1)}, u32[]{:S(2)}, u32[]{:S(2)}) collective-permute-start(bf16[512,384]{1,0:T(8,128)(2,1)} %bitcast.12.a_ref), channel_id=1, source_target_pairs={{0,64},{4,452},{8,72},{12,460},{16,80},{20,468},{24,88},{28,476},{... | collective-permute-start | bytes 1179656 | tf_op jit(solution)/shard_map/ppermute | solution.py:218
  98.8 0.8 copy-start.6
  99.6 37.6 %collective-permute-start.8 = (bf16[512,384]{1,0:T(8,128)(2,1)}, bf16[512,384]{1,0:T(8,128)(2,1)}, u32[]{:S(2)}, u32[]{:S(2)}) collective-permute-start(bf16[512,384]{1,0:T(8,128)(2,1)} %bitcast.12.a_ref), channel_id=1, source_target_pairs={{0,72},{4,508},{8,64},{12,468},{16,88},{20,460},{24,80},{28,484},{... | collective-permute-start | bytes 1179656 | tf_op jit(solution)/shard_map/ppermute | solution.py:218
  105.5 12.8 %collective-permute-start.1 = (bf16[512,512]{1,0:T(8,128)(2,1)}, bf16[512,512]{1,0:T(8,128)(2,1)S(1)}, u32[]{:S(2)}, u32[]{:S(2)}) collective-permute-start(bf16[512,512]{1,0:T(8,128)(2,1)} %bitcast.6.a_ref), channel_id=1, source_target_pairs={{0,8},{4,60},{8,0},{12,20},{16,24},{20,12},{24,16},{28,36},{32,40}... | collective-permute-start | bytes 1572872 | tf_op jit(solution)/shard_map/ppermute | solution.py:218
  108.4 1.0 copy-start.5
  109.4 1.0 copy-start.7
  110.5 1.0 copy-start.9
  111.5 3.6 %copy-start.10 = (bf16[512,2048]{1,0:T(8,128)(2,1)S(1)}, bf16[512,2048]{1,0:T(8,128)(2,1)}, u32[]{:S(2)}) copy-start(bf16[512,2048]{1,0:T(8,128)(2,1)} %param.12) | copy-start | bytes 6291460
  112.2 14.3 %collective-permute-start.2 = (bf16[512,512]{1,0:T(8,128)(2,1)}, bf16[512,512]{1,0:T(8,128)(2,1)S(1)}, u32[]{:S(2)}, u32[]{:S(2)}) collective-permute-start(bf16[512,512]{1,0:T(8,128)(2,1)} %bitcast.6.a_ref), channel_id=1, source_target_pairs={{0,64},{4,452},{8,72},{12,460},{16,80},{20,468},{24,88},{28,476},{... | collective-permute-start | bytes 1572872 | tf_op jit(solution)/shard_map/ppermute | solution.py:218
  118.3 13.5 %collective-permute-start.3 = (bf16[512,512]{1,0:T(8,128)(2,1)}, bf16[512,512]{1,0:T(8,128)(2,1)S(1)}, u32[]{:S(2)}, u32[]{:S(2)}) collective-permute-start(bf16[512,512]{1,0:T(8,128)(2,1)} %bitcast.6.a_ref), channel_id=1, source_target_pairs={{0,72},{4,508},{8,64},{12,468},{16,88},{20,460},{24,80},{28,484},{... | collective-permute-start | bytes 1572872 | tf_op jit(solution)/shard_map/ppermute | solution.py:218
  126.5 10.8 %copy-start.2 = (f32[1024,128]{1,0:T(8,128)S(1)}, f32[1024,128]{1,0:T(8,128)}, u32[]{:S(2)}) copy-start(f32[1024,128]{1,0:T(8,128)} %get-tuple-element.36.sin_ref) | copy-start | bytes 1572868
  126.6 53.0 %collective-permute-start.14 = (bf16[1024,1024]{1,0:T(8,128)(2,1)S(1)}, bf16[1024,1024]{1,0:T(8,128)(2,1)}, u32[]{:S(2)}, u32[]{:S(2)}) collective-permute-start(bf16[1024,1024]{1,0:T(8,128)(2,1)S(1)} %shard_map.134.own_ref), channel_id=1, source_target_pairs={{0,4},{4,0},{8,12},{12,8},{16,20},{20,16},{24,28},{28,24},{32,36},... | collective-permute-start | bytes 6291464 | tf_op jit(solution)/shard_map/ppermute | solution.py:236
  136.0 14.0 %collective-permute-start.4 = (bf16[32,256]{1,0:T(8,128)(2,1)S(1)}, bf16[32,256]{1,0:T(8,128)(2,1)S(1)}, u32[]{:S(2)}, u32[]{:S(2)}) collective-permute-start(bf16[32,256]{1,0:T(8,128)(2,1)S(1)} %slice.106), channel_id=1, source_target_pairs={{0,8},{4,12},{8,16},{12,20},{16,24},{20,28},{24,32},{28,36},{32,40... | collective-permute-start | bytes 49160 | tf_op jit(solution)/shard_map/ppermute | solution.py:285
  146.7 13.0 %collective-permute-start.9 = (bf16[128,128]{1,0:T(8,128)(2,1)S(1)}, bf16[128,128]{1,0:T(8,128)(2,1)S(1)}, u32[]{:S(2)}, u32[]{:S(2)}) collective-permute-start(bf16[128,128]{1,0:T(8,128)(2,1)S(1)} %slice.109), channel_id=1, source_target_pairs={{0,8},{4,12},{8,16},{12,20},{16,24},{20,28},{24,32},{28,36},{32,40... | collective-permute-start | bytes 98312 | tf_op jit(solution)/shard_map/ppermute | solution.py:286
  153.6 1.0 copy-start.3
  155.3 18.1 %all-to-all-start.1 = ((f32[8,2,1024]{2,1,0:T(2,128)}), f32[8,2,1024]{2,1,0:T(2,128)}, u32[]{:S(2)}, u32[]{:S(2)}) async-start(f32[8,2,1024]{2,1,0:T(2,128)} %broadcast_in_dim.21), calls=%async_computation.1 | async-start | bytes 131072 | tf_op jit(solution)/shard_map/all_to_all | solution.py:305
  159.8 4.8 %copy-start.11 = (pred[8,128,256]{1,2,0:T(8,128)(4,1)S(1)}, pred[8,128,256]{1,2,0:T(8,128)(4,1)}, u32[]{:S(2)}) copy-start(pred[8,128,256]{1,2,0:T(8,128)(4,1)} %broadcast_and_fusion) | copy-start | bytes 786436
  171.4 6.9 %collective-permute-start.10 = (bf16[512,256]{1,0:T(8,128)(2,1)S(1)}, bf16[512,256]{1,0:T(8,128)(2,1)S(1)}, u32[]{:S(2)}, u32[]{:S(2)}) collective-permute-start(bf16[512,256]{1,0:T(8,128)(2,1)S(1)} %get-tuple-element.9), channel_id=1, source_target_pairs={{0,4},{4,0},{8,12},{12,8},{16,20},{20,16},{24,28},{28,24},{32,36},... | collective-permute-start | bytes 786440 | tf_op jit(solution)/shard_map/ppermute | solution.py:344
  175.9 3.6 %collective-permute-start.5 = (bf16[512,256]{1,0:T(8,128)(2,1)S(1)}, bf16[512,256]{1,0:T(8,128)(2,1)S(1)}, u32[]{:S(2)}, u32[]{:S(2)}) collective-permute-start(bf16[512,256]{1,0:T(8,128)(2,1)S(1)} %get-tuple-element.11), channel_id=1, source_target_pairs={{0,4},{4,0},{8,12},{12,8},{16,20},{20,16},{24,28},{28,24},{32,36},... | collective-permute-start | bytes 786440 | tf_op jit(solution)/shard_map/ppermute | solution.py:344
  185.3 1.4 copy-start.1
  186.6 30.4 %all-to-all-start.4 = ((bf16[4,128,2048]{2,1,0:T(8,128)(2,1)}), bf16[4,128,2048]{2,1,0:T(8,128)(2,1)S(1)}, u32[]{:S(2)}, u32[]{:S(2)}) async-start(bf16[4,128,2048]{2,1,0:T(8,128)(2,1)} %bitcast.65), calls=%async_computation.4 | async-start | bytes 4194304 | tf_op jit(solution)/shard_map/all_to_all | solution.py:369
  191.1 3.2 %collective-permute-start.15 = (f32[4,512]{1,0:T(4,128)S(1)}, f32[4,512]{1,0:T(4,128)S(1)}, u32[]{:S(2)}, u32[]{:S(2)}) collective-permute-start(f32[4,512]{1,0:T(4,128)S(1)} %get-tuple-element.15), channel_id=1, source_target_pairs={{0,4},{4,0},{8,12},{12,8},{16,20},{20,16},{24,28},{28,24},{32,36},... | collective-permute-start | bytes 24584 | tf_op jit(solution)/shard_map/ppermute | solution.py:344
  (2 other events, 1.6 us)
where the time goes:
time: 223 us; the launch traced here: 218 us
  starting transfers between devices  91.4 us (41%)
  waiting for transfers between devices  56.5 us (25%)
  local copies, waits for them, and re-layouts  24.9 us (11%)
  Pallas kernels  19.1 us (9%)
  other arithmetic  17.7 us (8%)
  matrix products  7.56 us (3%)
    ppermute x9, starting transfers between devices, from_square(): return (own, *(lax.ppermute(own, SP, pairs) for pairs in NEAR))  39.3 us
    all_to_all x3, waiting for transfers between devices, exchanged(): lax.all_to_all(pieces, SP, 0, 0, tiled=True, axis_index_groups=groups)  29.3 us
    all_to_all x3, starting transfers between devices, exchanged(): lax.all_to_all(pieces, SP, 0, 0, tiled=True, axis_index_groups=groups)  28.5 us
    all_to_all x1, waiting for transfers between devices, layer(): lax.all_to_all(partial.reshape(peers, own_rows // peers, -1), 'tp', split...  22.1 us
    pallas_call x5, Pallas kernels, call(): pl.pallas_call(body, out_shape=outs, in_specs=[SMEM] + [VMEM] * (len(oper...  19.1 us
    unnamed x26, local copies, waits for them, and re-layouts  7.84 us
    ppermute x3, starting transfers between devices, swapped(): return (kept, lax.ppermute(given, SP, OTHER_CORE))  6.66 us
  transfers between devices with their start and end apart: 21, of which 7 were waited for; matrix products, arithmetic and copies ran while one was open for 17% of the time, Pallas kernels for 6%

commit v1 on v0

v1 whole, which is shorter than its diff:
```python
import functools

import jax
import jax.numpy as jnp
from jax import lax
from jax.experimental import pallas as pl
from jax.experimental.pallas import tpu as pltpu
from jax.sharding import Mesh, PartitionSpec as P

CONV_CH = 2048
HEAD_DIM = 64
WINDOW = 128

NORM_EPS = 1e-06
CHANNEL_EPS = 1e-05
ROPE_BASE = 10000.0

SIDE = 8
CHIPS = SIDE * SIDE
CORES = 2
SP = ("chip", "core")
CHIP = ("core", "tp")


def place(z, y, core):
    return ((z % SIDE) * SIDE + y % SIDE) * CORES + core


def at_line(line, step, core):
    return place(line, step, core) if core == 0 else place(step, line, core)


LINES = [[at_line(i, j, c) for j in range(SIDE)] for c in range(CORES) for i in range(SIDE)]
AHEAD, BEHIND = (
    [
        (at_line(i, j, c), at_line(i + by, j, c))
        for c in range(CORES)
        for i in range(SIDE)
        for j in range(SIDE)
    ]
    for by in (1, -1)
)
OTHER_CORE = [(i, i ^ 1) for i in range(CHIPS * CORES)]
NEXT_CHIP = [(i, i + CORES) for i in range(CHIPS * CORES - CORES)]

VMEM = pl.BlockSpec(memory_space=pltpu.VMEM)
SMEM = pl.BlockSpec(memory_space=pltpu.SMEM)
ANY = pl.BlockSpec(memory_space=pl.ANY)
TILE = 256


def call(body, outs, flops, in_specs, operands, scratch=(), limit=12):
    return pl.pallas_call(
        body,
        out_shape=outs,
        in_specs=in_specs,
        out_specs=jax.tree.map(lambda _: VMEM, outs),
        scratch_shapes=list(scratch),
        compiler_params=pltpu.CompilerParams(vmem_limit_bytes=limit << 20),
        cost_estimate=pl.CostEstimate(flops=flops, bytes_accessed=1 << 20, transcendentals=0),
    )(*operands)


def shape(dims, dtype=jnp.bfloat16):
    return jax.ShapeDtypeStruct(dims, dtype)


def pack_kernel(at_ref, value_ref, gate_ref, query_ref, key_ref, v_ref, conv_ref, attn_ref, out_ref):
    core = at_ref[3]
    lane = lax.broadcasted_iota(jnp.int32, key_ref.shape, 1)
    key = key_ref[...].astype(jnp.float32)
    value = v_ref[...].astype(jnp.float32)
    both = (
        jnp.where(lane < HEAD_DIM, key, pltpu.roll(value, HEAD_DIM, 1)),
        jnp.where(lane < HEAD_DIM, pltpu.roll(key, HEAD_DIM, 1), value),
    )
    for half in range(CORES):
        to = jnp.bitwise_xor(core, half)
        at = 0
        for source in (value_ref, gate_ref, query_ref, None, conv_ref, attn_ref):
            if source is None:
                part = both[half].astype(jnp.bfloat16)
            else:
                width = source.shape[1] // CORES
                part = source[:, half * width : (half + 1) * width]
            out_ref[to, :, at : at + part.shape[1]] = part
            at += part.shape[1]


def repeat_kernel(at_ref, kept_ref, got_ref, out_ref):
    core, rows = at_ref[3], kept_ref.shape[0]
    for source, to_core in ((kept_ref, core), (got_ref, 1 - core)):
        to = pl.ds(pl.multiple_of(to_core * rows, rows), rows)
        for member in range(out_ref.shape[0]):
            out_ref[member, to, :] = source[...]


def fetch(at_ref, pieces, out_ref, sem, columns):
    block = pieces[0].shape[1]
    line, line_rows, step_rows = at_ref[0], at_ref[1], at_ref[2]
    for index, piece in enumerate(pieces):
        away = (index + 1) // 2 * (1 if index % 2 == 0 else -1)
        from_line = jnp.bitwise_and(line + away, SIDE - 1)
        count = piece.shape[0]
        first = SIDE - count if index == SIDE else 0
        for step in range(count):
            to = pl.multiple_of(from_line * line_rows + (first + step) * step_rows, block)
            pltpu.make_async_copy(
                piece.at[step, :, pl.ds(*columns)], out_ref.at[pl.ds(to, block), :], sem
            ).start()
    pltpu.make_async_copy(out_ref, out_ref, sem).wait()


def gated_kernel(columns, at_ref, x_ref, *refs):
    pieces, (out_ref, w_ref, sem) = refs[:-3], refs[-3:]
    fetch(at_ref, pieces, w_ref, sem, columns)
    half = out_ref.shape[1]

    @pl.loop(0, x_ref.shape[0] // TILE)
    def _(step):
        rows = pl.ds(pl.multiple_of(step * TILE, TILE), TILE)
        both = jnp.dot(x_ref[rows, :], w_ref[...], preferred_element_type=jnp.float32)
        both = both.astype(jnp.bfloat16).astype(jnp.float32)
        out_ref[rows, :] = (both[:, :half] * jax.nn.sigmoid(both[:, half:])).astype(jnp.bfloat16)


def rotated_kernel(columns, at_ref, x_ref, cos_ref, sin_ref, *refs):
    pieces, (out_ref, w_ref, sem) = refs[:-3], refs[-3:]
    fetch(at_ref, pieces, w_ref, sem, columns)
    width = out_ref.shape[1]

    @pl.loop(0, x_ref.shape[0] // TILE)
    def _(step):
        rows = pl.ds(pl.multiple_of(step * TILE, TILE), TILE)
        raw = jnp.dot(x_ref[rows, :], w_ref[...], preferred_element_type=jnp.float32)
        raw = raw.astype(jnp.bfloat16).astype(jnp.float32)
        lane = lax.broadcasted_iota(jnp.int32, (TILE, 128), 1)
        front = jnp.bitwise_and(lane, HEAD_DIM - 1) < HEAD_DIM // 2
        cosine, sine = cos_ref[rows, :], sin_ref[rows, :]
        for at in range(0, width, 128):
            part = raw[:, at : at + 128]
            other = jnp.where(
                front,
                pltpu.roll(part, 128 - HEAD_DIM // 2, 1),
                pltpu.roll(part, HEAD_DIM // 2, 1),
            )
            turned = part * cosine + other * sine
            if at + 128 == width:
                turned = jnp.where(lane < HEAD_DIM, turned, part)
            out_ref[rows, at : at + 128] = turned.astype(jnp.bfloat16)


def order_kernel(columns, at_ref, *refs):
    pieces, (out_ref, sem) = refs[:-2], refs[-2:]
    fetch(at_ref, pieces, out_ref, sem, columns)


def conv_kernel(before_ref, glu_ref, taps_ref, out_ref, sums_ref, ext_ref):
    count, rows = taps_ref.shape[0], glu_ref.shape[0]
    lead = before_ref.shape[0]
    for part in range(2):
        lanes = pl.ds(part * 128, 128)
        ext_ref[part, pl.ds(0, lead), :] = before_ref[:, lanes].astype(jnp.float32)
        ext_ref[part, pl.ds(lead, rows), :] = glu_ref[:, lanes].astype(jnp.float32)

    @pl.loop(0, rows // 128)
    def _(step):
        base = pl.multiple_of(step * 128, 128)
        first = jnp.zeros((128, 128), jnp.float32)
        second = jnp.zeros((128, 128), jnp.float32)
        for part in range(2):
            lanes = pl.ds(part * 128, 128)
            total = jnp.zeros((128, 128), jnp.float32)
            for tap in range(count):
                rows_at = pl.ds(base + (lead - count + 1 + tap), 128)
                total = total + taps_ref[pl.ds(tap, 1), lanes] * ext_ref[part, rows_at, :]
            out_ref[pl.ds(base, 128), lanes] = total
            first = first + total
            second = second + total * total
        sums_ref[pl.ds(0, 1), pl.ds(base, 128)] = jnp.sum(first.T, axis=0, keepdims=True)
        sums_ref[pl.ds(1, 1), pl.ds(base, 128)] = jnp.sum(second.T, axis=0, keepdims=True)


def scaled_kernel(at_ref, conv_ref, sums_ref, gain_ref, kept_ref, given_ref):
    core = at_ref[3]
    totals = sums_ref[0]
    for member in range(1, sums_ref.shape[0]):
        totals = totals + sums_ref[member]
    mean = totals[0:1] / CONV_CH
    scale = lax.rsqrt(totals[1:2] / CONV_CH - mean * mean + CHANNEL_EPS)
    half = kept_ref.shape[0]
    for base in range(0, conv_ref.shape[0], 128):
        at = slice(base, base + 128)
        mean_at = jnp.broadcast_to(mean[:, at], (128, 128)).T
        scale_at = jnp.broadcast_to(scale[:, at], (128, 128)).T
        parts = []
        for lanes in (slice(0, 128), slice(128, 256)):
            normed = (conv_ref[at, lanes] - mean_at) * scale_at * gain_ref[0:1, lanes]
            parts.append((normed * jax.nn.sigmoid(normed)).astype(jnp.bfloat16))
        out = jnp.concatenate(parts, axis=1)
        to = slice(base % half, base % half + 128)

        @pl.when(core == base // half)
        def _():
            kept_ref[to, :] = out

        @pl.when(core != base // half)
        def _():
            given_ref[to, :] = out


def attention_kernel(
    at_ref, sinks_ref, qkv_ref, before_ref, kept_ref, given_ref, logs_ref, k_lo, k_hi, v_lo, v_hi
):
    core, first_chip = at_ref[3], at_ref[4]
    cols = kept_ref.shape[1]
    lead = before_ref.shape[0]
    for source, to in ((before_ref, 0), (qkv_ref, lead)):
        both = source[:, source.shape[1] - 128 :].astype(jnp.float32)
        low = lax.broadcasted_iota(jnp.int32, both.shape, 1) < HEAD_DIM
        turned = pltpu.roll(both, HEAD_DIM, 1)
        rows = slice(to, to + both.shape[0])
        k_lo[rows, :] = jnp.where(low, both, 0.0).astype(jnp.bfloat16)
        k_hi[rows, :] = jnp.where(low, 0.0, turned).astype(jnp.bfloat16)
        v_lo[rows, :] = jnp.where(low, turned, 0.0).astype(jnp.bfloat16)
        v_hi[rows, :] = jnp.where(low, 0.0, both).astype(jnp.bfloat16)
    blocks = qkv_ref.shape[0] // WINDOW
    half_blocks = blocks // CORES
    heads = cols // HEAD_DIM

    @pl.loop(0, blocks)
    def _(block):
        base = pl.multiple_of(block * WINDOW, WINDOW)
        window = pl.ds(base, 2 * WINDOW)
        key_at = lax.broadcasted_iota(jnp.int32, (2 * WINDOW, WINDOW), 0)
        query_at = lax.broadcasted_iota(jnp.int32, (2 * WINDOW, WINDOW), 1)
        lowest = jnp.where((first_chip == 1) & (block == 0), WINDOW, 0)
        allowed = (key_at > query_at) & (key_at <= query_at + WINDOW) & (key_at >= lowest)
        outs = []
        for pair in range(heads // 2):
            query = qkv_ref[pl.ds(base, WINDOW), pair * 128 : (pair + 1) * 128]
            total = jnp.zeros((WINDOW, 128), jnp.float32)
            for which, (keys, values) in enumerate(((k_lo, v_lo), (k_hi, v_hi))):
                head = 2 * pair + which
                scores = (
                    lax.dot_general(
                        keys[window, :],
                        query,
                        (((1,), (1,)), ((), ())),
                        preferred_element_type=jnp.float32,
                    )
                    * HEAD_DIM ** (-0.5)
                )
                sums = jnp.sum(jnp.where(allowed, jnp.exp(scores), 0.0), axis=0, keepdims=True)
                sink = jnp.full((1, WINDOW), sinks_ref[core * heads + head], jnp.float32)
                log_total = jnp.log(sums + jnp.exp(sink))
                logs_ref[pl.ds(head, 1), pl.ds(base, WINDOW)] = log_total
                weights = jnp.where(allowed, jnp.exp(scores - log_total), 0.0).astype(jnp.bfloat16)
                total = total + lax.dot_general(
                    weights,
                    values[window, :],
                    (((0,), (0,)), ((), ())),
                    preferred_element_type=jnp.float32,
                )
            outs.append(total.astype(jnp.bfloat16))
        out = jnp.concatenate(outs, axis=1)
        own = block // half_blocks == core
        to = pl.ds(pl.multiple_of((block % half_blocks) * WINDOW, WINDOW), WINDOW)

        @pl.when(own)
        def _():
            kept_ref[to, :] = out

        @pl.when(jnp.logical_not(own))
        def _():
            given_ref[to, :] = out


def output_kernel(
    steps, at_ref, conv_ref, attn_ref, conv_got, attn_got, own_ref, other_ref, *out_refs
):
    member, half = at_ref[5], conv_ref.shape[1]
    peers = conv_ref.shape[0] // out_refs[0].shape[0]
    count = out_refs[0].shape[0]
    for away, out_ref in zip(steps, out_refs):
        to = jnp.bitwise_and(member + away, peers - 1)
        rows = pl.ds(pl.multiple_of(to * count, count), count)

        @pl.loop(0, out_ref.shape[1] // TILE)
        def _(step):
            cols = pl.ds(pl.multiple_of(step * TILE, TILE), TILE)
            total = jnp.zeros((count, TILE), jnp.float32)
            for left, right, at in (
                (conv_ref, own_ref, 0),
                (attn_ref, own_ref, half),
                (conv_got, other_ref, 0),
                (attn_got, other_ref, half),
            ):
                total = total + lax.dot_general(
                    left[rows, :],
                    right[cols, at : at + half],
                    (((1,), (1,)), ((), ())),
                    preferred_element_type=jnp.float32,
                )
            out_ref[:, cols] = total.astype(jnp.bfloat16)


def layer(
    tokens,
    norm_gain,
    w_conv_value,
    w_conv_gate,
    w_query,
    w_key,
    w_value,
    conv_taps,
    ln_gain,
    sinks,
    out_conv,
    out_attn,
):
    core = lax.axis_index("core")
    chip = lax.axis_index("chip")
    member = lax.axis_index("tp")
    own_rows, model = tokens.shape
    row_count = own_rows * CORES
    depth = w_conv_value.shape[0]
    channels = w_conv_value.shape[1] // CORES
    q_cols = w_query.shape[1] // CORES
    query_heads = q_cols // HEAD_DIM
    block = CORES * depth

    z, y = chip // SIDE, chip % SIDE
    at = jnp.stack(
        [
            jnp.where(core == 0, z, y),
            jnp.where(core == 0, SIDE * block, block),
            jnp.where(core == 0, block, SIDE * block),
            core,
            (chip == 0).astype(jnp.int32),
            member,
        ]
    ).astype(jnp.int32)

    conv_cols = (0, 2 * channels)
    qkv_cols = (2 * channels, q_cols + 2 * HEAD_DIM)
    out_cols = (2 * channels + q_cols + 2 * HEAD_DIM, channels + q_cols)
    width = sum(out_cols)
    halves = call(
        pack_kernel,
        shape((CORES, depth, width)),
        1 << 20,
        [SMEM] + [VMEM] * 7,
        (at, w_conv_value, w_conv_gate, w_query, w_key, w_value, out_conv.T, out_attn.T),
    )
    got = lax.ppermute(halves[1], SP, OTHER_CORE)
    sent = call(
        repeat_kernel,
        shape((SIDE, block, width)),
        1 << 20,
        [SMEM, VMEM, VMEM],
        (at, halves[0], got),
    )
    own_line = lax.all_to_all(sent, SP, 0, 0, tiled=True, axis_index_groups=LINES)
    pieces = [own_line]
    ahead = behind = own_line
    for step in range(SIDE // 2):
        if step == SIDE // 2 - 1:
            ahead, behind = ahead[: SIDE // 2], behind[SIDE // 2 :]
        ahead = lax.ppermute(ahead, SP, AHEAD)
        behind = lax.ppermute(behind, SP, BEHIND)
        pieces += [ahead, behind]

    tokens_other = lax.ppermute(tokens, SP, OTHER_CORE)
    both = jnp.where(
        core == 0,
        jnp.concatenate([tokens, tokens_other], axis=0),
        jnp.concatenate([tokens_other, tokens], axis=0),
    )
    as_float = both.astype(jnp.float32)
    normed = (
        as_float
        * lax.rsqrt(jnp.mean(as_float * as_float, axis=-1, keepdims=True) + NORM_EPS)
        * norm_gain.astype(jnp.float32)
    ).astype(jnp.bfloat16)

    positions = chip * row_count + jnp.arange(row_count, dtype=jnp.int32)
    half_dim = HEAD_DIM // 2
    inverse = ROPE_BASE ** (-jnp.arange(half_dim, dtype=jnp.float32) / half_dim)
    angles = positions.astype(jnp.float32)[:, None] * inverse[None, :]
    cosine, sine = jnp.cos(angles), jnp.sin(angles)
    cosines = jnp.concatenate([cosine] * 4, axis=1)
    sines = jnp.concatenate([-sine, sine] * 2, axis=1)

    spots = [ANY] * len(pieces)
    glu = call(
        functools.partial(gated_kernel, conv_cols),
        shape((row_count, channels)),
        2 * row_count * model * conv_cols[1],
        [SMEM, VMEM] + spots,
        (at, normed, *pieces),
        (pltpu.VMEM((model, conv_cols[1]), jnp.bfloat16), pltpu.SemaphoreType.DMA),
    )
    glu_before = lax.ppermute(glu[row_count - 32 :], SP, NEXT_CHIP)
    qkv = call(
        functools.partial(rotated_kernel, qkv_cols),
        shape((row_count, qkv_cols[1])),
        2 * row_count * model * qkv_cols[1],
        [SMEM, VMEM, VMEM, VMEM] + spots,
        (at, normed, cosines, sines, *pieces),
        (pltpu.VMEM((model, qkv_cols[1]), jnp.bfloat16), pltpu.SemaphoreType.DMA),
    )
    kv_before = lax.ppermute(qkv[row_count - WINDOW :, q_cols:], SP, NEXT_CHIP)
    out_own = call(
        functools.partial(order_kernel, out_cols),
        shape((model, out_cols[1])),
        1 << 28,
        [SMEM] + spots,
        (at, *pieces),
        (pltpu.SemaphoreType.DMA,),
    )
    out_other = lax.ppermute(out_own, SP, OTHER_CORE)

    taps = lax.dynamic_slice_in_dim(conv_taps, core * channels, channels, 1)
    conv_out, sums = call(
        conv_kernel,
        (shape((row_count, channels), jnp.float32), shape((2, row_count), jnp.float32)),
        1 << 32,
        [VMEM] * 3,
        (glu_before, glu, taps),
        (pltpu.VMEM((2, row_count + 32, 128), jnp.float32),),
    )
    members = CORES * lax.axis_size("tp")
    everyones = lax.all_to_all(
        jnp.broadcast_to(sums[None], (members, *sums.shape)), CHIP, 0, 0, tiled=True
    )
    extended = pltpu.VMEM((row_count + WINDOW, 128), jnp.bfloat16)
    attn_kept, attn_given, log_rows = call(
        attention_kernel,
        (
            shape((own_rows, q_cols)),
            shape((own_rows, q_cols)),
            shape((query_heads, row_count), jnp.float32),
        ),
        1 << 32,
        [SMEM, SMEM, VMEM, VMEM],
        (at, sinks, qkv, kv_before),
        (extended,) * 4,
    )
    attn_got = lax.ppermute(attn_given, SP, OTHER_CORE)
    gain = lax.dynamic_slice_in_dim(ln_gain, core * channels, channels, 0)
    conv_kept, conv_given = call(
        scaled_kernel,
        (shape((own_rows, channels)),) * 2,
        1 << 28,
        [SMEM, VMEM, VMEM, VMEM],
        (at, conv_out, everyones, gain[None]),
    )
    conv_got = lax.ppermute(conv_given, SP, OTHER_CORE)

    kept = lax.dynamic_slice_in_dim(log_rows, core * own_rows, own_rows, 1)
    given = lax.dynamic_slice_in_dim(log_rows, (1 - core) * own_rows, own_rows, 1)
    logs_got = lax.ppermute(given, SP, OTHER_CORE)
    log_sums = jnp.where(
        core == 0,
        jnp.concatenate([kept, logs_got], axis=0),
        jnp.concatenate([logs_got, kept], axis=0),
    )

    peers = lax.axis_size("tp")
    share = own_rows // peers

    def output(steps):
        return call(
            functools.partial(output_kernel, steps),
            (shape((share, model)),) * len(steps),
            2 * share * len(steps) * model * 2 * out_cols[1],
            [SMEM] + [VMEM] * 6,
            (at, conv_kept, attn_kept, conv_got, attn_got, out_own, out_other),
        )

    def to_member(value, away):
        return lax.ppermute(value, "tp", [(i, (i + away) % peers) for i in range(peers)])

    (far,) = output((2,))
    far = to_member(far, 2)
    up, down, mine = output((1, 3, 0))
    up, down = to_member(up, 1), to_member(down, 3)
    mixed = (
        mine.astype(jnp.float32)
        + far.astype(jnp.float32)
        + up.astype(jnp.float32)
        + down.astype(jnp.float32)
    )
    return (mixed.astype(jnp.bfloat16), log_sums)


def solution(mesh):
    split = Mesh(mesh.devices.reshape(-1, CORES, mesh.shape["tp"]), ("chip", "core", "tp"))
    in_specs = (
        P(SP, None),
        P(),
        P(SP, "tp"),
        P(SP, "tp"),
        P(SP, "tp"),
        P(SP, "tp"),
        P(SP, "tp"),
        P(None, "tp"),
        P("tp"),
        P("tp"),
        P("tp", SP),
        P("tp", SP),
    )
    out_specs = (P((*SP, "tp"), None), P("tp", SP))
    return jax.shard_map(layer, mesh=split, in_specs=in_specs, out_specs=out_specs, check_vma=False)
```

time: 223 us -> 193 us (0.87); the launches traced: 218 us -> 191 us
  waiting for transfers between devices: 56.5 us -> 24.9 us
  Pallas kernels: 19.1 us -> 38.7 us
  blocking collectives: 0 us -> 18.7 us
  starting transfers between devices: 91.4 us -> 78.2 us
  local copies, waits for them, and re-layouts: 24.9 us -> 16.1 us
  matrix products: 7.56 us -> 0 us
  other arithmetic: 17.7 us -> 12.8 us
    all_to_all x5 -> x1, waiting for transfers between devices: 51.5 us -> 0.01 us  [layer(): lax.all_to_all(jnp.broadcast_to(sums[None], (members, *sums.shape)), CHIP...]
    all_to_all x5 -> x1, starting transfers between devices: 37.3 us -> 4.87 us  [layer(): lax.all_to_all(jnp.broadcast_to(sums[None], (members, *sums.shape)), CHIP...]
    ppermute x13 -> x16, waiting for transfers between devices: 5.03 us -> 24.9 us  [the longest x3 10.8 us: to_member(): lax.ppermute(value, 'tp', [(i, (i + away) % peers) for i in range(peers)])]
    pallas_call x5 -> x10, Pallas kernels: 19.1 us -> 38.7 us  [call(): pl.pallas_call(body, out_shape=outs, in_specs=in_specs, out_specs=jax.tre...]
    all_to_all x0 -> x1, blocking collectives: none -> 18.7 us  [layer(): lax.all_to_all(sent, SP, 0, 0, tiled=True, axis_index_groups=LINES)]
    ppermute x1, starting transfers between devices: 2.05 us -> 9.98 us  [layer(): out_other = lax.ppermute(out_own, SP, OTHER_CORE)]
    dot_general x2 -> x0, matrix products: 7.56 us -> none  [the longest x1 4.36 us: layer(): jnp.einsum('nqgd,nkd->ngqk', q_blocks, key_window, preferred_element_type...]
    slice x13 -> x3, local copies, waits for them, and re-layouts: 6.71 us -> 0.06 us  [the longest x2 0.06 us: layer(): ahead, behind = (ahead[:SIDE // 2], behind[SIDE // 2:])]
  transfers between devices with their start and end apart: 21 -> 20, of which waited for: 7 -> 9; matrix products, arithmetic and copies ran while one was open for 17% -> 6% of each run, Pallas kernels for 6% -> 14%
where the time goes in v1:
time: 193 us; the launch traced here: 191 us
  starting transfers between devices  78.2 us (41%)
  Pallas kernels  38.7 us (20%)
  waiting for transfers between devices  24.9 us (13%)
  blocking collectives  18.7 us (10%)
  local copies, waits for them, and re-layouts  16.1 us (8%)
  other arithmetic  12.8 us (7%)
    pallas_call x10, Pallas kernels, call(): pl.pallas_call(body, out_shape=outs, in_specs=in_specs, out_specs=jax.tre...  38.7 us
    all_to_all x1, blocking collectives, layer(): lax.all_to_all(sent, SP, 0, 0, tiled=True, axis_index_groups=LINES)  18.7 us
    ppermute x4, starting transfers between devices, layer(): behind = lax.ppermute(behind, SP, BEHIND)  17.5 us
    unnamed x54, local copies, waits for them, and re-layouts  14.4 us
    ppermute x3, waiting for transfers between devices, to_member(): lax.ppermute(value, 'tp', [(i, (i + away) % peers) for i in range(peers)])  10.8 us
    ppermute x3, starting transfers between devices, to_member(): lax.ppermute(value, 'tp', [(i, (i + away) % peers) for i in range(peers)])  10.3 us
    ppermute x4, waiting for transfers between devices, layer(): ahead = lax.ppermute(ahead, SP, AHEAD)  10.2 us
    ppermute x1, starting transfers between devices, layer(): out_other = lax.ppermute(out_own, SP, OTHER_CORE)  9.98 us
  transfers between devices with their start and end apart: 20, of which 9 were waited for; matrix products, arithmetic and copies ran while one was open for 6% of the time, Pallas kernels for 14%

profile of v1, /device:TPU:1, one launch (start us, length us, event | category | flops | bytes accessed | tf_op | source)
XLA Modules:
  0.0 190.7 jit_solution(3815995338196587854)
XLA Ops:
  6.4 8.7 %collective-permute-start.1 = (bf16[16,1408]{1,0:T(8,128)(2,1)S(1)}, bf16[16,1408]{1,0:T(8,128)(2,1)S(1)}, u32[]{:S(2)}, u32[]{:S(2)}) collective-permute-start(bf16[16,1408]{1,0:T(8,128)(2,1)S(1)} %get-tuple-element.22), channel_id=1, source_target_pairs={{0,4},{4,0},{8,12},{12,8},{16,20},{20,16},{24,28},{28,24},{32,36},... | collective-permute-start | bytes 135176 | tf_op jit(solution)/shard_map/ppermute | solution.py:356
  16.6 18.7 %all_to_all.10.refs_0_ = bf16[8,32,1408]{2,1,0:T(8,128)(2,1)S(1)} all-to-all(bf16[8,32,1408]{2,1,0:T(8,128)(2,1)S(1)} %shard_map.132), channel_id=1, replica_groups={{0,8,16,24,32,40,48,56},{64,72,80,88,96,104,112,120},{128,136,144,152,1..., dimensions={0} | all-to-all | bytes 1441792 | tf_op jit(solution)/shard_map/all_to_all | solution.py:364
  35.3 3.2 %collective-permute-start.2 = (bf16[8,32,1408]{2,1,0:T(8,128)(2,1)S(1)}, bf16[8,32,1408]{2,1,0:T(8,128)(2,1)S(1)}, u32[]{:S(2)}, u32[]{:S(2)}) collective-permute-start(bf16[8,32,1408]{2,1,0:T(8,128)(2,1)S(1)} %all_to_all.10.refs_0_), channel_id=1, source_target_pairs={{0,64},{8,72},{16,80},{24,88},{32,96},{40,104},{48,112},{56,120},{... | collective-permute-start | bytes 2162696 | tf_op jit(solution)/shard_map/ppermute | solution.py:370
  38.5 3.8 %collective-permute-start.3 = (bf16[8,32,1408]{2,1,0:T(8,128)(2,1)S(1)}, bf16[8,32,1408]{2,1,0:T(8,128)(2,1)S(1)}, u32[]{:S(2)}, u32[]{:S(2)}) collective-permute-start(bf16[8,32,1408]{2,1,0:T(8,128)(2,1)S(1)} %all_to_all.10.refs_0_), channel_id=1, source_target_pairs={{0,448},{8,456},{16,464},{24,472},{32,480},{40,488},{48,496},{56,5... | collective-permute-start | bytes 2162696 | tf_op jit(solution)/shard_map/ppermute | solution.py:371
  42.3 6.4 %collective-permute-start = (bf16[512,2048]{1,0:T(8,128)(2,1)}, bf16[512,2048]{1,0:T(8,128)(2,1)}, u32[]{:S(2)}, u32[]{:S(2)}) collective-permute-start(bf16[512,2048]{1,0:T(8,128)(2,1)} %param.12), channel_id=1, source_target_pairs={{0,4},{4,0},{8,12},{12,8},{16,20},{20,16},{24,28},{28,24},{32,36},... | collective-permute-start | bytes 6291464 | tf_op jit(solution)/shard_map/ppermute | solution.py:374
  49.4 1.9 %collective-permute-start.4 = (bf16[8,32,1408]{2,1,0:T(8,128)(2,1)S(1)}, bf16[8,32,1408]{2,1,0:T(8,128)(2,1)S(1)}, u32[]{:S(2)}, u32[]{:S(2)}) collective-permute-start(bf16[8,32,1408]{2,1,0:T(8,128)(2,1)S(1)} %collective-permute-done.2.refs_1_), channel_id=1, source_target_pairs={{0,64},{8,72},{16,80},{24,88},{32,96},{40,104},{48,112},{56,120},{... | collective-permute-start | bytes 2162696 | tf_op jit(solution)/shard_map/ppermute | solution.py:370
  51.3 4.6 %collective-permute-start.5 = (bf16[8,32,1408]{2,1,0:T(8,128)(2,1)S(1)}, bf16[8,32,1408]{2,1,0:T(8,128)(2,1)}, u32[]{:S(2)}, u32[]{:S(2)}) collective-permute-start(bf16[8,32,1408]{2,1,0:T(8,128)(2,1)S(1)} %collective-permute-done.3.refs_2_), channel_id=1, source_target_pairs={{0,448},{8,456},{16,464},{24,472},{32,480},{40,488},{48,496},{56,5... | collective-permute-start | bytes 2162696 | tf_op jit(solution)/shard_map/ppermute | solution.py:371
  57.5 5.4 %collective-permute-done.4.refs_3_ = bf16[8,32,1408]{2,1,0:T(8,128)(2,1)S(1)} collective-permute-done((bf16[8,32,1408]{2,1,0:T(8,128)(2,1)S(1)}, bf16[8,32,1408]{2,1,0:T(8,128)(2,1)S(1)}, u32[]{:S(2)}, u32[]{:S(2)}) %collective-permute-start.4) | collective-permute-done | bytes 720928 | tf_op jit(solution)/shard_map/ppermute | solution.py:370
  64.8 4.6 %collective-permute-start.7 = (bf16[8,32,1408]{2,1,0:T(8,128)(2,1)}, bf16[8,32,1408]{2,1,0:T(8,128)(2,1)S(1)}, u32[]{:S(2)}, u32[]{:S(2)}) collective-permute-start(bf16[8,32,1408]{2,1,0:T(8,128)(2,1)} %collective-permute-done.5.refs_4_), channel_id=1, source_target_pairs={{0,448},{8,456},{16,464},{24,472},{32,480},{40,488},{48,496},{56,5... | collective-permute-start | bytes 2162696 | tf_op jit(solution)/shard_map/ppermute | solution.py:371
  72.2 4.2 %collective-permute-done.6.refs_5_ = bf16[8,32,1408]{2,1,0:T(8,128)(2,1)S(1)} collective-permute-done((bf16[8,32,1408]{2,1,0:T(8,128)(2,1)S(1)}, bf16[8,32,1408]{2,1,0:T(8,128)(2,1)S(1)}, u32[]{:S(2)}, u32[]{:S(2)}) %collective-permute-start.6) | collective-permute-done | bytes 720928 | tf_op jit(solution)/shard_map/ppermute | solution.py:370
  76.4 1.9 %collective-permute-start.8 = (bf16[4,32,1408]{2,1,0:T(8,128)(2,1)S(1)}, bf16[4,32,1408]{2,1,0:T(8,128)(2,1)S(1)}, u32[]{:S(2)}, u32[]{:S(2)}) collective-permute-start(bf16[4,32,1408]{2,1,0:T(8,128)(2,1)S(1)} %slice.26), channel_id=1, source_target_pairs={{0,64},{8,72},{16,80},{24,88},{32,96},{40,104},{48,112},{56,120},{... | collective-permute-start | bytes 1081352 | tf_op jit(solution)/shard_map/ppermute | solution.py:370
  78.4 4.6 %collective-permute-start.9 = (bf16[4,32,1408]{2,1,0:T(8,128)(2,1)S(1)}, bf16[4,32,1408]{2,1,0:T(8,128)(2,1)S(1)}, u32[]{:S(2)}, u32[]{:S(2)}) collective-permute-start(bf16[4,32,1408]{2,1,0:T(8,128)(2,1)S(1)} %slice.27), channel_id=1, source_target_pairs={{0,448},{8,456},{16,464},{24,472},{32,480},{40,488},{48,496},{56,5... | collective-permute-start | bytes 1081352 | tf_op jit(solution)/shard_map/ppermute | solution.py:371
  83.0 3.2 %fusion = f32[1024]{0:T(1024)S(1)} fusion(bf16[512,2048]{1,0:T(8,128)(2,1)S(1)} %copy-done.26, bf16[512,2048]{1,0:T(8,128)(2,1)} %collective-permute-done, pred[]{:T(512)S(6)} %eq.6), kind=kLoop, calls=%fused_computation.2 | loop fusion | flops 25164800 | bytes 4198401 | tf_op jit(solution)/shard_map/reduce_sum | solution.py:383
  92.5 10.0 %collective-permute-start.14 = (bf16[2048,512]{1,0:T(8,128)(2,1)S(1)}, bf16[2048,512]{1,0:T(8,128)(2,1)}, u32[]{:S(2)}, u32[]{:S(2)}) collective-permute-start(bf16[2048,512]{1,0:T(8,128)(2,1)S(1)} %shard_map.138.own_ref), channel_id=1, source_target_pairs={{0,4},{4,0},{8,12},{12,8},{16,20},{20,16},{24,28},{28,24},{32,36},... | collective-permute-start | bytes 6291464 | tf_op jit(solution)/shard_map/ppermute | solution.py:422
  102.5 3.2 %fusion.2.x_ref = bf16[1024,2048]{1,0:T(8,128)(2,1)S(1)} fusion(f32[2048]{0:T(1024)S(1)} %convert_element_type.33, f32[1024]{0:T(1024)S(1)} %add_rsqrt_fusion, bf16[512,2048]{1,0:T(8,128)(2,1)S(1)} %copy-done.26, bf16[512,2048]{1,0:T(8,128)(2,1)} %collective-permute-done, pred[]{:T(512)S(6)} %eq.6), kind=kLoop, calls=%fused_computation.4 | loop fusion | flops 27262976 | bytes 8400897 | tf_op jit(solution)/shard_map/convert_element_type | solution.py:385
  105.8 4.8 %shard_map.133.glu_ref = bf16[1024,256]{1,0:T(8,128)(2,1)S(1)} custom-call(s32[6]{0:T(128)S(1)} %stack.31.at_ref, bf16[1024,2048]{1,0:T(8,128)(2,1)S(1)} %fusion.2.x_ref, bf16[8,32,1408]{2,1,0:T(8,128)(2,1)S(1)} %all_to_all.10.refs_0_, bf16[8,32,1408]{2,1,0:T(8,128)(2,1)S(1)} %copy-done.3, bf16[8,32,1408]{2,1,0:T(8,128)(2,1)S(1)} %copy-done.6, ...), custom_call_target="tpu_custom_call" | custom-call | flops 2147483648 | bytes 1048576 | tf_op jit(solution)/shard_map/pallas_call | solution.py:53
  110.6 2.1 %collective-permute-start.10 = (bf16[32,256]{1,0:T(8,128)(2,1)S(1)}, bf16[32,256]{1,0:T(8,128)(2,1)S(1)}, u32[]{:S(2)}, u32[]{:S(2)}) collective-permute-start(bf16[32,256]{1,0:T(8,128)(2,1)S(1)} %slice.28), channel_id=1, source_target_pairs={{0,8},{4,12},{8,16},{12,20},{16,24},{20,28},{24,32},{28,36},{32,40... | collective-permute-start | bytes 49160 | tf_op jit(solution)/shard_map/ppermute | solution.py:404
  112.7 5.0 %shard_map.136.qkv_ref = bf16[1024,384]{1,0:T(8,128)(2,1)S(1)} custom-call(s32[6]{0:T(128)S(1)} %stack.31.at_ref, bf16[1024,2048]{1,0:T(8,128)(2,1)S(1)} %fusion.2.x_ref, f32[1024,128]{1,0:T(8,128)S(1)} %get-tuple-element.29.cos_ref, f32[1024,128]{1,0:T(8,128)S(1)} %get-tuple-element.30.sin_ref, bf16[8,32,1408]{2,1,0:T(8,128)(2,1)S(1)} %all_to_all.10.refs_0_, ...), custom_call_target="tpu_custom_call" | custom-call | flops 1610612736 | bytes 1048576 | tf_op jit(solution)/shard_map/pallas_call | solution.py:53
  118.6 2.0 %collective-permute-start.11 = (bf16[128,128]{1,0:T(8,128)(2,1)S(1)}, bf16[128,128]{1,0:T(8,128)(2,1)S(1)}, u32[]{:S(2)}, u32[]{:S(2)}) collective-permute-start(bf16[128,128]{1,0:T(8,128)(2,1)S(1)} %slice.29), channel_id=1, source_target_pairs={{0,8},{4,12},{8,16},{12,20},{16,24},{20,28},{24,32},{28,36},{32,40... | collective-permute-start | bytes 98312 | tf_op jit(solution)/shard_map/ppermute | solution.py:413
  120.7 3.4 %shard_map.134 = (f32[1024,256]{1,0:T(8,128)S(1)}, f32[2,1024]{1,0:T(2,128)S(1)}) custom-call(bf16[32,256]{1,0:T(8,128)(2,1)S(1)} %collective-permute-done.10.before_ref, bf16[1024,256]{1,0:T(8,128)(2,1)S(1)} %shard_map.133.glu_ref, f32[31,256]{1,0:T(8,128)S(1)} %constant_dynamic-slice_fusion.2.taps_ref), custom_call_target="tpu_custom_call" | custom-call | flops 4294967296 | bytes 1048576 | tf_op jit(solution)/shard_map/pallas_call | solution.py:53
  125.7 4.9 %all-to-all-start.1 = ((f32[8,2,1024]{2,1,0:T(2,128)}), f32[8,2,1024]{2,1,0:T(2,128)S(1)}, u32[]{:S(2)}, u32[]{:S(2)}) async-start(f32[8,2,1024]{2,1,0:T(2,128)} %broadcast_in_dim.4), calls=%async_computation.1 | async-start | bytes 131072 | tf_op jit(solution)/shard_map/all_to_all | solution.py:434
  131.7 7.2 %shard_map.137 = (bf16[512,256]{1,0:T(8,128)(2,1)S(1)}, bf16[512,256]{1,0:T(8,128)(2,1)S(1)}, f32[4,1024]{1,0:T(4,128)S(1)}) custom-call(s32[6]{0:T(128)S(1)} %stack.31.at_ref, f32[8]{0:T(128)S(1)} %copy-done.25, bf16[1024,384]{1,0:T(8,128)(2,1)S(1)} %copy-done.13, bf16[128,128]{1,0:T(8,128)(2,1)S(1)} %collective-permute-done.11.before_ref), custom_call_target="tpu_custom_call" | custom-call | flops 4294967296 | bytes 1048576 | tf_op jit(solution)/shard_map/pallas_call | solution.py:53
  138.9 1.9 %collective-permute-start.13 = (bf16[512,256]{1,0:T(8,128)(2,1)S(1)}, bf16[512,256]{1,0:T(8,128)(2,1)S(1)}, u32[]{:S(2)}, u32[]{:S(2)}) collective-permute-start(bf16[512,256]{1,0:T(8,128)(2,1)S(1)} %get-tuple-element.17), channel_id=1, source_target_pairs={{0,4},{4,0},{8,12},{12,8},{16,20},{20,16},{24,28},{28,24},{32,36},... | collective-permute-start | bytes 786440 | tf_op jit(solution)/shard_map/ppermute | solution.py:450
  143.5 2.4 %collective-permute-start.12 = (bf16[512,256]{1,0:T(8,128)(2,1)S(1)}, bf16[512,256]{1,0:T(8,128)(2,1)S(1)}, u32[]{:S(2)}, u32[]{:S(2)}) collective-permute-start(bf16[512,256]{1,0:T(8,128)(2,1)S(1)} %get-tuple-element.16), channel_id=1, source_target_pairs={{0,4},{4,0},{8,12},{12,8},{16,20},{20,16},{24,28},{28,24},{32,36},... | collective-permute-start | bytes 786440 | tf_op jit(solution)/shard_map/ppermute | solution.py:459
  147.1 9.7 %shard_map.139 = (bf16[128,2048]{1,0:T(8,128)(2,1)}, bf16[128,2048]{1,0:T(8,128)(2,1)}, bf16[128,2048]{1,0:T(8,128)(2,1)S(1)}) custom-call(s32[6]{0:T(128)S(1)} %stack.31.at_ref, bf16[512,256]{1,0:T(8,128)(2,1)S(1)} %get-tuple-element.14.conv_ref, bf16[512,256]{1,0:T(8,128)(2,1)S(1)} %get-tuple-element.15.attn_ref, ...), custom_call_target="tpu_custom_call" | custom-call | flops 1610612736 | bytes 1048576 | tf_op jit(solution)/shard_map/pallas_call | solution.py:53
  156.8 4.8 %collective-permute-start.17 = (bf16[128,2048]{1,0:T(8,128)(2,1)}, bf16[128,2048]{1,0:T(8,128)(2,1)}, u32[]{:S(2)}, u32[]{:S(2)}) collective-permute-start(bf16[128,2048]{1,0:T(8,128)(2,1)} %get-tuple-element.20), channel_id=1, source_target_pairs={{0,3},{1,0},{2,1},{3,2},{4,7},{5,4},{6,5},{7,6},{8,11},{9,8},{10,9... | collective-permute-start | bytes 1572872 | tf_op jit(solution)/shard_map/ppermute | solution.py:483
  161.6 1.9 %collective-permute-start.16 = (bf16[128,2048]{1,0:T(8,128)(2,1)}, bf16[128,2048]{1,0:T(8,128)(2,1)}, u32[]{:S(2)}, u32[]{:S(2)}) collective-permute-start(bf16[128,2048]{1,0:T(8,128)(2,1)} %get-tuple-element.19), channel_id=1, source_target_pairs={{0,1},{1,2},{2,3},{3,0},{4,5},{5,6},{6,7},{7,4},{8,9},{9,10},{10,1... | collective-permute-start | bytes 1572872 | tf_op jit(solution)/shard_map/ppermute | solution.py:483
  165.4 4.1 %shard_map.140 = bf16[128,2048]{1,0:T(8,128)(2,1)S(1)} custom-call(s32[6]{0:T(128)S(1)} %stack.31.at_ref, bf16[512,256]{1,0:T(8,128)(2,1)S(1)} %get-tuple-element.14.conv_ref, bf16[512,256]{1,0:T(8,128)(2,1)S(1)} %copy-done.15, bf16[512,256]{1,0:T(8,128)(2,1)S(1)} %collective-permute-done.12.conv_got, bf16[512,256]{1,0:T(8,128)(2,1)S(1)} %copy-done.17, ...), custom_call_target="tpu_custom_call" | custom-call | flops 536870912 | bytes 1048576 | tf_op jit(solution)/shard_map/pallas_call | solution.py:53
  169.5 3.6 %collective-permute-start.15 = (bf16[128,2048]{1,0:T(8,128)(2,1)S(1)}, bf16[128,2048]{1,0:T(8,128)(2,1)S(1)}, u32[]{:S(2)}, u32[]{:S(2)}) collective-permute-start(bf16[128,2048]{1,0:T(8,128)(2,1)S(1)} %shard_map.140), channel_id=1, source_target_pairs={{0,2},{1,3},{2,0},{3,1},{4,6},{5,7},{6,4},{7,5},{8,10},{9,11},{10,... | collective-permute-start | bytes 1572872 | tf_op jit(solution)/shard_map/ppermute | solution.py:483
  173.2 2.9 %collective-permute-start.18 = (f32[4,512]{1,0:T(4,128)S(1)}, f32[4,512]{1,0:T(4,128)S(1)}, u32[]{:S(2)}, u32[]{:S(2)}) collective-permute-start(f32[4,512]{1,0:T(4,128)S(1)} %get-tuple-element.25), channel_id=1, source_target_pairs={{0,4},{4,0},{8,12},{12,8},{16,20},{20,16},{24,28},{28,24},{32,36},... | collective-permute-start | bytes 24584 | tf_op jit(solution)/shard_map/ppermute | solution.py:463
  179.0 9.4 %collective-permute-done.15 = bf16[128,2048]{1,0:T(8,128)(2,1)S(1)} collective-permute-done((bf16[128,2048]{1,0:T(8,128)(2,1)S(1)}, bf16[128,2048]{1,0:T(8,128)(2,1)S(1)}, u32[]{:S(2)}, u32[]{:S(2)}) %collective-permute-start.15) | collective-permute-done | bytes 524320 | tf_op jit(solution)/shard_map/ppermute | solution.py:483
  188.4 2.3 %add_convert_fusion = bf16[128,2048]{1,0:T(8,128)(2,1)} fusion(bf16[128,2048]{1,0:T(8,128)(2,1)} %collective-permute-done.17, bf16[128,2048]{1,0:T(8,128)(2,1)} %collective-permute-done.16, bf16[128,2048]{1,0:T(8,128)(2,1)S(1)} %collective-permute-done.15, bf16[128,2048]{1,0:T(8,128)(2,1)S(1)} %get-tuple-element.18), kind=kLoop, calls=%fused_computation.6 | loop fusion | flops 2097152 | bytes 2621440 | tf_op jit(solution)/shard_map/convert_element_type | solution.py:495
  (93 shorter events, 32.7 us)
Async XLA Ops:
  0.6 68.8 %copy-start = (f32[31,512]{1,0:T(8,128)S(1)}, f32[31,512]{1,0:T(8,128)}, u32[]{:S(2)}) copy-start(f32[31,512]{1,0:T(8,128)} %param.19) | copy-start | bytes 190468
  6.4 9.6 %collective-permute-start.1 = (bf16[16,1408]{1,0:T(8,128)(2,1)S(1)}, bf16[16,1408]{1,0:T(8,128)(2,1)S(1)}, u32[]{:S(2)}, u32[]{:S(2)}) collective-permute-start(bf16[16,1408]{1,0:T(8,128)(2,1)S(1)} %get-tuple-element.22), channel_id=1, source_target_pairs={{0,4},{4,0},{8,12},{12,8},{16,20},{20,16},{24,28},{28,24},{32,36},... | collective-permute-start | bytes 135176 | tf_op jit(solution)/shard_map/ppermute | solution.py:356
  35.3 14.1 %collective-permute-start.2 = (bf16[8,32,1408]{2,1,0:T(8,128)(2,1)S(1)}, bf16[8,32,1408]{2,1,0:T(8,128)(2,1)S(1)}, u32[]{:S(2)}, u32[]{:S(2)}) collective-permute-start(bf16[8,32,1408]{2,1,0:T(8,128)(2,1)S(1)} %all_to_all.10.refs_0_), channel_id=1, source_target_pairs={{0,64},{8,72},{16,80},{24,88},{32,96},{40,104},{48,112},{56,120},{... | collective-permute-start | bytes 2162696 | tf_op jit(solution)/shard_map/ppermute | solution.py:370
  38.5 12.8 %collective-permute-start.3 = (bf16[8,32,1408]{2,1,0:T(8,128)(2,1)S(1)}, bf16[8,32,1408]{2,1,0:T(8,128)(2,1)S(1)}, u32[]{:S(2)}, u32[]{:S(2)}) collective-permute-start(bf16[8,32,1408]{2,1,0:T(8,128)(2,1)S(1)} %all_to_all.10.refs_0_), channel_id=1, source_target_pairs={{0,448},{8,456},{16,464},{24,472},{32,480},{40,488},{48,496},{56,5... | collective-permute-start | bytes 2162696 | tf_op jit(solution)/shard_map/ppermute | solution.py:371
  42.3 40.7 %collective-permute-start = (bf16[512,2048]{1,0:T(8,128)(2,1)}, bf16[512,2048]{1,0:T(8,128)(2,1)}, u32[]{:S(2)}, u32[]{:S(2)}) collective-permute-start(bf16[512,2048]{1,0:T(8,128)(2,1)} %param.12), channel_id=1, source_target_pairs={{0,4},{4,0},{8,12},{12,8},{16,20},{20,16},{24,28},{28,24},{32,36},... | collective-permute-start | bytes 6291464 | tf_op jit(solution)/shard_map/ppermute | solution.py:374
  49.4 36.8 %copy-start.1 = (bf16[8,32,1408]{2,1,0:T(8,128)(2,1)}, bf16[8,32,1408]{2,1,0:T(8,128)(2,1)S(1)}, u32[]{:S(2)}) copy-start(bf16[8,32,1408]{2,1,0:T(8,128)(2,1)S(1)} %collective-permute-done.2.refs_1_) | copy-start | bytes 2162692
  49.4 13.5 %collective-permute-start.4 = (bf16[8,32,1408]{2,1,0:T(8,128)(2,1)S(1)}, bf16[8,32,1408]{2,1,0:T(8,128)(2,1)S(1)}, u32[]{:S(2)}, u32[]{:S(2)}) collective-permute-start(bf16[8,32,1408]{2,1,0:T(8,128)(2,1)S(1)} %collective-permute-done.2.refs_1_), channel_id=1, source_target_pairs={{0,64},{8,72},{16,80},{24,88},{32,96},{40,104},{48,112},{56,120},{... | collective-permute-start | bytes 2162696 | tf_op jit(solution)/shard_map/ppermute | solution.py:370
  51.3 34.9 %copy-start.4 = (bf16[8,32,1408]{2,1,0:T(8,128)(2,1)}, bf16[8,32,1408]{2,1,0:T(8,128)(2,1)S(1)}, u32[]{:S(2)}) copy-start(bf16[8,32,1408]{2,1,0:T(8,128)(2,1)S(1)} %collective-permute-done.3.refs_2_) | copy-start | bytes 2162692
  51.3 13.5 %collective-permute-start.5 = (bf16[8,32,1408]{2,1,0:T(8,128)(2,1)S(1)}, bf16[8,32,1408]{2,1,0:T(8,128)(2,1)}, u32[]{:S(2)}, u32[]{:S(2)}) collective-permute-start(bf16[8,32,1408]{2,1,0:T(8,128)(2,1)S(1)} %collective-permute-done.3.refs_2_), channel_id=1, source_target_pairs={{0,448},{8,456},{16,464},{24,472},{32,480},{40,488},{48,496},{56,5... | collective-permute-start | bytes 2162696 | tf_op jit(solution)/shard_map/ppermute | solution.py:371
  56.6 26.4 %copy-start.26 = (bf16[512,2048]{1,0:T(8,128)(2,1)S(1)}, bf16[512,2048]{1,0:T(8,128)(2,1)}, u32[]{:S(2)}) copy-start(bf16[512,2048]{1,0:T(8,128)(2,1)} %param.12) | copy-start | bytes 6291460
  62.9 23.3 %copy-start.7 = (bf16[8,32,1408]{2,1,0:T(8,128)(2,1)}, bf16[8,32,1408]{2,1,0:T(8,128)(2,1)S(1)}, u32[]{:S(2)}) copy-start(bf16[8,32,1408]{2,1,0:T(8,128)(2,1)S(1)} %collective-permute-done.4.refs_3_) | copy-start | bytes 2162692
  62.9 13.5 %collective-permute-start.6 = (bf16[8,32,1408]{2,1,0:T(8,128)(2,1)S(1)}, bf16[8,32,1408]{2,1,0:T(8,128)(2,1)S(1)}, u32[]{:S(2)}, u32[]{:S(2)}) collective-permute-start(bf16[8,32,1408]{2,1,0:T(8,128)(2,1)S(1)} %collective-permute-done.4.refs_3_), channel_id=1, source_target_pairs={{0,64},{8,72},{16,80},{24,88},{32,96},{40,104},{48,112},{56,120},{... | collective-permute-start | bytes 2162696 | tf_op jit(solution)/shard_map/ppermute | solution.py:370
  64.8 13.6 %collective-permute-start.7 = (bf16[8,32,1408]{2,1,0:T(8,128)(2,1)}, bf16[8,32,1408]{2,1,0:T(8,128)(2,1)S(1)}, u32[]{:S(2)}, u32[]{:S(2)}) collective-permute-start(bf16[8,32,1408]{2,1,0:T(8,128)(2,1)} %collective-permute-done.5.refs_4_), channel_id=1, source_target_pairs={{0,448},{8,456},{16,464},{24,472},{32,480},{40,488},{48,496},{56,5... | collective-permute-start | bytes 2162696 | tf_op jit(solution)/shard_map/ppermute | solution.py:371
  76.4 9.8 %collective-permute-start.8 = (bf16[4,32,1408]{2,1,0:T(8,128)(2,1)S(1)}, bf16[4,32,1408]{2,1,0:T(8,128)(2,1)S(1)}, u32[]{:S(2)}, u32[]{:S(2)}) collective-permute-start(bf16[4,32,1408]{2,1,0:T(8,128)(2,1)S(1)} %slice.26), channel_id=1, source_target_pairs={{0,64},{8,72},{16,80},{24,88},{32,96},{40,104},{48,112},{56,120},{... | collective-permute-start | bytes 1081352 | tf_op jit(solution)/shard_map/ppermute | solution.py:370
  78.4 8.9 %collective-permute-start.9 = (bf16[4,32,1408]{2,1,0:T(8,128)(2,1)S(1)}, bf16[4,32,1408]{2,1,0:T(8,128)(2,1)S(1)}, u32[]{:S(2)}, u32[]{:S(2)}) collective-permute-start(bf16[4,32,1408]{2,1,0:T(8,128)(2,1)S(1)} %slice.27), channel_id=1, source_target_pairs={{0,448},{8,456},{16,464},{24,472},{32,480},{40,488},{48,496},{56,5... | collective-permute-start | bytes 1081352 | tf_op jit(solution)/shard_map/ppermute | solution.py:371
  92.5 13.2 %copy-start.3 = (bf16[8,32,1408]{2,1,0:T(8,128)(2,1)S(1)}, bf16[8,32,1408]{2,1,0:T(8,128)(2,1)}, u32[]{:S(2)}) copy-start(bf16[8,32,1408]{2,1,0:T(8,128)(2,1)} %copy-done.1) | copy-start | bytes 2162692
  92.5 13.2 %copy-start.6 = (bf16[8,32,1408]{2,1,0:T(8,128)(2,1)S(1)}, bf16[8,32,1408]{2,1,0:T(8,128)(2,1)}, u32[]{:S(2)}) copy-start(bf16[8,32,1408]{2,1,0:T(8,128)(2,1)} %copy-done.4) | copy-start | bytes 2162692
  92.5 13.2 %copy-start.9 = (bf16[8,32,1408]{2,1,0:T(8,128)(2,1)S(1)}, bf16[8,32,1408]{2,1,0:T(8,128)(2,1)}, u32[]{:S(2)}) copy-start(bf16[8,32,1408]{2,1,0:T(8,128)(2,1)} %copy-done.7) | copy-start | bytes 2162692
  92.5 54.5 %collective-permute-start.14 = (bf16[2048,512]{1,0:T(8,128)(2,1)S(1)}, bf16[2048,512]{1,0:T(8,128)(2,1)}, u32[]{:S(2)}, u32[]{:S(2)}) collective-permute-start(bf16[2048,512]{1,0:T(8,128)(2,1)S(1)} %shard_map.138.own_ref), channel_id=1, source_target_pairs={{0,4},{4,0},{8,12},{12,8},{16,20},{20,16},{24,28},{28,24},{32,36},... | collective-permute-start | bytes 6291464 | tf_op jit(solution)/shard_map/ppermute | solution.py:422
  110.6 10.1 %collective-permute-start.10 = (bf16[32,256]{1,0:T(8,128)(2,1)S(1)}, bf16[32,256]{1,0:T(8,128)(2,1)S(1)}, u32[]{:S(2)}, u32[]{:S(2)}) collective-permute-start(bf16[32,256]{1,0:T(8,128)(2,1)S(1)} %slice.28), channel_id=1, source_target_pairs={{0,8},{4,12},{8,16},{12,20},{16,24},{20,28},{24,32},{28,36},{32,40... | collective-permute-start | bytes 49160 | tf_op jit(solution)/shard_map/ppermute | solution.py:404
  118.6 11.9 %copy-start.25 = (f32[8]{0:T(128)S(1)}, f32[8]{0:T(128)}, u32[]{:S(2)}) copy-start(f32[8]{0:T(128)} %sinks_ref.1) | copy-start | bytes 100
  118.6 11.9 %collective-permute-start.11 = (bf16[128,128]{1,0:T(8,128)(2,1)S(1)}, bf16[128,128]{1,0:T(8,128)(2,1)S(1)}, u32[]{:S(2)}, u32[]{:S(2)}) collective-permute-start(bf16[128,128]{1,0:T(8,128)(2,1)S(1)} %slice.29), channel_id=1, source_target_pairs={{0,8},{4,12},{8,16},{12,20},{16,24},{20,28},{24,32},{28,36},{32,40... | collective-permute-start | bytes 98312 | tf_op jit(solution)/shard_map/ppermute | solution.py:413
  125.7 15.1 %all-to-all-start.1 = ((f32[8,2,1024]{2,1,0:T(2,128)}), f32[8,2,1024]{2,1,0:T(2,128)S(1)}, u32[]{:S(2)}, u32[]{:S(2)}) async-start(f32[8,2,1024]{2,1,0:T(2,128)} %broadcast_in_dim.4), calls=%async_computation.1 | async-start | bytes 131072 | tf_op jit(solution)/shard_map/all_to_all | solution.py:434
  138.9 22.7 %copy-start.14 = (bf16[512,256]{1,0:T(8,128)(2,1)}, bf16[512,256]{1,0:T(8,128)(2,1)S(1)}, u32[]{:S(2)}) copy-start(bf16[512,256]{1,0:T(8,128)(2,1)S(1)} %get-tuple-element.15.attn_ref) | copy-start | bytes 786436
  138.9 7.1 %collective-permute-start.13 = (bf16[512,256]{1,0:T(8,128)(2,1)S(1)}, bf16[512,256]{1,0:T(8,128)(2,1)S(1)}, u32[]{:S(2)}, u32[]{:S(2)}) collective-permute-start(bf16[512,256]{1,0:T(8,128)(2,1)S(1)} %get-tuple-element.17), channel_id=1, source_target_pairs={{0,4},{4,0},{8,12},{12,8},{16,20},{20,16},{24,28},{28,24},{32,36},... | collective-permute-start | bytes 786440 | tf_op jit(solution)/shard_map/ppermute | solution.py:450
  140.8 1.2 copy-start.11
  143.5 3.6 %collective-permute-start.12 = (bf16[512,256]{1,0:T(8,128)(2,1)S(1)}, bf16[512,256]{1,0:T(8,128)(2,1)S(1)}, u32[]{:S(2)}, u32[]{:S(2)}) collective-permute-start(bf16[512,256]{1,0:T(8,128)(2,1)S(1)} %get-tuple-element.16), channel_id=1, source_target_pairs={{0,4},{4,0},{8,12},{12,8},{16,20},{20,16},{24,28},{28,24},{32,36},... | collective-permute-start | bytes 786440 | tf_op jit(solution)/shard_map/ppermute | solution.py:459
  145.9 15.7 %copy-start.16 = (bf16[512,256]{1,0:T(8,128)(2,1)}, bf16[512,256]{1,0:T(8,128)(2,1)S(1)}, u32[]{:S(2)}) copy-start(bf16[512,256]{1,0:T(8,128)(2,1)S(1)} %collective-permute-done.13.attn_got) | copy-start | bytes 786436
  156.8 20.7 %collective-permute-start.17 = (bf16[128,2048]{1,0:T(8,128)(2,1)}, bf16[128,2048]{1,0:T(8,128)(2,1)}, u32[]{:S(2)}, u32[]{:S(2)}) collective-permute-start(bf16[128,2048]{1,0:T(8,128)(2,1)} %get-tuple-element.20), channel_id=1, source_target_pairs={{0,3},{1,0},{2,1},{3,2},{4,7},{5,4},{6,5},{7,6},{8,11},{9,8},{10,9... | collective-permute-start | bytes 1572872 | tf_op jit(solution)/shard_map/ppermute | solution.py:483
  161.6 17.4 %collective-permute-start.16 = (bf16[128,2048]{1,0:T(8,128)(2,1)}, bf16[128,2048]{1,0:T(8,128)(2,1)}, u32[]{:S(2)}, u32[]{:S(2)}) collective-permute-start(bf16[128,2048]{1,0:T(8,128)(2,1)} %get-tuple-element.19), channel_id=1, source_target_pairs={{0,1},{1,2},{2,3},{3,0},{4,5},{5,6},{6,7},{7,4},{8,9},{9,10},{10,1... | collective-permute-start | bytes 1572872 | tf_op jit(solution)/shard_map/ppermute | solution.py:483
  169.5 18.8 %collective-permute-start.15 = (bf16[128,2048]{1,0:T(8,128)(2,1)S(1)}, bf16[128,2048]{1,0:T(8,128)(2,1)S(1)}, u32[]{:S(2)}, u32[]{:S(2)}) collective-permute-start(bf16[128,2048]{1,0:T(8,128)(2,1)S(1)} %shard_map.140), channel_id=1, source_target_pairs={{0,2},{1,3},{2,0},{3,1},{4,6},{5,7},{6,4},{7,5},{8,10},{9,11},{10,... | collective-permute-start | bytes 1572872 | tf_op jit(solution)/shard_map/ppermute | solution.py:483
  173.2 3.7 %collective-permute-start.18 = (f32[4,512]{1,0:T(4,128)S(1)}, f32[4,512]{1,0:T(4,128)S(1)}, u32[]{:S(2)}, u32[]{:S(2)}) collective-permute-start(f32[4,512]{1,0:T(4,128)S(1)} %get-tuple-element.25), channel_id=1, source_target_pairs={{0,4},{4,0},{8,12},{12,8},{16,20},{20,16},{24,28},{28,24},{32,36},... | collective-permute-start | bytes 24584 | tf_op jit(solution)/shard_map/ppermute | solution.py:463
  (15 other events, 13.2 us)

commit v2 on v1

--- a/solution.py
+++ b/solution.py
@@ -45,18 +45,18 @@
 
 VMEM = pl.BlockSpec(memory_space=pltpu.VMEM)
 SMEM = pl.BlockSpec(memory_space=pltpu.SMEM)
-ANY = pl.BlockSpec(memory_space=pl.ANY)
+HBM = pl.BlockSpec(memory_space=pltpu.MemorySpace.HBM)
 TILE = 256
 
 
-def call(body, outs, flops, in_specs, operands, scratch=(), limit=12):
+def call(body, outs, flops, in_specs, operands, scratch=(), limit=None):
     return pl.pallas_call(
         body,
         out_shape=outs,
         in_specs=in_specs,
         out_specs=jax.tree.map(lambda _: VMEM, outs),
         scratch_shapes=list(scratch),
-        compiler_params=pltpu.CompilerParams(vmem_limit_bytes=limit << 20),
+        compiler_params=pltpu.CompilerParams(vmem_limit_bytes=limit and limit << 20),
         cost_estimate=pl.CostEstimate(flops=flops, bytes_accessed=1 << 20, transcendentals=0),
     )(*operands)
 
@@ -65,7 +65,18 @@
     return jax.ShapeDtypeStruct(dims, dtype)
 
 
-def pack_kernel(at_ref, value_ref, gate_ref, query_ref, key_ref, v_ref, conv_ref, attn_ref, out_ref):
+def pack_kernel(at_ref, *refs):
+    count = (len(refs) - 2) // 2
+    shards, out_ref, held, sems = refs[:count], refs[count], refs[count + 1 : -1], refs[-1]
+    copies = [
+        pltpu.make_async_copy(shard, here, sems.at[index])
+        for index, (shard, here) in enumerate(zip(shards, held))
+    ]
+    for copy in copies:
+        copy.start()
+    for copy in copies:
+        copy.wait()
+    value_ref, gate_ref, query_ref, key_ref, v_ref, conv_ref, attn_ref = held
     core = at_ref[3]
     lane = lax.broadcasted_iota(jnp.int32, key_ref.shape, 1)
     key = key_ref[...].astype(jnp.float32)
@@ -111,32 +122,60 @@
     pltpu.make_async_copy(out_ref, out_ref, sem).wait()
 
 
+def rows_of(step):
+    return pl.ds(pl.multiple_of(step * TILE, TILE), TILE)
+
+
+def tile_copy(x_ref, x_here, sems, step):
+    rows = rows_of(step)
+    return pltpu.make_async_copy(x_ref.at[rows, :], x_here.at[rows, :], sems.at[step])
+
+
 def gated_kernel(columns, at_ref, x_ref, *refs):
-    pieces, (out_ref, w_ref, sem) = refs[:-3], refs[-3:]
+    pieces, (out_ref, w_ref, sem, x_here, x_sems) = refs[:-5], refs[-5:]
+    tiles = x_ref.shape[0] // TILE
+    for step in range(tiles):
+        tile_copy(x_ref, x_here, x_sems, step).start()
     fetch(at_ref, pieces, w_ref, sem, columns)
     half = out_ref.shape[1]
 
-    @pl.loop(0, x_ref.shape[0] // TILE)
+    @pl.loop(0, tiles)
     def _(step):
-        rows = pl.ds(pl.multiple_of(step * TILE, TILE), TILE)
-        both = jnp.dot(x_ref[rows, :], w_ref[...], preferred_element_type=jnp.float32)
+        tile_copy(x_ref, x_here, x_sems, step).wait()
+        rows = rows_of(step)
+        both = jnp.dot(x_here[rows, :], w_ref[...], preferred_element_type=jnp.float32)
         both = both.astype(jnp.bfloat16).astype(jnp.float32)
         out_ref[rows, :] = (both[:, :half] * jax.nn.sigmoid(both[:, half:])).astype(jnp.bfloat16)
 
 
 def rotated_kernel(columns, at_ref, x_ref, cos_ref, sin_ref, *refs):
-    pieces, (out_ref, w_ref, sem) = refs[:-3], refs[-3:]
+    pieces, (out_ref, w_ref, sem, x_here, x_sems, cos_here, sin_here, table_sems) = (
+        refs[:-8],
+        refs[-8:],
+    )
+    tiles = x_ref.shape[0] // TILE
+    for step in range(tiles):
+        tile_copy(x_ref, x_here, x_sems, step).start()
+    tables = (
+        pltpu.make_async_copy(cos_ref, cos_here, table_sems.at[0]),
+        pltpu.make_async_copy(sin_ref, sin_here, table_sems.at[1]),
+    )
+    for table in tables:
+        table.start()
     fetch(at_ref, pieces, w_ref, sem, columns)
+    for table in tables:
+        table.wait()
     width = out_ref.shape[1]
 
-    @pl.loop(0, x_ref.shape[0] // TILE)
+    @pl.loop(0, tiles)
     def _(step):
-        rows = pl.ds(pl.multiple_of(step * TILE, TILE), TILE)
-        raw = jnp.dot(x_ref[rows, :], w_ref[...], preferred_element_type=jnp.float32)
+        tile_copy(x_ref, x_here, x_sems, step).wait()
+        rows = rows_of(step)
+        raw = jnp.dot(x_here[rows, :], w_ref[...], preferred_element_type=jnp.float32)
         raw = raw.astype(jnp.bfloat16).astype(jnp.float32)
         lane = lax.broadcasted_iota(jnp.int32, (TILE, 128), 1)
         front = jnp.bitwise_and(lane, HEAD_DIM - 1) < HEAD_DIM // 2
-        cosine, sine = cos_ref[rows, :], sin_ref[rows, :]
+        cosine, sine = cos_here[rows, :], sin_here[rows, :]
         for at in range(0, width, 128):
             part = raw[:, at : at + 128]
             other = jnp.where(
@@ -280,29 +319,32 @@
     steps, at_ref, conv_ref, attn_ref, conv_got, attn_got, own_ref, other_ref, *out_refs
 ):
     member, half = at_ref[5], conv_ref.shape[1]
-    peers = conv_ref.shape[0] // out_refs[0].shape[0]
     count = out_refs[0].shape[0]
-    for away, out_ref in zip(steps, out_refs):
-        to = jnp.bitwise_and(member + away, peers - 1)
-        rows = pl.ds(pl.multiple_of(to * count, count), count)
-
-        @pl.loop(0, out_ref.shape[1] // TILE)
-        def _(step):
-            cols = pl.ds(pl.multiple_of(step * TILE, TILE), TILE)
-            total = jnp.zeros((count, TILE), jnp.float32)
-            for left, right, at in (
-                (conv_ref, own_ref, 0),
-                (attn_ref, own_ref, half),
-                (conv_got, other_ref, 0),
-                (attn_got, other_ref, half),
-            ):
-                total = total + lax.dot_general(
-                    left[rows, :],
-                    right[cols, at : at + half],
-                    (((1,), (1,)), ((), ())),
-                    preferred_element_type=jnp.float32,
-                )
-            out_ref[:, cols] = total.astype(jnp.bfloat16)
+    peers = conv_ref.shape[0] // count
+
+    @pl.loop(0, out_refs[0].shape[1] // TILE)
+    def _(step):
+        cols = pl.ds(pl.multiple_of(step * TILE, TILE), TILE)
+        total = jnp.zeros((conv_ref.shape[0], TILE), jnp.float32)
+        for left, right, at in (
+            (conv_ref, own_ref, 0),
+            (attn_ref, own_ref, half),
+            (conv_got, other_ref, 0),
+            (attn_got, other_ref, half),
+        ):
+            total = total + lax.dot_general(
+                left[...],
+                right[cols, at : at + half],
+                (((1,), (1,)), ((), ())),
+                preferred_element_type=jnp.float32,
+            )
+        for to in range(peers):
+            out = total[to * count : (to + 1) * count].astype(jnp.bfloat16)
+            for away, out_ref in zip(steps, out_refs):
+
+                @pl.when(jnp.bitwise_and(to - member, peers - 1) == away)
+                def _():
+                    out_ref[:, cols] = out
 
 
 def layer(
@@ -346,12 +388,17 @@
     qkv_cols = (2 * channels, q_cols + 2 * HEAD_DIM)
     out_cols = (2 * channels + q_cols + 2 * HEAD_DIM, channels + q_cols)
     width = sum(out_cols)
+    shards_in = (w_conv_value, w_conv_gate, w_query, w_key, w_value, out_conv.T, out_attn.T)
     halves = call(
         pack_kernel,
         shape((CORES, depth, width)),
         1 << 20,
-        [SMEM] + [VMEM] * 7,
-        (at, w_conv_value, w_conv_gate, w_query, w_key, w_value, out_conv.T, out_attn.T),
+        [SMEM] + [HBM] * len(shards_in),
+        (at, *shards_in),
+        (
+            *(pltpu.VMEM(w.shape, w.dtype) for w in shards_in),
+            pltpu.SemaphoreType.DMA((len(shards_in),)),
+        ),
     )
     got = lax.ppermute(halves[1], SP, OTHER_CORE)
     sent = call(
@@ -360,6 +407,7 @@
         1 << 20,
         [SMEM, VMEM, VMEM],
         (at, halves[0], got),
+        limit=12,
     )
     own_line = lax.all_to_all(sent, SP, 0, 0, tiled=True, axis_index_groups=LINES)
     pieces = [own_line]
@@ -392,23 +440,36 @@
     cosines = jnp.concatenate([cosine] * 4, axis=1)
     sines = jnp.concatenate([-sine, sine] * 2, axis=1)
 
-    spots = [ANY] * len(pieces)
+    spots = [HBM] * len(pieces)
     glu = call(
         functools.partial(gated_kernel, conv_cols),
         shape((row_count, channels)),
         2 * row_count * model * conv_cols[1],
-        [SMEM, VMEM] + spots,
+        [SMEM, HBM] + spots,
         (at, normed, *pieces),
-        (pltpu.VMEM((model, conv_cols[1]), jnp.bfloat16), pltpu.SemaphoreType.DMA),
+        (
+            pltpu.VMEM((model, conv_cols[1]), jnp.bfloat16),
+            pltpu.SemaphoreType.DMA,
+            pltpu.VMEM(normed.shape, jnp.bfloat16),
+            pltpu.SemaphoreType.DMA((row_count // TILE,)),
+        ),
     )
     glu_before = lax.ppermute(glu[row_count - 32 :], SP, NEXT_CHIP)
     qkv = call(
         functools.partial(rotated_kernel, qkv_cols),
         shape((row_count, qkv_cols[1])),
         2 * row_count * model * qkv_cols[1],
-        [SMEM, VMEM, VMEM, VMEM] + spots,
+        [SMEM, HBM, HBM, HBM] + spots,
         (at, normed, cosines, sines, *pieces),
-        (pltpu.VMEM((model, qkv_cols[1]), jnp.bfloat16), pltpu.SemaphoreType.DMA),
+        (
+            pltpu.VMEM((model, qkv_cols[1]), jnp.bfloat16),
+            pltpu.SemaphoreType.DMA,
+            pltpu.VMEM(normed.shape, jnp.bfloat16),
+            pltpu.SemaphoreType.DMA((row_count // TILE,)),
+            pltpu.VMEM(cosines.shape, jnp.float32),
+            pltpu.VMEM(sines.shape, jnp.float32),
+            pltpu.SemaphoreType.DMA((2,)),
+        ),
     )
     kv_before = lax.ppermute(qkv[row_count - WINDOW :, q_cols:], SP, NEXT_CHIP)
     out_own = call(
@@ -429,6 +490,7 @@
         [VMEM] * 3,
         (glu_before, glu, taps),
         (pltpu.VMEM((2, row_count + 32, 128), jnp.float32),),
+        limit=12,
     )
     members = CORES * lax.axis_size("tp")
     everyones = lax.all_to_all(
@@ -446,6 +508,7 @@
         [SMEM, SMEM, VMEM, VMEM],
         (at, sinks, qkv, kv_before),
         (extended,) * 4,
+        limit=12,
     )
     attn_got = lax.ppermute(attn_given, SP, OTHER_CORE)
     gain = lax.dynamic_slice_in_dim(ln_gain, core * channels, channels, 0)
@@ -455,6 +518,7 @@
         1 << 28,
         [SMEM, VMEM, VMEM, VMEM],
         (at, conv_out, everyones, gain[None]),
+        limit=12,
     )
     conv_got = lax.ppermute(conv_given, SP, OTHER_CORE)
 
@@ -477,14 +541,14 @@
             2 * share * len(steps) * model * 2 * out_cols[1],
             [SMEM] + [VMEM] * 6,
             (at, conv_kept, attn_kept, conv_got, attn_got, out_own, out_other),
+            limit=16,
         )
 
     def to_member(value, away):
         return lax.ppermute(value, "tp", [(i, (i + away) % peers) for i in range(peers)])
 
-    (far,) = output((2,))
+    far, up, down, mine = output((2, 1, 3, 0))
     far = to_member(far, 2)
-    up, down, mine = output((1, 3, 0))
     up, down = to_member(up, 1), to_member(down, 3)
     mixed = (
         mine.astype(jnp.float32)

time: 193 us -> 195 us (1.010)
  local copies, waits for them, and re-layouts: 16.1 us -> 9.49 us
  waiting for transfers between devices: 24.9 us -> 29.3 us
  other arithmetic: 12.8 us -> 16.4 us
  Pallas kernels: 38.7 us -> 41.4 us
    unnamed x54 -> x32, local copies, waits for them, and re-layouts: 14.4 us -> 5.04 us
    ppermute x3, waiting for transfers between devices: 10.8 us -> 16.8 us  [to_member(): lax.ppermute(value, 'tp', [(i, (i + away) % peers) for i in range(peers)])]
    pallas_call x10 -> x9, Pallas kernels: 38.7 us -> 41.4 us  [call(): pl.pallas_call(body, out_shape=outs, in_specs=in_specs, out_specs=jax.tre...]
    convert_element_type x1, other arithmetic: 3.18 us -> 5.76 us  [layer(): normed = (as_float * lax.rsqrt(jnp.mean(as_float * as_float, axis=-1, kee...]
  transfers between devices with their start and end apart: 20 -> 20, of which waited for: 9 -> 8; matrix products, arithmetic and copies ran while one was open for 6% -> 9% of each run, Pallas kernels for 14% -> 14%
where the time goes in v2:
time: 195 us; the launch traced here: 193 us
  starting transfers between devices  77.1 us (40%)
  Pallas kernels  41.4 us (21%)
  waiting for transfers between devices  29.3 us (15%)
  blocking collectives  18.7 us (10%)
  other arithmetic  16.4 us (8%)
  local copies, waits for them, and re-layouts  9.49 us (5%)
    pallas_call x9, Pallas kernels, call(): pl.pallas_call(body, out_shape=outs, in_specs=in_specs, out_specs=jax.tre...  41.4 us
    all_to_all x1, blocking collectives, layer(): lax.all_to_all(sent, SP, 0, 0, tiled=True, axis_index_groups=LINES)  18.7 us
    ppermute x4, starting transfers between devices, layer(): behind = lax.ppermute(behind, SP, BEHIND)  17.5 us
    ppermute x3, waiting for transfers between devices, to_member(): lax.ppermute(value, 'tp', [(i, (i + away) % peers) for i in range(peers)])  16.8 us
    ppermute x3, starting transfers between devices, to_member(): lax.ppermute(value, 'tp', [(i, (i + away) % peers) for i in range(peers)])  10.3 us
    ppermute x4, waiting for transfers between devices, layer(): ahead = lax.ppermute(ahead, SP, AHEAD)  9.63 us
    ppermute x1, starting transfers between devices, layer(): out_other = lax.ppermute(out_own, SP, OTHER_CORE)  8.99 us
    ppermute x4, starting transfers between devices, layer(): ahead = lax.ppermute(ahead, SP, AHEAD)  8.93 us
  transfers between devices with their start and end apart: 20, of which 8 were waited for; matrix products, arithmetic and copies ran while one was open for 9% of the time, Pallas kernels for 14%

profile of v2, /device:TPU:1, one launch (start us, length us, event | category | flops | bytes accessed | tf_op | source)
XLA Modules:
  0.0 193.5 jit_solution(7108237597255638743)
XLA Ops:
  1.3 2.3 %shard_map.131 = bf16[2,16,1408]{2,1,0:T(8,128)(2,1)} custom-call(s32[6]{0:T(128)} %stack.31.at_ref, bf16[16,512]{1,0:T(8,128)(2,1)} %refs_0_.1, bf16[16,512]{1,0:T(8,128)(2,1)} %refs_1_.1, bf16[16,512]{1,0:T(8,128)(2,1)} %refs_2_.1, bf16[16,128]{1,0:T(8,128)(2,1)} %refs_3_.1, bf16[16,128]{1,0:T(8,128)(2,1)} %refs_4_.1, bf16[16,512]{1,0:T(8,128)(2,1)} %bitcast.14, ...), custom_call_target="tpu_custom_call" | custom-call | flops 1048576 | bytes 1048576 | tf_op jit(solution)/shard_map/pallas_call | solution.py:53
  4.4 8.7 %collective-permute-start.1 = (bf16[16,1408]{1,0:T(8,128)(2,1)S(1)}, bf16[16,1408]{1,0:T(8,128)(2,1)S(1)}, u32[]{:S(2)}, u32[]{:S(2)}) collective-permute-start(bf16[16,1408]{1,0:T(8,128)(2,1)S(1)} %get-tuple-element.24), channel_id=1, source_target_pairs={{0,4},{4,0},{8,12},{12,8},{16,20},{20,16},{24,28},{28,24},{32,36},... | collective-permute-start | bytes 135176 | tf_op jit(solution)/shard_map/ppermute | solution.py:403
  15.3 18.7 %all_to_all.10.refs_0_ = bf16[8,32,1408]{2,1,0:T(8,128)(2,1)S(1)} all-to-all(bf16[8,32,1408]{2,1,0:T(8,128)(2,1)S(1)} %shard_map.132), channel_id=1, replica_groups={{0,8,16,24,32,40,48,56},{64,72,80,88,96,104,112,120},{128,136,144,152,1..., dimensions={0} | all-to-all | bytes 1441792 | tf_op jit(solution)/shard_map/all_to_all | solution.py:412
  34.0 3.2 %collective-permute-start.2 = (bf16[8,32,1408]{2,1,0:T(8,128)(2,1)S(1)}, bf16[8,32,1408]{2,1,0:T(8,128)(2,1)S(1)}, u32[]{:S(2)}, u32[]{:S(2)}) collective-permute-start(bf16[8,32,1408]{2,1,0:T(8,128)(2,1)S(1)} %all_to_all.10.refs_0_), channel_id=1, source_target_pairs={{0,64},{8,72},{16,80},{24,88},{32,96},{40,104},{48,112},{56,120},{... | collective-permute-start | bytes 2162696 | tf_op jit(solution)/shard_map/ppermute | solution.py:418
  37.2 3.8 %collective-permute-start.3 = (bf16[8,32,1408]{2,1,0:T(8,128)(2,1)S(1)}, bf16[8,32,1408]{2,1,0:T(8,128)(2,1)S(1)}, u32[]{:S(2)}, u32[]{:S(2)}) collective-permute-start(bf16[8,32,1408]{2,1,0:T(8,128)(2,1)S(1)} %all_to_all.10.refs_0_), channel_id=1, source_target_pairs={{0,448},{8,456},{16,464},{24,472},{32,480},{40,488},{48,496},{56,5... | collective-permute-start | bytes 2162696 | tf_op jit(solution)/shard_map/ppermute | solution.py:419
  41.0 6.4 %collective-permute-start = (bf16[512,2048]{1,0:T(8,128)(2,1)}, bf16[512,2048]{1,0:T(8,128)(2,1)}, u32[]{:S(2)}, u32[]{:S(2)}) collective-permute-start(bf16[512,2048]{1,0:T(8,128)(2,1)} %param.12), channel_id=1, source_target_pairs={{0,4},{4,0},{8,12},{12,8},{16,20},{20,16},{24,28},{28,24},{32,36},... | collective-permute-start | bytes 6291464 | tf_op jit(solution)/shard_map/ppermute | solution.py:422
  48.1 1.9 collective-permute-start.4
  50.0 4.6 %collective-permute-start.5 = (bf16[8,32,1408]{2,1,0:T(8,128)(2,1)S(1)}, bf16[8,32,1408]{2,1,0:T(8,128)(2,1)}, u32[]{:S(2)}, u32[]{:S(2)}) collective-permute-start(bf16[8,32,1408]{2,1,0:T(8,128)(2,1)S(1)} %collective-permute-done.3.refs_2_), channel_id=1, source_target_pairs={{0,448},{8,456},{16,464},{24,472},{32,480},{40,488},{48,496},{56,5... | collective-permute-start | bytes 2162696 | tf_op jit(solution)/shard_map/ppermute | solution.py:419
  56.0 5.7 %collective-permute-done.4.refs_3_ = bf16[8,32,1408]{2,1,0:T(8,128)(2,1)} collective-permute-done((bf16[8,32,1408]{2,1,0:T(8,128)(2,1)S(1)}, bf16[8,32,1408]{2,1,0:T(8,128)(2,1)}, u32[]{:S(2)}, u32[]{:S(2)}) %collective-permute-start.4) | collective-permute-done | bytes 720928 | tf_op jit(solution)/shard_map/ppermute | solution.py:418
  63.6 4.6 %collective-permute-start.7 = (bf16[8,32,1408]{2,1,0:T(8,128)(2,1)}, bf16[8,32,1408]{2,1,0:T(8,128)(2,1)S(1)}, u32[]{:S(2)}, u32[]{:S(2)}) collective-permute-start(bf16[8,32,1408]{2,1,0:T(8,128)(2,1)} %collective-permute-done.5.refs_4_), channel_id=1, source_target_pairs={{0,448},{8,456},{16,464},{24,472},{32,480},{40,488},{48,496},{56,5... | collective-permute-start | bytes 2162696 | tf_op jit(solution)/shard_map/ppermute | solution.py:419
  72.1 3.4 %collective-permute-done.6.refs_5_ = bf16[8,32,1408]{2,1,0:T(8,128)(2,1)S(1)} collective-permute-done((bf16[8,32,1408]{2,1,0:T(8,128)(2,1)}, bf16[8,32,1408]{2,1,0:T(8,128)(2,1)S(1)}, u32[]{:S(2)}, u32[]{:S(2)}) %collective-permute-start.6) | collective-permute-done | bytes 720928 | tf_op jit(solution)/shard_map/ppermute | solution.py:418
  75.5 1.9 collective-permute-start.8
  77.5 4.6 %collective-permute-start.9 = (bf16[4,32,1408]{2,1,0:T(8,128)(2,1)S(1)}, bf16[4,32,1408]{2,1,0:T(8,128)(2,1)S(1)}, u32[]{:S(2)}, u32[]{:S(2)}) collective-permute-start(bf16[4,32,1408]{2,1,0:T(8,128)(2,1)S(1)} %slice.27), channel_id=1, source_target_pairs={{0,448},{8,456},{16,464},{24,472},{32,480},{40,488},{48,496},{56,5... | collective-permute-start | bytes 1081352 | tf_op jit(solution)/shard_map/ppermute | solution.py:419
  82.1 4.4 %fusion = f32[1024]{0:T(1024)S(1)} fusion(bf16[512,2048]{1,0:T(8,128)(2,1)} %param.12, bf16[512,2048]{1,0:T(8,128)(2,1)} %collective-permute-done, pred[]{:T(512)S(6)} %eq.6), kind=kLoop, calls=%fused_computation.2 | loop fusion | flops 25164800 | bytes 4198401 | tf_op jit(solution)/shard_map/reduce_sum | solution.py:431
  87.9 3.6 %shard_map.138.own_ref = bf16[2048,512]{1,0:T(8,128)(2,1)} custom-call(s32[6]{0:T(128)} %stack.31.at_ref, bf16[8,32,1408]{2,1,0:T(8,128)(2,1)} %copy-done.9, bf16[8,32,1408]{2,1,0:T(8,128)(2,1)} %copy-done.12, bf16[8,32,1408]{2,1,0:T(8,128)(2,1)} %copy-done.13, bf16[8,32,1408]{2,1,0:T(8,128)(2,1)} %collective-permute-done.4.refs_3_, ...), custom_call_target="tpu_custom_call" | custom-call | flops 268435456 | bytes 1048576 | tf_op jit(solution)/shard_map/pallas_call | solution.py:53
  91.5 9.0 %collective-permute-start.14 = (bf16[2048,512]{1,0:T(8,128)(2,1)}, bf16[2048,512]{1,0:T(8,128)(2,1)}, u32[]{:S(2)}, u32[]{:S(2)}) collective-permute-start(bf16[2048,512]{1,0:T(8,128)(2,1)} %shard_map.138.own_ref), channel_id=1, source_target_pairs={{0,4},{4,0},{8,12},{12,8},{16,20},{20,16},{24,28},{28,24},{32,36},... | collective-permute-start | bytes 6291464 | tf_op jit(solution)/shard_map/ppermute | solution.py:483
  100.5 5.8 %fusion.2.x_ref = bf16[1024,2048]{1,0:T(8,128)(2,1)} fusion(f32[2048]{0:T(1024)S(1)} %convert_element_type.33, f32[1024]{0:T(1024)S(1)} %add_rsqrt_fusion, bf16[512,2048]{1,0:T(8,128)(2,1)} %param.12, bf16[512,2048]{1,0:T(8,128)(2,1)} %collective-permute-done, pred[]{:T(512)S(6)} %eq.6), kind=kLoop, calls=%fused_computation.4 | loop fusion | flops 27262976 | bytes 8400897 | tf_op jit(solution)/shard_map/convert_element_type | solution.py:433
  106.3 7.1 %shard_map.133.glu_ref = bf16[1024,256]{1,0:T(8,128)(2,1)} custom-call(s32[6]{0:T(128)} %stack.31.at_ref, bf16[1024,2048]{1,0:T(8,128)(2,1)} %fusion.2.x_ref, bf16[8,32,1408]{2,1,0:T(8,128)(2,1)} %copy-done.9, bf16[8,32,1408]{2,1,0:T(8,128)(2,1)} %copy-done.12, bf16[8,32,1408]{2,1,0:T(8,128)(2,1)} %copy-done.13, ...), custom_call_target="tpu_custom_call" | custom-call | flops 2147483648 | bytes 1048576 | tf_op jit(solution)/shard_map/pallas_call | solution.py:53
  114.2 2.1 %collective-permute-start.10 = (bf16[32,256]{1,0:T(8,128)(2,1)S(1)}, bf16[32,256]{1,0:T(8,128)(2,1)S(1)}, u32[]{:S(2)}, u32[]{:S(2)}) collective-permute-start(bf16[32,256]{1,0:T(8,128)(2,1)S(1)} %slice.28), channel_id=1, source_target_pairs={{0,8},{4,12},{8,16},{12,20},{16,24},{20,28},{24,32},{28,36},{32,40... | collective-permute-start | bytes 49160 | tf_op jit(solution)/shard_map/ppermute | solution.py:457
  116.3 8.2 %shard_map.136.qkv_ref = bf16[1024,384]{1,0:T(8,128)(2,1)} custom-call(s32[6]{0:T(128)} %stack.31.at_ref, bf16[1024,2048]{1,0:T(8,128)(2,1)} %fusion.2.x_ref, f32[1024,128]{1,0:T(8,128)} %get-tuple-element.31.cos_ref, f32[1024,128]{1,0:T(8,128)} %get-tuple-element.32.sin_ref, bf16[8,32,1408]{2,1,0:T(8,128)(2,1)} %copy-done.9, ...), custom_call_target="tpu_custom_call" | custom-call | flops 1610612736 | bytes 1048576 | tf_op jit(solution)/shard_map/pallas_call | solution.py:53
  125.2 2.1 %collective-permute-start.11 = (bf16[128,128]{1,0:T(8,128)(2,1)S(1)}, bf16[128,128]{1,0:T(8,128)(2,1)S(1)}, u32[]{:S(2)}, u32[]{:S(2)}) collective-permute-start(bf16[128,128]{1,0:T(8,128)(2,1)S(1)} %slice.29), channel_id=1, source_target_pairs={{0,8},{4,12},{8,16},{12,20},{16,24},{20,28},{24,32},{28,36},{32,40... | collective-permute-start | bytes 98312 | tf_op jit(solution)/shard_map/ppermute | solution.py:474
  127.3 3.1 %shard_map.134 = (f32[1024,256]{1,0:T(8,128)S(1)}, f32[2,1024]{1,0:T(2,128)S(1)}) custom-call(bf16[32,256]{1,0:T(8,128)(2,1)S(1)} %collective-permute-done.10.before_ref, bf16[1024,256]{1,0:T(8,128)(2,1)S(1)} %copy-done.3, f32[31,256]{1,0:T(8,128)S(1)} %constant_dynamic-slice_fusion.2.taps_ref), custom_call_target="tpu_custom_call" | custom-call | flops 4294967296 | bytes 1048576 | tf_op jit(solution)/shard_map/pallas_call | solution.py:53
  131.0 4.9 %all-to-all-start.1 = ((f32[8,2,1024]{2,1,0:T(2,128)}), f32[8,2,1024]{2,1,0:T(2,128)S(1)}, u32[]{:S(2)}, u32[]{:S(2)}) async-start(f32[8,2,1024]{2,1,0:T(2,128)} %broadcast_in_dim.4), calls=%async_computation.1 | async-start | bytes 131072 | tf_op jit(solution)/shard_map/all_to_all | solution.py:496
  137.2 7.9 %shard_map.137 = (bf16[512,256]{1,0:T(8,128)(2,1)S(1)}, bf16[512,256]{1,0:T(8,128)(2,1)}, f32[4,1024]{1,0:T(4,128)S(1)}) custom-call(s32[6]{0:T(128)S(1)} %copy-done.5, f32[8]{0:T(128)S(1)} %copy-done.6, bf16[1024,384]{1,0:T(8,128)(2,1)S(1)} %copy-done.2, bf16[128,128]{1,0:T(8,128)(2,1)S(1)} %collective-permute-done.11.before_ref), custom_call_target="tpu_custom_call" | custom-call | flops 4294967296 | bytes 1048576 | tf_op jit(solution)/shard_map/pallas_call | solution.py:53
  149.2 2.4 %collective-permute-start.12 = (bf16[512,256]{1,0:T(8,128)(2,1)S(1)}, bf16[512,256]{1,0:T(8,128)(2,1)S(1)}, u32[]{:S(2)}, u32[]{:S(2)}) collective-permute-start(bf16[512,256]{1,0:T(8,128)(2,1)S(1)} %get-tuple-element.17), channel_id=1, source_target_pairs={{0,4},{4,0},{8,12},{12,8},{16,20},{20,16},{24,28},{28,24},{32,36},... | collective-permute-start | bytes 786440 | tf_op jit(solution)/shard_map/ppermute | solution.py:523
  153.7 7.2 %shard_map.139 = (bf16[128,2048]{1,0:T(8,128)(2,1)S(1)}, bf16[128,2048]{1,0:T(8,128)(2,1)}, bf16[128,2048]{1,0:T(8,128)(2,1)}, bf16[128,2048]{1,0:T(8,128)(2,1)S(1)}) custom-call(s32[6]{0:T(128)S(1)} %copy-done.5, bf16[512,256]{1,0:T(8,128)(2,1)S(1)} %get-tuple-element.15.conv_ref, bf16[512,256]{1,0:T(8,128)(2,1)S(1)} %copy-done.8, ...), custom_call_target="tpu_custom_call" | custom-call | flops 2147483648 | bytes 1048576 | tf_op jit(solution)/shard_map/pallas_call | solution.py:53
  160.9 4.7 %collective-permute-start.17 = (bf16[128,2048]{1,0:T(8,128)(2,1)}, bf16[128,2048]{1,0:T(8,128)(2,1)S(1)}, u32[]{:S(2)}, u32[]{:S(2)}) collective-permute-start(bf16[128,2048]{1,0:T(8,128)(2,1)} %get-tuple-element.22), channel_id=1, source_target_pairs={{0,3},{1,0},{2,1},{3,2},{4,7},{5,4},{6,5},{7,6},{8,11},{9,8},{10,9... | collective-permute-start | bytes 1572872 | tf_op jit(solution)/shard_map/ppermute | solution.py:548
  165.6 1.9 collective-permute-start.16
  167.5 3.6 %collective-permute-start.15 = (bf16[128,2048]{1,0:T(8,128)(2,1)S(1)}, bf16[128,2048]{1,0:T(8,128)(2,1)S(1)}, u32[]{:S(2)}, u32[]{:S(2)}) collective-permute-start(bf16[128,2048]{1,0:T(8,128)(2,1)S(1)} %get-tuple-element.20), channel_id=1, source_target_pairs={{0,2},{1,3},{2,0},{3,1},{4,6},{5,7},{6,4},{7,5},{8,10},{9,11},{10,... | collective-permute-start | bytes 1572872 | tf_op jit(solution)/shard_map/ppermute | solution.py:548
  171.2 2.9 %collective-permute-start.18 = (f32[4,512]{1,0:T(4,128)S(1)}, f32[4,512]{1,0:T(4,128)S(1)}, u32[]{:S(2)}, u32[]{:S(2)}) collective-permute-start(f32[4,512]{1,0:T(4,128)S(1)} %get-tuple-element.27), channel_id=1, source_target_pairs={{0,4},{4,0},{8,12},{12,8},{16,20},{20,16},{24,28},{28,24},{32,36},... | collective-permute-start | bytes 24584 | tf_op jit(solution)/shard_map/ppermute | solution.py:527
  175.5 12.6 %collective-permute-done.17 = bf16[128,2048]{1,0:T(8,128)(2,1)S(1)} collective-permute-done((bf16[128,2048]{1,0:T(8,128)(2,1)}, bf16[128,2048]{1,0:T(8,128)(2,1)S(1)}, u32[]{:S(2)}, u32[]{:S(2)}) %collective-permute-start.17) | collective-permute-done | bytes 524320 | tf_op jit(solution)/shard_map/ppermute | solution.py:548
  188.1 4.2 %collective-permute-done.15 = bf16[128,2048]{1,0:T(8,128)(2,1)S(1)} collective-permute-done((bf16[128,2048]{1,0:T(8,128)(2,1)S(1)}, bf16[128,2048]{1,0:T(8,128)(2,1)S(1)}, u32[]{:S(2)}, u32[]{:S(2)}) %collective-permute-start.15) | collective-permute-done | bytes 524320 | tf_op jit(solution)/shard_map/ppermute | solution.py:548
  (70 shorter events, 25.0 us)
Async XLA Ops:
  0.6 67.6 %copy-start = (f32[31,512]{1,0:T(8,128)S(1)}, f32[31,512]{1,0:T(8,128)}, u32[]{:S(2)}) copy-start(f32[31,512]{1,0:T(8,128)} %param.19) | copy-start | bytes 190468
  4.4 9.6 %collective-permute-start.1 = (bf16[16,1408]{1,0:T(8,128)(2,1)S(1)}, bf16[16,1408]{1,0:T(8,128)(2,1)S(1)}, u32[]{:S(2)}, u32[]{:S(2)}) collective-permute-start(bf16[16,1408]{1,0:T(8,128)(2,1)S(1)} %get-tuple-element.24), channel_id=1, source_target_pairs={{0,4},{4,0},{8,12},{12,8},{16,20},{20,16},{24,28},{28,24},{32,36},... | collective-permute-start | bytes 135176 | tf_op jit(solution)/shard_map/ppermute | solution.py:403
  34.0 52.4 %copy-start.9 = (bf16[8,32,1408]{2,1,0:T(8,128)(2,1)}, bf16[8,32,1408]{2,1,0:T(8,128)(2,1)S(1)}, u32[]{:S(2)}) copy-start(bf16[8,32,1408]{2,1,0:T(8,128)(2,1)S(1)} %all_to_all.10.refs_0_) | copy-start | bytes 2162692
  34.0 14.1 %collective-permute-start.2 = (bf16[8,32,1408]{2,1,0:T(8,128)(2,1)S(1)}, bf16[8,32,1408]{2,1,0:T(8,128)(2,1)S(1)}, u32[]{:S(2)}, u32[]{:S(2)}) collective-permute-start(bf16[8,32,1408]{2,1,0:T(8,128)(2,1)S(1)} %all_to_all.10.refs_0_), channel_id=1, source_target_pairs={{0,64},{8,72},{16,80},{24,88},{32,96},{40,104},{48,112},{56,120},{... | collective-permute-start | bytes 2162696 | tf_op jit(solution)/shard_map/ppermute | solution.py:418
  37.2 12.8 %collective-permute-start.3 = (bf16[8,32,1408]{2,1,0:T(8,128)(2,1)S(1)}, bf16[8,32,1408]{2,1,0:T(8,128)(2,1)S(1)}, u32[]{:S(2)}, u32[]{:S(2)}) collective-permute-start(bf16[8,32,1408]{2,1,0:T(8,128)(2,1)S(1)} %all_to_all.10.refs_0_), channel_id=1, source_target_pairs={{0,448},{8,456},{16,464},{24,472},{32,480},{40,488},{48,496},{56,5... | collective-permute-start | bytes 2162696 | tf_op jit(solution)/shard_map/ppermute | solution.py:419
  41.0 41.0 %collective-permute-start = (bf16[512,2048]{1,0:T(8,128)(2,1)}, bf16[512,2048]{1,0:T(8,128)(2,1)}, u32[]{:S(2)}, u32[]{:S(2)}) collective-permute-start(bf16[512,2048]{1,0:T(8,128)(2,1)} %param.12), channel_id=1, source_target_pairs={{0,4},{4,0},{8,12},{12,8},{16,20},{20,16},{24,28},{28,24},{32,36},... | collective-permute-start | bytes 6291464 | tf_op jit(solution)/shard_map/ppermute | solution.py:422
  48.1 8.0 %copy-start.12 = (bf16[8,32,1408]{2,1,0:T(8,128)(2,1)}, bf16[8,32,1408]{2,1,0:T(8,128)(2,1)S(1)}, u32[]{:S(2)}) copy-start(bf16[8,32,1408]{2,1,0:T(8,128)(2,1)S(1)} %collective-permute-done.2.refs_1_) | copy-start | bytes 2162692
  48.1 13.6 %collective-permute-start.4 = (bf16[8,32,1408]{2,1,0:T(8,128)(2,1)S(1)}, bf16[8,32,1408]{2,1,0:T(8,128)(2,1)}, u32[]{:S(2)}, u32[]{:S(2)}) collective-permute-start(bf16[8,32,1408]{2,1,0:T(8,128)(2,1)S(1)} %collective-permute-done.2.refs_1_), channel_id=1, source_target_pairs={{0,64},{8,72},{16,80},{24,88},{32,96},{40,104},{48,112},{56,120},{... | collective-permute-start | bytes 2162696 | tf_op jit(solution)/shard_map/ppermute | solution.py:418
  50.0 13.6 %copy-start.13 = (bf16[8,32,1408]{2,1,0:T(8,128)(2,1)}, bf16[8,32,1408]{2,1,0:T(8,128)(2,1)S(1)}, u32[]{:S(2)}) copy-start(bf16[8,32,1408]{2,1,0:T(8,128)(2,1)S(1)} %collective-permute-done.3.refs_2_) | copy-start | bytes 2162692
  50.0 13.6 %collective-permute-start.5 = (bf16[8,32,1408]{2,1,0:T(8,128)(2,1)S(1)}, bf16[8,32,1408]{2,1,0:T(8,128)(2,1)}, u32[]{:S(2)}, u32[]{:S(2)}) collective-permute-start(bf16[8,32,1408]{2,1,0:T(8,128)(2,1)S(1)} %collective-permute-done.3.refs_2_), channel_id=1, source_target_pairs={{0,448},{8,456},{16,464},{24,472},{32,480},{40,488},{48,496},{56,5... | collective-permute-start | bytes 2162696 | tf_op jit(solution)/shard_map/ppermute | solution.py:419
  61.7 13.7 %collective-permute-start.6 = (bf16[8,32,1408]{2,1,0:T(8,128)(2,1)}, bf16[8,32,1408]{2,1,0:T(8,128)(2,1)S(1)}, u32[]{:S(2)}, u32[]{:S(2)}) collective-permute-start(bf16[8,32,1408]{2,1,0:T(8,128)(2,1)} %collective-permute-done.4.refs_3_), channel_id=1, source_target_pairs={{0,64},{8,72},{16,80},{24,88},{32,96},{40,104},{48,112},{56,120},{... | collective-permute-start | bytes 2162696 | tf_op jit(solution)/shard_map/ppermute | solution.py:418
  63.6 13.8 %collective-permute-start.7 = (bf16[8,32,1408]{2,1,0:T(8,128)(2,1)}, bf16[8,32,1408]{2,1,0:T(8,128)(2,1)S(1)}, u32[]{:S(2)}, u32[]{:S(2)}) collective-permute-start(bf16[8,32,1408]{2,1,0:T(8,128)(2,1)} %collective-permute-done.5.refs_4_), channel_id=1, source_target_pairs={{0,448},{8,456},{16,464},{24,472},{32,480},{40,488},{48,496},{56,5... | collective-permute-start | bytes 2162696 | tf_op jit(solution)/shard_map/ppermute | solution.py:419
  75.4 11.0 %copy-start.10 = (bf16[8,32,1408]{2,1,0:T(8,128)(2,1)}, bf16[8,32,1408]{2,1,0:T(8,128)(2,1)S(1)}, u32[]{:S(2)}) copy-start(bf16[8,32,1408]{2,1,0:T(8,128)(2,1)S(1)} %collective-permute-done.6.refs_5_) | copy-start | bytes 2162692
  75.5 11.0 %collective-permute-start.8 = (bf16[4,32,1408]{2,1,0:T(8,128)(2,1)S(1)}, bf16[4,32,1408]{2,1,0:T(8,128)(2,1)S(1)}, u32[]{:S(2)}, u32[]{:S(2)}) collective-permute-start(bf16[4,32,1408]{2,1,0:T(8,128)(2,1)S(1)} %slice.26), channel_id=1, source_target_pairs={{0,64},{8,72},{16,80},{24,88},{32,96},{40,104},{48,112},{56,120},{... | collective-permute-start | bytes 1081352 | tf_op jit(solution)/shard_map/ppermute | solution.py:418
  77.4 9.1 %copy-start.11 = (bf16[8,32,1408]{2,1,0:T(8,128)(2,1)}, bf16[8,32,1408]{2,1,0:T(8,128)(2,1)S(1)}, u32[]{:S(2)}) copy-start(bf16[8,32,1408]{2,1,0:T(8,128)(2,1)S(1)} %collective-permute-done.7.refs_6_) | copy-start | bytes 2162692
  77.5 9.0 %collective-permute-start.9 = (bf16[4,32,1408]{2,1,0:T(8,128)(2,1)S(1)}, bf16[4,32,1408]{2,1,0:T(8,128)(2,1)S(1)}, u32[]{:S(2)}, u32[]{:S(2)}) collective-permute-start(bf16[4,32,1408]{2,1,0:T(8,128)(2,1)S(1)} %slice.27), channel_id=1, source_target_pairs={{0,448},{8,456},{16,464},{24,472},{32,480},{40,488},{48,496},{56,5... | collective-permute-start | bytes 1081352 | tf_op jit(solution)/shard_map/ppermute | solution.py:419
  91.5 61.2 %collective-permute-start.14 = (bf16[2048,512]{1,0:T(8,128)(2,1)}, bf16[2048,512]{1,0:T(8,128)(2,1)}, u32[]{:S(2)}, u32[]{:S(2)}) collective-permute-start(bf16[2048,512]{1,0:T(8,128)(2,1)} %shard_map.138.own_ref), channel_id=1, source_target_pairs={{0,4},{4,0},{8,12},{12,8},{16,20},{20,16},{24,28},{28,24},{32,36},... | collective-permute-start | bytes 6291464 | tf_op jit(solution)/shard_map/ppermute | solution.py:483
  114.2 13.1 %collective-permute-start.10 = (bf16[32,256]{1,0:T(8,128)(2,1)S(1)}, bf16[32,256]{1,0:T(8,128)(2,1)S(1)}, u32[]{:S(2)}, u32[]{:S(2)}) collective-permute-start(bf16[32,256]{1,0:T(8,128)(2,1)S(1)} %slice.28), channel_id=1, source_target_pairs={{0,8},{4,12},{8,16},{12,20},{16,24},{20,28},{24,32},{28,36},{32,40... | collective-permute-start | bytes 49160 | tf_op jit(solution)/shard_map/ppermute | solution.py:457
  116.2 11.0 %copy-start.3 = (bf16[1024,256]{1,0:T(8,128)(2,1)S(1)}, bf16[1024,256]{1,0:T(8,128)(2,1)}, u32[]{:S(2)}) copy-start(bf16[1024,256]{1,0:T(8,128)(2,1)} %shard_map.133.glu_ref) | copy-start | bytes 1572868
  125.2 10.7 %copy-start.5 = (s32[6]{0:T(128)S(1)}, s32[6]{0:T(128)}, u32[]{:S(2)}) copy-start(s32[6]{0:T(128)} %stack.31.at_ref) | copy-start | bytes 76
  125.2 10.7 %copy-start.6 = (f32[8]{0:T(128)S(1)}, f32[8]{0:T(128)}, u32[]{:S(2)}) copy-start(f32[8]{0:T(128)} %sinks_ref.1) | copy-start | bytes 100
  125.2 10.7 %collective-permute-start.11 = (bf16[128,128]{1,0:T(8,128)(2,1)S(1)}, bf16[128,128]{1,0:T(8,128)(2,1)S(1)}, u32[]{:S(2)}, u32[]{:S(2)}) collective-permute-start(bf16[128,128]{1,0:T(8,128)(2,1)S(1)} %slice.29), channel_id=1, source_target_pairs={{0,8},{4,12},{8,16},{12,20},{16,24},{20,28},{24,32},{28,36},{32,40... | collective-permute-start | bytes 98312 | tf_op jit(solution)/shard_map/ppermute | solution.py:474
  131.0 16.7 %all-to-all-start.1 = ((f32[8,2,1024]{2,1,0:T(2,128)}), f32[8,2,1024]{2,1,0:T(2,128)S(1)}, u32[]{:S(2)}, u32[]{:S(2)}) async-start(f32[8,2,1024]{2,1,0:T(2,128)} %broadcast_in_dim.4), calls=%async_computation.1 | async-start | bytes 131072 | tf_op jit(solution)/shard_map/all_to_all | solution.py:496
  135.9 16.9 %copy-start.1 = (bf16[2048,512]{1,0:T(8,128)(2,1)S(1)}, bf16[2048,512]{1,0:T(8,128)(2,1)}, u32[]{:S(2)}) copy-start(bf16[2048,512]{1,0:T(8,128)(2,1)} %shard_map.138.own_ref) | copy-start | bytes 6291460
  135.9 1.3 copy-start.2
  145.8 5.8 %collective-permute-start.13 = (bf16[512,256]{1,0:T(8,128)(2,1)}, bf16[512,256]{1,0:T(8,128)(2,1)}, u32[]{:S(2)}, u32[]{:S(2)}) collective-permute-start(bf16[512,256]{1,0:T(8,128)(2,1)} %get-tuple-element.18), channel_id=1, source_target_pairs={{0,4},{4,0},{8,12},{12,8},{16,20},{20,16},{24,28},{28,24},{32,36},... | collective-permute-start | bytes 786440 | tf_op jit(solution)/shard_map/ppermute | solution.py:513
  149.2 3.6 %collective-permute-start.12 = (bf16[512,256]{1,0:T(8,128)(2,1)S(1)}, bf16[512,256]{1,0:T(8,128)(2,1)S(1)}, u32[]{:S(2)}, u32[]{:S(2)}) collective-permute-start(bf16[512,256]{1,0:T(8,128)(2,1)S(1)} %get-tuple-element.17), channel_id=1, source_target_pairs={{0,4},{4,0},{8,12},{12,8},{16,20},{20,16},{24,28},{28,24},{32,36},... | collective-permute-start | bytes 786440 | tf_op jit(solution)/shard_map/ppermute | solution.py:523
  152.7 1.0 copy-start.8
  160.9 27.2 %collective-permute-start.17 = (bf16[128,2048]{1,0:T(8,128)(2,1)}, bf16[128,2048]{1,0:T(8,128)(2,1)S(1)}, u32[]{:S(2)}, u32[]{:S(2)}) collective-permute-start(bf16[128,2048]{1,0:T(8,128)(2,1)} %get-tuple-element.22), channel_id=1, source_target_pairs={{0,3},{1,0},{2,1},{3,2},{4,7},{5,4},{6,5},{7,6},{8,11},{9,8},{10,9... | collective-permute-start | bytes 1572872 | tf_op jit(solution)/shard_map/ppermute | solution.py:548
  165.6 22.5 %collective-permute-start.16 = (bf16[128,2048]{1,0:T(8,128)(2,1)}, bf16[128,2048]{1,0:T(8,128)(2,1)S(1)}, u32[]{:S(2)}, u32[]{:S(2)}) collective-permute-start(bf16[128,2048]{1,0:T(8,128)(2,1)} %get-tuple-element.21), channel_id=1, source_target_pairs={{0,1},{1,2},{2,3},{3,0},{4,5},{5,6},{6,7},{7,4},{8,9},{9,10},{10,1... | collective-permute-start | bytes 1572872 | tf_op jit(solution)/shard_map/ppermute | solution.py:548
  167.5 24.8 %collective-permute-start.15 = (bf16[128,2048]{1,0:T(8,128)(2,1)S(1)}, bf16[128,2048]{1,0:T(8,128)(2,1)S(1)}, u32[]{:S(2)}, u32[]{:S(2)}) collective-permute-start(bf16[128,2048]{1,0:T(8,128)(2,1)S(1)} %get-tuple-element.20), channel_id=1, source_target_pairs={{0,2},{1,3},{2,0},{3,1},{4,6},{5,7},{6,4},{7,5},{8,10},{9,11},{10,... | collective-permute-start | bytes 1572872 | tf_op jit(solution)/shard_map/ppermute | solution.py:548
  171.2 3.7 %collective-permute-start.18 = (f32[4,512]{1,0:T(4,128)S(1)}, f32[4,512]{1,0:T(4,128)S(1)}, u32[]{:S(2)}, u32[]{:S(2)}) collective-permute-start(f32[4,512]{1,0:T(4,128)S(1)} %get-tuple-element.27), channel_id=1, source_target_pairs={{0,4},{4,0},{8,12},{12,8},{16,20},{20,16},{24,28},{28,24},{32,36},... | collective-permute-start | bytes 24584 | tf_op jit(solution)/shard_map/ppermute | solution.py:527
  (4 other events, 2.8 us)

commit v3 on v2

--- a/solution.py
+++ b/solution.py
@@ -66,8 +66,9 @@
 
 
 def pack_kernel(at_ref, *refs):
-    count = (len(refs) - 2) // 2
-    shards, out_ref, held, sems = refs[:count], refs[count], refs[count + 1 : -1], refs[-1]
+    count = (len(refs) - 3) // 2
+    shards, held, sems = refs[:count], refs[count + 2 : -1], refs[-1]
+    kept_ref, given_ref = refs[count : count + 2]
     copies = [
         pltpu.make_async_copy(shard, here, sems.at[index])
         for index, (shard, here) in enumerate(zip(shards, held))
@@ -86,16 +87,22 @@
         jnp.where(lane < HEAD_DIM, pltpu.roll(key, HEAD_DIM, 1), value),
     )
     for half in range(CORES):
-        to = jnp.bitwise_xor(core, half)
-        at = 0
+        parts = []
         for source in (value_ref, gate_ref, query_ref, None, conv_ref, attn_ref):
             if source is None:
-                part = both[half].astype(jnp.bfloat16)
+                parts.append(both[half].astype(jnp.bfloat16))
             else:
                 width = source.shape[1] // CORES
-                part = source[:, half * width : (half + 1) * width]
-            out_ref[to, :, at : at + part.shape[1]] = part
-            at += part.shape[1]
+                parts.append(source[:, half * width : (half + 1) * width])
+        whole = jnp.concatenate(parts, axis=1)
+
+        @pl.when(core == half)
+        def _():
+            kept_ref[...] = whole
+
+        @pl.when(core != half)
+        def _():
+            given_ref[...] = whole
 
 
 def repeat_kernel(at_ref, kept_ref, got_ref, out_ref):
@@ -106,78 +113,105 @@
             out_ref[member, to, :] = source[...]
 
 
-def fetch(at_ref, pieces, out_ref, sem, columns):
-    block = pieces[0].shape[1]
-    line, line_rows, step_rows = at_ref[0], at_ref[1], at_ref[2]
-    for index, piece in enumerate(pieces):
-        away = (index + 1) // 2 * (1 if index % 2 == 0 else -1)
-        from_line = jnp.bitwise_and(line + away, SIDE - 1)
-        count = piece.shape[0]
-        first = SIDE - count if index == SIDE else 0
-        for step in range(count):
-            to = pl.multiple_of(from_line * line_rows + (first + step) * step_rows, block)
-            pltpu.make_async_copy(
-                piece.at[step, :, pl.ds(*columns)], out_ref.at[pl.ds(to, block), :], sem
-            ).start()
-    pltpu.make_async_copy(out_ref, out_ref, sem).wait()
+def norm_kernel(at_ref, own_ref, other_ref, gain_ref, out_ref):
+    core = at_ref[3]
+    count, model = own_ref.shape
+    group = model // CHIPS
+    tile = 32
+    lane = lax.broadcasted_iota(jnp.int32, (tile, 128), 1)
+    gain = gain_ref[...].astype(jnp.float32)
+
+    @pl.loop(0, count // tile)
+    def _(step):
+        at = pl.multiple_of(step * tile, tile)
+        for source, to_core in ((own_ref, core), (other_ref, 1 - core)):
+            x = source[pl.ds(at, tile), :].astype(jnp.float32)
+            scale = lax.rsqrt(jnp.mean(x * x, axis=-1, keepdims=True) + NORM_EPS)
+            normed = x * scale * gain
+            rows = pl.ds(pl.multiple_of(to_core * count + at, tile), tile)
+
+            @pl.when(core == 0)
+            def _():
+                out_ref[rows, :] = normed.astype(jnp.bfloat16)
+
+            @pl.when(core == 1)
+            def _():
+                for to in range(0, model, 128):
+                    y, z = to // group // SIDE, to // group % SIDE
+                    out = jnp.zeros((tile, 128), jnp.float32)
+                    for part in range(128 // group):
+                        start = ((z + part) * SIDE + y) * group
+                        tile_at = start // 128 * 128
+                        turned = pltpu.roll(
+                            normed[:, tile_at : tile_at + 128],
+                            (part * group - start % 128) % 128,
+                            1,
+                        )
+                        out = jnp.where(lane // group == part, turned, out)
+                    out_ref[rows, to : to + 128] = out.astype(jnp.bfloat16)
+
+
+def line_of(at_ref, index):
+    away = (index + 1) // 2 * (1 if index % 2 == 0 else -1)
+    first = SIDE // 2 if index == SIDE else 0
+    return jnp.bitwise_and(at_ref[0] + away, SIDE - 1), first
+
+
+def products(at_ref, x_ref, rows, pieces, first, held_ref):
+    parts = []
+    for index, piece in enumerate(pieces, first):
+        line, step = line_of(at_ref, index)
+        block = piece.shape[1]
+        size = piece.shape[0] * block
+        start = pl.multiple_of(line * (SIDE * block) + step * block, 128)
+        parts.append(x_ref[rows, pl.ds(start, size)])
+    return jnp.dot(jnp.concatenate(parts, axis=1), held_ref[...], preferred_element_type=jnp.float32)
+
+
+def hold(pieces, held_ref):
+    to = 0
+    for piece in pieces:
+        for step in range(piece.shape[0]):
+            held_ref[to : to + piece.shape[1], :] = piece[step, :, : held_ref.shape[1]]
+            to += piece.shape[1]
 
 
 def rows_of(step):
     return pl.ds(pl.multiple_of(step * TILE, TILE), TILE)
 
 
-def tile_copy(x_ref, x_here, sems, step):
-    rows = rows_of(step)
-    return pltpu.make_async_copy(x_ref.at[rows, :], x_here.at[rows, :], sems.at[step])
-
-
-def gated_kernel(columns, at_ref, x_ref, *refs):
-    pieces, (out_ref, w_ref, sem, x_here, x_sems) = refs[:-5], refs[-5:]
-    tiles = x_ref.shape[0] // TILE
-    for step in range(tiles):
-        tile_copy(x_ref, x_here, x_sems, step).start()
-    fetch(at_ref, pieces, w_ref, sem, columns)
-    half = out_ref.shape[1]
-
-    @pl.loop(0, tiles)
+def early_kernel(first, count, at_ref, x_ref, *refs):
+    pieces, before, (out_ref, held_ref) = refs[:count], refs[count:-2], refs[-2:]
+    hold(pieces, held_ref)
+
+    @pl.loop(0, x_ref.shape[0] // TILE)
     def _(step):
-        tile_copy(x_ref, x_here, x_sems, step).wait()
         rows = rows_of(step)
-        both = jnp.dot(x_here[rows, :], w_ref[...], preferred_element_type=jnp.float32)
-        both = both.astype(jnp.bfloat16).astype(jnp.float32)
-        out_ref[rows, :] = (both[:, :half] * jax.nn.sigmoid(both[:, half:])).astype(jnp.bfloat16)
-
-
-def rotated_kernel(columns, at_ref, x_ref, cos_ref, sin_ref, *refs):
-    pieces, (out_ref, w_ref, sem, x_here, x_sems, cos_here, sin_here, table_sems) = (
-        refs[:-8],
-        refs[-8:],
-    )
-    tiles = x_ref.shape[0] // TILE
-    for step in range(tiles):
-        tile_copy(x_ref, x_here, x_sems, step).start()
-    tables = (
-        pltpu.make_async_copy(cos_ref, cos_here, table_sems.at[0]),
-        pltpu.make_async_copy(sin_ref, sin_here, table_sems.at[1]),
-    )
-    for table in tables:
-        table.start()
-    fetch(at_ref, pieces, w_ref, sem, columns)
-    for table in tables:
-        table.wait()
-    width = out_ref.shape[1]
-
-    @pl.loop(0, tiles)
+        total = products(at_ref, x_ref, rows, pieces, first, held_ref)
+        for other in before:
+            total = total + other[rows, :]
+        out_ref[rows, :] = total
+
+
+def late_kernel(
+    first, at_ref, x_ref, cos_ref, sin_ref, before_ref, a_ref, b_ref, glu_ref, qkv_ref, tail_ref, held_ref
+):
+    pieces = (a_ref, b_ref)
+    hold(pieces, held_ref)
+    channels, width = glu_ref.shape[1], qkv_ref.shape[1]
+
+    @pl.loop(0, x_ref.shape[0] // TILE)
     def _(step):
-        tile_copy(x_ref, x_here, x_sems, step).wait()
         rows = rows_of(step)
-        raw = jnp.dot(x_here[rows, :], w_ref[...], preferred_element_type=jnp.float32)
-        raw = raw.astype(jnp.bfloat16).astype(jnp.float32)
+        total = products(at_ref, x_ref, rows, pieces, first, held_ref) + before_ref[rows, :]
+        raw = total.astype(jnp.bfloat16).astype(jnp.float32)
+        value, gate = raw[:, :channels], raw[:, channels : 2 * channels]
+        glu_ref[rows, :] = (value * jax.nn.sigmoid(gate)).astype(jnp.bfloat16)
         lane = lax.broadcasted_iota(jnp.int32, (TILE, 128), 1)
         front = jnp.bitwise_and(lane, HEAD_DIM - 1) < HEAD_DIM // 2
-        cosine, sine = cos_here[rows, :], sin_here[rows, :]
+        cosine, sine = cos_ref[rows, :], sin_ref[rows, :]
         for at in range(0, width, 128):
-            part = raw[:, at : at + 128]
+            part = raw[:, 2 * channels + at : 2 * channels + at + 128]
             other = jnp.where(
                 front,
                 pltpu.roll(part, 128 - HEAD_DIM // 2, 1),
@@ -186,20 +220,31 @@
             turned = part * cosine + other * sine
             if at + 128 == width:
                 turned = jnp.where(lane < HEAD_DIM, turned, part)
-            out_ref[rows, at : at + 128] = turned.astype(jnp.bfloat16)
-
-
-def order_kernel(columns, at_ref, *refs):
-    pieces, (out_ref, sem) = refs[:-2], refs[-2:]
-    fetch(at_ref, pieces, out_ref, sem, columns)
+            qkv_ref[rows, at : at + 128] = turned.astype(jnp.bfloat16)
+
+    end = x_ref.shape[0]
+    tail_ref[0:WINDOW, :] = qkv_ref[end - WINDOW : end, width - 128 : width]
+    tail_ref[WINDOW : WINDOW + 32, :] = glu_ref[end - 32 : end, :128]
+    tail_ref[WINDOW + 32 : WINDOW + 64, :] = glu_ref[end - 32 : end, 128:]
+
+
+def join_kernel(column, at_ref, *refs):
+    pieces, out_ref = refs[:-1], refs[-1]
+    for index, piece in enumerate(pieces):
+        line, first = line_of(at_ref, index)
+        block = piece.shape[1]
+        for step in range(piece.shape[0]):
+            to = pl.multiple_of(line * (SIDE * block) + (first + step) * block, block)
+            out_ref[pl.ds(to, block), :] = piece[step, :, column:]
 
 
 def conv_kernel(before_ref, glu_ref, taps_ref, out_ref, sums_ref, ext_ref):
     count, rows = taps_ref.shape[0], glu_ref.shape[0]
-    lead = before_ref.shape[0]
+    lead = 32
     for part in range(2):
         lanes = pl.ds(part * 128, 128)
-        ext_ref[part, pl.ds(0, lead), :] = before_ref[:, lanes].astype(jnp.float32)
+        held = pl.ds(WINDOW + part * lead, lead)
+        ext_ref[part, pl.ds(0, lead), :] = before_ref[held, :].astype(jnp.float32)
         ext_ref[part, pl.ds(lead, rows), :] = glu_ref[:, lanes].astype(jnp.float32)
 
     @pl.loop(0, rows // 128)
@@ -216,18 +261,22 @@
             out_ref[pl.ds(base, 128), lanes] = total
             first = first + total
             second = second + total * total
-        sums_ref[pl.ds(0, 1), pl.ds(base, 128)] = jnp.sum(first.T, axis=0, keepdims=True)
-        sums_ref[pl.ds(1, 1), pl.ds(base, 128)] = jnp.sum(second.T, axis=0, keepdims=True)
-
-
-def scaled_kernel(at_ref, conv_ref, sums_ref, gain_ref, kept_ref, given_ref):
+        first = jnp.sum(first.T, axis=0, keepdims=True)
+        second = jnp.sum(second.T, axis=0, keepdims=True)
+        for member in range(sums_ref.shape[0]):
+            sums_ref[member, pl.ds(0, 1), pl.ds(base, 128)] = first
+            sums_ref[member, pl.ds(1, 1), pl.ds(base, 128)] = second
+
+
+def scaled_kernel(at_ref, conv_ref, sums_ref, gain_ref, attn_ref, kept_ref, given_ref):
     core = at_ref[3]
     totals = sums_ref[0]
     for member in range(1, sums_ref.shape[0]):
         totals = totals + sums_ref[member]
     mean = totals[0:1] / CONV_CH
     scale = lax.rsqrt(totals[1:2] / CONV_CH - mean * mean + CHANNEL_EPS)
-    half = kept_ref.shape[0]
+    half, channels = kept_ref.shape
+    given_ref[:, channels:] = attn_ref[...]
     for base in range(0, conv_ref.shape[0], 128):
         at = slice(base, base + 128)
         mean_at = jnp.broadcast_to(mean[:, at], (128, 128)).T
@@ -245,7 +294,7 @@
 
         @pl.when(core != base // half)
         def _():
-            given_ref[to, :] = out
+            given_ref[to, :channels] = out
 
 
 def attention_kernel(
@@ -253,9 +302,8 @@
 ):
     core, first_chip = at_ref[3], at_ref[4]
     cols = kept_ref.shape[1]
-    lead = before_ref.shape[0]
-    for source, to in ((before_ref, 0), (qkv_ref, lead)):
-        both = source[:, source.shape[1] - 128 :].astype(jnp.float32)
+    for source, to, count in ((before_ref, 0, WINDOW), (qkv_ref, WINDOW, qkv_ref.shape[0])):
+        both = source[:count, source.shape[1] - 128 :].astype(jnp.float32)
         low = lax.broadcasted_iota(jnp.int32, both.shape, 1) < HEAD_DIM
         turned = pltpu.roll(both, HEAD_DIM, 1)
         rows = slice(to, to + both.shape[0])
@@ -316,25 +364,30 @@
 
 
 def output_kernel(
-    steps, at_ref, conv_ref, attn_ref, conv_got, attn_got, own_ref, other_ref, *out_refs
+    steps, at_ref, conv_ref, attn_ref, got_ref, own_ref, other_ref, *rest
 ):
-    member, half = at_ref[5], conv_ref.shape[1]
+    out_refs, w_ref = rest[:-1], rest[-1]
+    core, member, half = at_ref[3], at_ref[5], conv_ref.shape[1]
     count = out_refs[0].shape[0]
     peers = conv_ref.shape[0] // count
-
-    @pl.loop(0, out_refs[0].shape[1] // TILE)
-    def _(step):
-        cols = pl.ds(pl.multiple_of(step * TILE, TILE), TILE)
-        total = jnp.zeros((conv_ref.shape[0], TILE), jnp.float32)
-        for left, right, at in (
-            (conv_ref, own_ref, 0),
-            (attn_ref, own_ref, half),
-            (conv_got, other_ref, 0),
-            (attn_got, other_ref, half),
-        ):
+    block = own_ref.shape[0] // CHIPS
+    width = own_ref.shape[1]
+
+    @pl.loop(0, SIDE)
+    def _(z):
+        cols = pl.ds(pl.multiple_of(z * SIDE * block, TILE), SIDE * block)
+        by_z, by_y = z * SIDE * block, z * block
+        for source, at, along_z in ((own_ref, 0, core == 0), (other_ref, width, core == 1)):
+            first = jnp.where(along_z, by_z, by_y)
+            stride = jnp.where(along_z, block, SIDE * block)
+            for y in range(SIDE):
+                start = pl.multiple_of(first + y * stride, block)
+                w_ref[y * block : (y + 1) * block, at : at + width] = source[pl.ds(start, block), :]
+        total = jnp.zeros((conv_ref.shape[0], SIDE * block), jnp.float32)
+        for left, at in ((conv_ref, 0), (attn_ref, half), (got_ref, width)):
             total = total + lax.dot_general(
                 left[...],
-                right[cols, at : at + half],
+                w_ref[:, at : at + left.shape[1]],
                 (((1,), (1,)), ((), ())),
                 preferred_element_type=jnp.float32,
             )
@@ -389,9 +442,9 @@
     out_cols = (2 * channels + q_cols + 2 * HEAD_DIM, channels + q_cols)
     width = sum(out_cols)
     shards_in = (w_conv_value, w_conv_gate, w_query, w_key, w_value, out_conv.T, out_attn.T)
-    halves = call(
+    kept, given = call(
         pack_kernel,
-        shape((CORES, depth, width)),
+        (shape((depth, width)),) * 2,
         1 << 20,
         [SMEM] + [HBM] * len(shards_in),
         (at, *shards_in),
@@ -400,13 +453,13 @@
             pltpu.SemaphoreType.DMA((len(shards_in),)),
         ),
     )
-    got = lax.ppermute(halves[1], SP, OTHER_CORE)
+    got = lax.ppermute(given, SP, OTHER_CORE)
     sent = call(
         repeat_kernel,
         shape((SIDE, block, width)),
         1 << 20,
         [SMEM, VMEM, VMEM],
-        (at, halves[0], got),
+        (at, kept, got),
         limit=12,
     )
     own_line = lax.all_to_all(sent, SP, 0, 0, tiled=True, axis_index_groups=LINES)
@@ -420,17 +473,14 @@
         pieces += [ahead, behind]
 
     tokens_other = lax.ppermute(tokens, SP, OTHER_CORE)
-    both = jnp.where(
-        core == 0,
-        jnp.concatenate([tokens, tokens_other], axis=0),
-        jnp.concatenate([tokens_other, tokens], axis=0),
-    )
-    as_float = both.astype(jnp.float32)
-    normed = (
-        as_float
-        * lax.rsqrt(jnp.mean(as_float * as_float, axis=-1, keepdims=True) + NORM_EPS)
-        * norm_gain.astype(jnp.float32)
-    ).astype(jnp.bfloat16)
+    normed = call(
+        norm_kernel,
+        shape((row_count, model)),
+        1 << 30,
+        [SMEM, VMEM, VMEM, VMEM],
+        (at, tokens, tokens_other, norm_gain[None]),
+        limit=16,
+    )
 
     positions = chip * row_count + jnp.arange(row_count, dtype=jnp.int32)
     half_dim = HEAD_DIM // 2
@@ -440,62 +490,55 @@
     cosines = jnp.concatenate([cosine] * 4, axis=1)
     sines = jnp.concatenate([-sine, sine] * 2, axis=1)
 
-    spots = [HBM] * len(pieces)
-    glu = call(
-        functools.partial(gated_kernel, conv_cols),
-        shape((row_count, channels)),
-        2 * row_count * model * conv_cols[1],
-        [SMEM, HBM] + spots,
-        (at, normed, *pieces),
-        (
-            pltpu.VMEM((model, conv_cols[1]), jnp.bfloat16),
-            pltpu.SemaphoreType.DMA,
-            pltpu.VMEM(normed.shape, jnp.bfloat16),
-            pltpu.SemaphoreType.DMA((row_count // TILE,)),
-        ),
-    )
-    glu_before = lax.ppermute(glu[row_count - 32 :], SP, NEXT_CHIP)
-    qkv = call(
-        functools.partial(rotated_kernel, qkv_cols),
-        shape((row_count, qkv_cols[1])),
-        2 * row_count * model * qkv_cols[1],
-        [SMEM, HBM, HBM, HBM] + spots,
-        (at, normed, cosines, sines, *pieces),
-        (
-            pltpu.VMEM((model, qkv_cols[1]), jnp.bfloat16),
-            pltpu.SemaphoreType.DMA,
-            pltpu.VMEM(normed.shape, jnp.bfloat16),
-            pltpu.SemaphoreType.DMA((row_count // TILE,)),
-            pltpu.VMEM(cosines.shape, jnp.float32),
-            pltpu.VMEM(sines.shape, jnp.float32),
-            pltpu.SemaphoreType.DMA((2,)),
-        ),
-    )
-    kv_before = lax.ppermute(qkv[row_count - WINDOW :, q_cols:], SP, NEXT_CHIP)
+    in_cols = conv_cols[1] + qkv_cols[1]
+    lines = SIDE * block
+
+    def early(first, last, before):
+        held = pieces[first:last]
+        return call(
+            functools.partial(early_kernel, first, len(held)),
+            shape((row_count, in_cols), jnp.float32),
+            2 * row_count * lines * len(held) * in_cols,
+            [SMEM] + [VMEM] * (1 + len(held) + len(before)),
+            (at, normed, *held, *before),
+            (pltpu.VMEM((lines * len(held), in_cols), jnp.bfloat16),),
+            limit=16,
+        )
+
+    total = early(0, 5, ())
+    total = early(5, 7, (total,))
+    glu, qkv, tail = call(
+        functools.partial(late_kernel, 7),
+        (shape((row_count, channels)), shape((row_count, qkv_cols[1])), shape((WINDOW + 64, 128))),
+        2 * row_count * lines * in_cols,
+        [SMEM] + [VMEM] * 6,
+        (at, normed, cosines, sines, total, *pieces[7:]),
+        (pltpu.VMEM((lines, in_cols), jnp.bfloat16),),
+        limit=16,
+    )
+    before = lax.ppermute(tail, SP, NEXT_CHIP)
     out_own = call(
-        functools.partial(order_kernel, out_cols),
+        functools.partial(join_kernel, out_cols[0]),
         shape((model, out_cols[1])),
         1 << 28,
-        [SMEM] + spots,
+        [SMEM] + [VMEM] * len(pieces),
         (at, *pieces),
-        (pltpu.SemaphoreType.DMA,),
+        limit=12,
     )
     out_other = lax.ppermute(out_own, SP, OTHER_CORE)
 
     taps = lax.dynamic_slice_in_dim(conv_taps, core * channels, channels, 1)
+    members = CORES * lax.axis_size("tp")
     conv_out, sums = call(
         conv_kernel,
-        (shape((row_count, channels), jnp.float32), shape((2, row_count), jnp.float32)),
+        (shape((row_count, channels), jnp.float32), shape((members, 2, row_count), jnp.float32)),
         1 << 32,
         [VMEM] * 3,
-        (glu_before, glu, taps),
+        (before, glu, taps),
         (pltpu.VMEM((2, row_count + 32, 128), jnp.float32),),
         limit=12,
     )
-    members = CORES * lax.axis_size("tp")
-    everyones = lax.all_to_all(
-        jnp.broadcast_to(sums[None], (members, *sums.shape)), CHIP, 0, 0, tiled=True
-    )
+    everyones = lax.all_to_all(sums, CHIP, 0, 0, tiled=True)
     extended = pltpu.VMEM((row_count + WINDOW, 128), jnp.bfloat16)
     attn_kept, attn_given, log_rows = call(
         attention_kernel,
@@ -506,21 +549,20 @@
         ),
         1 << 32,
         [SMEM, SMEM, VMEM, VMEM],
-        (at, sinks, qkv, kv_before),
+        (at, sinks, qkv, before),
         (extended,) * 4,
         limit=12,
     )
-    attn_got = lax.ppermute(attn_given, SP, OTHER_CORE)
     gain = lax.dynamic_slice_in_dim(ln_gain, core * channels, channels, 0)
-    conv_kept, conv_given = call(
+    conv_kept, given = call(
         scaled_kernel,
-        (shape((own_rows, channels)),) * 2,
+        (shape((own_rows, channels)), shape((own_rows, channels + q_cols))),
         1 << 28,
-        [SMEM, VMEM, VMEM, VMEM],
-        (at, conv_out, everyones, gain[None]),
+        [SMEM] + [VMEM] * 4,
+        (at, conv_out, everyones, gain[None], attn_given),
         limit=12,
     )
-    conv_got = lax.ppermute(conv_given, SP, OTHER_CORE)
+    rows_got = lax.ppermute(given, SP, OTHER_CORE)
 
     kept = lax.dynamic_slice_in_dim(log_rows, core * own_rows, own_rows, 1)
     given = lax.dynamic_slice_in_dim(log_rows, (1 - core) * own_rows, own_rows, 1)
@@ -539,8 +581,9 @@
             functools.partial(output_kernel, steps),
             (shape((share, model)),) * len(steps),
             2 * share * len(steps) * model * 2 * out_cols[1],
-            [SMEM] + [VMEM] * 6,
-            (at, conv_kept, attn_kept, conv_got, attn_got, out_own, out_other),
+            [SMEM] + [VMEM] * 5,
+            (at, conv_kept, attn_kept, rows_got, out_own, out_other),
+            (pltpu.VMEM((TILE, 2 * out_cols[1]), jnp.bfloat16),),
             limit=16,
         )
 

time: 195 us -> 195 us (level)
  other arithmetic: 16.4 us -> 9.25 us
  waiting for transfers between devices: 29.3 us -> 35.2 us
  Pallas kernels: 41.4 us -> 46.1 us
  starting transfers between devices: 77.1 us -> 73.8 us
    convert_element_type x2 -> x0, other arithmetic: 6.45 us -> none  [the longest x1 5.76 us: layer(): normed = (as_float * lax.rsqrt(jnp.mean(as_float * as_float, axis=-1, kee...]
    ppermute x4, waiting for transfers between devices: 9.63 us -> 15.4 us  [layer(): ahead = lax.ppermute(ahead, SP, AHEAD)]
    pallas_call x9 -> x11, Pallas kernels: 41.4 us -> 46.1 us  [call(): pl.pallas_call(body, out_shape=outs, in_specs=in_specs, out_specs=jax.tre...]
    ppermute x5 -> x3, starting transfers between devices: 17.2 us -> 12.8 us  [the longest x1 8.74 us: layer(): got = lax.ppermute(given, SP, OTHER_CORE)]
    reduce_sum x1 -> x0, other arithmetic: 4.36 us -> none  [layer(): jnp.mean(as_float * as_float, axis=-1, keepdims=True) + NORM_EPS]
    ppermute x3, waiting for transfers between devices: 16.8 us -> 12.6 us  [to_member(): lax.ppermute(value, 'tp', [(i, (i + away) % peers) for i in range(peers)])]
    ppermute x4, waiting for transfers between devices: 0.01 us -> 2.39 us  [layer(): behind = lax.ppermute(behind, SP, BEHIND)]
    ppermute x5 -> x3, waiting for transfers between devices: 1.99 us -> 3.98 us  [the longest x1 1.88 us: layer(): rows_got = lax.ppermute(given, SP, OTHER_CORE)]
  transfers between devices with their start and end apart: 20 -> 18, of which waited for: 8 -> 10; matrix products, arithmetic and copies ran while one was open for 9% -> 5% of each run, Pallas kernels for 14% -> 19%
where the time goes in v3:
time: 195 us; the launch traced here: 193 us
  starting transfers between devices  73.8 us (38%)
  Pallas kernels  46.1 us (24%)
  waiting for transfers between devices  35.2 us (18%)
  blocking collectives  18.7 us (10%)
  other arithmetic  9.25 us (5%)
  local copies, waits for them, and re-layouts  8.77 us (4%)
    pallas_call x11, Pallas kernels, call(): pl.pallas_call(body, out_shape=outs, in_specs=in_specs, out_specs=jax.tre...  46.1 us
    all_to_all x1, blocking collectives, layer(): lax.all_to_all(sent, SP, 0, 0, tiled=True, axis_index_groups=LINES)  18.7 us
    ppermute x4, starting transfers between devices, layer(): behind = lax.ppermute(behind, SP, BEHIND)  17.3 us
    ppermute x4, waiting for transfers between devices, layer(): ahead = lax.ppermute(ahead, SP, AHEAD)  15.4 us
    ppermute x3, waiting for transfers between devices, to_member(): lax.ppermute(value, 'tp', [(i, (i + away) % peers) for i in range(peers)])  12.6 us
    ppermute x3, starting transfers between devices, to_member(): lax.ppermute(value, 'tp', [(i, (i + away) % peers) for i in range(peers)])  11.3 us
    ppermute x4, starting transfers between devices, layer(): ahead = lax.ppermute(ahead, SP, AHEAD)  9.1 us
    ppermute x1, starting transfers between devices, layer(): got = lax.ppermute(given, SP, OTHER_CORE)  8.74 us
  transfers between devices with their start and end apart: 18, of which 10 were waited for; matrix products, arithmetic and copies ran while one was open for 5% of the time, Pallas kernels for 19%

profile of v3, /device:TPU:1, one launch (start us, length us, event | category | flops | bytes accessed | tf_op | source)
XLA Modules:
  0.0 192.9 jit_solution(4641543957612570300)
XLA Ops:
  1.3 2.4 %shard_map.132 = (bf16[16,1408]{1,0:T(8,128)(2,1)}, bf16[16,1408]{1,0:T(8,128)(2,1)}) custom-call(s32[6]{0:T(128)} %stack.31.at_ref, bf16[16,512]{1,0:T(8,128)(2,1)} %refs_0_.1, bf16[16,512]{1,0:T(8,128)(2,1)} %refs_1_.1, bf16[16,512]{1,0:T(8,128)(2,1)} %refs_2_.1, bf16[16,128]{1,0:T(8,128)(2,1)} %refs_3_.1, bf16[16,128]{1,0:T(8,128)(2,1)} %refs_4_.1, ...), custom_call_target="tpu_custom_call" | custom-call | flops 1048576 | bytes 1048576 | tf_op jit(solution)/shard_map/pallas_call | solution.py:53
  3.7 8.7 %collective-permute-start.1 = (bf16[16,1408]{1,0:T(8,128)(2,1)}, bf16[16,1408]{1,0:T(8,128)(2,1)S(1)}, u32[]{:S(2)}, u32[]{:S(2)}) collective-permute-start(bf16[16,1408]{1,0:T(8,128)(2,1)} %get-tuple-element.19), channel_id=1, source_target_pairs={{0,4},{4,0},{8,12},{12,8},{16,20},{20,16},{24,28},{28,24},{32,36},... | collective-permute-start | bytes 135176 | tf_op jit(solution)/shard_map/ppermute | solution.py:456
  15.5 18.7 %all_to_all.10.refs_0_ = bf16[8,32,1408]{2,1,0:T(8,128)(2,1)S(1)} all-to-all(bf16[8,32,1408]{2,1,0:T(8,128)(2,1)S(1)} %shard_map.133), channel_id=1, replica_groups={{0,8,16,24,32,40,48,56},{64,72,80,88,96,104,112,120},{128,136,144,152,1..., dimensions={0} | all-to-all | bytes 1441792 | tf_op jit(solution)/shard_map/all_to_all | solution.py:465
  34.2 3.2 %collective-permute-start.2 = (bf16[8,32,1408]{2,1,0:T(8,128)(2,1)S(1)}, bf16[8,32,1408]{2,1,0:T(8,128)(2,1)S(1)}, u32[]{:S(2)}, u32[]{:S(2)}) collective-permute-start(bf16[8,32,1408]{2,1,0:T(8,128)(2,1)S(1)} %all_to_all.10.refs_0_), channel_id=1, source_target_pairs={{0,64},{8,72},{16,80},{24,88},{32,96},{40,104},{48,112},{56,120},{... | collective-permute-start | bytes 2162696 | tf_op jit(solution)/shard_map/ppermute | solution.py:471
  37.4 3.8 %collective-permute-start.5 = (bf16[8,32,1408]{2,1,0:T(8,128)(2,1)S(1)}, bf16[8,32,1408]{2,1,0:T(8,128)(2,1)S(1)}, u32[]{:S(2)}, u32[]{:S(2)}) collective-permute-start(bf16[8,32,1408]{2,1,0:T(8,128)(2,1)S(1)} %all_to_all.10.refs_0_), channel_id=1, source_target_pairs={{0,448},{8,456},{16,464},{24,472},{32,480},{40,488},{48,496},{56,5... | collective-permute-start | bytes 2162696 | tf_op jit(solution)/shard_map/ppermute | solution.py:472
  41.3 7.0 %collective-permute-done.2.refs_1_ = bf16[8,32,1408]{2,1,0:T(8,128)(2,1)S(1)} collective-permute-done((bf16[8,32,1408]{2,1,0:T(8,128)(2,1)S(1)}, bf16[8,32,1408]{2,1,0:T(8,128)(2,1)S(1)}, u32[]{:S(2)}, u32[]{:S(2)}) %collective-permute-start.2) | collective-permute-done | bytes 720928 | tf_op jit(solution)/shard_map/ppermute | solution.py:471
  50.2 4.6 %collective-permute-start.6 = (bf16[8,32,1408]{2,1,0:T(8,128)(2,1)S(1)}, bf16[8,32,1408]{2,1,0:T(8,128)(2,1)S(1)}, u32[]{:S(2)}, u32[]{:S(2)}) collective-permute-start(bf16[8,32,1408]{2,1,0:T(8,128)(2,1)S(1)} %collective-permute-done.5.refs_2_), channel_id=1, source_target_pairs={{0,448},{8,456},{16,464},{24,472},{32,480},{40,488},{48,496},{56,5... | collective-permute-start | bytes 2162696 | tf_op jit(solution)/shard_map/ppermute | solution.py:472
  55.6 7.3 %collective-permute-start = (bf16[512,2048]{1,0:T(8,128)(2,1)}, bf16[512,2048]{1,0:T(8,128)(2,1)}, u32[]{:S(2)}, u32[]{:S(2)}) collective-permute-start(bf16[512,2048]{1,0:T(8,128)(2,1)} %own_ref.1), channel_id=1, source_target_pairs={{0,4},{4,0},{8,12},{12,8},{16,20},{20,16},{24,28},{28,24},{32,36},... | collective-permute-start | bytes 6291464 | tf_op jit(solution)/shard_map/ppermute | solution.py:475
  65.9 4.4 %collective-permute-start.7 = (bf16[8,32,1408]{2,1,0:T(8,128)(2,1)S(1)}, bf16[8,32,1408]{2,1,0:T(8,128)(2,1)S(1)}, u32[]{:S(2)}, u32[]{:S(2)}) collective-permute-start(bf16[8,32,1408]{2,1,0:T(8,128)(2,1)S(1)} %collective-permute-done.6.refs_4_), channel_id=1, source_target_pairs={{0,448},{8,456},{16,464},{24,472},{32,480},{40,488},{48,496},{56,5... | collective-permute-start | bytes 2162696 | tf_op jit(solution)/shard_map/ppermute | solution.py:472
  70.3 6.1 %collective-permute-done.4.refs_0_.refs_5_ = bf16[8,32,1408]{2,1,0:T(8,128)(2,1)S(1)} collective-permute-done((bf16[8,32,1408]{2,1,0:T(8,128)(2,1)S(1)}, bf16[8,32,1408]{2,1,0:T(8,128)(2,1)S(1)}, u32[]{:S(2)}, u32[]{:S(2)}) %collective-permute-start.4) | collective-permute-done | bytes 720928 | tf_op jit(solution)/shard_map/ppermute | solution.py:471
  80.0 4.6 %collective-permute-start.9 = (bf16[4,32,1408]{2,1,0:T(8,128)(2,1)}, bf16[4,32,1408]{2,1,0:T(8,128)(2,1)}, u32[]{:S(2)}, u32[]{:S(2)}) collective-permute-start(bf16[4,32,1408]{2,1,0:T(8,128)(2,1)} %slice.9), channel_id=1, source_target_pairs={{0,448},{8,456},{16,464},{24,472},{32,480},{40,488},{48,496},{56,5... | collective-permute-start | bytes 1081352 | tf_op jit(solution)/shard_map/ppermute | solution.py:472
  84.6 2.2 %collective-permute-done.8.a_ref.refs_7_ = bf16[4,32,1408]{2,1,0:T(8,128)(2,1)S(1)} collective-permute-done((bf16[4,32,1408]{2,1,0:T(8,128)(2,1)}, bf16[4,32,1408]{2,1,0:T(8,128)(2,1)S(1)}, u32[]{:S(2)}, u32[]{:S(2)}) %collective-permute-start.8) | collective-permute-done | bytes 360480 | tf_op jit(solution)/shard_map/ppermute | solution.py:471
  86.8 2.4 %collective-permute-done.9.b_ref.refs_8_ = bf16[4,32,1408]{2,1,0:T(8,128)(2,1)} collective-permute-done((bf16[4,32,1408]{2,1,0:T(8,128)(2,1)}, bf16[4,32,1408]{2,1,0:T(8,128)(2,1)}, u32[]{:S(2)}, u32[]{:S(2)}) %collective-permute-start.9) | collective-permute-done | bytes 360480 | tf_op jit(solution)/shard_map/ppermute | solution.py:472
  92.5 2.5 %shard_map.140.own_ref = bf16[2048,512]{1,0:T(8,128)(2,1)} custom-call(s32[6]{0:T(128)S(1)} %copy-done.12, bf16[8,32,1408]{2,1,0:T(8,128)(2,1)S(1)} %all_to_all.10.refs_0_, bf16[8,32,1408]{2,1,0:T(8,128)(2,1)S(1)} %collective-permute-done.2.refs_1_, bf16[8,32,1408]{2,1,0:T(8,128)(2,1)S(1)} %copy-done.2, bf16[8,32,1408]{2,1,0:T(8,128)(2,1)S(1)} %copy-done.5, ...), custom_call_target="tpu_custom_call" | custom-call | flops 268435456 | bytes 1048576 | tf_op jit(solution)/shard_map/pallas_call | solution.py:53
  95.0 8.5 %collective-permute-start.12 = (bf16[2048,512]{1,0:T(8,128)(2,1)}, bf16[2048,512]{1,0:T(8,128)(2,1)}, u32[]{:S(2)}, u32[]{:S(2)}) collective-permute-start(bf16[2048,512]{1,0:T(8,128)(2,1)} %shard_map.140.own_ref), channel_id=1, source_target_pairs={{0,4},{4,0},{8,12},{12,8},{16,20},{20,16},{24,28},{28,24},{32,36},... | collective-permute-start | bytes 6291464 | tf_op jit(solution)/shard_map/ppermute | solution.py:528
  103.5 3.1 %fusion = (f32[1024,32]{1,0:T(8,128)}, f32[1024,32]{1,0:T(8,128)}, f32[1024,32]{1,0:T(8,128)}) fusion(f32[32]{0:T(128)S(1)} %multiply_power_fusion, f32[1024]{0:T(1024)S(1)} %add_convert_fusion.1), kind=kLoop, calls=%fused_computation.5 | loop fusion | flops 65536 | bytes 397440 | tf_op jit(solution)/shard_map/neg | solution.py:491
  106.7 3.3 %pad_maximum_fusion = (f32[1024,128]{1,0:T(8,128)S(1)}, f32[1024,128]{1,0:T(8,128)S(1)}) fusion(f32[1024,32]{1,0:T(8,128)} %get-tuple-element.38, f32[1024,32]{1,0:T(8,128)} %get-tuple-element.37, f32[1024,32]{1,0:T(8,128)} %get-tuple-element.36), kind=kLoop, calls=%fused_computation.3 | loop fusion | flops 786432 | bytes 1441792 | tf_op jit(solution)/shard_map/concatenate | solution.py:490
  110.0 12.0 %shard_map.131.x_ref = bf16[1024,2048]{1,0:T(8,128)(2,1)S(1)} custom-call(s32[6]{0:T(128)S(1)} %copy-done.12, bf16[512,2048]{1,0:T(8,128)(2,1)} %own_ref.1, bf16[512,2048]{1,0:T(8,128)(2,1)} %collective-permute-done.other_ref, bf16[1,2048]{1,0:T(2,128)(2,1)S(1)} %broadcast_in_dim.8.gain_ref), custom_call_target="tpu_custom_call" | custom-call | flops 1073741824 | bytes 1048576 | tf_op jit(solution)/shard_map/pallas_call | solution.py:53
  122.1 4.1 %shard_map.134.refs_2_ = f32[1024,896]{1,0:T(8,128)S(1)} custom-call(s32[6]{0:T(128)S(1)} %copy-done.12, bf16[1024,2048]{1,0:T(8,128)(2,1)S(1)} %shard_map.131.x_ref, bf16[8,32,1408]{2,1,0:T(8,128)(2,1)S(1)} %all_to_all.10.refs_0_, bf16[8,32,1408]{2,1,0:T(8,128)(2,1)S(1)} %collective-permute-done.2.refs_1_, bf16[8,32,1408]{2,1,0:T(8,128)(2,1)S(1)} %copy-done.3, ...), custom_call_target="tpu_custom_call" | custom-call | flops 2348810240 | bytes 1048576 | tf_op jit(solution)/shard_map/pallas_call | solution.py:53
  126.2 2.4 %shard_map.135.before_ref = f32[1024,896]{1,0:T(8,128)S(1)} custom-call(s32[6]{0:T(128)S(1)} %copy-done.12, bf16[1024,2048]{1,0:T(8,128)(2,1)S(1)} %shard_map.131.x_ref, bf16[8,32,1408]{2,1,0:T(8,128)(2,1)S(1)} %collective-permute-done.4.refs_0_.refs_5_, bf16[8,32,1408]{2,1,0:T(8,128)(2,1)S(1)} %collective-permute-done.7.refs_1_.refs_6_, ...), custom_call_target="tpu_custom_call" | custom-call | flops 939524096 | bytes 1048576 | tf_op jit(solution)/shard_map/pallas_call | solution.py:53
  128.6 2.7 %shard_map.136 = (bf16[1024,256]{1,0:T(8,128)(2,1)S(1)}, bf16[1024,384]{1,0:T(8,128)(2,1)S(1)}, bf16[192,128]{1,0:T(8,128)(2,1)S(1)}) custom-call(s32[6]{0:T(128)S(1)} %copy-done.12, bf16[1024,2048]{1,0:T(8,128)(2,1)S(1)} %shard_map.131.x_ref, f32[1024,128]{1,0:T(8,128)S(1)} %get-tuple-element.39.cos_ref, f32[1024,128]{1,0:T(8,128)S(1)} %get-tuple-element.40.sin_ref, ...), custom_call_target="tpu_custom_call" | custom-call | flops 469762048 | bytes 1048576 | tf_op jit(solution)/shard_map/pallas_call | solution.py:53
  131.4 2.1 %collective-permute-start.10 = (bf16[192,128]{1,0:T(8,128)(2,1)S(1)}, bf16[192,128]{1,0:T(8,128)(2,1)S(1)}, u32[]{:S(2)}, u32[]{:S(2)}) collective-permute-start(bf16[192,128]{1,0:T(8,128)(2,1)S(1)} %get-tuple-element.20), channel_id=1, source_target_pairs={{0,8},{4,12},{8,16},{12,20},{16,24},{20,28},{24,32},{28,36},{32,40... | collective-permute-start | bytes 147464 | tf_op jit(solution)/shard_map/ppermute | solution.py:519
  134.6 3.8 %shard_map.137 = (f32[1024,256]{1,0:T(8,128)S(1)}, f32[8,2,1024]{2,1,0:T(2,128)}) custom-call(bf16[192,128]{1,0:T(8,128)(2,1)S(1)} %collective-permute-done.10.before_ref, bf16[1024,256]{1,0:T(8,128)(2,1)S(1)} %get-tuple-element.21.glu_ref, f32[31,256]{1,0:T(8,128)S(1)} %constant_dynamic-slice_fusion.2.taps_ref), custom_call_target="tpu_custom_call" | custom-call | flops 4294967296 | bytes 1048576 | tf_op jit(solution)/shard_map/pallas_call | solution.py:53
  138.4 4.4 %all-to-all-start.1 = ((f32[8,2,1024]{2,1,0:T(2,128)}), f32[8,2,1024]{2,1,0:T(2,128)S(1)}, u32[]{:S(2)}, u32[]{:S(2)}) async-start(f32[8,2,1024]{2,1,0:T(2,128)} %get-tuple-element.23), calls=%async_computation.1 | async-start | bytes 131072 | tf_op jit(solution)/shard_map/all_to_all | solution.py:541
  142.8 7.2 %shard_map.138 = (bf16[512,256]{1,0:T(8,128)(2,1)S(1)}, bf16[512,256]{1,0:T(8,128)(2,1)S(1)}, f32[4,1024]{1,0:T(4,128)S(1)}) custom-call(s32[6]{0:T(128)S(1)} %copy-done.12, f32[8]{0:T(128)S(1)} %copy-done.13, bf16[1024,384]{1,0:T(8,128)(2,1)S(1)} %get-tuple-element.24.qkv_ref, bf16[192,128]{1,0:T(8,128)(2,1)S(1)} %collective-permute-done.10.before_ref), custom_call_target="tpu_custom_call" | custom-call | flops 4294967296 | bytes 1048576 | tf_op jit(solution)/shard_map/pallas_call | solution.py:53
  155.3 7.0 %shard_map.141 = (bf16[128,2048]{1,0:T(8,128)(2,1)S(1)}, bf16[128,2048]{1,0:T(8,128)(2,1)S(1)}, bf16[128,2048]{1,0:T(8,128)(2,1)S(1)}, bf16[128,2048]{1,0:T(8,128)(2,1)S(1)}) custom-call(s32[6]{0:T(128)S(1)} %copy-done.12, bf16[512,256]{1,0:T(8,128)(2,1)S(1)} %get-tuple-element.26.conv_ref, bf16[512,256]{1,0:T(8,128)(2,1)S(1)} %get-tuple-element.27.attn_ref, ...), custom_call_target="tpu_custom_call" | custom-call | flops 2147483648 | bytes 1048576 | tf_op jit(solution)/shard_map/pallas_call | solution.py:53
  162.3 4.8 %collective-permute-start.13 = (bf16[128,2048]{1,0:T(8,128)(2,1)S(1)}, bf16[128,2048]{1,0:T(8,128)(2,1)S(1)}, u32[]{:S(2)}, u32[]{:S(2)}) collective-permute-start(bf16[128,2048]{1,0:T(8,128)(2,1)S(1)} %get-tuple-element.30), channel_id=1, source_target_pairs={{0,2},{1,3},{2,0},{3,1},{4,6},{5,7},{6,4},{7,5},{8,10},{9,11},{10,... | collective-permute-start | bytes 1572872 | tf_op jit(solution)/shard_map/ppermute | solution.py:591
  167.1 2.2 %collective-permute-start.14 = (bf16[128,2048]{1,0:T(8,128)(2,1)S(1)}, bf16[128,2048]{1,0:T(8,128)(2,1)S(1)}, u32[]{:S(2)}, u32[]{:S(2)}) collective-permute-start(bf16[128,2048]{1,0:T(8,128)(2,1)S(1)} %get-tuple-element.31), channel_id=1, source_target_pairs={{0,1},{1,2},{2,3},{3,0},{4,5},{5,6},{6,7},{7,4},{8,9},{9,10},{10,1... | collective-permute-start | bytes 1572872 | tf_op jit(solution)/shard_map/ppermute | solution.py:591
  169.3 4.3 %collective-permute-start.15 = (bf16[128,2048]{1,0:T(8,128)(2,1)S(1)}, bf16[128,2048]{1,0:T(8,128)(2,1)}, u32[]{:S(2)}, u32[]{:S(2)}) collective-permute-start(bf16[128,2048]{1,0:T(8,128)(2,1)S(1)} %get-tuple-element.32), channel_id=1, source_target_pairs={{0,3},{1,0},{2,1},{3,2},{4,7},{5,4},{6,5},{7,6},{8,11},{9,8},{10,9... | collective-permute-start | bytes 1572872 | tf_op jit(solution)/shard_map/ppermute | solution.py:591
  173.6 3.1 %collective-permute-start.16 = (f32[4,512]{1,0:T(4,128)S(1)}, f32[4,512]{1,0:T(4,128)S(1)}, u32[]{:S(2)}, u32[]{:S(2)}) collective-permute-start(f32[4,512]{1,0:T(4,128)S(1)} %get-tuple-element.35), channel_id=1, source_target_pairs={{0,4},{4,0},{8,12},{12,8},{16,20},{20,16},{24,28},{28,24},{32,36},... | collective-permute-start | bytes 24584 | tf_op jit(solution)/shard_map/ppermute | solution.py:569
  179.1 11.7 %collective-permute-done.14 = bf16[128,2048]{1,0:T(8,128)(2,1)S(1)} collective-permute-done((bf16[128,2048]{1,0:T(8,128)(2,1)S(1)}, bf16[128,2048]{1,0:T(8,128)(2,1)S(1)}, u32[]{:S(2)}, u32[]{:S(2)}) %collective-permute-start.14) | collective-permute-done | bytes 524320 | tf_op jit(solution)/shard_map/ppermute | solution.py:591
  190.8 2.2 %add_convert_fusion = bf16[128,2048]{1,0:T(8,128)(2,1)} fusion(bf16[128,2048]{1,0:T(8,128)(2,1)} %collective-permute-done.15, bf16[128,2048]{1,0:T(8,128)(2,1)S(1)} %collective-permute-done.14, bf16[128,2048]{1,0:T(8,128)(2,1)S(1)} %collective-permute-done.13, bf16[128,2048]{1,0:T(8,128)(2,1)S(1)} %get-tuple-element.29), kind=kLoop, calls=%fused_computation | loop fusion | flops 2097152 | bytes 2621440 | tf_op jit(solution)/shard_map/convert_element_type | solution.py:602
  (61 shorter events, 25.0 us)
Async XLA Ops:
  0.6 132.8 %copy-start = (f32[31,512]{1,0:T(8,128)S(1)}, f32[31,512]{1,0:T(8,128)}, u32[]{:S(2)}) copy-start(f32[31,512]{1,0:T(8,128)} %param.19) | copy-start | bytes 190468
  1.3 87.9 %copy-start.12 = (s32[6]{0:T(128)S(1)}, s32[6]{0:T(128)}, u32[]{:S(2)}) copy-start(s32[6]{0:T(128)} %stack.31.at_ref) | copy-start | bytes 76
  3.7 9.8 %collective-permute-start.1 = (bf16[16,1408]{1,0:T(8,128)(2,1)}, bf16[16,1408]{1,0:T(8,128)(2,1)S(1)}, u32[]{:S(2)}, u32[]{:S(2)}) collective-permute-start(bf16[16,1408]{1,0:T(8,128)(2,1)} %get-tuple-element.19), channel_id=1, source_target_pairs={{0,4},{4,0},{8,12},{12,8},{16,20},{20,16},{24,28},{28,24},{32,36},... | collective-permute-start | bytes 135176 | tf_op jit(solution)/shard_map/ppermute | solution.py:456
  34.2 14.1 %collective-permute-start.2 = (bf16[8,32,1408]{2,1,0:T(8,128)(2,1)S(1)}, bf16[8,32,1408]{2,1,0:T(8,128)(2,1)S(1)}, u32[]{:S(2)}, u32[]{:S(2)}) collective-permute-start(bf16[8,32,1408]{2,1,0:T(8,128)(2,1)S(1)} %all_to_all.10.refs_0_), channel_id=1, source_target_pairs={{0,64},{8,72},{16,80},{24,88},{32,96},{40,104},{48,112},{56,120},{... | collective-permute-start | bytes 2162696 | tf_op jit(solution)/shard_map/ppermute | solution.py:471
  37.4 12.8 %collective-permute-start.5 = (bf16[8,32,1408]{2,1,0:T(8,128)(2,1)S(1)}, bf16[8,32,1408]{2,1,0:T(8,128)(2,1)S(1)}, u32[]{:S(2)}, u32[]{:S(2)}) collective-permute-start(bf16[8,32,1408]{2,1,0:T(8,128)(2,1)S(1)} %all_to_all.10.refs_0_), channel_id=1, source_target_pairs={{0,448},{8,456},{16,464},{24,472},{32,480},{40,488},{48,496},{56,5... | collective-permute-start | bytes 2162696 | tf_op jit(solution)/shard_map/ppermute | solution.py:472
  48.3 14.6 %collective-permute-start.3 = (bf16[8,32,1408]{2,1,0:T(8,128)(2,1)S(1)}, bf16[8,32,1408]{2,1,0:T(8,128)(2,1)S(1)}, u32[]{:S(2)}, u32[]{:S(2)}) collective-permute-start(bf16[8,32,1408]{2,1,0:T(8,128)(2,1)S(1)} %collective-permute-done.2.refs_1_), channel_id=1, source_target_pairs={{0,64},{8,72},{16,80},{24,88},{32,96},{40,104},{48,112},{56,120},{... | collective-permute-start | bytes 2162696 | tf_op jit(solution)/shard_map/ppermute | solution.py:471
  50.2 15.7 %collective-permute-start.6 = (bf16[8,32,1408]{2,1,0:T(8,128)(2,1)S(1)}, bf16[8,32,1408]{2,1,0:T(8,128)(2,1)S(1)}, u32[]{:S(2)}, u32[]{:S(2)}) collective-permute-start(bf16[8,32,1408]{2,1,0:T(8,128)(2,1)S(1)} %collective-permute-done.5.refs_2_), channel_id=1, source_target_pairs={{0,448},{8,456},{16,464},{24,472},{32,480},{40,488},{48,496},{56,5... | collective-permute-start | bytes 2162696 | tf_op jit(solution)/shard_map/ppermute | solution.py:472
  54.8 0.9 copy-start.1
  55.6 54.4 %collective-permute-start = (bf16[512,2048]{1,0:T(8,128)(2,1)}, bf16[512,2048]{1,0:T(8,128)(2,1)}, u32[]{:S(2)}, u32[]{:S(2)}) collective-permute-start(bf16[512,2048]{1,0:T(8,128)(2,1)} %own_ref.1), channel_id=1, source_target_pairs={{0,4},{4,0},{8,12},{12,8},{16,20},{20,16},{24,28},{28,24},{32,36},... | collective-permute-start | bytes 6291464 | tf_op jit(solution)/shard_map/ppermute | solution.py:475
  62.9 13.5 %collective-permute-start.4 = (bf16[8,32,1408]{2,1,0:T(8,128)(2,1)S(1)}, bf16[8,32,1408]{2,1,0:T(8,128)(2,1)S(1)}, u32[]{:S(2)}, u32[]{:S(2)}) collective-permute-start(bf16[8,32,1408]{2,1,0:T(8,128)(2,1)S(1)} %collective-permute-done.3.refs_3_), channel_id=1, source_target_pairs={{0,64},{8,72},{16,80},{24,88},{32,96},{40,104},{48,112},{56,120},{... | collective-permute-start | bytes 2162696 | tf_op jit(solution)/shard_map/ppermute | solution.py:471
  65.0 0.9 copy-start.4
  65.9 13.2 %copy-start.7 = (bf16[8,32,1408]{2,1,0:T(8,128)(2,1)}, bf16[8,32,1408]{2,1,0:T(8,128)(2,1)S(1)}, u32[]{:S(2)}) copy-start(bf16[8,32,1408]{2,1,0:T(8,128)(2,1)S(1)} %collective-permute-done.6.refs_4_) | copy-start | bytes 2162692
  65.9 13.2 %collective-permute-start.7 = (bf16[8,32,1408]{2,1,0:T(8,128)(2,1)S(1)}, bf16[8,32,1408]{2,1,0:T(8,128)(2,1)S(1)}, u32[]{:S(2)}, u32[]{:S(2)}) collective-permute-start(bf16[8,32,1408]{2,1,0:T(8,128)(2,1)S(1)} %collective-permute-done.6.refs_4_), channel_id=1, source_target_pairs={{0,448},{8,456},{16,464},{24,472},{32,480},{40,488},{48,496},{56,5... | collective-permute-start | bytes 2162696 | tf_op jit(solution)/shard_map/ppermute | solution.py:472
  77.2 9.6 %collective-permute-start.8 = (bf16[4,32,1408]{2,1,0:T(8,128)(2,1)}, bf16[4,32,1408]{2,1,0:T(8,128)(2,1)S(1)}, u32[]{:S(2)}, u32[]{:S(2)}) collective-permute-start(bf16[4,32,1408]{2,1,0:T(8,128)(2,1)} %slice.8), channel_id=1, source_target_pairs={{0,64},{8,72},{16,80},{24,88},{32,96},{40,104},{48,112},{56,120},{... | collective-permute-start | bytes 1081352 | tf_op jit(solution)/shard_map/ppermute | solution.py:471
  80.0 9.2 %collective-permute-start.9 = (bf16[4,32,1408]{2,1,0:T(8,128)(2,1)}, bf16[4,32,1408]{2,1,0:T(8,128)(2,1)}, u32[]{:S(2)}, u32[]{:S(2)}) collective-permute-start(bf16[4,32,1408]{2,1,0:T(8,128)(2,1)} %slice.9), channel_id=1, source_target_pairs={{0,448},{8,456},{16,464},{24,472},{32,480},{40,488},{48,496},{56,5... | collective-permute-start | bytes 1081352 | tf_op jit(solution)/shard_map/ppermute | solution.py:472
  84.5 22.1 %copy-start.14 = (bf16[2048]{0:T(1024)(128)(2,1)S(1)}, bf16[2048]{0:T(1024)(128)(2,1)}, u32[]{:S(2)}) copy-start(bf16[2048]{0:T(1024)(128)(2,1)} %param.13) | copy-start | bytes 12292
  89.2 1.1 copy-start.2
  90.3 1.1 copy-start.5
  91.4 1.1 copy-start.8
  95.0 60.3 %collective-permute-start.12 = (bf16[2048,512]{1,0:T(8,128)(2,1)}, bf16[2048,512]{1,0:T(8,128)(2,1)}, u32[]{:S(2)}, u32[]{:S(2)}) collective-permute-start(bf16[2048,512]{1,0:T(8,128)(2,1)} %shard_map.140.own_ref), channel_id=1, source_target_pairs={{0,4},{4,0},{8,12},{12,8},{16,20},{20,16},{24,28},{28,24},{32,36},... | collective-permute-start | bytes 6291464 | tf_op jit(solution)/shard_map/ppermute | solution.py:528
  110.0 12.1 %copy-start.3 = (bf16[8,32,1408]{2,1,0:T(8,128)(2,1)S(1)}, bf16[8,32,1408]{2,1,0:T(8,128)(2,1)}, u32[]{:S(2)}) copy-start(bf16[8,32,1408]{2,1,0:T(8,128)(2,1)} %copy-done.1) | copy-start | bytes 2162692
  110.0 12.1 %copy-start.6 = (bf16[8,32,1408]{2,1,0:T(8,128)(2,1)S(1)}, bf16[8,32,1408]{2,1,0:T(8,128)(2,1)}, u32[]{:S(2)}) copy-start(bf16[8,32,1408]{2,1,0:T(8,128)(2,1)} %copy-done.4) | copy-start | bytes 2162692
  110.0 12.1 %copy-start.9 = (bf16[8,32,1408]{2,1,0:T(8,128)(2,1)S(1)}, bf16[8,32,1408]{2,1,0:T(8,128)(2,1)}, u32[]{:S(2)}) copy-start(bf16[8,32,1408]{2,1,0:T(8,128)(2,1)} %copy-done.7) | copy-start | bytes 2162692
  128.6 4.9 %copy-start.15 = (f32[512]{0:T(512)S(1)}, f32[512]{0:T(512)}, u32[]{:S(2)}) copy-start(f32[512]{0:T(512)} %param.20) | copy-start | bytes 6148
  131.4 3.3 %collective-permute-start.10 = (bf16[192,128]{1,0:T(8,128)(2,1)S(1)}, bf16[192,128]{1,0:T(8,128)(2,1)S(1)}, u32[]{:S(2)}, u32[]{:S(2)}) collective-permute-start(bf16[192,128]{1,0:T(8,128)(2,1)S(1)} %get-tuple-element.20), channel_id=1, source_target_pairs={{0,8},{4,12},{8,16},{12,20},{16,24},{20,28},{24,32},{28,36},{32,40... | collective-permute-start | bytes 147464 | tf_op jit(solution)/shard_map/ppermute | solution.py:519
  134.6 8.2 %copy-start.13 = (f32[8]{0:T(128)S(1)}, f32[8]{0:T(128)}, u32[]{:S(2)}) copy-start(f32[8]{0:T(128)} %sinks_ref.1) | copy-start | bytes 100
  138.4 11.6 %all-to-all-start.1 = ((f32[8,2,1024]{2,1,0:T(2,128)}), f32[8,2,1024]{2,1,0:T(2,128)S(1)}, u32[]{:S(2)}, u32[]{:S(2)}) async-start(f32[8,2,1024]{2,1,0:T(2,128)} %get-tuple-element.23), calls=%async_computation.1 | async-start | bytes 131072 | tf_op jit(solution)/shard_map/all_to_all | solution.py:541
  151.5 3.8 %collective-permute-start.11 = (bf16[512,512]{1,0:T(8,128)(2,1)S(1)}, bf16[512,512]{1,0:T(8,128)(2,1)S(1)}, u32[]{:S(2)}, u32[]{:S(2)}) collective-permute-start(bf16[512,512]{1,0:T(8,128)(2,1)S(1)} %get-tuple-element.28), channel_id=1, source_target_pairs={{0,4},{4,0},{8,12},{12,8},{16,20},{20,16},{24,28},{28,24},{32,36},... | collective-permute-start | bytes 1572872 | tf_op jit(solution)/shard_map/ppermute | solution.py:565
  162.3 16.8 %collective-permute-start.13 = (bf16[128,2048]{1,0:T(8,128)(2,1)S(1)}, bf16[128,2048]{1,0:T(8,128)(2,1)S(1)}, u32[]{:S(2)}, u32[]{:S(2)}) collective-permute-start(bf16[128,2048]{1,0:T(8,128)(2,1)S(1)} %get-tuple-element.30), channel_id=1, source_target_pairs={{0,2},{1,3},{2,0},{3,1},{4,6},{5,7},{6,4},{7,5},{8,10},{9,11},{10,... | collective-permute-start | bytes 1572872 | tf_op jit(solution)/shard_map/ppermute | solution.py:591
  167.1 23.7 %collective-permute-start.14 = (bf16[128,2048]{1,0:T(8,128)(2,1)S(1)}, bf16[128,2048]{1,0:T(8,128)(2,1)S(1)}, u32[]{:S(2)}, u32[]{:S(2)}) collective-permute-start(bf16[128,2048]{1,0:T(8,128)(2,1)S(1)} %get-tuple-element.31), channel_id=1, source_target_pairs={{0,1},{1,2},{2,3},{3,0},{4,5},{5,6},{6,7},{7,4},{8,9},{9,10},{10,1... | collective-permute-start | bytes 1572872 | tf_op jit(solution)/shard_map/ppermute | solution.py:591
  169.3 21.5 %collective-permute-start.15 = (bf16[128,2048]{1,0:T(8,128)(2,1)S(1)}, bf16[128,2048]{1,0:T(8,128)(2,1)}, u32[]{:S(2)}, u32[]{:S(2)}) collective-permute-start(bf16[128,2048]{1,0:T(8,128)(2,1)S(1)} %get-tuple-element.32), channel_id=1, source_target_pairs={{0,3},{1,0},{2,1},{3,2},{4,7},{5,4},{6,5},{7,6},{8,11},{9,8},{10,9... | collective-permute-start | bytes 1572872 | tf_op jit(solution)/shard_map/ppermute | solution.py:591
  173.6 3.9 %collective-permute-start.16 = (f32[4,512]{1,0:T(4,128)S(1)}, f32[4,512]{1,0:T(4,128)S(1)}, u32[]{:S(2)}, u32[]{:S(2)}) collective-permute-start(f32[4,512]{1,0:T(4,128)S(1)} %get-tuple-element.35), channel_id=1, source_target_pairs={{0,4},{4,0},{8,12},{12,8},{16,20},{20,16},{24,28},{28,24},{32,36},... | collective-permute-start | bytes 24584 | tf_op jit(solution)/shard_map/ppermute | solution.py:569
  (2 other events, 1.4 us)

commit v4 on v3

--- a/solution.py
+++ b/solution.py
@@ -65,7 +65,7 @@
     return jax.ShapeDtypeStruct(dims, dtype)
 
 
-def pack_kernel(at_ref, *refs):
+def pack_kernel(*refs):
     count = (len(refs) - 3) // 2
     shards, held, sems = refs[:count], refs[count + 2 : -1], refs[-1]
     kept_ref, given_ref = refs[count : count + 2]
@@ -78,7 +78,7 @@
     for copy in copies:
         copy.wait()
     value_ref, gate_ref, query_ref, key_ref, v_ref, conv_ref, attn_ref = held
-    core = at_ref[3]
+    core = lax.axis_index("core")
     lane = lax.broadcasted_iota(jnp.int32, key_ref.shape, 1)
     key = key_ref[...].astype(jnp.float32)
     value = v_ref[...].astype(jnp.float32)
@@ -105,16 +105,16 @@
             given_ref[...] = whole
 
 
-def repeat_kernel(at_ref, kept_ref, got_ref, out_ref):
-    core, rows = at_ref[3], kept_ref.shape[0]
+def repeat_kernel(kept_ref, got_ref, out_ref):
+    core, rows = lax.axis_index("core"), kept_ref.shape[0]
     for source, to_core in ((kept_ref, core), (got_ref, 1 - core)):
         to = pl.ds(pl.multiple_of(to_core * rows, rows), rows)
         for member in range(out_ref.shape[0]):
             out_ref[member, to, :] = source[...]
 
 
-def norm_kernel(at_ref, own_ref, other_ref, gain_ref, out_ref):
-    core = at_ref[3]
+def norm_kernel(own_ref, other_ref, gain_ref, out_ref):
+    core = lax.axis_index("core")
     count, model = own_ref.shape
     group = model // CHIPS
     tile = 32
@@ -151,16 +151,18 @@
                     out_ref[rows, to : to + 128] = out.astype(jnp.bfloat16)
 
 
-def line_of(at_ref, index):
+def line_of(index):
     away = (index + 1) // 2 * (1 if index % 2 == 0 else -1)
     first = SIDE // 2 if index == SIDE else 0
-    return jnp.bitwise_and(at_ref[0] + away, SIDE - 1), first
-
-
-def products(at_ref, x_ref, rows, pieces, first, held_ref):
+    chip = lax.axis_index("chip")
+    line = jnp.where(lax.axis_index("core") == 0, chip // SIDE, chip % SIDE)
+    return jnp.bitwise_and(line + away, SIDE - 1), first
+
+
+def products(x_ref, rows, pieces, first, held_ref):
     parts = []
     for index, piece in enumerate(pieces, first):
-        line, step = line_of(at_ref, index)
+        line, step = line_of(index)
         block = piece.shape[1]
         size = piece.shape[0] * block
         start = pl.multiple_of(line * (SIDE * block) + step * block, 128)
@@ -180,21 +182,21 @@
     return pl.ds(pl.multiple_of(step * TILE, TILE), TILE)
 
 
-def early_kernel(first, count, at_ref, x_ref, *refs):
+def early_kernel(first, count, x_ref, *refs):
     pieces, before, (out_ref, held_ref) = refs[:count], refs[count:-2], refs[-2:]
     hold(pieces, held_ref)
 
     @pl.loop(0, x_ref.shape[0] // TILE)
     def _(step):
         rows = rows_of(step)
-        total = products(at_ref, x_ref, rows, pieces, first, held_ref)
+        total = products(x_ref, rows, pieces, first, held_ref)
         for other in before:
             total = total + other[rows, :]
         out_ref[rows, :] = total
 
 
 def late_kernel(
-    first, at_ref, x_ref, cos_ref, sin_ref, before_ref, a_ref, b_ref, glu_ref, qkv_ref, tail_ref, held_ref
+    first, x_ref, cos_ref, sin_ref, before_ref, a_ref, b_ref, glu_ref, qkv_ref, tail_ref, held_ref
 ):
     pieces = (a_ref, b_ref)
     hold(pieces, held_ref)
@@ -203,7 +205,7 @@
     @pl.loop(0, x_ref.shape[0] // TILE)
     def _(step):
         rows = rows_of(step)
-        total = products(at_ref, x_ref, rows, pieces, first, held_ref) + before_ref[rows, :]
+        total = products(x_ref, rows, pieces, first, held_ref) + before_ref[rows, :]
         raw = total.astype(jnp.bfloat16).astype(jnp.float32)
         value, gate = raw[:, :channels], raw[:, channels : 2 * channels]
         glu_ref[rows, :] = (value * jax.nn.sigmoid(gate)).astype(jnp.bfloat16)
@@ -228,10 +230,10 @@
     tail_ref[WINDOW + 32 : WINDOW + 64, :] = glu_ref[end - 32 : end, 128:]
 
 
-def join_kernel(column, at_ref, *refs):
+def join_kernel(column, *refs):
     pieces, out_ref = refs[:-1], refs[-1]
     for index, piece in enumerate(pieces):
-        line, first = line_of(at_ref, index)
+        line, first = line_of(index)
         block = piece.shape[1]
         for step in range(piece.shape[0]):
             to = pl.multiple_of(line * (SIDE * block) + (first + step) * block, block)
@@ -239,7 +241,8 @@
 
 
 def conv_kernel(before_ref, glu_ref, taps_ref, out_ref, sums_ref, ext_ref):
-    count, rows = taps_ref.shape[0], glu_ref.shape[0]
+    count, (rows, channels) = taps_ref.shape[0], glu_ref.shape
+    first_channel = lax.axis_index("core") * channels
     lead = 32
     for part in range(2):
         lanes = pl.ds(part * 128, 128)
@@ -254,10 +257,11 @@
         second = jnp.zeros((128, 128), jnp.float32)
         for part in range(2):
             lanes = pl.ds(part * 128, 128)
+            own = pl.ds(pl.multiple_of(first_channel + part * 128, 128), 128)
             total = jnp.zeros((128, 128), jnp.float32)
             for tap in range(count):
                 rows_at = pl.ds(base + (lead - count + 1 + tap), 128)
-                total = total + taps_ref[pl.ds(tap, 1), lanes] * ext_ref[part, rows_at, :]
+                total = total + taps_ref[pl.ds(tap, 1), own] * ext_ref[part, rows_at, :]
             out_ref[pl.ds(base, 128), lanes] = total
             first = first + total
             second = second + total * total
@@ -268,8 +272,8 @@
             sums_ref[member, pl.ds(1, 1), pl.ds(base, 128)] = second
 
 
-def scaled_kernel(at_ref, conv_ref, sums_ref, gain_ref, attn_ref, kept_ref, given_ref):
-    core = at_ref[3]
+def scaled_kernel(conv_ref, sums_ref, gain_ref, attn_ref, kept_ref, given_ref):
+    core = lax.axis_index("core")
     totals = sums_ref[0]
     for member in range(1, sums_ref.shape[0]):
         totals = totals + sums_ref[member]
@@ -282,8 +286,9 @@
         mean_at = jnp.broadcast_to(mean[:, at], (128, 128)).T
         scale_at = jnp.broadcast_to(scale[:, at], (128, 128)).T
         parts = []
-        for lanes in (slice(0, 128), slice(128, 256)):
-            normed = (conv_ref[at, lanes] - mean_at) * scale_at * gain_ref[0:1, lanes]
+        for lane in range(0, channels, 128):
+            own = pl.ds(pl.multiple_of(core * channels + lane, 128), 128)
+            normed = (conv_ref[at, lane : lane + 128] - mean_at) * scale_at * gain_ref[0:1, own]
             parts.append((normed * jax.nn.sigmoid(normed)).astype(jnp.bfloat16))
         out = jnp.concatenate(parts, axis=1)
         to = slice(base % half, base % half + 128)
@@ -298,9 +303,9 @@
 
 
 def attention_kernel(
-    at_ref, sinks_ref, qkv_ref, before_ref, kept_ref, given_ref, logs_ref, k_lo, k_hi, v_lo, v_hi
+    sinks_ref, qkv_ref, before_ref, kept_ref, given_ref, logs_ref, k_lo, k_hi, v_lo, v_hi
 ):
-    core, first_chip = at_ref[3], at_ref[4]
+    core, chip = lax.axis_index("core"), lax.axis_index("chip")
     cols = kept_ref.shape[1]
     for source, to, count in ((before_ref, 0, WINDOW), (qkv_ref, WINDOW, qkv_ref.shape[0])):
         both = source[:count, source.shape[1] - 128 :].astype(jnp.float32)
@@ -321,7 +326,7 @@
         window = pl.ds(base, 2 * WINDOW)
         key_at = lax.broadcasted_iota(jnp.int32, (2 * WINDOW, WINDOW), 0)
         query_at = lax.broadcasted_iota(jnp.int32, (2 * WINDOW, WINDOW), 1)
-        lowest = jnp.where((first_chip == 1) & (block == 0), WINDOW, 0)
+        lowest = jnp.where((chip == 0) & (block == 0), WINDOW, 0)
         allowed = (key_at > query_at) & (key_at <= query_at + WINDOW) & (key_at >= lowest)
         outs = []
         for pair in range(heads // 2):
@@ -363,15 +368,19 @@
             given_ref[to, :] = out
 
 
-def output_kernel(
-    steps, at_ref, conv_ref, attn_ref, got_ref, own_ref, other_ref, *rest
-):
-    out_refs, w_ref = rest[:-1], rest[-1]
-    core, member, half = at_ref[3], at_ref[5], conv_ref.shape[1]
+def output_kernel(steps, conv_ref, attn_ref, got_ref, own_ref, other_ref, *rest):
+    out_refs, (x_ref, w_ref) = rest[:-2], rest[-2:]
+    core, member = lax.axis_index("core"), lax.axis_index("tp")
     count = out_refs[0].shape[0]
     peers = conv_ref.shape[0] // count
     block = own_ref.shape[0] // CHIPS
     width = own_ref.shape[1]
+    for index, away in enumerate(steps):
+        to = jnp.bitwise_and(member + away, peers - 1)
+        rows = pl.ds(pl.multiple_of(to * count, count), count)
+        x_ref[index * count : (index + 1) * count, :] = jnp.concatenate(
+            [conv_ref[rows, :], attn_ref[rows, :], got_ref[rows, :]], axis=1
+        )
 
     @pl.loop(0, SIDE)
     def _(z):
@@ -383,21 +392,11 @@
             for y in range(SIDE):
                 start = pl.multiple_of(first + y * stride, block)
                 w_ref[y * block : (y + 1) * block, at : at + width] = source[pl.ds(start, block), :]
-        total = jnp.zeros((conv_ref.shape[0], SIDE * block), jnp.float32)
-        for left, at in ((conv_ref, 0), (attn_ref, half), (got_ref, width)):
-            total = total + lax.dot_general(
-                left[...],
-                w_ref[:, at : at + left.shape[1]],
-                (((1,), (1,)), ((), ())),
-                preferred_element_type=jnp.float32,
-            )
-        for to in range(peers):
-            out = total[to * count : (to + 1) * count].astype(jnp.bfloat16)
-            for away, out_ref in zip(steps, out_refs):
-
-                @pl.when(jnp.bitwise_and(to - member, peers - 1) == away)
-                def _():
-                    out_ref[:, cols] = out
+        total = lax.dot_general(
+            x_ref[...], w_ref[...], (((1,), (1,)), ((), ())), preferred_element_type=jnp.float32
+        )
+        for index, out_ref in enumerate(out_refs):
+            out_ref[:, cols] = total[index * count : (index + 1) * count].astype(jnp.bfloat16)
 
 
 def layer(
@@ -416,7 +415,6 @@
 ):
     core = lax.axis_index("core")
     chip = lax.axis_index("chip")
-    member = lax.axis_index("tp")
     own_rows, model = tokens.shape
     row_count = own_rows * CORES
     depth = w_conv_value.shape[0]
@@ -424,18 +422,6 @@
     q_cols = w_query.shape[1] // CORES
     query_heads = q_cols // HEAD_DIM
     block = CORES * depth
-
-    z, y = chip // SIDE, chip % SIDE
-    at = jnp.stack(
-        [
-            jnp.where(core == 0, z, y),
-            jnp.where(core == 0, SIDE * block, block),
-            jnp.where(core == 0, block, SIDE * block),
-            core,
-            (chip == 0).astype(jnp.int32),
-            member,
-        ]
-    ).astype(jnp.int32)
 
     conv_cols = (0, 2 * channels)
     qkv_cols = (2 * channels, q_cols + 2 * HEAD_DIM)
@@ -446,22 +432,15 @@
         pack_kernel,
         (shape((depth, width)),) * 2,
         1 << 20,
-        [SMEM] + [HBM] * len(shards_in),
-        (at, *shards_in),
+        [HBM] * len(shards_in),
+        shards_in,
         (
             *(pltpu.VMEM(w.shape, w.dtype) for w in shards_in),
             pltpu.SemaphoreType.DMA((len(shards_in),)),
         ),
     )
     got = lax.ppermute(given, SP, OTHER_CORE)
-    sent = call(
-        repeat_kernel,
-        shape((SIDE, block, width)),
-        1 << 20,
-        [SMEM, VMEM, VMEM],
-        (at, kept, got),
-        limit=12,
-    )
+    sent = call(repeat_kernel, shape((SIDE, block, width)), 1 << 20, [VMEM, VMEM], (kept, got))
     own_line = lax.all_to_all(sent, SP, 0, 0, tiled=True, axis_index_groups=LINES)
     pieces = [own_line]
     ahead = behind = own_line
@@ -477,8 +456,8 @@
         norm_kernel,
         shape((row_count, model)),
         1 << 30,
-        [SMEM, VMEM, VMEM, VMEM],
-        (at, tokens, tokens_other, norm_gain[None]),
+        [VMEM, VMEM, VMEM],
+        (tokens, tokens_other, norm_gain[None]),
         limit=16,
     )
 
@@ -499,8 +478,8 @@
             functools.partial(early_kernel, first, len(held)),
             shape((row_count, in_cols), jnp.float32),
             2 * row_count * lines * len(held) * in_cols,
-            [SMEM] + [VMEM] * (1 + len(held) + len(before)),
-            (at, normed, *held, *before),
+            [VMEM] * (1 + len(held) + len(before)),
+            (normed, *held, *before),
             (pltpu.VMEM((lines * len(held), in_cols), jnp.bfloat16),),
             limit=16,
         )
@@ -511,8 +490,8 @@
         functools.partial(late_kernel, 7),
         (shape((row_count, channels)), shape((row_count, qkv_cols[1])), shape((WINDOW + 64, 128))),
         2 * row_count * lines * in_cols,
-        [SMEM] + [VMEM] * 6,
-        (at, normed, cosines, sines, total, *pieces[7:]),
+        [VMEM] * 6,
+        (normed, cosines, sines, total, *pieces[7:]),
         (pltpu.VMEM((lines, in_cols), jnp.bfloat16),),
         limit=16,
     )
@@ -521,20 +500,19 @@
         functools.partial(join_kernel, out_cols[0]),
         shape((model, out_cols[1])),
         1 << 28,
-        [SMEM] + [VMEM] * len(pieces),
-        (at, *pieces),
+        [VMEM] * len(pieces),
+        pieces,
         limit=12,
     )
     out_other = lax.ppermute(out_own, SP, OTHER_CORE)
 
-    taps = lax.dynamic_slice_in_dim(conv_taps, core * channels, channels, 1)
     members = CORES * lax.axis_size("tp")
     conv_out, sums = call(
         conv_kernel,
         (shape((row_count, channels), jnp.float32), shape((members, 2, row_count), jnp.float32)),
         1 << 32,
         [VMEM] * 3,
-        (before, glu, taps),
+        (before, glu, conv_taps),
         (pltpu.VMEM((2, row_count + 32, 128), jnp.float32),),
         limit=12,
     )
@@ -548,18 +526,17 @@
             shape((query_heads, row_count), jnp.float32),
         ),
         1 << 32,
-        [SMEM, SMEM, VMEM, VMEM],
-        (at, sinks, qkv, before),
+        [SMEM, VMEM, VMEM],
+        (sinks, qkv, before),
         (extended,) * 4,
         limit=12,
     )
-    gain = lax.dynamic_slice_in_dim(ln_gain, core * channels, channels, 0)
     conv_kept, given = call(
         scaled_kernel,
         (shape((own_rows, channels)), shape((own_rows, channels + q_cols))),
         1 << 28,
-        [SMEM] + [VMEM] * 4,
-        (at, conv_out, everyones, gain[None], attn_given),
+        [VMEM] * 4,
+        (conv_out, everyones, ln_gain[None], attn_given),
         limit=12,
     )
     rows_got = lax.ppermute(given, SP, OTHER_CORE)
@@ -581,18 +558,22 @@
             functools.partial(output_kernel, steps),
             (shape((share, model)),) * len(steps),
             2 * share * len(steps) * model * 2 * out_cols[1],
-            [SMEM] + [VMEM] * 5,
-            (at, conv_kept, attn_kept, rows_got, out_own, out_other),
-            (pltpu.VMEM((TILE, 2 * out_cols[1]), jnp.bfloat16),),
-            limit=16,
+            [VMEM] * 5,
+            (conv_kept, attn_kept, rows_got, out_own, out_other),
+            (
+                pltpu.VMEM((share * len(steps), 2 * out_cols[1]), jnp.bfloat16),
+                pltpu.VMEM((TILE, 2 * out_cols[1]), jnp.bfloat16),
+            ),
+            limit=12,
         )
 
     def to_member(value, away):
         return lax.ppermute(value, "tp", [(i, (i + away) % peers) for i in range(peers)])
 
-    far, up, down, mine = output((2, 1, 3, 0))
-    far = to_member(far, 2)
-    up, down = to_member(up, 1), to_member(down, 3)
+    far, up = output((2, 1))
+    far, up = to_member(far, 2), to_member(up, 1)
+    down, mine = output((3, 0))
+    down = to_member(down, 3)
     mixed = (
         mine.astype(jnp.float32)
         + far.astype(jnp.float32)

time: 195 us -> 193 us (0.990)
  local copies, waits for them, and re-layouts: 8.77 us -> 16 us
  waiting for transfers between devices: 35.2 us -> 29.6 us
  other arithmetic: 9.25 us -> 5.74 us
    unnamed x32 -> x60, local copies, waits for them, and re-layouts: 6.51 us -> 16 us
    ppermute x3, waiting for transfers between devices: 12.6 us -> 7.84 us  [to_member(): lax.ppermute(value, 'tp', [(i, (i + away) % peers) for i in range(peers)])]
    concatenate x1, other arithmetic: 3.3 us -> 0.88 us  [layer(): cosines = jnp.concatenate([cosine] * 4, axis=1)]
    pallas_call x11 -> x12, Pallas kernels: 46.1 us -> 45.1 us  [call(): pl.pallas_call(body, out_shape=outs, in_specs=in_specs, out_specs=jax.tre...]
  transfers between devices with their start and end apart: 18 -> 18, of which waited for: 10 -> 10; matrix products, arithmetic and copies ran while one was open for 5% -> 2% of each run, Pallas kernels for 19% -> 19%
where the time goes in v4:
time: 193 us; the launch traced here: 190 us
  starting transfers between devices  73.5 us (38%)
  Pallas kernels  45.1 us (23%)
  waiting for transfers between devices  29.6 us (15%)
  blocking collectives  18.9 us (10%)
  local copies, waits for them, and re-layouts  16 us (8%)
  other arithmetic  5.74 us (3%)
    pallas_call x12, Pallas kernels, call(): pl.pallas_call(body, out_shape=outs, in_specs=in_specs, out_specs=jax.tre...  45.1 us
    all_to_all x1, blocking collectives, layer(): lax.all_to_all(sent, SP, 0, 0, tiled=True, axis_index_groups=LINES)  18.9 us
    ppermute x4, starting transfers between devices, layer(): behind = lax.ppermute(behind, SP, BEHIND)  17.8 us
    unnamed x60, local copies, waits for them, and re-layouts  16 us
    ppermute x4, waiting for transfers between devices, layer(): ahead = lax.ppermute(ahead, SP, AHEAD)  14.6 us
    ppermute x3, starting transfers between devices, to_member(): lax.ppermute(value, 'tp', [(i, (i + away) % peers) for i in range(peers)])  11.2 us
    ppermute x4, starting transfers between devices, layer(): ahead = lax.ppermute(ahead, SP, AHEAD)  9.11 us
    ppermute x1, starting transfers between devices, layer(): got = lax.ppermute(given, SP, OTHER_CORE)  8.74 us
  transfers between devices with their start and end apart: 18, of which 10 were waited for; matrix products, arithmetic and copies ran while one was open for 2% of the time, Pallas kernels for 19%

profile of v4, /device:TPU:1, one launch (start us, length us, event | category | flops | bytes accessed | tf_op | source)
XLA Modules:
  0.0 190.0 jit_solution(814821285991953541)
XLA Ops:
  2.2 8.7 %collective-permute-start.1 = (bf16[16,1408]{1,0:T(8,128)(2,1)}, bf16[16,1408]{1,0:T(8,128)(2,1)S(1)}, u32[]{:S(2)}, u32[]{:S(2)}) collective-permute-start(bf16[16,1408]{1,0:T(8,128)(2,1)} %get-tuple-element.19), channel_id=1, source_target_pairs={{0,4},{4,0},{8,12},{12,8},{16,20},{20,16},{24,28},{28,24},{32,36},... | collective-permute-start | bytes 135176 | tf_op jit(solution)/shard_map/ppermute | solution.py:442
  14.4 18.9 %all_to_all.10.refs_0_ = bf16[8,32,1408]{2,1,0:T(8,128)(2,1)S(1)} all-to-all(bf16[8,32,1408]{2,1,0:T(8,128)(2,1)} %shard_map.133), channel_id=1, replica_groups={{0,8,16,24,32,40,48,56},{64,72,80,88,96,104,112,120},{128,136,144,152,1..., dimensions={0} | all-to-all | bytes 1441792 | tf_op jit(solution)/shard_map/all_to_all | solution.py:444
  33.3 3.2 %collective-permute-start.2 = (bf16[8,32,1408]{2,1,0:T(8,128)(2,1)S(1)}, bf16[8,32,1408]{2,1,0:T(8,128)(2,1)S(1)}, u32[]{:S(2)}, u32[]{:S(2)}) collective-permute-start(bf16[8,32,1408]{2,1,0:T(8,128)(2,1)S(1)} %all_to_all.10.refs_0_), channel_id=1, source_target_pairs={{0,64},{8,72},{16,80},{24,88},{32,96},{40,104},{48,112},{56,120},{... | collective-permute-start | bytes 2162696 | tf_op jit(solution)/shard_map/ppermute | solution.py:450
  36.5 3.8 %collective-permute-start.5 = (bf16[8,32,1408]{2,1,0:T(8,128)(2,1)S(1)}, bf16[8,32,1408]{2,1,0:T(8,128)(2,1)S(1)}, u32[]{:S(2)}, u32[]{:S(2)}) collective-permute-start(bf16[8,32,1408]{2,1,0:T(8,128)(2,1)S(1)} %all_to_all.10.refs_0_), channel_id=1, source_target_pairs={{0,448},{8,456},{16,464},{24,472},{32,480},{40,488},{48,496},{56,5... | collective-permute-start | bytes 2162696 | tf_op jit(solution)/shard_map/ppermute | solution.py:451
  40.3 7.0 %collective-permute-done.2.refs_1_ = bf16[8,32,1408]{2,1,0:T(8,128)(2,1)S(1)} collective-permute-done((bf16[8,32,1408]{2,1,0:T(8,128)(2,1)S(1)}, bf16[8,32,1408]{2,1,0:T(8,128)(2,1)S(1)}, u32[]{:S(2)}, u32[]{:S(2)}) %collective-permute-start.2) | collective-permute-done | bytes 720928 | tf_op jit(solution)/shard_map/ppermute | solution.py:450
  47.4 1.9 %collective-permute-start.3 = (bf16[8,32,1408]{2,1,0:T(8,128)(2,1)S(1)}, bf16[8,32,1408]{2,1,0:T(8,128)(2,1)S(1)}, u32[]{:S(2)}, u32[]{:S(2)}) collective-permute-start(bf16[8,32,1408]{2,1,0:T(8,128)(2,1)S(1)} %collective-permute-done.2.refs_1_), channel_id=1, source_target_pairs={{0,64},{8,72},{16,80},{24,88},{32,96},{40,104},{48,112},{56,120},{... | collective-permute-start | bytes 2162696 | tf_op jit(solution)/shard_map/ppermute | solution.py:450
  50.2 4.6 %collective-permute-start.6 = (bf16[8,32,1408]{2,1,0:T(8,128)(2,1)S(1)}, bf16[8,32,1408]{2,1,0:T(8,128)(2,1)S(1)}, u32[]{:S(2)}, u32[]{:S(2)}) collective-permute-start(bf16[8,32,1408]{2,1,0:T(8,128)(2,1)S(1)} %collective-permute-done.5.refs_2_), channel_id=1, source_target_pairs={{0,448},{8,456},{16,464},{24,472},{32,480},{40,488},{48,496},{56,5... | collective-permute-start | bytes 2162696 | tf_op jit(solution)/shard_map/ppermute | solution.py:451
  55.6 7.3 %collective-permute-start = (bf16[512,2048]{1,0:T(8,128)(2,1)}, bf16[512,2048]{1,0:T(8,128)(2,1)}, u32[]{:S(2)}, u32[]{:S(2)}) collective-permute-start(bf16[512,2048]{1,0:T(8,128)(2,1)} %own_ref.1), channel_id=1, source_target_pairs={{0,4},{4,0},{8,12},{12,8},{16,20},{20,16},{24,28},{28,24},{32,36},... | collective-permute-start | bytes 6291464 | tf_op jit(solution)/shard_map/ppermute | solution.py:454
  62.9 2.1 %collective-permute-start.4 = (bf16[8,32,1408]{2,1,0:T(8,128)(2,1)S(1)}, bf16[8,32,1408]{2,1,0:T(8,128)(2,1)S(1)}, u32[]{:S(2)}, u32[]{:S(2)}) collective-permute-start(bf16[8,32,1408]{2,1,0:T(8,128)(2,1)S(1)} %collective-permute-done.3.refs_3_), channel_id=1, source_target_pairs={{0,64},{8,72},{16,80},{24,88},{32,96},{40,104},{48,112},{56,120},{... | collective-permute-start | bytes 2162696 | tf_op jit(solution)/shard_map/ppermute | solution.py:450
  65.9 4.4 %collective-permute-start.7 = (bf16[8,32,1408]{2,1,0:T(8,128)(2,1)S(1)}, bf16[8,32,1408]{2,1,0:T(8,128)(2,1)S(1)}, u32[]{:S(2)}, u32[]{:S(2)}) collective-permute-start(bf16[8,32,1408]{2,1,0:T(8,128)(2,1)S(1)} %collective-permute-done.6.refs_4_), channel_id=1, source_target_pairs={{0,448},{8,456},{16,464},{24,472},{32,480},{40,488},{48,496},{56,5... | collective-permute-start | bytes 2162696 | tf_op jit(solution)/shard_map/ppermute | solution.py:451
  70.3 6.2 %collective-permute-done.4.refs_0_.refs_5_ = bf16[8,32,1408]{2,1,0:T(8,128)(2,1)S(1)} collective-permute-done((bf16[8,32,1408]{2,1,0:T(8,128)(2,1)S(1)}, bf16[8,32,1408]{2,1,0:T(8,128)(2,1)S(1)}, u32[]{:S(2)}, u32[]{:S(2)}) %collective-permute-start.4) | collective-permute-done | bytes 720928 | tf_op jit(solution)/shard_map/ppermute | solution.py:450
  76.5 1.9 %collective-permute-start.8 = (bf16[4,32,1408]{2,1,0:T(8,128)(2,1)S(1)}, bf16[4,32,1408]{2,1,0:T(8,128)(2,1)S(1)}, u32[]{:S(2)}, u32[]{:S(2)}) collective-permute-start(bf16[4,32,1408]{2,1,0:T(8,128)(2,1)S(1)} %slice.8), channel_id=1, source_target_pairs={{0,64},{8,72},{16,80},{24,88},{32,96},{40,104},{48,112},{56,120},{... | collective-permute-start | bytes 1081352 | tf_op jit(solution)/shard_map/ppermute | solution.py:450
  79.4 5.0 %collective-permute-start.9 = (bf16[4,32,1408]{2,1,0:T(8,128)(2,1)S(1)}, bf16[4,32,1408]{2,1,0:T(8,128)(2,1)S(1)}, u32[]{:S(2)}, u32[]{:S(2)}) collective-permute-start(bf16[4,32,1408]{2,1,0:T(8,128)(2,1)S(1)} %slice.9), channel_id=1, source_target_pairs={{0,448},{8,456},{16,464},{24,472},{32,480},{40,488},{48,496},{56,5... | collective-permute-start | bytes 1081352 | tf_op jit(solution)/shard_map/ppermute | solution.py:451
  86.6 2.2 %collective-permute-done.9.b_ref.refs_8_ = bf16[4,32,1408]{2,1,0:T(8,128)(2,1)S(1)} collective-permute-done((bf16[4,32,1408]{2,1,0:T(8,128)(2,1)S(1)}, bf16[4,32,1408]{2,1,0:T(8,128)(2,1)S(1)}, u32[]{:S(2)}, u32[]{:S(2)}) %collective-permute-start.9) | collective-permute-done | bytes 360480 | tf_op jit(solution)/shard_map/ppermute | solution.py:451
  97.2 7.8 %collective-permute-start.12 = (bf16[2048,512]{1,0:T(8,128)(2,1)S(1)}, bf16[2048,512]{1,0:T(8,128)(2,1)}, u32[]{:S(2)}, u32[]{:S(2)}) collective-permute-start(bf16[2048,512]{1,0:T(8,128)(2,1)S(1)} %shard_map.140.own_ref), channel_id=1, source_target_pairs={{0,4},{4,0},{8,12},{12,8},{16,20},{20,16},{24,28},{28,24},{32,36},... | collective-permute-start | bytes 6291464 | tf_op jit(solution)/shard_map/ppermute | solution.py:507
  105.1 1.9 fusion
  108.0 12.0 %shard_map.131.x_ref = bf16[1024,2048]{1,0:T(8,128)(2,1)S(1)} custom-call(bf16[512,2048]{1,0:T(8,128)(2,1)} %own_ref.1, bf16[512,2048]{1,0:T(8,128)(2,1)} %collective-permute-done.other_ref, bf16[1,2048]{1,0:T(2,128)(2,1)S(1)} %broadcast_in_dim.8.gain_ref), custom_call_target="tpu_custom_call" | custom-call | flops 1073741824 | bytes 1048576 | tf_op jit(solution)/shard_map/pallas_call | solution.py:53
  120.0 3.6 %shard_map.134.refs_2_ = f32[1024,896]{1,0:T(8,128)S(1)} custom-call(bf16[1024,2048]{1,0:T(8,128)(2,1)S(1)} %shard_map.131.x_ref, bf16[8,32,1408]{2,1,0:T(8,128)(2,1)S(1)} %all_to_all.10.refs_0_, bf16[8,32,1408]{2,1,0:T(8,128)(2,1)S(1)} %copy-done.5, bf16[8,32,1408]{2,1,0:T(8,128)(2,1)S(1)} %copy-done.8, bf16[8,32,1408]{2,1,0:T(8,128)(2,1)S(1)} %copy-done.11, ...), custom_call_target="tpu_custom_call" | custom-call | flops 2348810240 | bytes 1048576 | tf_op jit(solution)/shard_map/pallas_call | solution.py:53
  127.3 2.1 %collective-permute-start.10 = (bf16[192,128]{1,0:T(8,128)(2,1)S(1)}, bf16[192,128]{1,0:T(8,128)(2,1)S(1)}, u32[]{:S(2)}, u32[]{:S(2)}) collective-permute-start(bf16[192,128]{1,0:T(8,128)(2,1)S(1)} %get-tuple-element.20), channel_id=1, source_target_pairs={{0,8},{4,12},{8,16},{12,20},{16,24},{20,28},{24,32},{28,36},{32,40... | collective-permute-start | bytes 147464 | tf_op jit(solution)/shard_map/ppermute | solution.py:498
  130.5 4.1 %shard_map.137 = (f32[1024,256]{1,0:T(8,128)S(1)}, f32[8,2,1024]{2,1,0:T(2,128)}) custom-call(bf16[192,128]{1,0:T(8,128)(2,1)S(1)} %collective-permute-done.10.before_ref, bf16[1024,256]{1,0:T(8,128)(2,1)S(1)} %get-tuple-element.21.glu_ref, f32[31,512]{1,0:T(8,128)S(1)} %copy-done.26), custom_call_target="tpu_custom_call" | custom-call | flops 4294967296 | bytes 1048576 | tf_op jit(solution)/shard_map/pallas_call | solution.py:53
  134.7 4.4 %all-to-all-start.1 = ((f32[8,2,1024]{2,1,0:T(2,128)}), f32[8,2,1024]{2,1,0:T(2,128)S(1)}, u32[]{:S(2)}, u32[]{:S(2)}) async-start(f32[8,2,1024]{2,1,0:T(2,128)} %get-tuple-element.23), calls=%async_computation.1 | async-start | bytes 131072 | tf_op jit(solution)/shard_map/all_to_all | solution.py:519
  140.2 7.2 %shard_map.138 = (bf16[512,256]{1,0:T(8,128)(2,1)S(1)}, bf16[512,256]{1,0:T(8,128)(2,1)S(1)}, f32[4,1024]{1,0:T(4,128)S(1)}) custom-call(f32[8]{0:T(128)S(1)} %copy-done.27, bf16[1024,384]{1,0:T(8,128)(2,1)S(1)} %copy-done.25, bf16[192,128]{1,0:T(8,128)(2,1)S(1)} %collective-permute-done.10.before_ref), custom_call_target="tpu_custom_call" | custom-call | flops 4294967296 | bytes 1048576 | tf_op jit(solution)/shard_map/pallas_call | solution.py:53
  150.0 1.9 %collective-permute-start.11 = (bf16[512,512]{1,0:T(8,128)(2,1)S(1)}, bf16[512,512]{1,0:T(8,128)(2,1)S(1)}, u32[]{:S(2)}, u32[]{:S(2)}) collective-permute-start(bf16[512,512]{1,0:T(8,128)(2,1)S(1)} %get-tuple-element.28), channel_id=1, source_target_pairs={{0,4},{4,0},{8,12},{12,8},{16,20},{20,16},{24,28},{28,24},{32,36},... | collective-permute-start | bytes 1572872 | tf_op jit(solution)/shard_map/ppermute | solution.py:542
  152.0 1.9 collective-permute-done.11.got_ref
  153.8 5.1 %shard_map.142 = (bf16[128,2048]{1,0:T(8,128)(2,1)}, bf16[128,2048]{1,0:T(8,128)(2,1)S(1)}) custom-call(bf16[512,256]{1,0:T(8,128)(2,1)S(1)} %get-tuple-element.26.conv_ref, bf16[512,256]{1,0:T(8,128)(2,1)S(1)} %get-tuple-element.27.attn_ref, bf16[512,512]{1,0:T(8,128)(2,1)S(1)} %collective-permute-done.11.got_ref, ...), custom_call_target="tpu_custom_call" | custom-call | flops 1073741824 | bytes 1048576 | tf_op jit(solution)/shard_map/pallas_call | solution.py:53
  158.9 4.8 %collective-permute-start.13 = (bf16[128,2048]{1,0:T(8,128)(2,1)}, bf16[128,2048]{1,0:T(8,128)(2,1)}, u32[]{:S(2)}, u32[]{:S(2)}) collective-permute-start(bf16[128,2048]{1,0:T(8,128)(2,1)} %get-tuple-element.30), channel_id=1, source_target_pairs={{0,2},{1,3},{2,0},{3,1},{4,6},{5,7},{6,4},{7,5},{8,10},{9,11},{10,... | collective-permute-start | bytes 1572872 | tf_op jit(solution)/shard_map/ppermute | solution.py:571
  163.7 2.2 %collective-permute-start.14 = (bf16[128,2048]{1,0:T(8,128)(2,1)S(1)}, bf16[128,2048]{1,0:T(8,128)(2,1)}, u32[]{:S(2)}, u32[]{:S(2)}) collective-permute-start(bf16[128,2048]{1,0:T(8,128)(2,1)S(1)} %get-tuple-element.31), channel_id=1, source_target_pairs={{0,1},{1,2},{2,3},{3,0},{4,5},{5,6},{6,7},{7,4},{8,9},{9,10},{10,1... | collective-permute-start | bytes 1572872 | tf_op jit(solution)/shard_map/ppermute | solution.py:571
  165.9 5.1 %shard_map.141 = (bf16[128,2048]{1,0:T(8,128)(2,1)}, bf16[128,2048]{1,0:T(8,128)(2,1)S(1)}) custom-call(bf16[512,256]{1,0:T(8,128)(2,1)S(1)} %get-tuple-element.26.conv_ref, bf16[512,256]{1,0:T(8,128)(2,1)S(1)} %get-tuple-element.27.attn_ref, bf16[512,512]{1,0:T(8,128)(2,1)S(1)} %collective-permute-done.11.got_ref, ...), custom_call_target="tpu_custom_call" | custom-call | flops 1073741824 | bytes 1048576 | tf_op jit(solution)/shard_map/pallas_call | solution.py:53
  171.0 4.3 %collective-permute-start.15 = (bf16[128,2048]{1,0:T(8,128)(2,1)}, bf16[128,2048]{1,0:T(8,128)(2,1)S(1)}, u32[]{:S(2)}, u32[]{:S(2)}) collective-permute-start(bf16[128,2048]{1,0:T(8,128)(2,1)} %get-tuple-element.32), channel_id=1, source_target_pairs={{0,3},{1,0},{2,1},{3,2},{4,7},{5,4},{6,5},{7,6},{8,11},{9,8},{10,9... | collective-permute-start | bytes 1572872 | tf_op jit(solution)/shard_map/ppermute | solution.py:571
  175.3 3.1 %collective-permute-start.16 = (f32[4,512]{1,0:T(4,128)S(1)}, f32[4,512]{1,0:T(4,128)S(1)}, u32[]{:S(2)}, u32[]{:S(2)}) collective-permute-start(f32[4,512]{1,0:T(4,128)S(1)} %get-tuple-element.35), channel_id=1, source_target_pairs={{0,4},{4,0},{8,12},{12,8},{16,20},{20,16},{24,28},{28,24},{32,36},... | collective-permute-start | bytes 24584 | tf_op jit(solution)/shard_map/ppermute | solution.py:546
  179.9 7.8 %collective-permute-done.14 = bf16[128,2048]{1,0:T(8,128)(2,1)} collective-permute-done((bf16[128,2048]{1,0:T(8,128)(2,1)S(1)}, bf16[128,2048]{1,0:T(8,128)(2,1)}, u32[]{:S(2)}, u32[]{:S(2)}) %collective-permute-start.14) | collective-permute-done | bytes 524320 | tf_op jit(solution)/shard_map/ppermute | solution.py:571
  187.7 2.3 %add_convert_fusion = bf16[128,2048]{1,0:T(8,128)(2,1)} fusion(bf16[128,2048]{1,0:T(8,128)(2,1)S(1)} %collective-permute-done.15, bf16[128,2048]{1,0:T(8,128)(2,1)} %collective-permute-done.14, bf16[128,2048]{1,0:T(8,128)(2,1)} %collective-permute-done.13, bf16[128,2048]{1,0:T(8,128)(2,1)S(1)} %get-tuple-element.29), kind=kLoop, calls=%fused_computation | loop fusion | flops 2097152 | bytes 2621440 | tf_op jit(solution)/shard_map/convert_element_type | solution.py:583
  (87 shorter events, 30.0 us)
Async XLA Ops:
  2.2 9.8 %collective-permute-start.1 = (bf16[16,1408]{1,0:T(8,128)(2,1)}, bf16[16,1408]{1,0:T(8,128)(2,1)S(1)}, u32[]{:S(2)}, u32[]{:S(2)}) collective-permute-start(bf16[16,1408]{1,0:T(8,128)(2,1)} %get-tuple-element.19), channel_id=1, source_target_pairs={{0,4},{4,0},{8,12},{12,8},{16,20},{20,16},{24,28},{28,24},{32,36},... | collective-permute-start | bytes 135176 | tf_op jit(solution)/shard_map/ppermute | solution.py:442
  33.3 14.1 %collective-permute-start.2 = (bf16[8,32,1408]{2,1,0:T(8,128)(2,1)S(1)}, bf16[8,32,1408]{2,1,0:T(8,128)(2,1)S(1)}, u32[]{:S(2)}, u32[]{:S(2)}) collective-permute-start(bf16[8,32,1408]{2,1,0:T(8,128)(2,1)S(1)} %all_to_all.10.refs_0_), channel_id=1, source_target_pairs={{0,64},{8,72},{16,80},{24,88},{32,96},{40,104},{48,112},{56,120},{... | collective-permute-start | bytes 2162696 | tf_op jit(solution)/shard_map/ppermute | solution.py:450
  36.5 13.6 %collective-permute-start.5 = (bf16[8,32,1408]{2,1,0:T(8,128)(2,1)S(1)}, bf16[8,32,1408]{2,1,0:T(8,128)(2,1)S(1)}, u32[]{:S(2)}, u32[]{:S(2)}) collective-permute-start(bf16[8,32,1408]{2,1,0:T(8,128)(2,1)S(1)} %all_to_all.10.refs_0_), channel_id=1, source_target_pairs={{0,448},{8,456},{16,464},{24,472},{32,480},{40,488},{48,496},{56,5... | collective-permute-start | bytes 2162696 | tf_op jit(solution)/shard_map/ppermute | solution.py:451
  47.4 15.5 %collective-permute-start.3 = (bf16[8,32,1408]{2,1,0:T(8,128)(2,1)S(1)}, bf16[8,32,1408]{2,1,0:T(8,128)(2,1)S(1)}, u32[]{:S(2)}, u32[]{:S(2)}) collective-permute-start(bf16[8,32,1408]{2,1,0:T(8,128)(2,1)S(1)} %collective-permute-done.2.refs_1_), channel_id=1, source_target_pairs={{0,64},{8,72},{16,80},{24,88},{32,96},{40,104},{48,112},{56,120},{... | collective-permute-start | bytes 2162696 | tf_op jit(solution)/shard_map/ppermute | solution.py:450
  50.2 15.7 %collective-permute-start.6 = (bf16[8,32,1408]{2,1,0:T(8,128)(2,1)S(1)}, bf16[8,32,1408]{2,1,0:T(8,128)(2,1)S(1)}, u32[]{:S(2)}, u32[]{:S(2)}) collective-permute-start(bf16[8,32,1408]{2,1,0:T(8,128)(2,1)S(1)} %collective-permute-done.5.refs_2_), channel_id=1, source_target_pairs={{0,448},{8,456},{16,464},{24,472},{32,480},{40,488},{48,496},{56,5... | collective-permute-start | bytes 2162696 | tf_op jit(solution)/shard_map/ppermute | solution.py:451
  55.6 52.3 %collective-permute-start = (bf16[512,2048]{1,0:T(8,128)(2,1)}, bf16[512,2048]{1,0:T(8,128)(2,1)}, u32[]{:S(2)}, u32[]{:S(2)}) collective-permute-start(bf16[512,2048]{1,0:T(8,128)(2,1)} %own_ref.1), channel_id=1, source_target_pairs={{0,4},{4,0},{8,12},{12,8},{16,20},{20,16},{24,28},{28,24},{32,36},... | collective-permute-start | bytes 6291464 | tf_op jit(solution)/shard_map/ppermute | solution.py:454
  62.9 13.5 %collective-permute-start.4 = (bf16[8,32,1408]{2,1,0:T(8,128)(2,1)S(1)}, bf16[8,32,1408]{2,1,0:T(8,128)(2,1)S(1)}, u32[]{:S(2)}, u32[]{:S(2)}) collective-permute-start(bf16[8,32,1408]{2,1,0:T(8,128)(2,1)S(1)} %collective-permute-done.3.refs_3_), channel_id=1, source_target_pairs={{0,64},{8,72},{16,80},{24,88},{32,96},{40,104},{48,112},{56,120},{... | collective-permute-start | bytes 2162696 | tf_op jit(solution)/shard_map/ppermute | solution.py:450
  65.9 12.6 %copy-start.12 = (bf16[8,32,1408]{2,1,0:T(8,128)(2,1)}, bf16[8,32,1408]{2,1,0:T(8,128)(2,1)S(1)}, u32[]{:S(2)}) copy-start(bf16[8,32,1408]{2,1,0:T(8,128)(2,1)S(1)} %collective-permute-done.6.refs_4_) | copy-start | bytes 2162692
  65.9 12.6 %collective-permute-start.7 = (bf16[8,32,1408]{2,1,0:T(8,128)(2,1)S(1)}, bf16[8,32,1408]{2,1,0:T(8,128)(2,1)S(1)}, u32[]{:S(2)}, u32[]{:S(2)}) collective-permute-start(bf16[8,32,1408]{2,1,0:T(8,128)(2,1)S(1)} %collective-permute-done.6.refs_4_), channel_id=1, source_target_pairs={{0,448},{8,456},{16,464},{24,472},{32,480},{40,488},{48,496},{56,5... | collective-permute-start | bytes 2162696 | tf_op jit(solution)/shard_map/ppermute | solution.py:451
  76.5 9.4 %collective-permute-start.8 = (bf16[4,32,1408]{2,1,0:T(8,128)(2,1)S(1)}, bf16[4,32,1408]{2,1,0:T(8,128)(2,1)S(1)}, u32[]{:S(2)}, u32[]{:S(2)}) collective-permute-start(bf16[4,32,1408]{2,1,0:T(8,128)(2,1)S(1)} %slice.8), channel_id=1, source_target_pairs={{0,64},{8,72},{16,80},{24,88},{32,96},{40,104},{48,112},{56,120},{... | collective-permute-start | bytes 1081352 | tf_op jit(solution)/shard_map/ppermute | solution.py:450
  79.4 9.4 %collective-permute-start.9 = (bf16[4,32,1408]{2,1,0:T(8,128)(2,1)S(1)}, bf16[4,32,1408]{2,1,0:T(8,128)(2,1)S(1)}, u32[]{:S(2)}, u32[]{:S(2)}) collective-permute-start(bf16[4,32,1408]{2,1,0:T(8,128)(2,1)S(1)} %slice.9), channel_id=1, source_target_pairs={{0,448},{8,456},{16,464},{24,472},{32,480},{40,488},{48,496},{56,5... | collective-permute-start | bytes 1081352 | tf_op jit(solution)/shard_map/ppermute | solution.py:451
  84.5 22.5 %copy-start.29 = (bf16[2048]{0:T(1024)(128)(2,1)S(1)}, bf16[2048]{0:T(1024)(128)(2,1)}, u32[]{:S(2)}) copy-start(bf16[2048]{0:T(1024)(128)(2,1)} %param.13) | copy-start | bytes 12292
  97.2 56.6 %collective-permute-start.12 = (bf16[2048,512]{1,0:T(8,128)(2,1)S(1)}, bf16[2048,512]{1,0:T(8,128)(2,1)}, u32[]{:S(2)}, u32[]{:S(2)}) collective-permute-start(bf16[2048,512]{1,0:T(8,128)(2,1)S(1)} %shard_map.140.own_ref), channel_id=1, source_target_pairs={{0,4},{4,0},{8,12},{12,8},{16,20},{20,16},{24,28},{28,24},{32,36},... | collective-permute-start | bytes 6291464 | tf_op jit(solution)/shard_map/ppermute | solution.py:507
  107.9 12.1 %copy-start.5 = (bf16[8,32,1408]{2,1,0:T(8,128)(2,1)S(1)}, bf16[8,32,1408]{2,1,0:T(8,128)(2,1)}, u32[]{:S(2)}) copy-start(bf16[8,32,1408]{2,1,0:T(8,128)(2,1)} %copy-done.3) | copy-start | bytes 2162692
  107.9 12.1 %copy-start.8 = (bf16[8,32,1408]{2,1,0:T(8,128)(2,1)S(1)}, bf16[8,32,1408]{2,1,0:T(8,128)(2,1)}, u32[]{:S(2)}) copy-start(bf16[8,32,1408]{2,1,0:T(8,128)(2,1)} %copy-done.6) | copy-start | bytes 2162692
  107.9 12.1 %copy-start.11 = (bf16[8,32,1408]{2,1,0:T(8,128)(2,1)S(1)}, bf16[8,32,1408]{2,1,0:T(8,128)(2,1)}, u32[]{:S(2)}) copy-start(bf16[8,32,1408]{2,1,0:T(8,128)(2,1)} %copy-done.9) | copy-start | bytes 2162692
  107.9 12.1 %copy-start.14 = (bf16[8,32,1408]{2,1,0:T(8,128)(2,1)S(1)}, bf16[8,32,1408]{2,1,0:T(8,128)(2,1)}, u32[]{:S(2)}) copy-start(bf16[8,32,1408]{2,1,0:T(8,128)(2,1)} %copy-done.12) | copy-start | bytes 2162692
  120.0 3.6 %copy-start.2 = (bf16[8,32,1408]{2,1,0:T(8,128)(2,1)S(1)}, bf16[8,32,1408]{2,1,0:T(8,128)(2,1)}, u32[]{:S(2)}) copy-start(bf16[8,32,1408]{2,1,0:T(8,128)(2,1)} %copy-done) | copy-start | bytes 2162692
  123.7 1.9 copy-start.17
  123.7 1.9 copy-start.20
  125.5 5.0 %copy-start.26 = (f32[31,512]{1,0:T(8,128)S(1)}, f32[31,512]{1,0:T(8,128)}, u32[]{:S(2)}) copy-start(f32[31,512]{1,0:T(8,128)} %taps_ref.1) | copy-start | bytes 190468
  127.3 7.4 %copy-start.24 = (bf16[1024,384]{1,0:T(8,128)(2,1)}, bf16[1024,384]{1,0:T(8,128)(2,1)S(1)}, u32[]{:S(2)}) copy-start(bf16[1024,384]{1,0:T(8,128)(2,1)S(1)} %get-tuple-element.24.qkv_ref) | copy-start | bytes 2359300
  127.3 3.2 %collective-permute-start.10 = (bf16[192,128]{1,0:T(8,128)(2,1)S(1)}, bf16[192,128]{1,0:T(8,128)(2,1)S(1)}, u32[]{:S(2)}, u32[]{:S(2)}) collective-permute-start(bf16[192,128]{1,0:T(8,128)(2,1)S(1)} %get-tuple-element.20), channel_id=1, source_target_pairs={{0,8},{4,12},{8,16},{12,20},{16,24},{20,28},{24,32},{28,36},{32,40... | collective-permute-start | bytes 147464 | tf_op jit(solution)/shard_map/ppermute | solution.py:498
  130.5 8.6 %copy-start.27 = (f32[8]{0:T(128)S(1)}, f32[8]{0:T(128)}, u32[]{:S(2)}) copy-start(f32[8]{0:T(128)} %sinks_ref.1) | copy-start | bytes 100
  134.7 13.4 %all-to-all-start.1 = ((f32[8,2,1024]{2,1,0:T(2,128)}), f32[8,2,1024]{2,1,0:T(2,128)S(1)}, u32[]{:S(2)}, u32[]{:S(2)}) async-start(f32[8,2,1024]{2,1,0:T(2,128)} %get-tuple-element.23), calls=%async_computation.1 | async-start | bytes 131072 | tf_op jit(solution)/shard_map/all_to_all | solution.py:519
  139.1 1.1 copy-start.25
  140.2 7.9 %copy-start.23 = (f32[512]{0:T(512)S(1)}, f32[512]{0:T(512)}, u32[]{:S(2)}) copy-start(f32[512]{0:T(512)} %param.20) | copy-start | bytes 6148
  150.0 3.8 %collective-permute-start.11 = (bf16[512,512]{1,0:T(8,128)(2,1)S(1)}, bf16[512,512]{1,0:T(8,128)(2,1)S(1)}, u32[]{:S(2)}, u32[]{:S(2)}) collective-permute-start(bf16[512,512]{1,0:T(8,128)(2,1)S(1)} %get-tuple-element.28), channel_id=1, source_target_pairs={{0,4},{4,0},{8,12},{12,8},{16,20},{20,16},{24,28},{28,24},{32,36},... | collective-permute-start | bytes 1572872 | tf_op jit(solution)/shard_map/ppermute | solution.py:542
  158.9 20.9 %collective-permute-start.13 = (bf16[128,2048]{1,0:T(8,128)(2,1)}, bf16[128,2048]{1,0:T(8,128)(2,1)}, u32[]{:S(2)}, u32[]{:S(2)}) collective-permute-start(bf16[128,2048]{1,0:T(8,128)(2,1)} %get-tuple-element.30), channel_id=1, source_target_pairs={{0,2},{1,3},{2,0},{3,1},{4,6},{5,7},{6,4},{7,5},{8,10},{9,11},{10,... | collective-permute-start | bytes 1572872 | tf_op jit(solution)/shard_map/ppermute | solution.py:571
  163.7 24.0 %collective-permute-start.14 = (bf16[128,2048]{1,0:T(8,128)(2,1)S(1)}, bf16[128,2048]{1,0:T(8,128)(2,1)}, u32[]{:S(2)}, u32[]{:S(2)}) collective-permute-start(bf16[128,2048]{1,0:T(8,128)(2,1)S(1)} %get-tuple-element.31), channel_id=1, source_target_pairs={{0,1},{1,2},{2,3},{3,0},{4,5},{5,6},{6,7},{7,4},{8,9},{9,10},{10,1... | collective-permute-start | bytes 1572872 | tf_op jit(solution)/shard_map/ppermute | solution.py:571
  171.0 16.7 %collective-permute-start.15 = (bf16[128,2048]{1,0:T(8,128)(2,1)}, bf16[128,2048]{1,0:T(8,128)(2,1)S(1)}, u32[]{:S(2)}, u32[]{:S(2)}) collective-permute-start(bf16[128,2048]{1,0:T(8,128)(2,1)} %get-tuple-element.32), channel_id=1, source_target_pairs={{0,3},{1,0},{2,1},{3,2},{4,7},{5,4},{6,5},{7,6},{8,11},{9,8},{10,9... | collective-permute-start | bytes 1572872 | tf_op jit(solution)/shard_map/ppermute | solution.py:571
  175.3 3.9 %collective-permute-start.16 = (f32[4,512]{1,0:T(4,128)S(1)}, f32[4,512]{1,0:T(4,128)S(1)}, u32[]{:S(2)}, u32[]{:S(2)}) collective-permute-start(f32[4,512]{1,0:T(4,128)S(1)} %get-tuple-element.35), channel_id=1, source_target_pairs={{0,4},{4,0},{8,12},{12,8},{16,20},{20,16},{24,28},{28,24},{32,36},... | collective-permute-start | bytes 24584 | tf_op jit(solution)/shard_map/ppermute | solution.py:546
  (16 other events, 14.8 us)

commit v5 on v4

--- a/solution.py
+++ b/solution.py
@@ -115,8 +115,8 @@
 
 def norm_kernel(own_ref, other_ref, gain_ref, out_ref):
     core = lax.axis_index("core")
-    count, model = own_ref.shape
-    group = model // CHIPS
+    count, _ = own_ref.shape
+    group = 128 // 4
     tile = 32
     lane = lax.broadcasted_iota(jnp.int32, (tile, 128), 1)
     gain = gain_ref[...].astype(jnp.float32)
@@ -136,19 +136,25 @@
 
             @pl.when(core == 1)
             def _():
-                for to in range(0, model, 128):
-                    y, z = to // group // SIDE, to // group % SIDE
-                    out = jnp.zeros((tile, 128), jnp.float32)
-                    for part in range(128 // group):
-                        start = ((z + part) * SIDE + y) * group
-                        tile_at = start // 128 * 128
-                        turned = pltpu.roll(
-                            normed[:, tile_at : tile_at + 128],
-                            (part * group - start % 128) % 128,
-                            1,
-                        )
-                        out = jnp.where(lane // group == part, turned, out)
-                    out_ref[rows, to : to + 128] = out.astype(jnp.bfloat16)
+                for z in range(0, SIDE, 4):
+                    for y in range(0, SIDE, 4):
+                        tiles = []
+                        for part in range(4):
+                            start = ((z + part) * SIDE + y) * group
+                            tiles.append(normed[:, start : start + 128])
+                        for away in (2, 1):
+                            low = jnp.bitwise_and(lane // group, away) == 0
+                            tiles = [
+                                jnp.where(low, tiles[i], pltpu.roll(tiles[i + away], away * group, 1))
+                                if i & away == 0
+                                else jnp.where(
+                                    low, pltpu.roll(tiles[i - away], 128 - away * group, 1), tiles[i]
+                                )
+                                for i in range(4)
+                            ]
+                        for part in range(4):
+                            to = ((y + part) * SIDE + z) * group
+                            out_ref[rows, to : to + 128] = tiles[part].astype(jnp.bfloat16)
 
 
 def line_of(index):
@@ -320,7 +326,7 @@
     half_blocks = blocks // CORES
     heads = cols // HEAD_DIM
 
-    @pl.loop(0, blocks)
+    @pl.loop(0, blocks, unroll=2)
     def _(block):
         base = pl.multiple_of(block * WINDOW, WINDOW)
         window = pl.ds(base, 2 * WINDOW)
@@ -330,24 +336,22 @@
         allowed = (key_at > query_at) & (key_at <= query_at + WINDOW) & (key_at >= lowest)
         outs = []
         for pair in range(heads // 2):
-            query = qkv_ref[pl.ds(base, WINDOW), pair * 128 : (pair + 1) * 128]
+            query = qkv_ref[pl.ds(base, WINDOW), pair * 128 : (pair + 1) * 128] * HEAD_DIM ** (-0.5)
             total = jnp.zeros((WINDOW, 128), jnp.float32)
             for which, (keys, values) in enumerate(((k_lo, v_lo), (k_hi, v_hi))):
                 head = 2 * pair + which
-                scores = (
-                    lax.dot_general(
-                        keys[window, :],
-                        query,
-                        (((1,), (1,)), ((), ())),
-                        preferred_element_type=jnp.float32,
-                    )
-                    * HEAD_DIM ** (-0.5)
+                scores = lax.dot_general(
+                    keys[window, :],
+                    query,
+                    (((1,), (1,)), ((), ())),
+                    preferred_element_type=jnp.float32,
                 )
-                sums = jnp.sum(jnp.where(allowed, jnp.exp(scores), 0.0), axis=0, keepdims=True)
+                scores = jnp.where(allowed, scores, -jnp.inf)
+                sums = jnp.sum(jnp.exp(scores), axis=0, keepdims=True)
                 sink = jnp.full((1, WINDOW), sinks_ref[core * heads + head], jnp.float32)
                 log_total = jnp.log(sums + jnp.exp(sink))
                 logs_ref[pl.ds(head, 1), pl.ds(base, WINDOW)] = log_total
-                weights = jnp.where(allowed, jnp.exp(scores - log_total), 0.0).astype(jnp.bfloat16)
+                weights = jnp.exp(scores - log_total).astype(jnp.bfloat16)
                 total = total + lax.dot_general(
                     weights,
                     values[window, :],
@@ -382,7 +386,7 @@
             [conv_ref[rows, :], attn_ref[rows, :], got_ref[rows, :]], axis=1
         )
 
-    @pl.loop(0, SIDE)
+    @pl.loop(0, SIDE, unroll=4)
     def _(z):
         cols = pl.ds(pl.multiple_of(z * SIDE * block, TILE), SIDE * block)
         by_z, by_y = z * SIDE * block, z * block

time: 193 us -> 191 us (0.990)
  Pallas kernels: 45.1 us -> 42.7 us
    pallas_call x12, Pallas kernels: 45.1 us -> 42.7 us  [call(): pl.pallas_call(body, out_shape=outs, in_specs=in_specs, out_specs=jax.tre...]
where the time goes in v5:
time: 191 us; the launch traced here: 189 us
  starting transfers between devices  73.5 us (38%)
  Pallas kernels  42.7 us (22%)
  waiting for transfers between devices  30.8 us (16%)
  blocking collectives  18.9 us (10%)
  local copies, waits for them, and re-layouts  16 us (8%)
  other arithmetic  5.74 us (3%)
    pallas_call x12, Pallas kernels, call(): pl.pallas_call(body, out_shape=outs, in_specs=in_specs, out_specs=jax.tre...  42.7 us
    all_to_all x1, blocking collectives, layer(): lax.all_to_all(sent, SP, 0, 0, tiled=True, axis_index_groups=LINES)  18.9 us
    ppermute x4, starting transfers between devices, layer(): behind = lax.ppermute(behind, SP, BEHIND)  17.8 us
    unnamed x60, local copies, waits for them, and re-layouts  16 us
    ppermute x4, waiting for transfers between devices, layer(): ahead = lax.ppermute(ahead, SP, AHEAD)  14.6 us
    ppermute x3, starting transfers between devices, to_member(): lax.ppermute(value, 'tp', [(i, (i + away) % peers) for i in range(peers)])  11.2 us
    ppermute x4, starting transfers between devices, layer(): ahead = lax.ppermute(ahead, SP, AHEAD)  9.11 us
    ppermute x3, waiting for transfers between devices, to_member(): lax.ppermute(value, 'tp', [(i, (i + away) % peers) for i in range(peers)])  9.04 us
  transfers between devices with their start and end apart: 18, of which 10 were waited for; matrix products, arithmetic and copies ran while one was open for 2% of the time, Pallas kernels for 19%

profile of v5, /device:TPU:1, one launch (start us, length us, event | category | flops | bytes accessed | tf_op | source)
XLA Modules:
  0.0 188.9 jit_solution(3297880857902643919)
XLA Ops:
  2.2 8.7 %collective-permute-start.1 = (bf16[16,1408]{1,0:T(8,128)(2,1)}, bf16[16,1408]{1,0:T(8,128)(2,1)S(1)}, u32[]{:S(2)}, u32[]{:S(2)}) collective-permute-start(bf16[16,1408]{1,0:T(8,128)(2,1)} %get-tuple-element.19), channel_id=1, source_target_pairs={{0,4},{4,0},{8,12},{12,8},{16,20},{20,16},{24,28},{28,24},{32,36},... | collective-permute-start | bytes 135176 | tf_op jit(solution)/shard_map/ppermute | solution.py:446
  14.4 18.9 %all_to_all.10.refs_0_ = bf16[8,32,1408]{2,1,0:T(8,128)(2,1)S(1)} all-to-all(bf16[8,32,1408]{2,1,0:T(8,128)(2,1)} %shard_map.133), channel_id=1, replica_groups={{0,8,16,24,32,40,48,56},{64,72,80,88,96,104,112,120},{128,136,144,152,1..., dimensions={0} | all-to-all | bytes 1441792 | tf_op jit(solution)/shard_map/all_to_all | solution.py:448
  33.3 3.2 %collective-permute-start.2 = (bf16[8,32,1408]{2,1,0:T(8,128)(2,1)S(1)}, bf16[8,32,1408]{2,1,0:T(8,128)(2,1)S(1)}, u32[]{:S(2)}, u32[]{:S(2)}) collective-permute-start(bf16[8,32,1408]{2,1,0:T(8,128)(2,1)S(1)} %all_to_all.10.refs_0_), channel_id=1, source_target_pairs={{0,64},{8,72},{16,80},{24,88},{32,96},{40,104},{48,112},{56,120},{... | collective-permute-start | bytes 2162696 | tf_op jit(solution)/shard_map/ppermute | solution.py:454
  36.5 3.8 %collective-permute-start.5 = (bf16[8,32,1408]{2,1,0:T(8,128)(2,1)S(1)}, bf16[8,32,1408]{2,1,0:T(8,128)(2,1)S(1)}, u32[]{:S(2)}, u32[]{:S(2)}) collective-permute-start(bf16[8,32,1408]{2,1,0:T(8,128)(2,1)S(1)} %all_to_all.10.refs_0_), channel_id=1, source_target_pairs={{0,448},{8,456},{16,464},{24,472},{32,480},{40,488},{48,496},{56,5... | collective-permute-start | bytes 2162696 | tf_op jit(solution)/shard_map/ppermute | solution.py:455
  40.3 7.0 %collective-permute-done.2.refs_1_ = bf16[8,32,1408]{2,1,0:T(8,128)(2,1)S(1)} collective-permute-done((bf16[8,32,1408]{2,1,0:T(8,128)(2,1)S(1)}, bf16[8,32,1408]{2,1,0:T(8,128)(2,1)S(1)}, u32[]{:S(2)}, u32[]{:S(2)}) %collective-permute-start.2) | collective-permute-done | bytes 720928 | tf_op jit(solution)/shard_map/ppermute | solution.py:454
  47.4 1.9 %collective-permute-start.3 = (bf16[8,32,1408]{2,1,0:T(8,128)(2,1)S(1)}, bf16[8,32,1408]{2,1,0:T(8,128)(2,1)S(1)}, u32[]{:S(2)}, u32[]{:S(2)}) collective-permute-start(bf16[8,32,1408]{2,1,0:T(8,128)(2,1)S(1)} %collective-permute-done.2.refs_1_), channel_id=1, source_target_pairs={{0,64},{8,72},{16,80},{24,88},{32,96},{40,104},{48,112},{56,120},{... | collective-permute-start | bytes 2162696 | tf_op jit(solution)/shard_map/ppermute | solution.py:454
  50.2 4.6 %collective-permute-start.6 = (bf16[8,32,1408]{2,1,0:T(8,128)(2,1)S(1)}, bf16[8,32,1408]{2,1,0:T(8,128)(2,1)S(1)}, u32[]{:S(2)}, u32[]{:S(2)}) collective-permute-start(bf16[8,32,1408]{2,1,0:T(8,128)(2,1)S(1)} %collective-permute-done.5.refs_2_), channel_id=1, source_target_pairs={{0,448},{8,456},{16,464},{24,472},{32,480},{40,488},{48,496},{56,5... | collective-permute-start | bytes 2162696 | tf_op jit(solution)/shard_map/ppermute | solution.py:455
  55.6 7.3 %collective-permute-start = (bf16[512,2048]{1,0:T(8,128)(2,1)}, bf16[512,2048]{1,0:T(8,128)(2,1)}, u32[]{:S(2)}, u32[]{:S(2)}) collective-permute-start(bf16[512,2048]{1,0:T(8,128)(2,1)} %own_ref.1), channel_id=1, source_target_pairs={{0,4},{4,0},{8,12},{12,8},{16,20},{20,16},{24,28},{28,24},{32,36},... | collective-permute-start | bytes 6291464 | tf_op jit(solution)/shard_map/ppermute | solution.py:458
  62.9 2.1 %collective-permute-start.4 = (bf16[8,32,1408]{2,1,0:T(8,128)(2,1)S(1)}, bf16[8,32,1408]{2,1,0:T(8,128)(2,1)S(1)}, u32[]{:S(2)}, u32[]{:S(2)}) collective-permute-start(bf16[8,32,1408]{2,1,0:T(8,128)(2,1)S(1)} %collective-permute-done.3.refs_3_), channel_id=1, source_target_pairs={{0,64},{8,72},{16,80},{24,88},{32,96},{40,104},{48,112},{56,120},{... | collective-permute-start | bytes 2162696 | tf_op jit(solution)/shard_map/ppermute | solution.py:454
  65.9 4.4 %collective-permute-start.7 = (bf16[8,32,1408]{2,1,0:T(8,128)(2,1)S(1)}, bf16[8,32,1408]{2,1,0:T(8,128)(2,1)S(1)}, u32[]{:S(2)}, u32[]{:S(2)}) collective-permute-start(bf16[8,32,1408]{2,1,0:T(8,128)(2,1)S(1)} %collective-permute-done.6.refs_4_), channel_id=1, source_target_pairs={{0,448},{8,456},{16,464},{24,472},{32,480},{40,488},{48,496},{56,5... | collective-permute-start | bytes 2162696 | tf_op jit(solution)/shard_map/ppermute | solution.py:455
  70.3 6.2 %collective-permute-done.4.refs_0_.refs_5_ = bf16[8,32,1408]{2,1,0:T(8,128)(2,1)S(1)} collective-permute-done((bf16[8,32,1408]{2,1,0:T(8,128)(2,1)S(1)}, bf16[8,32,1408]{2,1,0:T(8,128)(2,1)S(1)}, u32[]{:S(2)}, u32[]{:S(2)}) %collective-permute-start.4) | collective-permute-done | bytes 720928 | tf_op jit(solution)/shard_map/ppermute | solution.py:454
  76.5 1.9 %collective-permute-start.8 = (bf16[4,32,1408]{2,1,0:T(8,128)(2,1)S(1)}, bf16[4,32,1408]{2,1,0:T(8,128)(2,1)S(1)}, u32[]{:S(2)}, u32[]{:S(2)}) collective-permute-start(bf16[4,32,1408]{2,1,0:T(8,128)(2,1)S(1)} %slice.8), channel_id=1, source_target_pairs={{0,64},{8,72},{16,80},{24,88},{32,96},{40,104},{48,112},{56,120},{... | collective-permute-start | bytes 1081352 | tf_op jit(solution)/shard_map/ppermute | solution.py:454
  79.4 5.0 %collective-permute-start.9 = (bf16[4,32,1408]{2,1,0:T(8,128)(2,1)S(1)}, bf16[4,32,1408]{2,1,0:T(8,128)(2,1)S(1)}, u32[]{:S(2)}, u32[]{:S(2)}) collective-permute-start(bf16[4,32,1408]{2,1,0:T(8,128)(2,1)S(1)} %slice.9), channel_id=1, source_target_pairs={{0,448},{8,456},{16,464},{24,472},{32,480},{40,488},{48,496},{56,5... | collective-permute-start | bytes 1081352 | tf_op jit(solution)/shard_map/ppermute | solution.py:455
  86.6 2.2 %collective-permute-done.9.b_ref.refs_8_ = bf16[4,32,1408]{2,1,0:T(8,128)(2,1)S(1)} collective-permute-done((bf16[4,32,1408]{2,1,0:T(8,128)(2,1)S(1)}, bf16[4,32,1408]{2,1,0:T(8,128)(2,1)S(1)}, u32[]{:S(2)}, u32[]{:S(2)}) %collective-permute-start.9) | collective-permute-done | bytes 360480 | tf_op jit(solution)/shard_map/ppermute | solution.py:455
  97.2 7.8 %collective-permute-start.12 = (bf16[2048,512]{1,0:T(8,128)(2,1)S(1)}, bf16[2048,512]{1,0:T(8,128)(2,1)}, u32[]{:S(2)}, u32[]{:S(2)}) collective-permute-start(bf16[2048,512]{1,0:T(8,128)(2,1)S(1)} %shard_map.140.own_ref), channel_id=1, source_target_pairs={{0,4},{4,0},{8,12},{12,8},{16,20},{20,16},{24,28},{28,24},{32,36},... | collective-permute-start | bytes 6291464 | tf_op jit(solution)/shard_map/ppermute | solution.py:511
  105.1 1.9 %fusion = (f32[1024,32]{1,0:T(8,128)S(1)}, f32[1024,32]{1,0:T(8,128)S(1)}, f32[1024,32]{1,0:T(8,128)S(1)}) fusion(f32[32]{0:T(128)S(1)} %multiply_power_fusion, f32[1024]{0:T(1024)S(1)} %add_convert_fusion.1), kind=kLoop, calls=%fused_computation.5 | loop fusion | flops 65536 | bytes 397440 | tf_op jit(solution)/shard_map/neg | solution.py:474
  108.0 12.1 %shard_map.131.x_ref = bf16[1024,2048]{1,0:T(8,128)(2,1)S(1)} custom-call(bf16[512,2048]{1,0:T(8,128)(2,1)} %own_ref.1, bf16[512,2048]{1,0:T(8,128)(2,1)} %collective-permute-done.other_ref, bf16[1,2048]{1,0:T(2,128)(2,1)S(1)} %broadcast_in_dim.8.gain_ref), custom_call_target="tpu_custom_call" | custom-call | flops 1073741824 | bytes 1048576 | tf_op jit(solution)/shard_map/pallas_call | solution.py:53
  120.2 3.6 %shard_map.134.refs_2_ = f32[1024,896]{1,0:T(8,128)S(1)} custom-call(bf16[1024,2048]{1,0:T(8,128)(2,1)S(1)} %shard_map.131.x_ref, bf16[8,32,1408]{2,1,0:T(8,128)(2,1)S(1)} %all_to_all.10.refs_0_, bf16[8,32,1408]{2,1,0:T(8,128)(2,1)S(1)} %copy-done.5, bf16[8,32,1408]{2,1,0:T(8,128)(2,1)S(1)} %copy-done.8, bf16[8,32,1408]{2,1,0:T(8,128)(2,1)S(1)} %copy-done.11, ...), custom_call_target="tpu_custom_call" | custom-call | flops 2348810240 | bytes 1048576 | tf_op jit(solution)/shard_map/pallas_call | solution.py:53
  127.4 2.1 %collective-permute-start.10 = (bf16[192,128]{1,0:T(8,128)(2,1)S(1)}, bf16[192,128]{1,0:T(8,128)(2,1)S(1)}, u32[]{:S(2)}, u32[]{:S(2)}) collective-permute-start(bf16[192,128]{1,0:T(8,128)(2,1)S(1)} %get-tuple-element.20), channel_id=1, source_target_pairs={{0,8},{4,12},{8,16},{12,20},{16,24},{20,28},{24,32},{28,36},{32,40... | collective-permute-start | bytes 147464 | tf_op jit(solution)/shard_map/ppermute | solution.py:502
  130.7 4.1 %shard_map.137 = (f32[1024,256]{1,0:T(8,128)S(1)}, f32[8,2,1024]{2,1,0:T(2,128)}) custom-call(bf16[192,128]{1,0:T(8,128)(2,1)S(1)} %collective-permute-done.10.before_ref, bf16[1024,256]{1,0:T(8,128)(2,1)S(1)} %get-tuple-element.21.glu_ref, f32[31,512]{1,0:T(8,128)S(1)} %copy-done.26), custom_call_target="tpu_custom_call" | custom-call | flops 4294967296 | bytes 1048576 | tf_op jit(solution)/shard_map/pallas_call | solution.py:53
  134.8 4.4 %all-to-all-start.1 = ((f32[8,2,1024]{2,1,0:T(2,128)}), f32[8,2,1024]{2,1,0:T(2,128)S(1)}, u32[]{:S(2)}, u32[]{:S(2)}) async-start(f32[8,2,1024]{2,1,0:T(2,128)} %get-tuple-element.23), calls=%async_computation.1 | async-start | bytes 131072 | tf_op jit(solution)/shard_map/all_to_all | solution.py:523
  140.4 7.1 %shard_map.138 = (bf16[512,256]{1,0:T(8,128)(2,1)S(1)}, bf16[512,256]{1,0:T(8,128)(2,1)S(1)}, f32[4,1024]{1,0:T(4,128)S(1)}) custom-call(f32[8]{0:T(128)S(1)} %copy-done.27, bf16[1024,384]{1,0:T(8,128)(2,1)S(1)} %copy-done.25, bf16[192,128]{1,0:T(8,128)(2,1)S(1)} %collective-permute-done.10.before_ref), custom_call_target="tpu_custom_call" | custom-call | flops 4294967296 | bytes 1048576 | tf_op jit(solution)/shard_map/pallas_call | solution.py:53
  150.1 1.9 %collective-permute-start.11 = (bf16[512,512]{1,0:T(8,128)(2,1)S(1)}, bf16[512,512]{1,0:T(8,128)(2,1)S(1)}, u32[]{:S(2)}, u32[]{:S(2)}) collective-permute-start(bf16[512,512]{1,0:T(8,128)(2,1)S(1)} %get-tuple-element.28), channel_id=1, source_target_pairs={{0,4},{4,0},{8,12},{12,8},{16,20},{20,16},{24,28},{28,24},{32,36},... | collective-permute-start | bytes 1572872 | tf_op jit(solution)/shard_map/ppermute | solution.py:546
  152.0 1.9 collective-permute-done.11.got_ref
  153.9 3.9 %shard_map.142 = (bf16[128,2048]{1,0:T(8,128)(2,1)}, bf16[128,2048]{1,0:T(8,128)(2,1)S(1)}) custom-call(bf16[512,256]{1,0:T(8,128)(2,1)S(1)} %get-tuple-element.26.conv_ref, bf16[512,256]{1,0:T(8,128)(2,1)S(1)} %get-tuple-element.27.attn_ref, bf16[512,512]{1,0:T(8,128)(2,1)S(1)} %collective-permute-done.11.got_ref, ...), custom_call_target="tpu_custom_call" | custom-call | flops 1073741824 | bytes 1048576 | tf_op jit(solution)/shard_map/pallas_call | solution.py:53
  157.8 4.8 %collective-permute-start.13 = (bf16[128,2048]{1,0:T(8,128)(2,1)}, bf16[128,2048]{1,0:T(8,128)(2,1)}, u32[]{:S(2)}, u32[]{:S(2)}) collective-permute-start(bf16[128,2048]{1,0:T(8,128)(2,1)} %get-tuple-element.30), channel_id=1, source_target_pairs={{0,2},{1,3},{2,0},{3,1},{4,6},{5,7},{6,4},{7,5},{8,10},{9,11},{10,... | collective-permute-start | bytes 1572872 | tf_op jit(solution)/shard_map/ppermute | solution.py:575
  162.5 2.2 %collective-permute-start.14 = (bf16[128,2048]{1,0:T(8,128)(2,1)S(1)}, bf16[128,2048]{1,0:T(8,128)(2,1)}, u32[]{:S(2)}, u32[]{:S(2)}) collective-permute-start(bf16[128,2048]{1,0:T(8,128)(2,1)S(1)} %get-tuple-element.31), channel_id=1, source_target_pairs={{0,1},{1,2},{2,3},{3,0},{4,5},{5,6},{6,7},{7,4},{8,9},{9,10},{10,1... | collective-permute-start | bytes 1572872 | tf_op jit(solution)/shard_map/ppermute | solution.py:575
  164.7 3.9 %shard_map.141 = (bf16[128,2048]{1,0:T(8,128)(2,1)}, bf16[128,2048]{1,0:T(8,128)(2,1)S(1)}) custom-call(bf16[512,256]{1,0:T(8,128)(2,1)S(1)} %get-tuple-element.26.conv_ref, bf16[512,256]{1,0:T(8,128)(2,1)S(1)} %get-tuple-element.27.attn_ref, bf16[512,512]{1,0:T(8,128)(2,1)S(1)} %collective-permute-done.11.got_ref, ...), custom_call_target="tpu_custom_call" | custom-call | flops 1073741824 | bytes 1048576 | tf_op jit(solution)/shard_map/pallas_call | solution.py:53
  168.6 4.3 %collective-permute-start.15 = (bf16[128,2048]{1,0:T(8,128)(2,1)}, bf16[128,2048]{1,0:T(8,128)(2,1)S(1)}, u32[]{:S(2)}, u32[]{:S(2)}) collective-permute-start(bf16[128,2048]{1,0:T(8,128)(2,1)} %get-tuple-element.32), channel_id=1, source_target_pairs={{0,3},{1,0},{2,1},{3,2},{4,7},{5,4},{6,5},{7,6},{8,11},{9,8},{10,9... | collective-permute-start | bytes 1572872 | tf_op jit(solution)/shard_map/ppermute | solution.py:575
  173.0 3.1 %collective-permute-start.16 = (f32[4,512]{1,0:T(4,128)S(1)}, f32[4,512]{1,0:T(4,128)S(1)}, u32[]{:S(2)}, u32[]{:S(2)}) collective-permute-start(f32[4,512]{1,0:T(4,128)S(1)} %get-tuple-element.35), channel_id=1, source_target_pairs={{0,4},{4,0},{8,12},{12,8},{16,20},{20,16},{24,28},{28,24},{32,36},... | collective-permute-start | bytes 24584 | tf_op jit(solution)/shard_map/ppermute | solution.py:550
  177.5 9.0 %collective-permute-done.14 = bf16[128,2048]{1,0:T(8,128)(2,1)} collective-permute-done((bf16[128,2048]{1,0:T(8,128)(2,1)S(1)}, bf16[128,2048]{1,0:T(8,128)(2,1)}, u32[]{:S(2)}, u32[]{:S(2)}) %collective-permute-start.14) | collective-permute-done | bytes 524320 | tf_op jit(solution)/shard_map/ppermute | solution.py:575
  186.5 2.3 %add_convert_fusion = bf16[128,2048]{1,0:T(8,128)(2,1)} fusion(bf16[128,2048]{1,0:T(8,128)(2,1)S(1)} %collective-permute-done.15, bf16[128,2048]{1,0:T(8,128)(2,1)} %collective-permute-done.14, bf16[128,2048]{1,0:T(8,128)(2,1)} %collective-permute-done.13, bf16[128,2048]{1,0:T(8,128)(2,1)S(1)} %get-tuple-element.29), kind=kLoop, calls=%fused_computation | loop fusion | flops 2097152 | bytes 2621440 | tf_op jit(solution)/shard_map/convert_element_type | solution.py:587
  (87 shorter events, 30.0 us)
Async XLA Ops:
  2.2 9.8 %collective-permute-start.1 = (bf16[16,1408]{1,0:T(8,128)(2,1)}, bf16[16,1408]{1,0:T(8,128)(2,1)S(1)}, u32[]{:S(2)}, u32[]{:S(2)}) collective-permute-start(bf16[16,1408]{1,0:T(8,128)(2,1)} %get-tuple-element.19), channel_id=1, source_target_pairs={{0,4},{4,0},{8,12},{12,8},{16,20},{20,16},{24,28},{28,24},{32,36},... | collective-permute-start | bytes 135176 | tf_op jit(solution)/shard_map/ppermute | solution.py:446
  33.3 14.1 %collective-permute-start.2 = (bf16[8,32,1408]{2,1,0:T(8,128)(2,1)S(1)}, bf16[8,32,1408]{2,1,0:T(8,128)(2,1)S(1)}, u32[]{:S(2)}, u32[]{:S(2)}) collective-permute-start(bf16[8,32,1408]{2,1,0:T(8,128)(2,1)S(1)} %all_to_all.10.refs_0_), channel_id=1, source_target_pairs={{0,64},{8,72},{16,80},{24,88},{32,96},{40,104},{48,112},{56,120},{... | collective-permute-start | bytes 2162696 | tf_op jit(solution)/shard_map/ppermute | solution.py:454
  36.5 13.6 %collective-permute-start.5 = (bf16[8,32,1408]{2,1,0:T(8,128)(2,1)S(1)}, bf16[8,32,1408]{2,1,0:T(8,128)(2,1)S(1)}, u32[]{:S(2)}, u32[]{:S(2)}) collective-permute-start(bf16[8,32,1408]{2,1,0:T(8,128)(2,1)S(1)} %all_to_all.10.refs_0_), channel_id=1, source_target_pairs={{0,448},{8,456},{16,464},{24,472},{32,480},{40,488},{48,496},{56,5... | collective-permute-start | bytes 2162696 | tf_op jit(solution)/shard_map/ppermute | solution.py:455
  47.4 15.5 %collective-permute-start.3 = (bf16[8,32,1408]{2,1,0:T(8,128)(2,1)S(1)}, bf16[8,32,1408]{2,1,0:T(8,128)(2,1)S(1)}, u32[]{:S(2)}, u32[]{:S(2)}) collective-permute-start(bf16[8,32,1408]{2,1,0:T(8,128)(2,1)S(1)} %collective-permute-done.2.refs_1_), channel_id=1, source_target_pairs={{0,64},{8,72},{16,80},{24,88},{32,96},{40,104},{48,112},{56,120},{... | collective-permute-start | bytes 2162696 | tf_op jit(solution)/shard_map/ppermute | solution.py:454
  50.2 15.7 %collective-permute-start.6 = (bf16[8,32,1408]{2,1,0:T(8,128)(2,1)S(1)}, bf16[8,32,1408]{2,1,0:T(8,128)(2,1)S(1)}, u32[]{:S(2)}, u32[]{:S(2)}) collective-permute-start(bf16[8,32,1408]{2,1,0:T(8,128)(2,1)S(1)} %collective-permute-done.5.refs_2_), channel_id=1, source_target_pairs={{0,448},{8,456},{16,464},{24,472},{32,480},{40,488},{48,496},{56,5... | collective-permute-start | bytes 2162696 | tf_op jit(solution)/shard_map/ppermute | solution.py:455
  55.6 52.3 %collective-permute-start = (bf16[512,2048]{1,0:T(8,128)(2,1)}, bf16[512,2048]{1,0:T(8,128)(2,1)}, u32[]{:S(2)}, u32[]{:S(2)}) collective-permute-start(bf16[512,2048]{1,0:T(8,128)(2,1)} %own_ref.1), channel_id=1, source_target_pairs={{0,4},{4,0},{8,12},{12,8},{16,20},{20,16},{24,28},{28,24},{32,36},... | collective-permute-start | bytes 6291464 | tf_op jit(solution)/shard_map/ppermute | solution.py:458
  62.9 13.5 %collective-permute-start.4 = (bf16[8,32,1408]{2,1,0:T(8,128)(2,1)S(1)}, bf16[8,32,1408]{2,1,0:T(8,128)(2,1)S(1)}, u32[]{:S(2)}, u32[]{:S(2)}) collective-permute-start(bf16[8,32,1408]{2,1,0:T(8,128)(2,1)S(1)} %collective-permute-done.3.refs_3_), channel_id=1, source_target_pairs={{0,64},{8,72},{16,80},{24,88},{32,96},{40,104},{48,112},{56,120},{... | collective-permute-start | bytes 2162696 | tf_op jit(solution)/shard_map/ppermute | solution.py:454
  65.9 12.6 %copy-start.12 = (bf16[8,32,1408]{2,1,0:T(8,128)(2,1)}, bf16[8,32,1408]{2,1,0:T(8,128)(2,1)S(1)}, u32[]{:S(2)}) copy-start(bf16[8,32,1408]{2,1,0:T(8,128)(2,1)S(1)} %collective-permute-done.6.refs_4_) | copy-start | bytes 2162692
  65.9 12.6 %collective-permute-start.7 = (bf16[8,32,1408]{2,1,0:T(8,128)(2,1)S(1)}, bf16[8,32,1408]{2,1,0:T(8,128)(2,1)S(1)}, u32[]{:S(2)}, u32[]{:S(2)}) collective-permute-start(bf16[8,32,1408]{2,1,0:T(8,128)(2,1)S(1)} %collective-permute-done.6.refs_4_), channel_id=1, source_target_pairs={{0,448},{8,456},{16,464},{24,472},{32,480},{40,488},{48,496},{56,5... | collective-permute-start | bytes 2162696 | tf_op jit(solution)/shard_map/ppermute | solution.py:455
  76.5 9.4 %collective-permute-start.8 = (bf16[4,32,1408]{2,1,0:T(8,128)(2,1)S(1)}, bf16[4,32,1408]{2,1,0:T(8,128)(2,1)S(1)}, u32[]{:S(2)}, u32[]{:S(2)}) collective-permute-start(bf16[4,32,1408]{2,1,0:T(8,128)(2,1)S(1)} %slice.8), channel_id=1, source_target_pairs={{0,64},{8,72},{16,80},{24,88},{32,96},{40,104},{48,112},{56,120},{... | collective-permute-start | bytes 1081352 | tf_op jit(solution)/shard_map/ppermute | solution.py:454
  79.4 9.4 %collective-permute-start.9 = (bf16[4,32,1408]{2,1,0:T(8,128)(2,1)S(1)}, bf16[4,32,1408]{2,1,0:T(8,128)(2,1)S(1)}, u32[]{:S(2)}, u32[]{:S(2)}) collective-permute-start(bf16[4,32,1408]{2,1,0:T(8,128)(2,1)S(1)} %slice.9), channel_id=1, source_target_pairs={{0,448},{8,456},{16,464},{24,472},{32,480},{40,488},{48,496},{56,5... | collective-permute-start | bytes 1081352 | tf_op jit(solution)/shard_map/ppermute | solution.py:455
  84.5 22.5 %copy-start.29 = (bf16[2048]{0:T(1024)(128)(2,1)S(1)}, bf16[2048]{0:T(1024)(128)(2,1)}, u32[]{:S(2)}) copy-start(bf16[2048]{0:T(1024)(128)(2,1)} %param.13) | copy-start | bytes 12292
  97.2 56.6 %collective-permute-start.12 = (bf16[2048,512]{1,0:T(8,128)(2,1)S(1)}, bf16[2048,512]{1,0:T(8,128)(2,1)}, u32[]{:S(2)}, u32[]{:S(2)}) collective-permute-start(bf16[2048,512]{1,0:T(8,128)(2,1)S(1)} %shard_map.140.own_ref), channel_id=1, source_target_pairs={{0,4},{4,0},{8,12},{12,8},{16,20},{20,16},{24,28},{28,24},{32,36},... | collective-permute-start | bytes 6291464 | tf_op jit(solution)/shard_map/ppermute | solution.py:511
  107.9 12.2 %copy-start.5 = (bf16[8,32,1408]{2,1,0:T(8,128)(2,1)S(1)}, bf16[8,32,1408]{2,1,0:T(8,128)(2,1)}, u32[]{:S(2)}) copy-start(bf16[8,32,1408]{2,1,0:T(8,128)(2,1)} %copy-done.3) | copy-start | bytes 2162692
  107.9 12.2 %copy-start.8 = (bf16[8,32,1408]{2,1,0:T(8,128)(2,1)S(1)}, bf16[8,32,1408]{2,1,0:T(8,128)(2,1)}, u32[]{:S(2)}) copy-start(bf16[8,32,1408]{2,1,0:T(8,128)(2,1)} %copy-done.6) | copy-start | bytes 2162692
  107.9 12.2 %copy-start.11 = (bf16[8,32,1408]{2,1,0:T(8,128)(2,1)S(1)}, bf16[8,32,1408]{2,1,0:T(8,128)(2,1)}, u32[]{:S(2)}) copy-start(bf16[8,32,1408]{2,1,0:T(8,128)(2,1)} %copy-done.9) | copy-start | bytes 2162692
  107.9 12.2 %copy-start.14 = (bf16[8,32,1408]{2,1,0:T(8,128)(2,1)S(1)}, bf16[8,32,1408]{2,1,0:T(8,128)(2,1)}, u32[]{:S(2)}) copy-start(bf16[8,32,1408]{2,1,0:T(8,128)(2,1)} %copy-done.12) | copy-start | bytes 2162692
  120.2 3.6 %copy-start.2 = (bf16[8,32,1408]{2,1,0:T(8,128)(2,1)S(1)}, bf16[8,32,1408]{2,1,0:T(8,128)(2,1)}, u32[]{:S(2)}) copy-start(bf16[8,32,1408]{2,1,0:T(8,128)(2,1)} %copy-done) | copy-start | bytes 2162692
  123.8 1.9 copy-start.17
  123.8 1.9 copy-start.20
  125.7 5.0 %copy-start.26 = (f32[31,512]{1,0:T(8,128)S(1)}, f32[31,512]{1,0:T(8,128)}, u32[]{:S(2)}) copy-start(f32[31,512]{1,0:T(8,128)} %taps_ref.1) | copy-start | bytes 190468
  127.4 7.4 %copy-start.24 = (bf16[1024,384]{1,0:T(8,128)(2,1)}, bf16[1024,384]{1,0:T(8,128)(2,1)S(1)}, u32[]{:S(2)}) copy-start(bf16[1024,384]{1,0:T(8,128)(2,1)S(1)} %get-tuple-element.24.qkv_ref) | copy-start | bytes 2359300
  127.4 3.2 %collective-permute-start.10 = (bf16[192,128]{1,0:T(8,128)(2,1)S(1)}, bf16[192,128]{1,0:T(8,128)(2,1)S(1)}, u32[]{:S(2)}, u32[]{:S(2)}) collective-permute-start(bf16[192,128]{1,0:T(8,128)(2,1)S(1)} %get-tuple-element.20), channel_id=1, source_target_pairs={{0,8},{4,12},{8,16},{12,20},{16,24},{20,28},{24,32},{28,36},{32,40... | collective-permute-start | bytes 147464 | tf_op jit(solution)/shard_map/ppermute | solution.py:502
  130.7 8.6 %copy-start.27 = (f32[8]{0:T(128)S(1)}, f32[8]{0:T(128)}, u32[]{:S(2)}) copy-start(f32[8]{0:T(128)} %sinks_ref.1) | copy-start | bytes 100
  134.8 13.3 %all-to-all-start.1 = ((f32[8,2,1024]{2,1,0:T(2,128)}), f32[8,2,1024]{2,1,0:T(2,128)S(1)}, u32[]{:S(2)}, u32[]{:S(2)}) async-start(f32[8,2,1024]{2,1,0:T(2,128)} %get-tuple-element.23), calls=%async_computation.1 | async-start | bytes 131072 | tf_op jit(solution)/shard_map/all_to_all | solution.py:523
  139.2 1.1 copy-start.25
  140.4 7.8 %copy-start.23 = (f32[512]{0:T(512)S(1)}, f32[512]{0:T(512)}, u32[]{:S(2)}) copy-start(f32[512]{0:T(512)} %param.20) | copy-start | bytes 6148
  150.1 3.8 %collective-permute-start.11 = (bf16[512,512]{1,0:T(8,128)(2,1)S(1)}, bf16[512,512]{1,0:T(8,128)(2,1)S(1)}, u32[]{:S(2)}, u32[]{:S(2)}) collective-permute-start(bf16[512,512]{1,0:T(8,128)(2,1)S(1)} %get-tuple-element.28), channel_id=1, source_target_pairs={{0,4},{4,0},{8,12},{12,8},{16,20},{20,16},{24,28},{28,24},{32,36},... | collective-permute-start | bytes 1572872 | tf_op jit(solution)/shard_map/ppermute | solution.py:546
  157.8 19.7 %collective-permute-start.13 = (bf16[128,2048]{1,0:T(8,128)(2,1)}, bf16[128,2048]{1,0:T(8,128)(2,1)}, u32[]{:S(2)}, u32[]{:S(2)}) collective-permute-start(bf16[128,2048]{1,0:T(8,128)(2,1)} %get-tuple-element.30), channel_id=1, source_target_pairs={{0,2},{1,3},{2,0},{3,1},{4,6},{5,7},{6,4},{7,5},{8,10},{9,11},{10,... | collective-permute-start | bytes 1572872 | tf_op jit(solution)/shard_map/ppermute | solution.py:575
  162.5 24.0 %collective-permute-start.14 = (bf16[128,2048]{1,0:T(8,128)(2,1)S(1)}, bf16[128,2048]{1,0:T(8,128)(2,1)}, u32[]{:S(2)}, u32[]{:S(2)}) collective-permute-start(bf16[128,2048]{1,0:T(8,128)(2,1)S(1)} %get-tuple-element.31), channel_id=1, source_target_pairs={{0,1},{1,2},{2,3},{3,0},{4,5},{5,6},{6,7},{7,4},{8,9},{9,10},{10,1... | collective-permute-start | bytes 1572872 | tf_op jit(solution)/shard_map/ppermute | solution.py:575
  168.6 17.9 %collective-permute-start.15 = (bf16[128,2048]{1,0:T(8,128)(2,1)}, bf16[128,2048]{1,0:T(8,128)(2,1)S(1)}, u32[]{:S(2)}, u32[]{:S(2)}) collective-permute-start(bf16[128,2048]{1,0:T(8,128)(2,1)} %get-tuple-element.32), channel_id=1, source_target_pairs={{0,3},{1,0},{2,1},{3,2},{4,7},{5,4},{6,5},{7,6},{8,11},{9,8},{10,9... | collective-permute-start | bytes 1572872 | tf_op jit(solution)/shard_map/ppermute | solution.py:575
  173.0 3.9 %collective-permute-start.16 = (f32[4,512]{1,0:T(4,128)S(1)}, f32[4,512]{1,0:T(4,128)S(1)}, u32[]{:S(2)}, u32[]{:S(2)}) collective-permute-start(f32[4,512]{1,0:T(4,128)S(1)} %get-tuple-element.35), channel_id=1, source_target_pairs={{0,4},{4,0},{8,12},{12,8},{16,20},{20,16},{24,28},{28,24},{32,36},... | collective-permute-start | bytes 24584 | tf_op jit(solution)/shard_map/ppermute | solution.py:550
  (16 other events, 14.8 us)

commit v6 on v5

--- a/solution.py
+++ b/solution.py
@@ -113,9 +113,9 @@
             out_ref[member, to, :] = source[...]
 
 
-def norm_kernel(own_ref, other_ref, gain_ref, out_ref):
+def norm_kernel(x_ref, gain_ref, out_ref):
     core = lax.axis_index("core")
-    count, _ = own_ref.shape
+    count, _ = x_ref.shape
     group = 128 // 4
     tile = 32
     lane = lax.broadcasted_iota(jnp.int32, (tile, 128), 1)
@@ -123,38 +123,36 @@
 
     @pl.loop(0, count // tile)
     def _(step):
-        at = pl.multiple_of(step * tile, tile)
-        for source, to_core in ((own_ref, core), (other_ref, 1 - core)):
-            x = source[pl.ds(at, tile), :].astype(jnp.float32)
-            scale = lax.rsqrt(jnp.mean(x * x, axis=-1, keepdims=True) + NORM_EPS)
-            normed = x * scale * gain
-            rows = pl.ds(pl.multiple_of(to_core * count + at, tile), tile)
-
-            @pl.when(core == 0)
-            def _():
-                out_ref[rows, :] = normed.astype(jnp.bfloat16)
-
-            @pl.when(core == 1)
-            def _():
-                for z in range(0, SIDE, 4):
-                    for y in range(0, SIDE, 4):
-                        tiles = []
-                        for part in range(4):
-                            start = ((z + part) * SIDE + y) * group
-                            tiles.append(normed[:, start : start + 128])
-                        for away in (2, 1):
-                            low = jnp.bitwise_and(lane // group, away) == 0
-                            tiles = [
-                                jnp.where(low, tiles[i], pltpu.roll(tiles[i + away], away * group, 1))
-                                if i & away == 0
-                                else jnp.where(
-                                    low, pltpu.roll(tiles[i - away], 128 - away * group, 1), tiles[i]
-                                )
-                                for i in range(4)
-                            ]
-                        for part in range(4):
-                            to = ((y + part) * SIDE + z) * group
-                            out_ref[rows, to : to + 128] = tiles[part].astype(jnp.bfloat16)
+        rows = pl.ds(pl.multiple_of(step * tile, tile), tile)
+        x = x_ref[rows, :].astype(jnp.float32)
+        scale = lax.rsqrt(jnp.mean(x * x, axis=-1, keepdims=True) + NORM_EPS)
+        normed = x * scale * gain
+
+        @pl.when(core == 0)
+        def _():
+            out_ref[rows, :] = normed.astype(jnp.bfloat16)
+
+        @pl.when(core == 1)
+        def _():
+            for z in range(0, SIDE, 4):
+                for y in range(0, SIDE, 4):
+                    tiles = []
+                    for part in range(4):
+                        start = ((z + part) * SIDE + y) * group
+                        tiles.append(normed[:, start : start + 128])
+                    for away in (2, 1):
+                        low = jnp.bitwise_and(lane // group, away) == 0
+                        tiles = [
+                            jnp.where(low, tiles[i], pltpu.roll(tiles[i + away], away * group, 1))
+                            if i & away == 0
+                            else jnp.where(
+                                low, pltpu.roll(tiles[i - away], 128 - away * group, 1), tiles[i]
+                            )
+                            for i in range(4)
+                        ]
+                    for part in range(4):
+                        to = ((y + part) * SIDE + z) * group
+                        out_ref[rows, to : to + 128] = tiles[part].astype(jnp.bfloat16)
 
 
 def line_of(index):
@@ -184,34 +182,39 @@
             to += piece.shape[1]
 
 
-def rows_of(step):
-    return pl.ds(pl.multiple_of(step * TILE, TILE), TILE)
-
-
-def early_kernel(first, count, x_ref, *refs):
+def row_tiles(own_ref, other_ref, body):
+    core, count = lax.axis_index("core"), own_ref.shape[0]
+    for x_ref, of_core in ((own_ref, core), (other_ref, 1 - core)):
+
+        @pl.loop(0, count // TILE)
+        def _(step):
+            here = pl.multiple_of(step * TILE, TILE)
+            there = pl.multiple_of(of_core * count + step * TILE, TILE)
+            body(x_ref, pl.ds(here, TILE), pl.ds(there, TILE))
+
+
+def early_kernel(first, count, own_ref, other_ref, *refs):
     pieces, before, (out_ref, held_ref) = refs[:count], refs[count:-2], refs[-2:]
     hold(pieces, held_ref)
 
-    @pl.loop(0, x_ref.shape[0] // TILE)
-    def _(step):
-        rows = rows_of(step)
-        total = products(x_ref, rows, pieces, first, held_ref)
+    def body(x_ref, here, rows):
+        total = products(x_ref, here, pieces, first, held_ref)
         for other in before:
             total = total + other[rows, :]
         out_ref[rows, :] = total
 
+    row_tiles(own_ref, other_ref, body)
+
 
 def late_kernel(
-    first, x_ref, cos_ref, sin_ref, before_ref, a_ref, b_ref, glu_ref, qkv_ref, tail_ref, held_ref
+    first, own_ref, other_ref, cos_ref, sin_ref, before_ref, a_ref, b_ref, glu_ref, qkv_ref, tail_ref, held_ref
 ):
     pieces = (a_ref, b_ref)
     hold(pieces, held_ref)
     channels, width = glu_ref.shape[1], qkv_ref.shape[1]
 
-    @pl.loop(0, x_ref.shape[0] // TILE)
-    def _(step):
-        rows = rows_of(step)
-        total = products(x_ref, rows, pieces, first, held_ref) + before_ref[rows, :]
+    def body(x_ref, here, rows):
+        total = products(x_ref, here, pieces, first, held_ref) + before_ref[rows, :]
         raw = total.astype(jnp.bfloat16).astype(jnp.float32)
         value, gate = raw[:, :channels], raw[:, channels : 2 * channels]
         glu_ref[rows, :] = (value * jax.nn.sigmoid(gate)).astype(jnp.bfloat16)
@@ -230,7 +233,8 @@
                 turned = jnp.where(lane < HEAD_DIM, turned, part)
             qkv_ref[rows, at : at + 128] = turned.astype(jnp.bfloat16)
 
-    end = x_ref.shape[0]
+    row_tiles(own_ref, other_ref, body)
+    end = glu_ref.shape[0]
     tail_ref[0:WINDOW, :] = qkv_ref[end - WINDOW : end, width - 128 : width]
     tail_ref[WINDOW : WINDOW + 32, :] = glu_ref[end - 32 : end, :128]
     tail_ref[WINDOW + 32 : WINDOW + 64, :] = glu_ref[end - 32 : end, 128:]
@@ -246,7 +250,7 @@
             out_ref[pl.ds(to, block), :] = piece[step, :, column:]
 
 
-def conv_kernel(before_ref, glu_ref, taps_ref, out_ref, sums_ref, ext_ref):
+def conv_kernel(before_ref, glu_ref, taps_ref, out_ref, sums_ref, ext_ref, pair_ref):
     count, (rows, channels) = taps_ref.shape[0], glu_ref.shape
     first_channel = lax.axis_index("core") * channels
     lead = 32
@@ -259,20 +263,22 @@
     @pl.loop(0, rows // 128)
     def _(step):
         base = pl.multiple_of(step * 128, 128)
-        first = jnp.zeros((128, 128), jnp.float32)
-        second = jnp.zeros((128, 128), jnp.float32)
-        for part in range(2):
-            lanes = pl.ds(part * 128, 128)
-            own = pl.ds(pl.multiple_of(first_channel + part * 128, 128), 128)
-            total = jnp.zeros((128, 128), jnp.float32)
-            for tap in range(count):
-                rows_at = pl.ds(base + (lead - count + 1 + tap), 128)
-                total = total + taps_ref[pl.ds(tap, 1), own] * ext_ref[part, rows_at, :]
-            out_ref[pl.ds(base, 128), lanes] = total
-            first = first + total
-            second = second + total * total
-        first = jnp.sum(first.T, axis=0, keepdims=True)
-        second = jnp.sum(second.T, axis=0, keepdims=True)
+        for half in range(0, 128, 64):
+            first = jnp.zeros((64, 128), jnp.float32)
+            second = jnp.zeros((64, 128), jnp.float32)
+            for part in range(2):
+                own = pl.ds(pl.multiple_of(first_channel + part * 128, 128), 128)
+                total = jnp.zeros((64, 128), jnp.float32)
+                for tap in range(count):
+                    rows_at = pl.ds(base + (half + lead - count + 1 + tap), 64)
+                    total = total + taps_ref[pl.ds(tap, 1), own] * ext_ref[part, rows_at, :]
+                out_ref[pl.ds(base + half, 64), pl.ds(part * 128, 128)] = total
+                first = first + total
+                second = second + total * total
+            pair_ref[0, half : half + 64, :] = first
+            pair_ref[1, half : half + 64, :] = second
+        first = jnp.sum(pair_ref[0].T, axis=0, keepdims=True)
+        second = jnp.sum(pair_ref[1].T, axis=0, keepdims=True)
         for member in range(sums_ref.shape[0]):
             sums_ref[member, pl.ds(0, 1), pl.ds(base, 128)] = first
             sums_ref[member, pl.ds(1, 1), pl.ds(base, 128)] = second
@@ -456,14 +462,13 @@
         pieces += [ahead, behind]
 
     tokens_other = lax.ppermute(tokens, SP, OTHER_CORE)
-    normed = call(
-        norm_kernel,
-        shape((row_count, model)),
-        1 << 30,
-        [VMEM, VMEM, VMEM],
-        (tokens, tokens_other, norm_gain[None]),
-        limit=16,
-    )
+
+    def rms_normed(rows):
+        return call(
+            norm_kernel, shape(rows.shape), 1 << 30, [VMEM, VMEM], (rows, norm_gain[None]), limit=12
+        )
+
+    normed = (rms_normed(tokens), rms_normed(tokens_other))
 
     positions = chip * row_count + jnp.arange(row_count, dtype=jnp.int32)
     half_dim = HEAD_DIM // 2
@@ -482,8 +487,8 @@
             functools.partial(early_kernel, first, len(held)),
             shape((row_count, in_cols), jnp.float32),
             2 * row_count * lines * len(held) * in_cols,
-            [VMEM] * (1 + len(held) + len(before)),
-            (normed, *held, *before),
+            [VMEM] * (2 + len(held) + len(before)),
+            (*normed, *held, *before),
             (pltpu.VMEM((lines * len(held), in_cols), jnp.bfloat16),),
             limit=16,
         )
@@ -494,8 +499,8 @@
         functools.partial(late_kernel, 7),
         (shape((row_count, channels)), shape((row_count, qkv_cols[1])), shape((WINDOW + 64, 128))),
         2 * row_count * lines * in_cols,
-        [VMEM] * 6,
-        (normed, cosines, sines, total, *pieces[7:]),
+        [VMEM] * 7,
+        (*normed, cosines, sines, total, *pieces[7:]),
         (pltpu.VMEM((lines, in_cols), jnp.bfloat16),),
         limit=16,
     )
@@ -517,7 +522,7 @@
         1 << 32,
         [VMEM] * 3,
         (before, glu, conv_taps),
-        (pltpu.VMEM((2, row_count + 32, 128), jnp.float32),),
+        (pltpu.VMEM((2, row_count + 32, 128), jnp.float32), pltpu.VMEM((2, 128, 128), jnp.float32)),
         limit=12,
     )
     everyones = lax.all_to_all(sums, CHIP, 0, 0, tiled=True)
@@ -574,9 +579,8 @@
     def to_member(value, away):
         return lax.ppermute(value, "tp", [(i, (i + away) % peers) for i in range(peers)])
 
-    far, up = output((2, 1))
+    far, up, down, mine = output((2, 1, 3, 0))
     far, up = to_member(far, 2), to_member(up, 1)
-    down, mine = output((3, 0))
     down = to_member(down, 3)
     mixed = (
         mine.astype(jnp.float32)

time: 191 us -> 188 us (0.984)
  local copies, waits for them, and re-layouts: 16 us -> 7.25 us
  waiting for transfers between devices: 30.8 us -> 35.3 us
    unnamed x60 -> x28, local copies, waits for them, and re-layouts: 16 us -> 5.7 us
    ppermute x3, waiting for transfers between devices: 9.04 us -> 12.6 us  [to_member(): lax.ppermute(value, 'tp', [(i, (i + away) % peers) for i in range(peers)])]
  transfers between devices with their start and end apart: 18 -> 18, of which waited for: 10 -> 10; matrix products, arithmetic and copies ran while one was open for 2% -> 3% of each run, Pallas kernels for 19% -> 19%
where the time goes in v6:
time: 188 us; the launch traced here: 186 us
  starting transfers between devices  73.8 us (39%)
  Pallas kernels  44.1 us (23%)
  waiting for transfers between devices  35.3 us (19%)
  blocking collectives  18.9 us (10%)
  local copies, waits for them, and re-layouts  7.25 us (4%)
  other arithmetic  5.58 us (3%)
    pallas_call x12, Pallas kernels, call(): pl.pallas_call(body, out_shape=outs, in_specs=in_specs, out_specs=jax.tre...  44.1 us
    all_to_all x1, blocking collectives, layer(): lax.all_to_all(sent, SP, 0, 0, tiled=True, axis_index_groups=LINES)  18.9 us
    ppermute x4, starting transfers between devices, layer(): behind = lax.ppermute(behind, SP, BEHIND)  17.3 us
    ppermute x4, waiting for transfers between devices, layer(): ahead = lax.ppermute(ahead, SP, AHEAD)  15.4 us
    ppermute x3, waiting for transfers between devices, to_member(): lax.ppermute(value, 'tp', [(i, (i + away) % peers) for i in range(peers)])  12.6 us
    ppermute x3, starting transfers between devices, to_member(): lax.ppermute(value, 'tp', [(i, (i + away) % peers) for i in range(peers)])  11.3 us
    ppermute x4, starting transfers between devices, layer(): ahead = lax.ppermute(ahead, SP, AHEAD)  9.1 us
    ppermute x1, starting transfers between devices, layer(): got = lax.ppermute(given, SP, OTHER_CORE)  8.74 us
  transfers between devices with their start and end apart: 18, of which 10 were waited for; matrix products, arithmetic and copies ran while one was open for 3% of the time, Pallas kernels for 19%

profile of v6, /device:TPU:1, one launch (start us, length us, event | category | flops | bytes accessed | tf_op | source)
XLA Modules:
  0.0 186.1 jit_solution(10949706418450904013)
XLA Ops:
  2.2 8.7 %collective-permute-start.1 = (bf16[16,1408]{1,0:T(8,128)(2,1)}, bf16[16,1408]{1,0:T(8,128)(2,1)S(1)}, u32[]{:S(2)}, u32[]{:S(2)}) collective-permute-start(bf16[16,1408]{1,0:T(8,128)(2,1)} %get-tuple-element.19), channel_id=1, source_target_pairs={{0,4},{4,0},{8,12},{12,8},{16,20},{20,16},{24,28},{28,24},{32,36},... | collective-permute-start | bytes 135176 | tf_op jit(solution)/shard_map/ppermute | solution.py:452
  14.4 18.9 %all_to_all.10.refs_0_ = bf16[8,32,1408]{2,1,0:T(8,128)(2,1)S(1)} all-to-all(bf16[8,32,1408]{2,1,0:T(8,128)(2,1)} %shard_map.134), channel_id=1, replica_groups={{0,8,16,24,32,40,48,56},{64,72,80,88,96,104,112,120},{128,136,144,152,1..., dimensions={0} | all-to-all | bytes 1441792 | tf_op jit(solution)/shard_map/all_to_all | solution.py:454
  33.3 3.2 %collective-permute-start.2 = (bf16[8,32,1408]{2,1,0:T(8,128)(2,1)S(1)}, bf16[8,32,1408]{2,1,0:T(8,128)(2,1)S(1)}, u32[]{:S(2)}, u32[]{:S(2)}) collective-permute-start(bf16[8,32,1408]{2,1,0:T(8,128)(2,1)S(1)} %all_to_all.10.refs_0_), channel_id=1, source_target_pairs={{0,64},{8,72},{16,80},{24,88},{32,96},{40,104},{48,112},{56,120},{... | collective-permute-start | bytes 2162696 | tf_op jit(solution)/shard_map/ppermute | solution.py:460
  36.5 3.8 %collective-permute-start.5 = (bf16[8,32,1408]{2,1,0:T(8,128)(2,1)S(1)}, bf16[8,32,1408]{2,1,0:T(8,128)(2,1)S(1)}, u32[]{:S(2)}, u32[]{:S(2)}) collective-permute-start(bf16[8,32,1408]{2,1,0:T(8,128)(2,1)S(1)} %all_to_all.10.refs_0_), channel_id=1, source_target_pairs={{0,448},{8,456},{16,464},{24,472},{32,480},{40,488},{48,496},{56,5... | collective-permute-start | bytes 2162696 | tf_op jit(solution)/shard_map/ppermute | solution.py:461
  40.3 7.0 %collective-permute-done.2.refs_1_ = bf16[8,32,1408]{2,1,0:T(8,128)(2,1)S(1)} collective-permute-done((bf16[8,32,1408]{2,1,0:T(8,128)(2,1)S(1)}, bf16[8,32,1408]{2,1,0:T(8,128)(2,1)S(1)}, u32[]{:S(2)}, u32[]{:S(2)}) %collective-permute-start.2) | collective-permute-done | bytes 720928 | tf_op jit(solution)/shard_map/ppermute | solution.py:460
  47.4 1.9 %collective-permute-start.3 = (bf16[8,32,1408]{2,1,0:T(8,128)(2,1)S(1)}, bf16[8,32,1408]{2,1,0:T(8,128)(2,1)S(1)}, u32[]{:S(2)}, u32[]{:S(2)}) collective-permute-start(bf16[8,32,1408]{2,1,0:T(8,128)(2,1)S(1)} %collective-permute-done.2.refs_1_), channel_id=1, source_target_pairs={{0,64},{8,72},{16,80},{24,88},{32,96},{40,104},{48,112},{56,120},{... | collective-permute-start | bytes 2162696 | tf_op jit(solution)/shard_map/ppermute | solution.py:460
  49.3 4.6 %collective-permute-start.6 = (bf16[8,32,1408]{2,1,0:T(8,128)(2,1)S(1)}, bf16[8,32,1408]{2,1,0:T(8,128)(2,1)S(1)}, u32[]{:S(2)}, u32[]{:S(2)}) collective-permute-start(bf16[8,32,1408]{2,1,0:T(8,128)(2,1)S(1)} %collective-permute-done.5.refs_2_), channel_id=1, source_target_pairs={{0,448},{8,456},{16,464},{24,472},{32,480},{40,488},{48,496},{56,5... | collective-permute-start | bytes 2162696 | tf_op jit(solution)/shard_map/ppermute | solution.py:461
  54.7 7.3 %collective-permute-start = (bf16[512,2048]{1,0:T(8,128)(2,1)}, bf16[512,2048]{1,0:T(8,128)(2,1)}, u32[]{:S(2)}, u32[]{:S(2)}) collective-permute-start(bf16[512,2048]{1,0:T(8,128)(2,1)} %x_ref.1), channel_id=1, source_target_pairs={{0,4},{4,0},{8,12},{12,8},{16,20},{20,16},{24,28},{28,24},{32,36},... | collective-permute-start | bytes 6291464 | tf_op jit(solution)/shard_map/ppermute | solution.py:464
  62.0 2.1 %collective-permute-start.4 = (bf16[8,32,1408]{2,1,0:T(8,128)(2,1)S(1)}, bf16[8,32,1408]{2,1,0:T(8,128)(2,1)S(1)}, u32[]{:S(2)}, u32[]{:S(2)}) collective-permute-start(bf16[8,32,1408]{2,1,0:T(8,128)(2,1)S(1)} %collective-permute-done.3.refs_3_), channel_id=1, source_target_pairs={{0,64},{8,72},{16,80},{24,88},{32,96},{40,104},{48,112},{56,120},{... | collective-permute-start | bytes 2162696 | tf_op jit(solution)/shard_map/ppermute | solution.py:460
  65.0 4.4 %collective-permute-start.7 = (bf16[8,32,1408]{2,1,0:T(8,128)(2,1)S(1)}, bf16[8,32,1408]{2,1,0:T(8,128)(2,1)S(1)}, u32[]{:S(2)}, u32[]{:S(2)}) collective-permute-start(bf16[8,32,1408]{2,1,0:T(8,128)(2,1)S(1)} %collective-permute-done.6.refs_4_), channel_id=1, source_target_pairs={{0,448},{8,456},{16,464},{24,472},{32,480},{40,488},{48,496},{56,5... | collective-permute-start | bytes 2162696 | tf_op jit(solution)/shard_map/ppermute | solution.py:461
  69.4 6.2 %collective-permute-done.4.refs_0_.refs_5_ = bf16[8,32,1408]{2,1,0:T(8,128)(2,1)S(1)} collective-permute-done((bf16[8,32,1408]{2,1,0:T(8,128)(2,1)S(1)}, bf16[8,32,1408]{2,1,0:T(8,128)(2,1)S(1)}, u32[]{:S(2)}, u32[]{:S(2)}) %collective-permute-start.4) | collective-permute-done | bytes 720928 | tf_op jit(solution)/shard_map/ppermute | solution.py:460
  79.0 4.6 %collective-permute-start.9 = (bf16[4,32,1408]{2,1,0:T(8,128)(2,1)}, bf16[4,32,1408]{2,1,0:T(8,128)(2,1)}, u32[]{:S(2)}, u32[]{:S(2)}) collective-permute-start(bf16[4,32,1408]{2,1,0:T(8,128)(2,1)} %slice.9), channel_id=1, source_target_pairs={{0,448},{8,456},{16,464},{24,472},{32,480},{40,488},{48,496},{56,5... | collective-permute-start | bytes 1081352 | tf_op jit(solution)/shard_map/ppermute | solution.py:461
  83.7 2.3 %collective-permute-done.8.a_ref.refs_7_ = bf16[4,32,1408]{2,1,0:T(8,128)(2,1)S(1)} collective-permute-done((bf16[4,32,1408]{2,1,0:T(8,128)(2,1)}, bf16[4,32,1408]{2,1,0:T(8,128)(2,1)S(1)}, u32[]{:S(2)}, u32[]{:S(2)}) %collective-permute-start.8) | collective-permute-done | bytes 360480 | tf_op jit(solution)/shard_map/ppermute | solution.py:460
  85.9 2.4 %collective-permute-done.9.b_ref.refs_8_ = bf16[4,32,1408]{2,1,0:T(8,128)(2,1)} collective-permute-done((bf16[4,32,1408]{2,1,0:T(8,128)(2,1)}, bf16[4,32,1408]{2,1,0:T(8,128)(2,1)}, u32[]{:S(2)}, u32[]{:S(2)}) %collective-permute-start.9) | collective-permute-done | bytes 360480 | tf_op jit(solution)/shard_map/ppermute | solution.py:461
  91.6 2.5 %shard_map.141.own_ref = bf16[2048,512]{1,0:T(8,128)(2,1)} custom-call(bf16[8,32,1408]{2,1,0:T(8,128)(2,1)S(1)} %all_to_all.10.refs_0_, bf16[8,32,1408]{2,1,0:T(8,128)(2,1)S(1)} %collective-permute-done.2.refs_1_, bf16[8,32,1408]{2,1,0:T(8,128)(2,1)S(1)} %copy-done.1, bf16[8,32,1408]{2,1,0:T(8,128)(2,1)S(1)} %copy-done.4, ...), custom_call_target="tpu_custom_call" | custom-call | flops 268435456 | bytes 1048576 | tf_op jit(solution)/shard_map/pallas_call | solution.py:53
  94.1 8.5 %collective-permute-start.12 = (bf16[2048,512]{1,0:T(8,128)(2,1)}, bf16[2048,512]{1,0:T(8,128)(2,1)}, u32[]{:S(2)}, u32[]{:S(2)}) collective-permute-start(bf16[2048,512]{1,0:T(8,128)(2,1)} %shard_map.141.own_ref), channel_id=1, source_target_pairs={{0,4},{4,0},{8,12},{12,8},{16,20},{20,16},{24,28},{28,24},{32,36},... | collective-permute-start | bytes 6291464 | tf_op jit(solution)/shard_map/ppermute | solution.py:516
  104.5 6.5 %shard_map.131.own_ref = bf16[512,2048]{1,0:T(8,128)(2,1)S(1)} custom-call(bf16[512,2048]{1,0:T(8,128)(2,1)} %x_ref.1, bf16[1,2048]{1,0:T(2,128)(2,1)S(1)} %broadcast_in_dim.4.gain_ref), custom_call_target="tpu_custom_call" | custom-call | flops 1073741824 | bytes 1048576 | tf_op jit(solution)/shard_map/pallas_call | solution.py:53
  112.0 6.7 %shard_map.132.other_ref = bf16[512,2048]{1,0:T(8,128)(2,1)S(1)} custom-call(bf16[512,2048]{1,0:T(8,128)(2,1)} %collective-permute-done.x_ref, bf16[1,2048]{1,0:T(2,128)(2,1)S(1)} %broadcast_in_dim.4.gain_ref), custom_call_target="tpu_custom_call" | custom-call | flops 1073741824 | bytes 1048576 | tf_op jit(solution)/shard_map/pallas_call | solution.py:53
  118.7 3.6 %shard_map.135.refs_2_ = f32[1024,896]{1,0:T(8,128)S(1)} custom-call(bf16[512,2048]{1,0:T(8,128)(2,1)S(1)} %shard_map.131.own_ref, bf16[512,2048]{1,0:T(8,128)(2,1)S(1)} %shard_map.132.other_ref, bf16[8,32,1408]{2,1,0:T(8,128)(2,1)S(1)} %all_to_all.10.refs_0_, bf16[8,32,1408]{2,1,0:T(8,128)(2,1)S(1)} %collective-permute-done.2.refs_1_, ...), custom_call_target="tpu_custom_call" | custom-call | flops 2348810240 | bytes 1048576 | tf_op jit(solution)/shard_map/pallas_call | solution.py:53
  124.1 2.8 %shard_map.137 = (bf16[1024,256]{1,0:T(8,128)(2,1)S(1)}, bf16[1024,384]{1,0:T(8,128)(2,1)S(1)}, bf16[192,128]{1,0:T(8,128)(2,1)S(1)}) custom-call(bf16[512,2048]{1,0:T(8,128)(2,1)S(1)} %shard_map.131.own_ref, bf16[512,2048]{1,0:T(8,128)(2,1)S(1)} %shard_map.132.other_ref, f32[1024,128]{1,0:T(8,128)S(1)} %get-tuple-element.39.cos_ref, ...), custom_call_target="tpu_custom_call" | custom-call | flops 469762048 | bytes 1048576 | tf_op jit(solution)/shard_map/pallas_call | solution.py:53
  126.9 2.1 %collective-permute-start.10 = (bf16[192,128]{1,0:T(8,128)(2,1)S(1)}, bf16[192,128]{1,0:T(8,128)(2,1)S(1)}, u32[]{:S(2)}, u32[]{:S(2)}) collective-permute-start(bf16[192,128]{1,0:T(8,128)(2,1)S(1)} %get-tuple-element.20), channel_id=1, source_target_pairs={{0,8},{4,12},{8,16},{12,20},{16,24},{20,28},{24,32},{28,36},{32,40... | collective-permute-start | bytes 147464 | tf_op jit(solution)/shard_map/ppermute | solution.py:507
  130.1 4.1 %shard_map.138 = (f32[1024,256]{1,0:T(8,128)S(1)}, f32[8,2,1024]{2,1,0:T(2,128)}) custom-call(bf16[192,128]{1,0:T(8,128)(2,1)S(1)} %collective-permute-done.10.before_ref, bf16[1024,256]{1,0:T(8,128)(2,1)S(1)} %get-tuple-element.21.glu_ref, f32[31,512]{1,0:T(8,128)S(1)} %copy-done.10), custom_call_target="tpu_custom_call" | custom-call | flops 4294967296 | bytes 1048576 | tf_op jit(solution)/shard_map/pallas_call | solution.py:53
  134.2 4.4 %all-to-all-start.1 = ((f32[8,2,1024]{2,1,0:T(2,128)}), f32[8,2,1024]{2,1,0:T(2,128)S(1)}, u32[]{:S(2)}, u32[]{:S(2)}) async-start(f32[8,2,1024]{2,1,0:T(2,128)} %get-tuple-element.23), calls=%async_computation.1 | async-start | bytes 131072 | tf_op jit(solution)/shard_map/all_to_all | solution.py:528
  138.7 7.1 %shard_map.139 = (bf16[512,256]{1,0:T(8,128)(2,1)S(1)}, bf16[512,256]{1,0:T(8,128)(2,1)S(1)}, f32[4,1024]{1,0:T(4,128)S(1)}) custom-call(f32[8]{0:T(128)S(1)} %copy-done.11, bf16[1024,384]{1,0:T(8,128)(2,1)S(1)} %get-tuple-element.24.qkv_ref, bf16[192,128]{1,0:T(8,128)(2,1)S(1)} %collective-permute-done.10.before_ref), custom_call_target="tpu_custom_call" | custom-call | flops 4294967296 | bytes 1048576 | tf_op jit(solution)/shard_map/pallas_call | solution.py:53
  146.7 1.9 %collective-permute-start.11 = (bf16[512,512]{1,0:T(8,128)(2,1)S(1)}, bf16[512,512]{1,0:T(8,128)(2,1)S(1)}, u32[]{:S(2)}, u32[]{:S(2)}) collective-permute-start(bf16[512,512]{1,0:T(8,128)(2,1)S(1)} %get-tuple-element.28), channel_id=1, source_target_pairs={{0,4},{4,0},{8,12},{12,8},{16,20},{20,16},{24,28},{28,24},{32,36},... | collective-permute-start | bytes 1572872 | tf_op jit(solution)/shard_map/ppermute | solution.py:551
  150.5 4.9 %shard_map.142 = (bf16[128,2048]{1,0:T(8,128)(2,1)S(1)}, bf16[128,2048]{1,0:T(8,128)(2,1)S(1)}, bf16[128,2048]{1,0:T(8,128)(2,1)S(1)}, bf16[128,2048]{1,0:T(8,128)(2,1)S(1)}) custom-call(bf16[512,256]{1,0:T(8,128)(2,1)S(1)} %get-tuple-element.26.conv_ref, bf16[512,256]{1,0:T(8,128)(2,1)S(1)} %get-tuple-element.27.attn_ref, ...), custom_call_target="tpu_custom_call" | custom-call | flops 2147483648 | bytes 1048576 | tf_op jit(solution)/shard_map/pallas_call | solution.py:53
  155.4 4.8 %collective-permute-start.13 = (bf16[128,2048]{1,0:T(8,128)(2,1)S(1)}, bf16[128,2048]{1,0:T(8,128)(2,1)S(1)}, u32[]{:S(2)}, u32[]{:S(2)}) collective-permute-start(bf16[128,2048]{1,0:T(8,128)(2,1)S(1)} %get-tuple-element.30), channel_id=1, source_target_pairs={{0,2},{1,3},{2,0},{3,1},{4,6},{5,7},{6,4},{7,5},{8,10},{9,11},{10,... | collective-permute-start | bytes 1572872 | tf_op jit(solution)/shard_map/ppermute | solution.py:580
  160.2 2.2 %collective-permute-start.14 = (bf16[128,2048]{1,0:T(8,128)(2,1)S(1)}, bf16[128,2048]{1,0:T(8,128)(2,1)S(1)}, u32[]{:S(2)}, u32[]{:S(2)}) collective-permute-start(bf16[128,2048]{1,0:T(8,128)(2,1)S(1)} %get-tuple-element.31), channel_id=1, source_target_pairs={{0,1},{1,2},{2,3},{3,0},{4,5},{5,6},{6,7},{7,4},{8,9},{9,10},{10,1... | collective-permute-start | bytes 1572872 | tf_op jit(solution)/shard_map/ppermute | solution.py:580
  162.4 4.3 %collective-permute-start.15 = (bf16[128,2048]{1,0:T(8,128)(2,1)S(1)}, bf16[128,2048]{1,0:T(8,128)(2,1)}, u32[]{:S(2)}, u32[]{:S(2)}) collective-permute-start(bf16[128,2048]{1,0:T(8,128)(2,1)S(1)} %get-tuple-element.32), channel_id=1, source_target_pairs={{0,3},{1,0},{2,1},{3,2},{4,7},{5,4},{6,5},{7,6},{8,11},{9,8},{10,9... | collective-permute-start | bytes 1572872 | tf_op jit(solution)/shard_map/ppermute | solution.py:580
  166.7 3.1 %collective-permute-start.16 = (f32[4,512]{1,0:T(4,128)S(1)}, f32[4,512]{1,0:T(4,128)S(1)}, u32[]{:S(2)}, u32[]{:S(2)}) collective-permute-start(f32[4,512]{1,0:T(4,128)S(1)} %get-tuple-element.35), channel_id=1, source_target_pairs={{0,4},{4,0},{8,12},{12,8},{16,20},{20,16},{24,28},{28,24},{32,36},... | collective-permute-start | bytes 24584 | tf_op jit(solution)/shard_map/ppermute | solution.py:555
  172.2 11.7 %collective-permute-done.14 = bf16[128,2048]{1,0:T(8,128)(2,1)S(1)} collective-permute-done((bf16[128,2048]{1,0:T(8,128)(2,1)S(1)}, bf16[128,2048]{1,0:T(8,128)(2,1)S(1)}, u32[]{:S(2)}, u32[]{:S(2)}) %collective-permute-start.14) | collective-permute-done | bytes 524320 | tf_op jit(solution)/shard_map/ppermute | solution.py:580
  183.9 2.2 %add_convert_fusion = bf16[128,2048]{1,0:T(8,128)(2,1)} fusion(bf16[128,2048]{1,0:T(8,128)(2,1)} %collective-permute-done.15, bf16[128,2048]{1,0:T(8,128)(2,1)S(1)} %collective-permute-done.14, bf16[128,2048]{1,0:T(8,128)(2,1)S(1)} %collective-permute-done.13, bf16[128,2048]{1,0:T(8,128)(2,1)S(1)} %get-tuple-element.29), kind=kLoop, calls=%fused_computation | loop fusion | flops 2097152 | bytes 2621440 | tf_op jit(solution)/shard_map/convert_element_type | solution.py:591
  (55 shorter events, 24.5 us)
Async XLA Ops:
  2.2 9.8 %collective-permute-start.1 = (bf16[16,1408]{1,0:T(8,128)(2,1)}, bf16[16,1408]{1,0:T(8,128)(2,1)S(1)}, u32[]{:S(2)}, u32[]{:S(2)}) collective-permute-start(bf16[16,1408]{1,0:T(8,128)(2,1)} %get-tuple-element.19), channel_id=1, source_target_pairs={{0,4},{4,0},{8,12},{12,8},{16,20},{20,16},{24,28},{28,24},{32,36},... | collective-permute-start | bytes 135176 | tf_op jit(solution)/shard_map/ppermute | solution.py:452
  12.0 0.6 copy-start.12
  33.3 14.1 %collective-permute-start.2 = (bf16[8,32,1408]{2,1,0:T(8,128)(2,1)S(1)}, bf16[8,32,1408]{2,1,0:T(8,128)(2,1)S(1)}, u32[]{:S(2)}, u32[]{:S(2)}) collective-permute-start(bf16[8,32,1408]{2,1,0:T(8,128)(2,1)S(1)} %all_to_all.10.refs_0_), channel_id=1, source_target_pairs={{0,64},{8,72},{16,80},{24,88},{32,96},{40,104},{48,112},{56,120},{... | collective-permute-start | bytes 2162696 | tf_op jit(solution)/shard_map/ppermute | solution.py:460
  36.5 12.8 %collective-permute-start.5 = (bf16[8,32,1408]{2,1,0:T(8,128)(2,1)S(1)}, bf16[8,32,1408]{2,1,0:T(8,128)(2,1)S(1)}, u32[]{:S(2)}, u32[]{:S(2)}) collective-permute-start(bf16[8,32,1408]{2,1,0:T(8,128)(2,1)S(1)} %all_to_all.10.refs_0_), channel_id=1, source_target_pairs={{0,448},{8,456},{16,464},{24,472},{32,480},{40,488},{48,496},{56,5... | collective-permute-start | bytes 2162696 | tf_op jit(solution)/shard_map/ppermute | solution.py:461
  47.4 14.6 %collective-permute-start.3 = (bf16[8,32,1408]{2,1,0:T(8,128)(2,1)S(1)}, bf16[8,32,1408]{2,1,0:T(8,128)(2,1)S(1)}, u32[]{:S(2)}, u32[]{:S(2)}) collective-permute-start(bf16[8,32,1408]{2,1,0:T(8,128)(2,1)S(1)} %collective-permute-done.2.refs_1_), channel_id=1, source_target_pairs={{0,64},{8,72},{16,80},{24,88},{32,96},{40,104},{48,112},{56,120},{... | collective-permute-start | bytes 2162696 | tf_op jit(solution)/shard_map/ppermute | solution.py:460
  49.3 15.7 %collective-permute-start.6 = (bf16[8,32,1408]{2,1,0:T(8,128)(2,1)S(1)}, bf16[8,32,1408]{2,1,0:T(8,128)(2,1)S(1)}, u32[]{:S(2)}, u32[]{:S(2)}) collective-permute-start(bf16[8,32,1408]{2,1,0:T(8,128)(2,1)S(1)} %collective-permute-done.5.refs_2_), channel_id=1, source_target_pairs={{0,448},{8,456},{16,464},{24,472},{32,480},{40,488},{48,496},{56,5... | collective-permute-start | bytes 2162696 | tf_op jit(solution)/shard_map/ppermute | solution.py:461
  53.9 0.9 copy-start
  54.7 57.2 %collective-permute-start = (bf16[512,2048]{1,0:T(8,128)(2,1)}, bf16[512,2048]{1,0:T(8,128)(2,1)}, u32[]{:S(2)}, u32[]{:S(2)}) collective-permute-start(bf16[512,2048]{1,0:T(8,128)(2,1)} %x_ref.1), channel_id=1, source_target_pairs={{0,4},{4,0},{8,12},{12,8},{16,20},{20,16},{24,28},{28,24},{32,36},... | collective-permute-start | bytes 6291464 | tf_op jit(solution)/shard_map/ppermute | solution.py:464
  62.0 13.5 %collective-permute-start.4 = (bf16[8,32,1408]{2,1,0:T(8,128)(2,1)S(1)}, bf16[8,32,1408]{2,1,0:T(8,128)(2,1)S(1)}, u32[]{:S(2)}, u32[]{:S(2)}) collective-permute-start(bf16[8,32,1408]{2,1,0:T(8,128)(2,1)S(1)} %collective-permute-done.3.refs_3_), channel_id=1, source_target_pairs={{0,64},{8,72},{16,80},{24,88},{32,96},{40,104},{48,112},{56,120},{... | collective-permute-start | bytes 2162696 | tf_op jit(solution)/shard_map/ppermute | solution.py:460
  64.1 0.9 copy-start.3
  65.0 13.2 %copy-start.6 = (bf16[8,32,1408]{2,1,0:T(8,128)(2,1)}, bf16[8,32,1408]{2,1,0:T(8,128)(2,1)S(1)}, u32[]{:S(2)}) copy-start(bf16[8,32,1408]{2,1,0:T(8,128)(2,1)S(1)} %collective-permute-done.6.refs_4_) | copy-start | bytes 2162692
  65.0 13.2 %collective-permute-start.7 = (bf16[8,32,1408]{2,1,0:T(8,128)(2,1)S(1)}, bf16[8,32,1408]{2,1,0:T(8,128)(2,1)S(1)}, u32[]{:S(2)}, u32[]{:S(2)}) collective-permute-start(bf16[8,32,1408]{2,1,0:T(8,128)(2,1)S(1)} %collective-permute-done.6.refs_4_), channel_id=1, source_target_pairs={{0,448},{8,456},{16,464},{24,472},{32,480},{40,488},{48,496},{56,5... | collective-permute-start | bytes 2162696 | tf_op jit(solution)/shard_map/ppermute | solution.py:461
  76.3 9.6 %collective-permute-start.8 = (bf16[4,32,1408]{2,1,0:T(8,128)(2,1)}, bf16[4,32,1408]{2,1,0:T(8,128)(2,1)S(1)}, u32[]{:S(2)}, u32[]{:S(2)}) collective-permute-start(bf16[4,32,1408]{2,1,0:T(8,128)(2,1)} %slice.8), channel_id=1, source_target_pairs={{0,64},{8,72},{16,80},{24,88},{32,96},{40,104},{48,112},{56,120},{... | collective-permute-start | bytes 1081352 | tf_op jit(solution)/shard_map/ppermute | solution.py:460
  79.0 9.2 %collective-permute-start.9 = (bf16[4,32,1408]{2,1,0:T(8,128)(2,1)}, bf16[4,32,1408]{2,1,0:T(8,128)(2,1)}, u32[]{:S(2)}, u32[]{:S(2)}) collective-permute-start(bf16[4,32,1408]{2,1,0:T(8,128)(2,1)} %slice.9), channel_id=1, source_target_pairs={{0,448},{8,456},{16,464},{24,472},{32,480},{40,488},{48,496},{56,5... | collective-permute-start | bytes 1081352 | tf_op jit(solution)/shard_map/ppermute | solution.py:461
  83.6 20.9 %copy-start.13 = (bf16[2048]{0:T(1024)(128)(2,1)S(1)}, bf16[2048]{0:T(1024)(128)(2,1)}, u32[]{:S(2)}) copy-start(bf16[2048]{0:T(1024)(128)(2,1)} %param.13) | copy-start | bytes 12292
  88.3 1.1 copy-start.1
  89.4 1.1 copy-start.4
  90.5 1.1 copy-start.7
  94.1 56.4 %collective-permute-start.12 = (bf16[2048,512]{1,0:T(8,128)(2,1)}, bf16[2048,512]{1,0:T(8,128)(2,1)}, u32[]{:S(2)}, u32[]{:S(2)}) collective-permute-start(bf16[2048,512]{1,0:T(8,128)(2,1)} %shard_map.141.own_ref), channel_id=1, source_target_pairs={{0,4},{4,0},{8,12},{12,8},{16,20},{20,16},{24,28},{28,24},{32,36},... | collective-permute-start | bytes 6291464 | tf_op jit(solution)/shard_map/ppermute | solution.py:516
  111.9 6.7 %copy-start.2 = (bf16[8,32,1408]{2,1,0:T(8,128)(2,1)S(1)}, bf16[8,32,1408]{2,1,0:T(8,128)(2,1)}, u32[]{:S(2)}) copy-start(bf16[8,32,1408]{2,1,0:T(8,128)(2,1)} %copy-done) | copy-start | bytes 2162692
  111.9 6.7 %copy-start.5 = (bf16[8,32,1408]{2,1,0:T(8,128)(2,1)S(1)}, bf16[8,32,1408]{2,1,0:T(8,128)(2,1)}, u32[]{:S(2)}) copy-start(bf16[8,32,1408]{2,1,0:T(8,128)(2,1)} %copy-done.3) | copy-start | bytes 2162692
  111.9 6.7 %copy-start.8 = (bf16[8,32,1408]{2,1,0:T(8,128)(2,1)S(1)}, bf16[8,32,1408]{2,1,0:T(8,128)(2,1)}, u32[]{:S(2)}) copy-start(bf16[8,32,1408]{2,1,0:T(8,128)(2,1)} %copy-done.6) | copy-start | bytes 2162692
  124.1 6.0 %copy-start.10 = (f32[31,512]{1,0:T(8,128)S(1)}, f32[31,512]{1,0:T(8,128)}, u32[]{:S(2)}) copy-start(f32[31,512]{1,0:T(8,128)} %taps_ref.1) | copy-start | bytes 190468
  126.9 3.3 %collective-permute-start.10 = (bf16[192,128]{1,0:T(8,128)(2,1)S(1)}, bf16[192,128]{1,0:T(8,128)(2,1)S(1)}, u32[]{:S(2)}, u32[]{:S(2)}) collective-permute-start(bf16[192,128]{1,0:T(8,128)(2,1)S(1)} %get-tuple-element.20), channel_id=1, source_target_pairs={{0,8},{4,12},{8,16},{12,20},{16,24},{20,28},{24,32},{28,36},{32,40... | collective-permute-start | bytes 147464 | tf_op jit(solution)/shard_map/ppermute | solution.py:507
  130.1 8.5 %copy-start.11 = (f32[8]{0:T(128)S(1)}, f32[8]{0:T(128)}, u32[]{:S(2)}) copy-start(f32[8]{0:T(128)} %sinks_ref.1) | copy-start | bytes 100
  134.2 11.5 %all-to-all-start.1 = ((f32[8,2,1024]{2,1,0:T(2,128)}), f32[8,2,1024]{2,1,0:T(2,128)S(1)}, u32[]{:S(2)}, u32[]{:S(2)}) async-start(f32[8,2,1024]{2,1,0:T(2,128)} %get-tuple-element.23), calls=%async_computation.1 | async-start | bytes 131072 | tf_op jit(solution)/shard_map/all_to_all | solution.py:528
  138.6 7.1 %copy-start.9 = (f32[512]{0:T(512)S(1)}, f32[512]{0:T(512)}, u32[]{:S(2)}) copy-start(f32[512]{0:T(512)} %param.20) | copy-start | bytes 6148
  146.7 3.8 %collective-permute-start.11 = (bf16[512,512]{1,0:T(8,128)(2,1)S(1)}, bf16[512,512]{1,0:T(8,128)(2,1)S(1)}, u32[]{:S(2)}, u32[]{:S(2)}) collective-permute-start(bf16[512,512]{1,0:T(8,128)(2,1)S(1)} %get-tuple-element.28), channel_id=1, source_target_pairs={{0,4},{4,0},{8,12},{12,8},{16,20},{20,16},{24,28},{28,24},{32,36},... | collective-permute-start | bytes 1572872 | tf_op jit(solution)/shard_map/ppermute | solution.py:551
  155.4 16.8 %collective-permute-start.13 = (bf16[128,2048]{1,0:T(8,128)(2,1)S(1)}, bf16[128,2048]{1,0:T(8,128)(2,1)S(1)}, u32[]{:S(2)}, u32[]{:S(2)}) collective-permute-start(bf16[128,2048]{1,0:T(8,128)(2,1)S(1)} %get-tuple-element.30), channel_id=1, source_target_pairs={{0,2},{1,3},{2,0},{3,1},{4,6},{5,7},{6,4},{7,5},{8,10},{9,11},{10,... | collective-permute-start | bytes 1572872 | tf_op jit(solution)/shard_map/ppermute | solution.py:580
  160.2 23.7 %collective-permute-start.14 = (bf16[128,2048]{1,0:T(8,128)(2,1)S(1)}, bf16[128,2048]{1,0:T(8,128)(2,1)S(1)}, u32[]{:S(2)}, u32[]{:S(2)}) collective-permute-start(bf16[128,2048]{1,0:T(8,128)(2,1)S(1)} %get-tuple-element.31), channel_id=1, source_target_pairs={{0,1},{1,2},{2,3},{3,0},{4,5},{5,6},{6,7},{7,4},{8,9},{9,10},{10,1... | collective-permute-start | bytes 1572872 | tf_op jit(solution)/shard_map/ppermute | solution.py:580
  162.4 21.5 %collective-permute-start.15 = (bf16[128,2048]{1,0:T(8,128)(2,1)S(1)}, bf16[128,2048]{1,0:T(8,128)(2,1)}, u32[]{:S(2)}, u32[]{:S(2)}) collective-permute-start(bf16[128,2048]{1,0:T(8,128)(2,1)S(1)} %get-tuple-element.32), channel_id=1, source_target_pairs={{0,3},{1,0},{2,1},{3,2},{4,7},{5,4},{6,5},{7,6},{8,11},{9,8},{10,9... | collective-permute-start | bytes 1572872 | tf_op jit(solution)/shard_map/ppermute | solution.py:580
  166.7 3.9 %collective-permute-start.16 = (f32[4,512]{1,0:T(4,128)S(1)}, f32[4,512]{1,0:T(4,128)S(1)}, u32[]{:S(2)}, u32[]{:S(2)}) collective-permute-start(f32[4,512]{1,0:T(4,128)S(1)} %get-tuple-element.35), channel_id=1, source_target_pairs={{0,4},{4,0},{8,12},{12,8},{16,20},{20,16},{24,28},{28,24},{32,36},... | collective-permute-start | bytes 24584 | tf_op jit(solution)/shard_map/ppermute | solution.py:555

commit v7 on v6

--- a/solution.py
+++ b/solution.py
@@ -336,8 +336,10 @@
     def _(block):
         base = pl.multiple_of(block * WINDOW, WINDOW)
         window = pl.ds(base, 2 * WINDOW)
-        key_at = lax.broadcasted_iota(jnp.int32, (2 * WINDOW, WINDOW), 0)
-        query_at = lax.broadcasted_iota(jnp.int32, (2 * WINDOW, WINDOW), 1)
+        query_at = lax.broadcasted_iota(jnp.int32, (WINDOW, 2 * WINDOW), 0)
+        key_at = lax.broadcasted_iota(jnp.int32, (WINDOW, 2 * WINDOW), 1)
+        head_at = lax.broadcasted_iota(jnp.int32, (WINDOW, 128), 1)
+        logs = jnp.zeros((WINDOW, 128), jnp.float32)
         lowest = jnp.where((chip == 0) & (block == 0), WINDOW, 0)
         allowed = (key_at > query_at) & (key_at <= query_at + WINDOW) & (key_at >= lowest)
         outs = []
@@ -347,25 +349,23 @@
             for which, (keys, values) in enumerate(((k_lo, v_lo), (k_hi, v_hi))):
                 head = 2 * pair + which
                 scores = lax.dot_general(
+                    query,
                     keys[window, :],
-                    query,
                     (((1,), (1,)), ((), ())),
                     preferred_element_type=jnp.float32,
                 )
                 scores = jnp.where(allowed, scores, -jnp.inf)
-                sums = jnp.sum(jnp.exp(scores), axis=0, keepdims=True)
-                sink = jnp.full((1, WINDOW), sinks_ref[core * heads + head], jnp.float32)
+                sums = jnp.sum(jnp.exp(scores), axis=1, keepdims=True)
+                sink = jnp.full((WINDOW, 1), sinks_ref[core * heads + head], jnp.float32)
                 log_total = jnp.log(sums + jnp.exp(sink))
-                logs_ref[pl.ds(head, 1), pl.ds(base, WINDOW)] = log_total
+                logs = jnp.where(head_at == head, log_total, logs)
                 weights = jnp.exp(scores - log_total).astype(jnp.bfloat16)
-                total = total + lax.dot_general(
-                    weights,
-                    values[window, :],
-                    (((0,), (0,)), ((), ())),
-                    preferred_element_type=jnp.float32,
+                total = total + jnp.dot(
+                    weights, values[window, :], preferred_element_type=jnp.float32
                 )
             outs.append(total.astype(jnp.bfloat16))
         out = jnp.concatenate(outs, axis=1)
+        logs_ref[:, pl.ds(base, WINDOW)] = logs.T[:heads]
         own = block // half_blocks == core
         to = pl.ds(pl.multiple_of((block % half_blocks) * WINDOW, WINDOW), WINDOW)
 
@@ -538,7 +538,6 @@
         [SMEM, VMEM, VMEM],
         (sinks, qkv, before),
         (extended,) * 4,
-        limit=12,
     )
     conv_kept, given = call(
         scaled_kernel,

time: 188 us -> 191 us (1.016)
  local copies, waits for them, and re-layouts: 7.25 us -> 9.17 us
    unnamed x28 -> x36, local copies, waits for them, and re-layouts: 5.7 us -> 7.64 us
  transfers between devices with their start and end apart: 18 -> 18, of which waited for: 10 -> 10; matrix products, arithmetic and copies ran while one was open for 3% -> 3% of each run, Pallas kernels for 19% -> 20%
where the time goes in v7:
time: 191 us; the launch traced here: 189 us
  starting transfers between devices  73.8 us (39%)
  Pallas kernels  45.1 us (24%)
  waiting for transfers between devices  35.3 us (18%)
  blocking collectives  18.9 us (10%)
  local copies, waits for them, and re-layouts  9.17 us (5%)
  other arithmetic  5.58 us (3%)
    pallas_call x12, Pallas kernels, call(): pl.pallas_call(body, out_shape=outs, in_specs=in_specs, out_specs=jax.tre...  45.1 us
    all_to_all x1, blocking collectives, layer(): lax.all_to_all(sent, SP, 0, 0, tiled=True, axis_index_groups=LINES)  18.9 us
    ppermute x4, starting transfers between devices, layer(): behind = lax.ppermute(behind, SP, BEHIND)  17.3 us
    ppermute x4, waiting for transfers between devices, layer(): ahead = lax.ppermute(ahead, SP, AHEAD)  15.4 us
    ppermute x3, waiting for transfers between devices, to_member(): lax.ppermute(value, 'tp', [(i, (i + away) % peers) for i in range(peers)])  12.6 us
    ppermute x3, starting transfers between devices, to_member(): lax.ppermute(value, 'tp', [(i, (i + away) % peers) for i in range(peers)])  11.3 us
    ppermute x4, starting transfers between devices, layer(): ahead = lax.ppermute(ahead, SP, AHEAD)  9.1 us
    ppermute x1, starting transfers between devices, layer(): got = lax.ppermute(given, SP, OTHER_CORE)  8.74 us
  transfers between devices with their start and end apart: 18, of which 10 were waited for; matrix products, arithmetic and copies ran while one was open for 3% of the time, Pallas kernels for 20%

profile of v7, /device:TPU:1, one launch (start us, length us, event | category | flops | bytes accessed | tf_op | source)
XLA Modules:
  0.0 189.0 jit_solution(9649341154066528395)
XLA Ops:
  2.2 8.7 %collective-permute-start.1 = (bf16[16,1408]{1,0:T(8,128)(2,1)}, bf16[16,1408]{1,0:T(8,128)(2,1)S(1)}, u32[]{:S(2)}, u32[]{:S(2)}) collective-permute-start(bf16[16,1408]{1,0:T(8,128)(2,1)} %get-tuple-element.19), channel_id=1, source_target_pairs={{0,4},{4,0},{8,12},{12,8},{16,20},{20,16},{24,28},{28,24},{32,36},... | collective-permute-start | bytes 135176 | tf_op jit(solution)/shard_map/ppermute | solution.py:452
  14.4 18.9 %all_to_all.10.refs_0_ = bf16[8,32,1408]{2,1,0:T(8,128)(2,1)S(1)} all-to-all(bf16[8,32,1408]{2,1,0:T(8,128)(2,1)} %shard_map.134), channel_id=1, replica_groups={{0,8,16,24,32,40,48,56},{64,72,80,88,96,104,112,120},{128,136,144,152,1..., dimensions={0} | all-to-all | bytes 1441792 | tf_op jit(solution)/shard_map/all_to_all | solution.py:454
  33.3 3.2 %collective-permute-start.2 = (bf16[8,32,1408]{2,1,0:T(8,128)(2,1)S(1)}, bf16[8,32,1408]{2,1,0:T(8,128)(2,1)S(1)}, u32[]{:S(2)}, u32[]{:S(2)}) collective-permute-start(bf16[8,32,1408]{2,1,0:T(8,128)(2,1)S(1)} %all_to_all.10.refs_0_), channel_id=1, source_target_pairs={{0,64},{8,72},{16,80},{24,88},{32,96},{40,104},{48,112},{56,120},{... | collective-permute-start | bytes 2162696 | tf_op jit(solution)/shard_map/ppermute | solution.py:460
  36.5 3.8 %collective-permute-start.5 = (bf16[8,32,1408]{2,1,0:T(8,128)(2,1)S(1)}, bf16[8,32,1408]{2,1,0:T(8,128)(2,1)S(1)}, u32[]{:S(2)}, u32[]{:S(2)}) collective-permute-start(bf16[8,32,1408]{2,1,0:T(8,128)(2,1)S(1)} %all_to_all.10.refs_0_), channel_id=1, source_target_pairs={{0,448},{8,456},{16,464},{24,472},{32,480},{40,488},{48,496},{56,5... | collective-permute-start | bytes 2162696 | tf_op jit(solution)/shard_map/ppermute | solution.py:461
  40.4 7.0 %collective-permute-done.2.refs_1_ = bf16[8,32,1408]{2,1,0:T(8,128)(2,1)S(1)} collective-permute-done((bf16[8,32,1408]{2,1,0:T(8,128)(2,1)S(1)}, bf16[8,32,1408]{2,1,0:T(8,128)(2,1)S(1)}, u32[]{:S(2)}, u32[]{:S(2)}) %collective-permute-start.2) | collective-permute-done | bytes 720928 | tf_op jit(solution)/shard_map/ppermute | solution.py:460
  47.4 1.9 %collective-permute-start.3 = (bf16[8,32,1408]{2,1,0:T(8,128)(2,1)S(1)}, bf16[8,32,1408]{2,1,0:T(8,128)(2,1)S(1)}, u32[]{:S(2)}, u32[]{:S(2)}) collective-permute-start(bf16[8,32,1408]{2,1,0:T(8,128)(2,1)S(1)} %collective-permute-done.2.refs_1_), channel_id=1, source_target_pairs={{0,64},{8,72},{16,80},{24,88},{32,96},{40,104},{48,112},{56,120},{... | collective-permute-start | bytes 2162696 | tf_op jit(solution)/shard_map/ppermute | solution.py:460
  49.3 4.6 %collective-permute-start.6 = (bf16[8,32,1408]{2,1,0:T(8,128)(2,1)S(1)}, bf16[8,32,1408]{2,1,0:T(8,128)(2,1)S(1)}, u32[]{:S(2)}, u32[]{:S(2)}) collective-permute-start(bf16[8,32,1408]{2,1,0:T(8,128)(2,1)S(1)} %collective-permute-done.5.refs_2_), channel_id=1, source_target_pairs={{0,448},{8,456},{16,464},{24,472},{32,480},{40,488},{48,496},{56,5... | collective-permute-start | bytes 2162696 | tf_op jit(solution)/shard_map/ppermute | solution.py:461
  54.8 7.3 %collective-permute-start = (bf16[512,2048]{1,0:T(8,128)(2,1)}, bf16[512,2048]{1,0:T(8,128)(2,1)}, u32[]{:S(2)}, u32[]{:S(2)}) collective-permute-start(bf16[512,2048]{1,0:T(8,128)(2,1)} %x_ref.1), channel_id=1, source_target_pairs={{0,4},{4,0},{8,12},{12,8},{16,20},{20,16},{24,28},{28,24},{32,36},... | collective-permute-start | bytes 6291464 | tf_op jit(solution)/shard_map/ppermute | solution.py:464
  62.0 2.1 %collective-permute-start.4 = (bf16[8,32,1408]{2,1,0:T(8,128)(2,1)S(1)}, bf16[8,32,1408]{2,1,0:T(8,128)(2,1)S(1)}, u32[]{:S(2)}, u32[]{:S(2)}) collective-permute-start(bf16[8,32,1408]{2,1,0:T(8,128)(2,1)S(1)} %collective-permute-done.3.refs_3_), channel_id=1, source_target_pairs={{0,64},{8,72},{16,80},{24,88},{32,96},{40,104},{48,112},{56,120},{... | collective-permute-start | bytes 2162696 | tf_op jit(solution)/shard_map/ppermute | solution.py:460
  65.1 4.4 %collective-permute-start.7 = (bf16[8,32,1408]{2,1,0:T(8,128)(2,1)S(1)}, bf16[8,32,1408]{2,1,0:T(8,128)(2,1)S(1)}, u32[]{:S(2)}, u32[]{:S(2)}) collective-permute-start(bf16[8,32,1408]{2,1,0:T(8,128)(2,1)S(1)} %collective-permute-done.6.refs_4_), channel_id=1, source_target_pairs={{0,448},{8,456},{16,464},{24,472},{32,480},{40,488},{48,496},{56,5... | collective-permute-start | bytes 2162696 | tf_op jit(solution)/shard_map/ppermute | solution.py:461
  69.5 6.1 %collective-permute-done.4.refs_0_.refs_5_ = bf16[8,32,1408]{2,1,0:T(8,128)(2,1)S(1)} collective-permute-done((bf16[8,32,1408]{2,1,0:T(8,128)(2,1)S(1)}, bf16[8,32,1408]{2,1,0:T(8,128)(2,1)S(1)}, u32[]{:S(2)}, u32[]{:S(2)}) %collective-permute-start.4) | collective-permute-done | bytes 720928 | tf_op jit(solution)/shard_map/ppermute | solution.py:460
  79.0 4.6 %collective-permute-start.9 = (bf16[4,32,1408]{2,1,0:T(8,128)(2,1)}, bf16[4,32,1408]{2,1,0:T(8,128)(2,1)}, u32[]{:S(2)}, u32[]{:S(2)}) collective-permute-start(bf16[4,32,1408]{2,1,0:T(8,128)(2,1)} %slice.9), channel_id=1, source_target_pairs={{0,448},{8,456},{16,464},{24,472},{32,480},{40,488},{48,496},{56,5... | collective-permute-start | bytes 1081352 | tf_op jit(solution)/shard_map/ppermute | solution.py:461
  83.6 2.3 %collective-permute-done.8.a_ref.refs_7_ = bf16[4,32,1408]{2,1,0:T(8,128)(2,1)S(1)} collective-permute-done((bf16[4,32,1408]{2,1,0:T(8,128)(2,1)}, bf16[4,32,1408]{2,1,0:T(8,128)(2,1)S(1)}, u32[]{:S(2)}, u32[]{:S(2)}) %collective-permute-start.8) | collective-permute-done | bytes 360480 | tf_op jit(solution)/shard_map/ppermute | solution.py:460
  85.9 2.3 %collective-permute-done.9.b_ref.refs_8_ = bf16[4,32,1408]{2,1,0:T(8,128)(2,1)} collective-permute-done((bf16[4,32,1408]{2,1,0:T(8,128)(2,1)}, bf16[4,32,1408]{2,1,0:T(8,128)(2,1)}, u32[]{:S(2)}, u32[]{:S(2)}) %collective-permute-start.9) | collective-permute-done | bytes 360480 | tf_op jit(solution)/shard_map/ppermute | solution.py:461
  91.6 2.5 %shard_map.141.own_ref = bf16[2048,512]{1,0:T(8,128)(2,1)} custom-call(bf16[8,32,1408]{2,1,0:T(8,128)(2,1)S(1)} %all_to_all.10.refs_0_, bf16[8,32,1408]{2,1,0:T(8,128)(2,1)S(1)} %collective-permute-done.2.refs_1_, bf16[8,32,1408]{2,1,0:T(8,128)(2,1)S(1)} %copy-done.1, bf16[8,32,1408]{2,1,0:T(8,128)(2,1)S(1)} %copy-done.4, ...), custom_call_target="tpu_custom_call" | custom-call | flops 268435456 | bytes 1048576 | tf_op jit(solution)/shard_map/pallas_call | solution.py:53
  94.1 8.5 %collective-permute-start.12 = (bf16[2048,512]{1,0:T(8,128)(2,1)}, bf16[2048,512]{1,0:T(8,128)(2,1)}, u32[]{:S(2)}, u32[]{:S(2)}) collective-permute-start(bf16[2048,512]{1,0:T(8,128)(2,1)} %shard_map.141.own_ref), channel_id=1, source_target_pairs={{0,4},{4,0},{8,12},{12,8},{16,20},{20,16},{24,28},{28,24},{32,36},... | collective-permute-start | bytes 6291464 | tf_op jit(solution)/shard_map/ppermute | solution.py:516
  104.6 6.5 %shard_map.131.own_ref = bf16[512,2048]{1,0:T(8,128)(2,1)S(1)} custom-call(bf16[512,2048]{1,0:T(8,128)(2,1)} %x_ref.1, bf16[1,2048]{1,0:T(2,128)(2,1)S(1)} %broadcast_in_dim.4.gain_ref), custom_call_target="tpu_custom_call" | custom-call | flops 1073741824 | bytes 1048576 | tf_op jit(solution)/shard_map/pallas_call | solution.py:53
  112.0 6.7 %shard_map.132.other_ref = bf16[512,2048]{1,0:T(8,128)(2,1)S(1)} custom-call(bf16[512,2048]{1,0:T(8,128)(2,1)} %collective-permute-done.x_ref, bf16[1,2048]{1,0:T(2,128)(2,1)S(1)} %broadcast_in_dim.4.gain_ref), custom_call_target="tpu_custom_call" | custom-call | flops 1073741824 | bytes 1048576 | tf_op jit(solution)/shard_map/pallas_call | solution.py:53
  118.7 3.6 %shard_map.135.refs_2_ = f32[1024,896]{1,0:T(8,128)S(1)} custom-call(bf16[512,2048]{1,0:T(8,128)(2,1)S(1)} %shard_map.131.own_ref, bf16[512,2048]{1,0:T(8,128)(2,1)S(1)} %shard_map.132.other_ref, bf16[8,32,1408]{2,1,0:T(8,128)(2,1)S(1)} %all_to_all.10.refs_0_, bf16[8,32,1408]{2,1,0:T(8,128)(2,1)S(1)} %collective-permute-done.2.refs_1_, ...), custom_call_target="tpu_custom_call" | custom-call | flops 2348810240 | bytes 1048576 | tf_op jit(solution)/shard_map/pallas_call | solution.py:53
  124.1 2.8 %shard_map.137 = (bf16[1024,256]{1,0:T(8,128)(2,1)S(1)}, bf16[1024,384]{1,0:T(8,128)(2,1)S(1)}, bf16[192,128]{1,0:T(8,128)(2,1)S(1)}) custom-call(bf16[512,2048]{1,0:T(8,128)(2,1)S(1)} %shard_map.131.own_ref, bf16[512,2048]{1,0:T(8,128)(2,1)S(1)} %shard_map.132.other_ref, f32[1024,128]{1,0:T(8,128)S(1)} %get-tuple-element.39.cos_ref, ...), custom_call_target="tpu_custom_call" | custom-call | flops 469762048 | bytes 1048576 | tf_op jit(solution)/shard_map/pallas_call | solution.py:53
  126.9 2.1 %collective-permute-start.10 = (bf16[192,128]{1,0:T(8,128)(2,1)S(1)}, bf16[192,128]{1,0:T(8,128)(2,1)S(1)}, u32[]{:S(2)}, u32[]{:S(2)}) collective-permute-start(bf16[192,128]{1,0:T(8,128)(2,1)S(1)} %get-tuple-element.20), channel_id=1, source_target_pairs={{0,8},{4,12},{8,16},{12,20},{16,24},{20,28},{24,32},{28,36},{32,40... | collective-permute-start | bytes 147464 | tf_op jit(solution)/shard_map/ppermute | solution.py:507
  130.2 4.1 %shard_map.138 = (f32[1024,256]{1,0:T(8,128)S(1)}, f32[8,2,1024]{2,1,0:T(2,128)}) custom-call(bf16[192,128]{1,0:T(8,128)(2,1)S(1)} %collective-permute-done.10.before_ref, bf16[1024,256]{1,0:T(8,128)(2,1)S(1)} %get-tuple-element.21.glu_ref, f32[31,512]{1,0:T(8,128)S(1)} %copy-done.12), custom_call_target="tpu_custom_call" | custom-call | flops 4294967296 | bytes 1048576 | tf_op jit(solution)/shard_map/pallas_call | solution.py:53
  134.3 4.4 %all-to-all-start.1 = ((f32[8,2,1024]{2,1,0:T(2,128)}), f32[8,2,1024]{2,1,0:T(2,128)S(1)}, u32[]{:S(2)}, u32[]{:S(2)}) async-start(f32[8,2,1024]{2,1,0:T(2,128)} %get-tuple-element.23), calls=%async_computation.1 | async-start | bytes 131072 | tf_op jit(solution)/shard_map/all_to_all | solution.py:528
  138.7 8.0 %shard_map.139 = (bf16[512,256]{1,0:T(8,128)(2,1)}, bf16[512,256]{1,0:T(8,128)(2,1)}, f32[4,1024]{1,0:T(4,128)}) custom-call(f32[8]{0:T(128)} %sinks_ref.1, bf16[1024,384]{1,0:T(8,128)(2,1)} %copy-done.11, bf16[192,128]{1,0:T(8,128)(2,1)} %copy-done.13), custom_call_target="tpu_custom_call" | custom-call | flops 4294967296 | bytes 1048576 | tf_op jit(solution)/shard_map/pallas_call | solution.py:53
  148.6 1.9 %collective-permute-start.11 = (bf16[512,512]{1,0:T(8,128)(2,1)S(1)}, bf16[512,512]{1,0:T(8,128)(2,1)S(1)}, u32[]{:S(2)}, u32[]{:S(2)}) collective-permute-start(bf16[512,512]{1,0:T(8,128)(2,1)S(1)} %get-tuple-element.28), channel_id=1, source_target_pairs={{0,4},{4,0},{8,12},{12,8},{16,20},{20,16},{24,28},{28,24},{32,36},... | collective-permute-start | bytes 1572872 | tf_op jit(solution)/shard_map/ppermute | solution.py:550
  153.4 4.9 %shard_map.142 = (bf16[128,2048]{1,0:T(8,128)(2,1)S(1)}, bf16[128,2048]{1,0:T(8,128)(2,1)S(1)}, bf16[128,2048]{1,0:T(8,128)(2,1)S(1)}, bf16[128,2048]{1,0:T(8,128)(2,1)S(1)}) custom-call(bf16[512,256]{1,0:T(8,128)(2,1)S(1)} %get-tuple-element.26.conv_ref, bf16[512,256]{1,0:T(8,128)(2,1)S(1)} %copy-done.14, ...), custom_call_target="tpu_custom_call" | custom-call | flops 2147483648 | bytes 1048576 | tf_op jit(solution)/shard_map/pallas_call | solution.py:53
  158.3 4.8 %collective-permute-start.13 = (bf16[128,2048]{1,0:T(8,128)(2,1)S(1)}, bf16[128,2048]{1,0:T(8,128)(2,1)S(1)}, u32[]{:S(2)}, u32[]{:S(2)}) collective-permute-start(bf16[128,2048]{1,0:T(8,128)(2,1)S(1)} %get-tuple-element.30), channel_id=1, source_target_pairs={{0,2},{1,3},{2,0},{3,1},{4,6},{5,7},{6,4},{7,5},{8,10},{9,11},{10,... | collective-permute-start | bytes 1572872 | tf_op jit(solution)/shard_map/ppermute | solution.py:579
  163.1 2.2 %collective-permute-start.14 = (bf16[128,2048]{1,0:T(8,128)(2,1)S(1)}, bf16[128,2048]{1,0:T(8,128)(2,1)S(1)}, u32[]{:S(2)}, u32[]{:S(2)}) collective-permute-start(bf16[128,2048]{1,0:T(8,128)(2,1)S(1)} %get-tuple-element.31), channel_id=1, source_target_pairs={{0,1},{1,2},{2,3},{3,0},{4,5},{5,6},{6,7},{7,4},{8,9},{9,10},{10,1... | collective-permute-start | bytes 1572872 | tf_op jit(solution)/shard_map/ppermute | solution.py:579
  165.3 4.3 %collective-permute-start.15 = (bf16[128,2048]{1,0:T(8,128)(2,1)S(1)}, bf16[128,2048]{1,0:T(8,128)(2,1)}, u32[]{:S(2)}, u32[]{:S(2)}) collective-permute-start(bf16[128,2048]{1,0:T(8,128)(2,1)S(1)} %get-tuple-element.32), channel_id=1, source_target_pairs={{0,3},{1,0},{2,1},{3,2},{4,7},{5,4},{6,5},{7,6},{8,11},{9,8},{10,9... | collective-permute-start | bytes 1572872 | tf_op jit(solution)/shard_map/ppermute | solution.py:579
  169.7 3.1 %collective-permute-start.16 = (f32[4,512]{1,0:T(4,128)S(1)}, f32[4,512]{1,0:T(4,128)S(1)}, u32[]{:S(2)}, u32[]{:S(2)}) collective-permute-start(f32[4,512]{1,0:T(4,128)S(1)} %get-tuple-element.35), channel_id=1, source_target_pairs={{0,4},{4,0},{8,12},{12,8},{16,20},{20,16},{24,28},{28,24},{32,36},... | collective-permute-start | bytes 24584 | tf_op jit(solution)/shard_map/ppermute | solution.py:554
  175.1 11.7 %collective-permute-done.14 = bf16[128,2048]{1,0:T(8,128)(2,1)S(1)} collective-permute-done((bf16[128,2048]{1,0:T(8,128)(2,1)S(1)}, bf16[128,2048]{1,0:T(8,128)(2,1)S(1)}, u32[]{:S(2)}, u32[]{:S(2)}) %collective-permute-start.14) | collective-permute-done | bytes 524320 | tf_op jit(solution)/shard_map/ppermute | solution.py:579
  186.8 2.2 %add_convert_fusion = bf16[128,2048]{1,0:T(8,128)(2,1)} fusion(bf16[128,2048]{1,0:T(8,128)(2,1)} %collective-permute-done.15, bf16[128,2048]{1,0:T(8,128)(2,1)S(1)} %collective-permute-done.14, bf16[128,2048]{1,0:T(8,128)(2,1)S(1)} %collective-permute-done.13, bf16[128,2048]{1,0:T(8,128)(2,1)S(1)} %get-tuple-element.29), kind=kLoop, calls=%fused_computation | loop fusion | flops 2097152 | bytes 2621440 | tf_op jit(solution)/shard_map/convert_element_type | solution.py:590
  (63 shorter events, 26.4 us)
Async XLA Ops:
  2.2 9.8 %collective-permute-start.1 = (bf16[16,1408]{1,0:T(8,128)(2,1)}, bf16[16,1408]{1,0:T(8,128)(2,1)S(1)}, u32[]{:S(2)}, u32[]{:S(2)}) collective-permute-start(bf16[16,1408]{1,0:T(8,128)(2,1)} %get-tuple-element.19), channel_id=1, source_target_pairs={{0,4},{4,0},{8,12},{12,8},{16,20},{20,16},{24,28},{28,24},{32,36},... | collective-permute-start | bytes 135176 | tf_op jit(solution)/shard_map/ppermute | solution.py:452
  33.3 14.1 %collective-permute-start.2 = (bf16[8,32,1408]{2,1,0:T(8,128)(2,1)S(1)}, bf16[8,32,1408]{2,1,0:T(8,128)(2,1)S(1)}, u32[]{:S(2)}, u32[]{:S(2)}) collective-permute-start(bf16[8,32,1408]{2,1,0:T(8,128)(2,1)S(1)} %all_to_all.10.refs_0_), channel_id=1, source_target_pairs={{0,64},{8,72},{16,80},{24,88},{32,96},{40,104},{48,112},{56,120},{... | collective-permute-start | bytes 2162696 | tf_op jit(solution)/shard_map/ppermute | solution.py:460
  36.5 12.8 %collective-permute-start.5 = (bf16[8,32,1408]{2,1,0:T(8,128)(2,1)S(1)}, bf16[8,32,1408]{2,1,0:T(8,128)(2,1)S(1)}, u32[]{:S(2)}, u32[]{:S(2)}) collective-permute-start(bf16[8,32,1408]{2,1,0:T(8,128)(2,1)S(1)} %all_to_all.10.refs_0_), channel_id=1, source_target_pairs={{0,448},{8,456},{16,464},{24,472},{32,480},{40,488},{48,496},{56,5... | collective-permute-start | bytes 2162696 | tf_op jit(solution)/shard_map/ppermute | solution.py:461
  47.4 14.6 %collective-permute-start.3 = (bf16[8,32,1408]{2,1,0:T(8,128)(2,1)S(1)}, bf16[8,32,1408]{2,1,0:T(8,128)(2,1)S(1)}, u32[]{:S(2)}, u32[]{:S(2)}) collective-permute-start(bf16[8,32,1408]{2,1,0:T(8,128)(2,1)S(1)} %collective-permute-done.2.refs_1_), channel_id=1, source_target_pairs={{0,64},{8,72},{16,80},{24,88},{32,96},{40,104},{48,112},{56,120},{... | collective-permute-start | bytes 2162696 | tf_op jit(solution)/shard_map/ppermute | solution.py:460
  49.3 15.7 %collective-permute-start.6 = (bf16[8,32,1408]{2,1,0:T(8,128)(2,1)S(1)}, bf16[8,32,1408]{2,1,0:T(8,128)(2,1)S(1)}, u32[]{:S(2)}, u32[]{:S(2)}) collective-permute-start(bf16[8,32,1408]{2,1,0:T(8,128)(2,1)S(1)} %collective-permute-done.5.refs_2_), channel_id=1, source_target_pairs={{0,448},{8,456},{16,464},{24,472},{32,480},{40,488},{48,496},{56,5... | collective-permute-start | bytes 2162696 | tf_op jit(solution)/shard_map/ppermute | solution.py:461
  54.8 57.2 %collective-permute-start = (bf16[512,2048]{1,0:T(8,128)(2,1)}, bf16[512,2048]{1,0:T(8,128)(2,1)}, u32[]{:S(2)}, u32[]{:S(2)}) collective-permute-start(bf16[512,2048]{1,0:T(8,128)(2,1)} %x_ref.1), channel_id=1, source_target_pairs={{0,4},{4,0},{8,12},{12,8},{16,20},{20,16},{24,28},{28,24},{32,36},... | collective-permute-start | bytes 6291464 | tf_op jit(solution)/shard_map/ppermute | solution.py:464
  62.0 13.5 %collective-permute-start.4 = (bf16[8,32,1408]{2,1,0:T(8,128)(2,1)S(1)}, bf16[8,32,1408]{2,1,0:T(8,128)(2,1)S(1)}, u32[]{:S(2)}, u32[]{:S(2)}) collective-permute-start(bf16[8,32,1408]{2,1,0:T(8,128)(2,1)S(1)} %collective-permute-done.3.refs_3_), channel_id=1, source_target_pairs={{0,64},{8,72},{16,80},{24,88},{32,96},{40,104},{48,112},{56,120},{... | collective-permute-start | bytes 2162696 | tf_op jit(solution)/shard_map/ppermute | solution.py:460
  65.1 13.2 %copy-start.6 = (bf16[8,32,1408]{2,1,0:T(8,128)(2,1)}, bf16[8,32,1408]{2,1,0:T(8,128)(2,1)S(1)}, u32[]{:S(2)}) copy-start(bf16[8,32,1408]{2,1,0:T(8,128)(2,1)S(1)} %collective-permute-done.6.refs_4_) | copy-start | bytes 2162692
  65.1 13.2 %collective-permute-start.7 = (bf16[8,32,1408]{2,1,0:T(8,128)(2,1)S(1)}, bf16[8,32,1408]{2,1,0:T(8,128)(2,1)S(1)}, u32[]{:S(2)}, u32[]{:S(2)}) collective-permute-start(bf16[8,32,1408]{2,1,0:T(8,128)(2,1)S(1)} %collective-permute-done.6.refs_4_), channel_id=1, source_target_pairs={{0,448},{8,456},{16,464},{24,472},{32,480},{40,488},{48,496},{56,5... | collective-permute-start | bytes 2162696 | tf_op jit(solution)/shard_map/ppermute | solution.py:461
  76.3 9.6 %collective-permute-start.8 = (bf16[4,32,1408]{2,1,0:T(8,128)(2,1)}, bf16[4,32,1408]{2,1,0:T(8,128)(2,1)S(1)}, u32[]{:S(2)}, u32[]{:S(2)}) collective-permute-start(bf16[4,32,1408]{2,1,0:T(8,128)(2,1)} %slice.8), channel_id=1, source_target_pairs={{0,64},{8,72},{16,80},{24,88},{32,96},{40,104},{48,112},{56,120},{... | collective-permute-start | bytes 1081352 | tf_op jit(solution)/shard_map/ppermute | solution.py:460
  79.0 9.2 %collective-permute-start.9 = (bf16[4,32,1408]{2,1,0:T(8,128)(2,1)}, bf16[4,32,1408]{2,1,0:T(8,128)(2,1)}, u32[]{:S(2)}, u32[]{:S(2)}) collective-permute-start(bf16[4,32,1408]{2,1,0:T(8,128)(2,1)} %slice.9), channel_id=1, source_target_pairs={{0,448},{8,456},{16,464},{24,472},{32,480},{40,488},{48,496},{56,5... | collective-permute-start | bytes 1081352 | tf_op jit(solution)/shard_map/ppermute | solution.py:461
  83.6 20.9 %copy-start.17 = (bf16[2048]{0:T(1024)(128)(2,1)S(1)}, bf16[2048]{0:T(1024)(128)(2,1)}, u32[]{:S(2)}) copy-start(bf16[2048]{0:T(1024)(128)(2,1)} %param.13) | copy-start | bytes 12292
  88.3 1.1 copy-start.1
  89.4 1.1 copy-start.4
  90.5 1.1 copy-start.7
  94.1 58.4 %collective-permute-start.12 = (bf16[2048,512]{1,0:T(8,128)(2,1)}, bf16[2048,512]{1,0:T(8,128)(2,1)}, u32[]{:S(2)}, u32[]{:S(2)}) collective-permute-start(bf16[2048,512]{1,0:T(8,128)(2,1)} %shard_map.141.own_ref), channel_id=1, source_target_pairs={{0,4},{4,0},{8,12},{12,8},{16,20},{20,16},{24,28},{28,24},{32,36},... | collective-permute-start | bytes 6291464 | tf_op jit(solution)/shard_map/ppermute | solution.py:516
  112.0 6.7 %copy-start.2 = (bf16[8,32,1408]{2,1,0:T(8,128)(2,1)S(1)}, bf16[8,32,1408]{2,1,0:T(8,128)(2,1)}, u32[]{:S(2)}) copy-start(bf16[8,32,1408]{2,1,0:T(8,128)(2,1)} %copy-done) | copy-start | bytes 2162692
  112.0 6.7 %copy-start.5 = (bf16[8,32,1408]{2,1,0:T(8,128)(2,1)S(1)}, bf16[8,32,1408]{2,1,0:T(8,128)(2,1)}, u32[]{:S(2)}) copy-start(bf16[8,32,1408]{2,1,0:T(8,128)(2,1)} %copy-done.3) | copy-start | bytes 2162692
  112.0 6.7 %copy-start.8 = (bf16[8,32,1408]{2,1,0:T(8,128)(2,1)S(1)}, bf16[8,32,1408]{2,1,0:T(8,128)(2,1)}, u32[]{:S(2)}) copy-start(bf16[8,32,1408]{2,1,0:T(8,128)(2,1)} %copy-done.6) | copy-start | bytes 2162692
  124.1 6.0 %copy-start.12 = (f32[31,512]{1,0:T(8,128)S(1)}, f32[31,512]{1,0:T(8,128)}, u32[]{:S(2)}) copy-start(f32[31,512]{1,0:T(8,128)} %taps_ref.1) | copy-start | bytes 190468
  126.9 7.4 %copy-start.11 = (bf16[1024,384]{1,0:T(8,128)(2,1)}, bf16[1024,384]{1,0:T(8,128)(2,1)S(1)}, u32[]{:S(2)}) copy-start(bf16[1024,384]{1,0:T(8,128)(2,1)S(1)} %get-tuple-element.24.qkv_ref) | copy-start | bytes 2359300
  126.9 3.3 %collective-permute-start.10 = (bf16[192,128]{1,0:T(8,128)(2,1)S(1)}, bf16[192,128]{1,0:T(8,128)(2,1)S(1)}, u32[]{:S(2)}, u32[]{:S(2)}) collective-permute-start(bf16[192,128]{1,0:T(8,128)(2,1)S(1)} %get-tuple-element.20), channel_id=1, source_target_pairs={{0,8},{4,12},{8,16},{12,20},{16,24},{20,28},{24,32},{28,36},{32,40... | collective-permute-start | bytes 147464 | tf_op jit(solution)/shard_map/ppermute | solution.py:507
  130.2 4.1 %copy-start.13 = (bf16[192,128]{1,0:T(8,128)(2,1)}, bf16[192,128]{1,0:T(8,128)(2,1)S(1)}, u32[]{:S(2)}) copy-start(bf16[192,128]{1,0:T(8,128)(2,1)S(1)} %collective-permute-done.10.before_ref) | copy-start | bytes 147460
  134.3 12.4 %all-to-all-start.1 = ((f32[8,2,1024]{2,1,0:T(2,128)}), f32[8,2,1024]{2,1,0:T(2,128)S(1)}, u32[]{:S(2)}, u32[]{:S(2)}) async-start(f32[8,2,1024]{2,1,0:T(2,128)} %get-tuple-element.23), calls=%async_computation.1 | async-start | bytes 131072 | tf_op jit(solution)/shard_map/all_to_all | solution.py:528
  138.7 8.0 %copy-start.10 = (f32[512]{0:T(512)S(1)}, f32[512]{0:T(512)}, u32[]{:S(2)}) copy-start(f32[512]{0:T(512)} %param.20) | copy-start | bytes 6148
  148.6 3.8 %collective-permute-start.11 = (bf16[512,512]{1,0:T(8,128)(2,1)S(1)}, bf16[512,512]{1,0:T(8,128)(2,1)S(1)}, u32[]{:S(2)}, u32[]{:S(2)}) collective-permute-start(bf16[512,512]{1,0:T(8,128)(2,1)S(1)} %get-tuple-element.28), channel_id=1, source_target_pairs={{0,4},{4,0},{8,12},{12,8},{16,20},{20,16},{24,28},{28,24},{32,36},... | collective-permute-start | bytes 1572872 | tf_op jit(solution)/shard_map/ppermute | solution.py:550
  152.4 1.0 copy-start.14
  153.4 16.2 %copy-start.16 = (f32[4,1024]{1,0:T(4,128)S(1)}, f32[4,1024]{1,0:T(4,128)}, u32[]{:S(2)}) copy-start(f32[4,1024]{1,0:T(4,128)} %get-tuple-element.33) | copy-start | bytes 49156
  158.3 16.8 %collective-permute-start.13 = (bf16[128,2048]{1,0:T(8,128)(2,1)S(1)}, bf16[128,2048]{1,0:T(8,128)(2,1)S(1)}, u32[]{:S(2)}, u32[]{:S(2)}) collective-permute-start(bf16[128,2048]{1,0:T(8,128)(2,1)S(1)} %get-tuple-element.30), channel_id=1, source_target_pairs={{0,2},{1,3},{2,0},{3,1},{4,6},{5,7},{6,4},{7,5},{8,10},{9,11},{10,... | collective-permute-start | bytes 1572872 | tf_op jit(solution)/shard_map/ppermute | solution.py:579
  163.1 23.7 %collective-permute-start.14 = (bf16[128,2048]{1,0:T(8,128)(2,1)S(1)}, bf16[128,2048]{1,0:T(8,128)(2,1)S(1)}, u32[]{:S(2)}, u32[]{:S(2)}) collective-permute-start(bf16[128,2048]{1,0:T(8,128)(2,1)S(1)} %get-tuple-element.31), channel_id=1, source_target_pairs={{0,1},{1,2},{2,3},{3,0},{4,5},{5,6},{6,7},{7,4},{8,9},{9,10},{10,1... | collective-permute-start | bytes 1572872 | tf_op jit(solution)/shard_map/ppermute | solution.py:579
  165.3 21.5 %collective-permute-start.15 = (bf16[128,2048]{1,0:T(8,128)(2,1)S(1)}, bf16[128,2048]{1,0:T(8,128)(2,1)}, u32[]{:S(2)}, u32[]{:S(2)}) collective-permute-start(bf16[128,2048]{1,0:T(8,128)(2,1)S(1)} %get-tuple-element.32), channel_id=1, source_target_pairs={{0,3},{1,0},{2,1},{3,2},{4,7},{5,4},{6,5},{7,6},{8,11},{9,8},{10,9... | collective-permute-start | bytes 1572872 | tf_op jit(solution)/shard_map/ppermute | solution.py:579
  169.7 3.9 %collective-permute-start.16 = (f32[4,512]{1,0:T(4,128)S(1)}, f32[4,512]{1,0:T(4,128)S(1)}, u32[]{:S(2)}, u32[]{:S(2)}) collective-permute-start(f32[4,512]{1,0:T(4,128)S(1)} %get-tuple-element.35), channel_id=1, source_target_pairs={{0,4},{4,0},{8,12},{12,8},{16,20},{20,16},{24,28},{28,24},{32,36},... | collective-permute-start | bytes 24584 | tf_op jit(solution)/shard_map/ppermute | solution.py:554
  (4 other events, 3.3 us)

commit v8 on v7

--- a/solution.py
+++ b/solution.py
@@ -314,9 +314,7 @@
             given_ref[to, :channels] = out
 
 
-def attention_kernel(
-    sinks_ref, qkv_ref, before_ref, kept_ref, given_ref, logs_ref, k_lo, k_hi, v_lo, v_hi
-):
+def attention_kernel(sinks_ref, qkv_ref, before_ref, kept_ref, given_ref, logs_ref, keys, values):
     core, chip = lax.axis_index("core"), lax.axis_index("chip")
     cols = kept_ref.shape[1]
     for source, to, count in ((before_ref, 0, WINDOW), (qkv_ref, WINDOW, qkv_ref.shape[0])):
@@ -324,10 +322,8 @@
         low = lax.broadcasted_iota(jnp.int32, both.shape, 1) < HEAD_DIM
         turned = pltpu.roll(both, HEAD_DIM, 1)
         rows = slice(to, to + both.shape[0])
-        k_lo[rows, :] = jnp.where(low, both, 0.0).astype(jnp.bfloat16)
-        k_hi[rows, :] = jnp.where(low, 0.0, turned).astype(jnp.bfloat16)
-        v_lo[rows, :] = jnp.where(low, turned, 0.0).astype(jnp.bfloat16)
-        v_hi[rows, :] = jnp.where(low, 0.0, both).astype(jnp.bfloat16)
+        keys[rows, :] = jnp.where(low, both, turned).astype(jnp.bfloat16)
+        values[rows, :] = jnp.where(low, turned, both).astype(jnp.bfloat16)
     blocks = qkv_ref.shape[0] // WINDOW
     half_blocks = blocks // CORES
     heads = cols // HEAD_DIM
@@ -338,32 +334,40 @@
         window = pl.ds(base, 2 * WINDOW)
         query_at = lax.broadcasted_iota(jnp.int32, (WINDOW, 2 * WINDOW), 0)
         key_at = lax.broadcasted_iota(jnp.int32, (WINDOW, 2 * WINDOW), 1)
-        head_at = lax.broadcasted_iota(jnp.int32, (WINDOW, 128), 1)
+        lane = lax.broadcasted_iota(jnp.int32, (WINDOW, 128), 1)
+        low = lane < HEAD_DIM
         logs = jnp.zeros((WINDOW, 128), jnp.float32)
         lowest = jnp.where((chip == 0) & (block == 0), WINDOW, 0)
         allowed = (key_at > query_at) & (key_at <= query_at + WINDOW) & (key_at >= lowest)
-        outs = []
-        for pair in range(heads // 2):
-            query = qkv_ref[pl.ds(base, WINDOW), pair * 128 : (pair + 1) * 128] * HEAD_DIM ** (-0.5)
-            total = jnp.zeros((WINDOW, 128), jnp.float32)
-            for which, (keys, values) in enumerate(((k_lo, v_lo), (k_hi, v_hi))):
-                head = 2 * pair + which
-                scores = lax.dot_general(
-                    query,
-                    keys[window, :],
-                    (((1,), (1,)), ((), ())),
-                    preferred_element_type=jnp.float32,
-                )
-                scores = jnp.where(allowed, scores, -jnp.inf)
-                sums = jnp.sum(jnp.exp(scores), axis=1, keepdims=True)
-                sink = jnp.full((WINDOW, 1), sinks_ref[core * heads + head], jnp.float32)
-                log_total = jnp.log(sums + jnp.exp(sink))
-                logs = jnp.where(head_at == head, log_total, logs)
-                weights = jnp.exp(scores - log_total).astype(jnp.bfloat16)
-                total = total + jnp.dot(
-                    weights, values[window, :], preferred_element_type=jnp.float32
-                )
-            outs.append(total.astype(jnp.bfloat16))
+        queries = []
+        for head in range(heads):
+            pair = head // 2 * 128
+            query = qkv_ref[pl.ds(base, WINDOW), pair : pair + 128].astype(jnp.float32)
+            query = jnp.where(low if head % 2 == 0 else jnp.logical_not(low), query, 0.0)
+            queries.append((query * HEAD_DIM ** (-0.5)).astype(jnp.bfloat16))
+        all_scores = lax.dot_general(
+            jnp.concatenate(queries, axis=0),
+            keys[window, :],
+            (((1,), (1,)), ((), ())),
+            preferred_element_type=jnp.float32,
+        )
+        weights = []
+        for head in range(heads):
+            scores = all_scores[head * WINDOW : (head + 1) * WINDOW]
+            scores = jnp.where(allowed, scores, -jnp.inf)
+            sums = jnp.sum(jnp.exp(scores), axis=1, keepdims=True)
+            sink = jnp.full((WINDOW, 1), sinks_ref[core * heads + head], jnp.float32)
+            log_total = jnp.log(sums + jnp.exp(sink))
+            logs = jnp.where(lane == head, log_total, logs)
+            weights.append(jnp.exp(scores - log_total).astype(jnp.bfloat16))
+        attended = jnp.dot(
+            jnp.concatenate(weights, axis=0), values[window, :], preferred_element_type=jnp.float32
+        )
+        parts = [attended[head * WINDOW : (head + 1) * WINDOW] for head in range(heads)]
+        outs = [
+            jnp.where(low, parts[head], parts[head + 1]).astype(jnp.bfloat16)
+            for head in range(0, heads, 2)
+        ]
         out = jnp.concatenate(outs, axis=1)
         logs_ref[:, pl.ds(base, WINDOW)] = logs.T[:heads]
         own = block // half_blocks == core
@@ -537,7 +541,7 @@
         1 << 32,
         [SMEM, VMEM, VMEM],
         (sinks, qkv, before),
-        (extended,) * 4,
+        (extended,) * 2,
     )
     conv_kept, given = call(
         scaled_kernel,

time: 191 us -> 190 us (level)
  transfers between devices with their start and end apart: 18 -> 18, of which waited for: 10 -> 10; matrix products, arithmetic and copies ran while one was open for 3% -> 3% of each run, Pallas kernels for 20% -> 19%
where the time goes in v8:
time: 190 us; the launch traced here: 187 us
  starting transfers between devices  73.8 us (39%)
  Pallas kernels  43.4 us (23%)
  waiting for transfers between devices  35.3 us (19%)
  blocking collectives  18.9 us (10%)
  local copies, waits for them, and re-layouts  9.17 us (5%)
  other arithmetic  5.58 us (3%)
    pallas_call x12, Pallas kernels, call(): pl.pallas_call(body, out_shape=outs, in_specs=in_specs, out_specs=jax.tre...  43.4 us
    all_to_all x1, blocking collectives, layer(): lax.all_to_all(sent, SP, 0, 0, tiled=True, axis_index_groups=LINES)  18.9 us
    ppermute x4, starting transfers between devices, layer(): behind = lax.ppermute(behind, SP, BEHIND)  17.3 us
    ppermute x4, waiting for transfers between devices, layer(): ahead = lax.ppermute(ahead, SP, AHEAD)  15.4 us
    ppermute x3, waiting for transfers between devices, to_member(): lax.ppermute(value, 'tp', [(i, (i + away) % peers) for i in range(peers)])  12.6 us
    ppermute x3, starting transfers between devices, to_member(): lax.ppermute(value, 'tp', [(i, (i + away) % peers) for i in range(peers)])  11.3 us
    ppermute x4, starting transfers between devices, layer(): ahead = lax.ppermute(ahead, SP, AHEAD)  9.1 us
    ppermute x1, starting transfers between devices, layer(): got = lax.ppermute(given, SP, OTHER_CORE)  8.74 us
  transfers between devices with their start and end apart: 18, of which 10 were waited for; matrix products, arithmetic and copies ran while one was open for 3% of the time, Pallas kernels for 19%

profile of v8, /device:TPU:1, one launch (start us, length us, event | category | flops | bytes accessed | tf_op | source)
XLA Modules:
  0.0 187.2 jit_solution(18389695548336950248)
XLA Ops:
  2.2 8.7 %collective-permute-start.1 = (bf16[16,1408]{1,0:T(8,128)(2,1)}, bf16[16,1408]{1,0:T(8,128)(2,1)S(1)}, u32[]{:S(2)}, u32[]{:S(2)}) collective-permute-start(bf16[16,1408]{1,0:T(8,128)(2,1)} %get-tuple-element.19), channel_id=1, source_target_pairs={{0,4},{4,0},{8,12},{12,8},{16,20},{20,16},{24,28},{28,24},{32,36},... | collective-permute-start | bytes 135176 | tf_op jit(solution)/shard_map/ppermute | solution.py:456
  14.4 18.9 %all_to_all.10.refs_0_ = bf16[8,32,1408]{2,1,0:T(8,128)(2,1)S(1)} all-to-all(bf16[8,32,1408]{2,1,0:T(8,128)(2,1)} %shard_map.134), channel_id=1, replica_groups={{0,8,16,24,32,40,48,56},{64,72,80,88,96,104,112,120},{128,136,144,152,1..., dimensions={0} | all-to-all | bytes 1441792 | tf_op jit(solution)/shard_map/all_to_all | solution.py:458
  33.3 3.2 %collective-permute-start.2 = (bf16[8,32,1408]{2,1,0:T(8,128)(2,1)S(1)}, bf16[8,32,1408]{2,1,0:T(8,128)(2,1)S(1)}, u32[]{:S(2)}, u32[]{:S(2)}) collective-permute-start(bf16[8,32,1408]{2,1,0:T(8,128)(2,1)S(1)} %all_to_all.10.refs_0_), channel_id=1, source_target_pairs={{0,64},{8,72},{16,80},{24,88},{32,96},{40,104},{48,112},{56,120},{... | collective-permute-start | bytes 2162696 | tf_op jit(solution)/shard_map/ppermute | solution.py:464
  36.5 3.8 %collective-permute-start.5 = (bf16[8,32,1408]{2,1,0:T(8,128)(2,1)S(1)}, bf16[8,32,1408]{2,1,0:T(8,128)(2,1)S(1)}, u32[]{:S(2)}, u32[]{:S(2)}) collective-permute-start(bf16[8,32,1408]{2,1,0:T(8,128)(2,1)S(1)} %all_to_all.10.refs_0_), channel_id=1, source_target_pairs={{0,448},{8,456},{16,464},{24,472},{32,480},{40,488},{48,496},{56,5... | collective-permute-start | bytes 2162696 | tf_op jit(solution)/shard_map/ppermute | solution.py:465
  40.4 7.0 %collective-permute-done.2.refs_1_ = bf16[8,32,1408]{2,1,0:T(8,128)(2,1)S(1)} collective-permute-done((bf16[8,32,1408]{2,1,0:T(8,128)(2,1)S(1)}, bf16[8,32,1408]{2,1,0:T(8,128)(2,1)S(1)}, u32[]{:S(2)}, u32[]{:S(2)}) %collective-permute-start.2) | collective-permute-done | bytes 720928 | tf_op jit(solution)/shard_map/ppermute | solution.py:464
  47.4 1.9 %collective-permute-start.3 = (bf16[8,32,1408]{2,1,0:T(8,128)(2,1)S(1)}, bf16[8,32,1408]{2,1,0:T(8,128)(2,1)S(1)}, u32[]{:S(2)}, u32[]{:S(2)}) collective-permute-start(bf16[8,32,1408]{2,1,0:T(8,128)(2,1)S(1)} %collective-permute-done.2.refs_1_), channel_id=1, source_target_pairs={{0,64},{8,72},{16,80},{24,88},{32,96},{40,104},{48,112},{56,120},{... | collective-permute-start | bytes 2162696 | tf_op jit(solution)/shard_map/ppermute | solution.py:464
  49.3 4.6 %collective-permute-start.6 = (bf16[8,32,1408]{2,1,0:T(8,128)(2,1)S(1)}, bf16[8,32,1408]{2,1,0:T(8,128)(2,1)S(1)}, u32[]{:S(2)}, u32[]{:S(2)}) collective-permute-start(bf16[8,32,1408]{2,1,0:T(8,128)(2,1)S(1)} %collective-permute-done.5.refs_2_), channel_id=1, source_target_pairs={{0,448},{8,456},{16,464},{24,472},{32,480},{40,488},{48,496},{56,5... | collective-permute-start | bytes 2162696 | tf_op jit(solution)/shard_map/ppermute | solution.py:465
  54.8 7.3 %collective-permute-start = (bf16[512,2048]{1,0:T(8,128)(2,1)}, bf16[512,2048]{1,0:T(8,128)(2,1)}, u32[]{:S(2)}, u32[]{:S(2)}) collective-permute-start(bf16[512,2048]{1,0:T(8,128)(2,1)} %x_ref.1), channel_id=1, source_target_pairs={{0,4},{4,0},{8,12},{12,8},{16,20},{20,16},{24,28},{28,24},{32,36},... | collective-permute-start | bytes 6291464 | tf_op jit(solution)/shard_map/ppermute | solution.py:468
  62.0 2.1 %collective-permute-start.4 = (bf16[8,32,1408]{2,1,0:T(8,128)(2,1)S(1)}, bf16[8,32,1408]{2,1,0:T(8,128)(2,1)S(1)}, u32[]{:S(2)}, u32[]{:S(2)}) collective-permute-start(bf16[8,32,1408]{2,1,0:T(8,128)(2,1)S(1)} %collective-permute-done.3.refs_3_), channel_id=1, source_target_pairs={{0,64},{8,72},{16,80},{24,88},{32,96},{40,104},{48,112},{56,120},{... | collective-permute-start | bytes 2162696 | tf_op jit(solution)/shard_map/ppermute | solution.py:464
  65.1 4.4 %collective-permute-start.7 = (bf16[8,32,1408]{2,1,0:T(8,128)(2,1)S(1)}, bf16[8,32,1408]{2,1,0:T(8,128)(2,1)S(1)}, u32[]{:S(2)}, u32[]{:S(2)}) collective-permute-start(bf16[8,32,1408]{2,1,0:T(8,128)(2,1)S(1)} %collective-permute-done.6.refs_4_), channel_id=1, source_target_pairs={{0,448},{8,456},{16,464},{24,472},{32,480},{40,488},{48,496},{56,5... | collective-permute-start | bytes 2162696 | tf_op jit(solution)/shard_map/ppermute | solution.py:465
  69.5 6.1 %collective-permute-done.4.refs_0_.refs_5_ = bf16[8,32,1408]{2,1,0:T(8,128)(2,1)S(1)} collective-permute-done((bf16[8,32,1408]{2,1,0:T(8,128)(2,1)S(1)}, bf16[8,32,1408]{2,1,0:T(8,128)(2,1)S(1)}, u32[]{:S(2)}, u32[]{:S(2)}) %collective-permute-start.4) | collective-permute-done | bytes 720928 | tf_op jit(solution)/shard_map/ppermute | solution.py:464
  79.0 4.6 %collective-permute-start.9 = (bf16[4,32,1408]{2,1,0:T(8,128)(2,1)}, bf16[4,32,1408]{2,1,0:T(8,128)(2,1)}, u32[]{:S(2)}, u32[]{:S(2)}) collective-permute-start(bf16[4,32,1408]{2,1,0:T(8,128)(2,1)} %slice.9), channel_id=1, source_target_pairs={{0,448},{8,456},{16,464},{24,472},{32,480},{40,488},{48,496},{56,5... | collective-permute-start | bytes 1081352 | tf_op jit(solution)/shard_map/ppermute | solution.py:465
  83.6 2.3 %collective-permute-done.8.a_ref.refs_7_ = bf16[4,32,1408]{2,1,0:T(8,128)(2,1)S(1)} collective-permute-done((bf16[4,32,1408]{2,1,0:T(8,128)(2,1)}, bf16[4,32,1408]{2,1,0:T(8,128)(2,1)S(1)}, u32[]{:S(2)}, u32[]{:S(2)}) %collective-permute-start.8) | collective-permute-done | bytes 360480 | tf_op jit(solution)/shard_map/ppermute | solution.py:464
  85.9 2.3 %collective-permute-done.9.b_ref.refs_8_ = bf16[4,32,1408]{2,1,0:T(8,128)(2,1)} collective-permute-done((bf16[4,32,1408]{2,1,0:T(8,128)(2,1)}, bf16[4,32,1408]{2,1,0:T(8,128)(2,1)}, u32[]{:S(2)}, u32[]{:S(2)}) %collective-permute-start.9) | collective-permute-done | bytes 360480 | tf_op jit(solution)/shard_map/ppermute | solution.py:465
  91.6 2.5 %shard_map.141.own_ref = bf16[2048,512]{1,0:T(8,128)(2,1)} custom-call(bf16[8,32,1408]{2,1,0:T(8,128)(2,1)S(1)} %all_to_all.10.refs_0_, bf16[8,32,1408]{2,1,0:T(8,128)(2,1)S(1)} %collective-permute-done.2.refs_1_, bf16[8,32,1408]{2,1,0:T(8,128)(2,1)S(1)} %copy-done.1, bf16[8,32,1408]{2,1,0:T(8,128)(2,1)S(1)} %copy-done.4, ...), custom_call_target="tpu_custom_call" | custom-call | flops 268435456 | bytes 1048576 | tf_op jit(solution)/shard_map/pallas_call | solution.py:53
  94.1 8.5 %collective-permute-start.12 = (bf16[2048,512]{1,0:T(8,128)(2,1)}, bf16[2048,512]{1,0:T(8,128)(2,1)}, u32[]{:S(2)}, u32[]{:S(2)}) collective-permute-start(bf16[2048,512]{1,0:T(8,128)(2,1)} %shard_map.141.own_ref), channel_id=1, source_target_pairs={{0,4},{4,0},{8,12},{12,8},{16,20},{20,16},{24,28},{28,24},{32,36},... | collective-permute-start | bytes 6291464 | tf_op jit(solution)/shard_map/ppermute | solution.py:520
  104.6 6.5 %shard_map.131.own_ref = bf16[512,2048]{1,0:T(8,128)(2,1)S(1)} custom-call(bf16[512,2048]{1,0:T(8,128)(2,1)} %x_ref.1, bf16[1,2048]{1,0:T(2,128)(2,1)S(1)} %broadcast_in_dim.4.gain_ref), custom_call_target="tpu_custom_call" | custom-call | flops 1073741824 | bytes 1048576 | tf_op jit(solution)/shard_map/pallas_call | solution.py:53
  112.0 6.7 %shard_map.132.other_ref = bf16[512,2048]{1,0:T(8,128)(2,1)S(1)} custom-call(bf16[512,2048]{1,0:T(8,128)(2,1)} %collective-permute-done.x_ref, bf16[1,2048]{1,0:T(2,128)(2,1)S(1)} %broadcast_in_dim.4.gain_ref), custom_call_target="tpu_custom_call" | custom-call | flops 1073741824 | bytes 1048576 | tf_op jit(solution)/shard_map/pallas_call | solution.py:53
  118.7 3.6 %shard_map.135.refs_2_ = f32[1024,896]{1,0:T(8,128)S(1)} custom-call(bf16[512,2048]{1,0:T(8,128)(2,1)S(1)} %shard_map.131.own_ref, bf16[512,2048]{1,0:T(8,128)(2,1)S(1)} %shard_map.132.other_ref, bf16[8,32,1408]{2,1,0:T(8,128)(2,1)S(1)} %all_to_all.10.refs_0_, bf16[8,32,1408]{2,1,0:T(8,128)(2,1)S(1)} %collective-permute-done.2.refs_1_, ...), custom_call_target="tpu_custom_call" | custom-call | flops 2348810240 | bytes 1048576 | tf_op jit(solution)/shard_map/pallas_call | solution.py:53
  124.1 2.8 %shard_map.137 = (bf16[1024,256]{1,0:T(8,128)(2,1)S(1)}, bf16[1024,384]{1,0:T(8,128)(2,1)S(1)}, bf16[192,128]{1,0:T(8,128)(2,1)S(1)}) custom-call(bf16[512,2048]{1,0:T(8,128)(2,1)S(1)} %shard_map.131.own_ref, bf16[512,2048]{1,0:T(8,128)(2,1)S(1)} %shard_map.132.other_ref, f32[1024,128]{1,0:T(8,128)S(1)} %get-tuple-element.39.cos_ref, ...), custom_call_target="tpu_custom_call" | custom-call | flops 469762048 | bytes 1048576 | tf_op jit(solution)/shard_map/pallas_call | solution.py:53
  126.9 2.1 %collective-permute-start.10 = (bf16[192,128]{1,0:T(8,128)(2,1)S(1)}, bf16[192,128]{1,0:T(8,128)(2,1)S(1)}, u32[]{:S(2)}, u32[]{:S(2)}) collective-permute-start(bf16[192,128]{1,0:T(8,128)(2,1)S(1)} %get-tuple-element.20), channel_id=1, source_target_pairs={{0,8},{4,12},{8,16},{12,20},{16,24},{20,28},{24,32},{28,36},{32,40... | collective-permute-start | bytes 147464 | tf_op jit(solution)/shard_map/ppermute | solution.py:511
  130.2 4.1 %shard_map.138 = (f32[1024,256]{1,0:T(8,128)S(1)}, f32[8,2,1024]{2,1,0:T(2,128)}) custom-call(bf16[192,128]{1,0:T(8,128)(2,1)S(1)} %collective-permute-done.10.before_ref, bf16[1024,256]{1,0:T(8,128)(2,1)S(1)} %get-tuple-element.21.glu_ref, f32[31,512]{1,0:T(8,128)S(1)} %copy-done.12), custom_call_target="tpu_custom_call" | custom-call | flops 4294967296 | bytes 1048576 | tf_op jit(solution)/shard_map/pallas_call | solution.py:53
  134.3 4.4 %all-to-all-start.1 = ((f32[8,2,1024]{2,1,0:T(2,128)}), f32[8,2,1024]{2,1,0:T(2,128)S(1)}, u32[]{:S(2)}, u32[]{:S(2)}) async-start(f32[8,2,1024]{2,1,0:T(2,128)} %get-tuple-element.23), calls=%async_computation.1 | async-start | bytes 131072 | tf_op jit(solution)/shard_map/all_to_all | solution.py:532
  138.7 6.3 %shard_map.139 = (bf16[512,256]{1,0:T(8,128)(2,1)}, bf16[512,256]{1,0:T(8,128)(2,1)}, f32[4,1024]{1,0:T(4,128)}) custom-call(f32[8]{0:T(128)} %sinks_ref.1, bf16[1024,384]{1,0:T(8,128)(2,1)} %copy-done.11, bf16[192,128]{1,0:T(8,128)(2,1)} %copy-done.13), custom_call_target="tpu_custom_call" | custom-call | flops 4294967296 | bytes 1048576 | tf_op jit(solution)/shard_map/pallas_call | solution.py:53
  146.9 1.9 %collective-permute-start.11 = (bf16[512,512]{1,0:T(8,128)(2,1)S(1)}, bf16[512,512]{1,0:T(8,128)(2,1)S(1)}, u32[]{:S(2)}, u32[]{:S(2)}) collective-permute-start(bf16[512,512]{1,0:T(8,128)(2,1)S(1)} %get-tuple-element.28), channel_id=1, source_target_pairs={{0,4},{4,0},{8,12},{12,8},{16,20},{20,16},{24,28},{28,24},{32,36},... | collective-permute-start | bytes 1572872 | tf_op jit(solution)/shard_map/ppermute | solution.py:554
  151.7 4.9 %shard_map.142 = (bf16[128,2048]{1,0:T(8,128)(2,1)S(1)}, bf16[128,2048]{1,0:T(8,128)(2,1)S(1)}, bf16[128,2048]{1,0:T(8,128)(2,1)S(1)}, bf16[128,2048]{1,0:T(8,128)(2,1)S(1)}) custom-call(bf16[512,256]{1,0:T(8,128)(2,1)S(1)} %get-tuple-element.26.conv_ref, bf16[512,256]{1,0:T(8,128)(2,1)S(1)} %copy-done.14, ...), custom_call_target="tpu_custom_call" | custom-call | flops 2147483648 | bytes 1048576 | tf_op jit(solution)/shard_map/pallas_call | solution.py:53
  156.6 4.8 %collective-permute-start.13 = (bf16[128,2048]{1,0:T(8,128)(2,1)S(1)}, bf16[128,2048]{1,0:T(8,128)(2,1)S(1)}, u32[]{:S(2)}, u32[]{:S(2)}) collective-permute-start(bf16[128,2048]{1,0:T(8,128)(2,1)S(1)} %get-tuple-element.30), channel_id=1, source_target_pairs={{0,2},{1,3},{2,0},{3,1},{4,6},{5,7},{6,4},{7,5},{8,10},{9,11},{10,... | collective-permute-start | bytes 1572872 | tf_op jit(solution)/shard_map/ppermute | solution.py:583
  161.4 2.2 %collective-permute-start.14 = (bf16[128,2048]{1,0:T(8,128)(2,1)S(1)}, bf16[128,2048]{1,0:T(8,128)(2,1)S(1)}, u32[]{:S(2)}, u32[]{:S(2)}) collective-permute-start(bf16[128,2048]{1,0:T(8,128)(2,1)S(1)} %get-tuple-element.31), channel_id=1, source_target_pairs={{0,1},{1,2},{2,3},{3,0},{4,5},{5,6},{6,7},{7,4},{8,9},{9,10},{10,1... | collective-permute-start | bytes 1572872 | tf_op jit(solution)/shard_map/ppermute | solution.py:583
  163.6 4.3 %collective-permute-start.15 = (bf16[128,2048]{1,0:T(8,128)(2,1)S(1)}, bf16[128,2048]{1,0:T(8,128)(2,1)}, u32[]{:S(2)}, u32[]{:S(2)}) collective-permute-start(bf16[128,2048]{1,0:T(8,128)(2,1)S(1)} %get-tuple-element.32), channel_id=1, source_target_pairs={{0,3},{1,0},{2,1},{3,2},{4,7},{5,4},{6,5},{7,6},{8,11},{9,8},{10,9... | collective-permute-start | bytes 1572872 | tf_op jit(solution)/shard_map/ppermute | solution.py:583
  167.9 3.1 %collective-permute-start.16 = (f32[4,512]{1,0:T(4,128)S(1)}, f32[4,512]{1,0:T(4,128)S(1)}, u32[]{:S(2)}, u32[]{:S(2)}) collective-permute-start(f32[4,512]{1,0:T(4,128)S(1)} %get-tuple-element.35), channel_id=1, source_target_pairs={{0,4},{4,0},{8,12},{12,8},{16,20},{20,16},{24,28},{28,24},{32,36},... | collective-permute-start | bytes 24584 | tf_op jit(solution)/shard_map/ppermute | solution.py:558
  173.4 11.7 %collective-permute-done.14 = bf16[128,2048]{1,0:T(8,128)(2,1)S(1)} collective-permute-done((bf16[128,2048]{1,0:T(8,128)(2,1)S(1)}, bf16[128,2048]{1,0:T(8,128)(2,1)S(1)}, u32[]{:S(2)}, u32[]{:S(2)}) %collective-permute-start.14) | collective-permute-done | bytes 524320 | tf_op jit(solution)/shard_map/ppermute | solution.py:583
  185.1 2.2 %add_convert_fusion = bf16[128,2048]{1,0:T(8,128)(2,1)} fusion(bf16[128,2048]{1,0:T(8,128)(2,1)} %collective-permute-done.15, bf16[128,2048]{1,0:T(8,128)(2,1)S(1)} %collective-permute-done.14, bf16[128,2048]{1,0:T(8,128)(2,1)S(1)} %collective-permute-done.13, bf16[128,2048]{1,0:T(8,128)(2,1)S(1)} %get-tuple-element.29), kind=kLoop, calls=%fused_computation | loop fusion | flops 2097152 | bytes 2621440 | tf_op jit(solution)/shard_map/convert_element_type | solution.py:594
  (63 shorter events, 26.4 us)
Async XLA Ops:
  2.2 9.8 %collective-permute-start.1 = (bf16[16,1408]{1,0:T(8,128)(2,1)}, bf16[16,1408]{1,0:T(8,128)(2,1)S(1)}, u32[]{:S(2)}, u32[]{:S(2)}) collective-permute-start(bf16[16,1408]{1,0:T(8,128)(2,1)} %get-tuple-element.19), channel_id=1, source_target_pairs={{0,4},{4,0},{8,12},{12,8},{16,20},{20,16},{24,28},{28,24},{32,36},... | collective-permute-start | bytes 135176 | tf_op jit(solution)/shard_map/ppermute | solution.py:456
  33.3 14.1 %collective-permute-start.2 = (bf16[8,32,1408]{2,1,0:T(8,128)(2,1)S(1)}, bf16[8,32,1408]{2,1,0:T(8,128)(2,1)S(1)}, u32[]{:S(2)}, u32[]{:S(2)}) collective-permute-start(bf16[8,32,1408]{2,1,0:T(8,128)(2,1)S(1)} %all_to_all.10.refs_0_), channel_id=1, source_target_pairs={{0,64},{8,72},{16,80},{24,88},{32,96},{40,104},{48,112},{56,120},{... | collective-permute-start | bytes 2162696 | tf_op jit(solution)/shard_map/ppermute | solution.py:464
  36.5 12.8 %collective-permute-start.5 = (bf16[8,32,1408]{2,1,0:T(8,128)(2,1)S(1)}, bf16[8,32,1408]{2,1,0:T(8,128)(2,1)S(1)}, u32[]{:S(2)}, u32[]{:S(2)}) collective-permute-start(bf16[8,32,1408]{2,1,0:T(8,128)(2,1)S(1)} %all_to_all.10.refs_0_), channel_id=1, source_target_pairs={{0,448},{8,456},{16,464},{24,472},{32,480},{40,488},{48,496},{56,5... | collective-permute-start | bytes 2162696 | tf_op jit(solution)/shard_map/ppermute | solution.py:465
  47.4 14.6 %collective-permute-start.3 = (bf16[8,32,1408]{2,1,0:T(8,128)(2,1)S(1)}, bf16[8,32,1408]{2,1,0:T(8,128)(2,1)S(1)}, u32[]{:S(2)}, u32[]{:S(2)}) collective-permute-start(bf16[8,32,1408]{2,1,0:T(8,128)(2,1)S(1)} %collective-permute-done.2.refs_1_), channel_id=1, source_target_pairs={{0,64},{8,72},{16,80},{24,88},{32,96},{40,104},{48,112},{56,120},{... | collective-permute-start | bytes 2162696 | tf_op jit(solution)/shard_map/ppermute | solution.py:464
  49.3 15.7 %collective-permute-start.6 = (bf16[8,32,1408]{2,1,0:T(8,128)(2,1)S(1)}, bf16[8,32,1408]{2,1,0:T(8,128)(2,1)S(1)}, u32[]{:S(2)}, u32[]{:S(2)}) collective-permute-start(bf16[8,32,1408]{2,1,0:T(8,128)(2,1)S(1)} %collective-permute-done.5.refs_2_), channel_id=1, source_target_pairs={{0,448},{8,456},{16,464},{24,472},{32,480},{40,488},{48,496},{56,5... | collective-permute-start | bytes 2162696 | tf_op jit(solution)/shard_map/ppermute | solution.py:465
  54.8 57.2 %collective-permute-start = (bf16[512,2048]{1,0:T(8,128)(2,1)}, bf16[512,2048]{1,0:T(8,128)(2,1)}, u32[]{:S(2)}, u32[]{:S(2)}) collective-permute-start(bf16[512,2048]{1,0:T(8,128)(2,1)} %x_ref.1), channel_id=1, source_target_pairs={{0,4},{4,0},{8,12},{12,8},{16,20},{20,16},{24,28},{28,24},{32,36},... | collective-permute-start | bytes 6291464 | tf_op jit(solution)/shard_map/ppermute | solution.py:468
  62.0 13.5 %collective-permute-start.4 = (bf16[8,32,1408]{2,1,0:T(8,128)(2,1)S(1)}, bf16[8,32,1408]{2,1,0:T(8,128)(2,1)S(1)}, u32[]{:S(2)}, u32[]{:S(2)}) collective-permute-start(bf16[8,32,1408]{2,1,0:T(8,128)(2,1)S(1)} %collective-permute-done.3.refs_3_), channel_id=1, source_target_pairs={{0,64},{8,72},{16,80},{24,88},{32,96},{40,104},{48,112},{56,120},{... | collective-permute-start | bytes 2162696 | tf_op jit(solution)/shard_map/ppermute | solution.py:464
  65.1 13.2 %copy-start.6 = (bf16[8,32,1408]{2,1,0:T(8,128)(2,1)}, bf16[8,32,1408]{2,1,0:T(8,128)(2,1)S(1)}, u32[]{:S(2)}) copy-start(bf16[8,32,1408]{2,1,0:T(8,128)(2,1)S(1)} %collective-permute-done.6.refs_4_) | copy-start | bytes 2162692
  65.1 13.2 %collective-permute-start.7 = (bf16[8,32,1408]{2,1,0:T(8,128)(2,1)S(1)}, bf16[8,32,1408]{2,1,0:T(8,128)(2,1)S(1)}, u32[]{:S(2)}, u32[]{:S(2)}) collective-permute-start(bf16[8,32,1408]{2,1,0:T(8,128)(2,1)S(1)} %collective-permute-done.6.refs_4_), channel_id=1, source_target_pairs={{0,448},{8,456},{16,464},{24,472},{32,480},{40,488},{48,496},{56,5... | collective-permute-start | bytes 2162696 | tf_op jit(solution)/shard_map/ppermute | solution.py:465
  76.3 9.6 %collective-permute-start.8 = (bf16[4,32,1408]{2,1,0:T(8,128)(2,1)}, bf16[4,32,1408]{2,1,0:T(8,128)(2,1)S(1)}, u32[]{:S(2)}, u32[]{:S(2)}) collective-permute-start(bf16[4,32,1408]{2,1,0:T(8,128)(2,1)} %slice.8), channel_id=1, source_target_pairs={{0,64},{8,72},{16,80},{24,88},{32,96},{40,104},{48,112},{56,120},{... | collective-permute-start | bytes 1081352 | tf_op jit(solution)/shard_map/ppermute | solution.py:464
  79.0 9.2 %collective-permute-start.9 = (bf16[4,32,1408]{2,1,0:T(8,128)(2,1)}, bf16[4,32,1408]{2,1,0:T(8,128)(2,1)}, u32[]{:S(2)}, u32[]{:S(2)}) collective-permute-start(bf16[4,32,1408]{2,1,0:T(8,128)(2,1)} %slice.9), channel_id=1, source_target_pairs={{0,448},{8,456},{16,464},{24,472},{32,480},{40,488},{48,496},{56,5... | collective-permute-start | bytes 1081352 | tf_op jit(solution)/shard_map/ppermute | solution.py:465
  83.6 20.9 %copy-start.17 = (bf16[2048]{0:T(1024)(128)(2,1)S(1)}, bf16[2048]{0:T(1024)(128)(2,1)}, u32[]{:S(2)}) copy-start(bf16[2048]{0:T(1024)(128)(2,1)} %param.13) | copy-start | bytes 12292
  88.3 1.1 copy-start.1
  89.4 1.1 copy-start.4
  90.5 1.1 copy-start.7
  94.1 56.6 %collective-permute-start.12 = (bf16[2048,512]{1,0:T(8,128)(2,1)}, bf16[2048,512]{1,0:T(8,128)(2,1)}, u32[]{:S(2)}, u32[]{:S(2)}) collective-permute-start(bf16[2048,512]{1,0:T(8,128)(2,1)} %shard_map.141.own_ref), channel_id=1, source_target_pairs={{0,4},{4,0},{8,12},{12,8},{16,20},{20,16},{24,28},{28,24},{32,36},... | collective-permute-start | bytes 6291464 | tf_op jit(solution)/shard_map/ppermute | solution.py:520
  112.0 6.7 %copy-start.2 = (bf16[8,32,1408]{2,1,0:T(8,128)(2,1)S(1)}, bf16[8,32,1408]{2,1,0:T(8,128)(2,1)}, u32[]{:S(2)}) copy-start(bf16[8,32,1408]{2,1,0:T(8,128)(2,1)} %copy-done) | copy-start | bytes 2162692
  112.0 6.7 %copy-start.5 = (bf16[8,32,1408]{2,1,0:T(8,128)(2,1)S(1)}, bf16[8,32,1408]{2,1,0:T(8,128)(2,1)}, u32[]{:S(2)}) copy-start(bf16[8,32,1408]{2,1,0:T(8,128)(2,1)} %copy-done.3) | copy-start | bytes 2162692
  112.0 6.7 %copy-start.8 = (bf16[8,32,1408]{2,1,0:T(8,128)(2,1)S(1)}, bf16[8,32,1408]{2,1,0:T(8,128)(2,1)}, u32[]{:S(2)}) copy-start(bf16[8,32,1408]{2,1,0:T(8,128)(2,1)} %copy-done.6) | copy-start | bytes 2162692
  124.1 6.0 %copy-start.12 = (f32[31,512]{1,0:T(8,128)S(1)}, f32[31,512]{1,0:T(8,128)}, u32[]{:S(2)}) copy-start(f32[31,512]{1,0:T(8,128)} %taps_ref.1) | copy-start | bytes 190468
  126.9 7.4 %copy-start.11 = (bf16[1024,384]{1,0:T(8,128)(2,1)}, bf16[1024,384]{1,0:T(8,128)(2,1)S(1)}, u32[]{:S(2)}) copy-start(bf16[1024,384]{1,0:T(8,128)(2,1)S(1)} %get-tuple-element.24.qkv_ref) | copy-start | bytes 2359300
  126.9 3.3 %collective-permute-start.10 = (bf16[192,128]{1,0:T(8,128)(2,1)S(1)}, bf16[192,128]{1,0:T(8,128)(2,1)S(1)}, u32[]{:S(2)}, u32[]{:S(2)}) collective-permute-start(bf16[192,128]{1,0:T(8,128)(2,1)S(1)} %get-tuple-element.20), channel_id=1, source_target_pairs={{0,8},{4,12},{8,16},{12,20},{16,24},{20,28},{24,32},{28,36},{32,40... | collective-permute-start | bytes 147464 | tf_op jit(solution)/shard_map/ppermute | solution.py:511
  130.2 4.1 %copy-start.13 = (bf16[192,128]{1,0:T(8,128)(2,1)}, bf16[192,128]{1,0:T(8,128)(2,1)S(1)}, u32[]{:S(2)}) copy-start(bf16[192,128]{1,0:T(8,128)(2,1)S(1)} %collective-permute-done.10.before_ref) | copy-start | bytes 147460
  134.3 10.7 %all-to-all-start.1 = ((f32[8,2,1024]{2,1,0:T(2,128)}), f32[8,2,1024]{2,1,0:T(2,128)S(1)}, u32[]{:S(2)}, u32[]{:S(2)}) async-start(f32[8,2,1024]{2,1,0:T(2,128)} %get-tuple-element.23), calls=%async_computation.1 | async-start | bytes 131072 | tf_op jit(solution)/shard_map/all_to_all | solution.py:532
  138.7 6.3 %copy-start.10 = (f32[512]{0:T(512)S(1)}, f32[512]{0:T(512)}, u32[]{:S(2)}) copy-start(f32[512]{0:T(512)} %param.20) | copy-start | bytes 6148
  146.9 3.8 %collective-permute-start.11 = (bf16[512,512]{1,0:T(8,128)(2,1)S(1)}, bf16[512,512]{1,0:T(8,128)(2,1)S(1)}, u32[]{:S(2)}, u32[]{:S(2)}) collective-permute-start(bf16[512,512]{1,0:T(8,128)(2,1)S(1)} %get-tuple-element.28), channel_id=1, source_target_pairs={{0,4},{4,0},{8,12},{12,8},{16,20},{20,16},{24,28},{28,24},{32,36},... | collective-permute-start | bytes 1572872 | tf_op jit(solution)/shard_map/ppermute | solution.py:554
  150.7 1.0 copy-start.14
  151.7 16.2 %copy-start.16 = (f32[4,1024]{1,0:T(4,128)S(1)}, f32[4,1024]{1,0:T(4,128)}, u32[]{:S(2)}) copy-start(f32[4,1024]{1,0:T(4,128)} %get-tuple-element.33) | copy-start | bytes 49156
  156.6 16.8 %collective-permute-start.13 = (bf16[128,2048]{1,0:T(8,128)(2,1)S(1)}, bf16[128,2048]{1,0:T(8,128)(2,1)S(1)}, u32[]{:S(2)}, u32[]{:S(2)}) collective-permute-start(bf16[128,2048]{1,0:T(8,128)(2,1)S(1)} %get-tuple-element.30), channel_id=1, source_target_pairs={{0,2},{1,3},{2,0},{3,1},{4,6},{5,7},{6,4},{7,5},{8,10},{9,11},{10,... | collective-permute-start | bytes 1572872 | tf_op jit(solution)/shard_map/ppermute | solution.py:583
  161.4 23.7 %collective-permute-start.14 = (bf16[128,2048]{1,0:T(8,128)(2,1)S(1)}, bf16[128,2048]{1,0:T(8,128)(2,1)S(1)}, u32[]{:S(2)}, u32[]{:S(2)}) collective-permute-start(bf16[128,2048]{1,0:T(8,128)(2,1)S(1)} %get-tuple-element.31), channel_id=1, source_target_pairs={{0,1},{1,2},{2,3},{3,0},{4,5},{5,6},{6,7},{7,4},{8,9},{9,10},{10,1... | collective-permute-start | bytes 1572872 | tf_op jit(solution)/shard_map/ppermute | solution.py:583
  163.6 21.5 %collective-permute-start.15 = (bf16[128,2048]{1,0:T(8,128)(2,1)S(1)}, bf16[128,2048]{1,0:T(8,128)(2,1)}, u32[]{:S(2)}, u32[]{:S(2)}) collective-permute-start(bf16[128,2048]{1,0:T(8,128)(2,1)S(1)} %get-tuple-element.32), channel_id=1, source_target_pairs={{0,3},{1,0},{2,1},{3,2},{4,7},{5,4},{6,5},{7,6},{8,11},{9,8},{10,9... | collective-permute-start | bytes 1572872 | tf_op jit(solution)/shard_map/ppermute | solution.py:583
  167.9 3.9 %collective-permute-start.16 = (f32[4,512]{1,0:T(4,128)S(1)}, f32[4,512]{1,0:T(4,128)S(1)}, u32[]{:S(2)}, u32[]{:S(2)}) collective-permute-start(f32[4,512]{1,0:T(4,128)S(1)} %get-tuple-element.35), channel_id=1, source_target_pairs={{0,4},{4,0},{8,12},{12,8},{16,20},{20,16},{24,28},{28,24},{32,36},... | collective-permute-start | bytes 24584 | tf_op jit(solution)/shard_map/ppermute | solution.py:558
  (4 other events, 3.3 us)
